TPU v7x, 512 devices: a whole 4x4x16 slice. The times are simulated.
512 devices in a mesh: fs: 32 (over z, core), tp: 16 (over y, x).
Axes of the slice: x: 4, y: 4, z: 16, core: 2. Of those that a mesh axis runs over, the one named last changes fastest.
Arguments:
- attn_out: bfloat16 [49152, 2048], P('fs', 'tp'), may hold values from -6 to 6
- out_cot: bfloat16 [49152, 4096], P('fs', 'tp'), may hold values from -6 to 6
- latent: bfloat16 [49152, 1024], P('fs', 'tp'), may hold values from -6 to 6
- value_cot: bfloat16 [49152, 2048], P('fs', 'tp'), may hold values from -6 to 6
- out_weight: float32 [2048, 4096], P('fs', 'tp'), may hold values from -0.125 to 0.125
- value_up_matrix: float32 [1024, 2048], P('fs', 'tp'), may hold values from -0.1875 to 0.1875
- out_basis: bfloat16 [2048, 256], P('fs'), as said below
- value_basis: bfloat16 [1024, 256], P('fs'), as said below
- out_mean: float32 [256, 4096], P(None, 'tp'), may hold values from -5320.86 to 5320.86
- out_square: float32 [256, 4096], P(None, 'tp'), may hold values from 49152 to 9830400, as said below
- value_mean: float32 [256, 2048], P(None, 'tp'), may hold values from -5320.86 to 5320.86
- value_square: float32 [256, 2048], P(None, 'tp'), may hold values from 49152 to 9830400, as said below
Outputs:
- out_step: float32 [2048, 4096], P('fs', 'tp')
- out_new: float32 [2048, 4096], P('fs', 'tp')
- out_copy: bfloat16 [2048, 4096], P(None, 'tp')
- out_mean_new: float32 [256, 4096], P(None, 'tp')
- out_square_new: float32 [256, 4096], P(None, 'tp')
- value_step: float32 [1024, 2048], P('fs', 'tp')
- value_new: float32 [1024, 2048], P('fs', 'tp')
- value_copy: bfloat16 [1024, 2048], P(None, 'tp')
- value_mean_new: float32 [256, 2048], P(None, 'tp')
- value_square_new: float32 [256, 2048], P(None, 'tp')
Inputs may be any that keep to these rules, and one draw needn't show every extreme that they name: `out_basis`: factors of full rank, rows of differing scales. `value_basis`: factors of full rank, rows of differing scales. `out_square`: Positive. `value_square`: Positive.
All inputs are finite; a program needn't handle non-finite values.
Results may differ from a plain program's by a relative error of at most 0.012.
Values may be sent and summed in bfloat16 or wider, within the bound.
No kernel may reach another device: no remote copies, remote signals or barrier semaphores. Data moves between devices by JAX's collectives and lax.ppermute only.
A program may use at most 64 MiB of HBM per device.

v0:
```python
import jax
import jax.numpy as jnp
from jax import lax
from jax.sharding import Mesh
from jax.sharding import PartitionSpec as P

TP = ("tp_0", "tp_1")
FS = ("fs_0", "fs_1")


LEARN_RATE = 0.01
MEAN_DECAY = 0.8
BETA_SQUARE = 0.9
EPS_RMS = 1e-06


def laid_out(pieces, dim):
    pieces = jnp.moveaxis(pieces, 0, dim)
    dims = pieces.shape
    return pieces.reshape(*dims[:dim], dims[dim] * dims[dim + 1], *dims[dim + 2 :])


def gather_packed(arrays, axis, dims):
    ravelled = jnp.concatenate([a.reshape(-1) for a in arrays])
    lines, at, done = (lax.all_gather(ravelled, axis), 0, [])
    for a, dim in zip(arrays, dims):
        pieces = lines[:, at : at + a.size].reshape(-1, *a.shape)
        done.append(laid_out(pieces, dim))
        at += a.size
    return tuple(done)


def from_everyone(value, axis):
    devices = lax.axis_size(axis)
    return lax.all_to_all(
        jnp.broadcast_to(value[None], (devices, *value.shape)), axis, 0, 0, tiled=True
    )


def gather_axes(value, axes, dim):
    far, near = axes
    pieces = from_everyone(from_everyone(value, far), near)
    return laid_out(pieces.swapaxes(0, 1).reshape(-1, *value.shape), dim)


def split_up(value, dim, devices):
    before, after = (value.shape[:dim], value.shape[dim + 1 :])
    return jnp.moveaxis(value.reshape(*before, devices, -1, *after), dim, 0)


def summed_on_arrival(value, axis, dim):
    pieces = split_up(value, dim, lax.axis_size(axis))
    arrived = lax.all_to_all(pieces, axis, split_axis=0, concat_axis=0, tiled=True)
    return arrived.astype(jnp.float32).sum(axis=0)


def filled_up(lines, devices):
    spare = -len(lines) % devices
    return jnp.pad(lines, [(0, spare)] + [(0, 0)] * (lines.ndim - 1))


def collect(value, axis, dim):
    pieces = from_everyone(value, axis)
    return laid_out(pieces, dim)


def nested_sum(value, axes):
    lines = value.reshape(-1, value.shape[-1])
    own = summed_on_arrival(filled_up(lines, lax.axis_size(axes)), axes, 0)
    whole = collect(own.astype(jnp.bfloat16), axes, 0)
    return whole[: len(lines)].reshape(value.shape).astype(jnp.float32)


def by_axis(value, axes):
    for axis in axes:
        value = lax.psum(value, axis)
    return value


def moments(proj, mean_in, square_in):
    mean_new = MEAN_DECAY * mean_in + (1.0 - MEAN_DECAY) * proj
    square_new = BETA_SQUARE * square_in + (1.0 - BETA_SQUARE) * proj * proj
    return (mean_new, square_new, mean_new / jnp.sqrt(square_new))


def gram_of(basis):
    return jnp.dot(basis.T, basis, preferred_element_type=jnp.float32)


def split_product(lifted, cotangent):
    upper = lifted.astype(jnp.bfloat16)
    lower = (lifted - upper.astype(jnp.float32)).astype(jnp.bfloat16)
    first = jnp.dot(upper.T, cotangent, preferred_element_type=jnp.float32)
    return first + jnp.dot(lower.T, cotangent, preferred_element_type=jnp.float32)


def per_device(
    attn_out,
    out_cot,
    latent,
    value_cot,
    out_weight,
    value_up_matrix,
    out_basis,
    value_basis,
    out_mean,
    out_square,
    value_mean,
    value_square,
):
    width_out = out_cot.shape[1]
    head_cols = value_cot.shape[1]
    rows_out = out_basis.shape[0]
    rows_value = value_basis.shape[0]
    all_heads, all_latent = gather_packed((attn_out, latent), TP, (1, 1))
    whole_o, whole_v = (
        gather_axes(out_basis, ("fs_0", "fs_1"), 0),
        gather_axes(value_basis, ("fs_0", "fs_1"), 0),
    )
    lifted_o = jnp.dot(all_heads, whole_o, preferred_element_type=jnp.float32)
    part_o = split_product(lifted_o, out_cot)
    lifted_v = jnp.dot(all_latent, whole_v, preferred_element_type=jnp.float32)
    part_v = split_product(lifted_v, value_cot)
    count_o = rows_out * lax.axis_size(FS) * width_out * lax.axis_size(TP)
    count_v = rows_value * lax.axis_size(FS) * head_cols * lax.axis_size(TP)
    proj_o, proj_v, gram_o, gram_v = (
        nested_sum(part_o.astype(jnp.bfloat16), FS),
        nested_sum(part_v.astype(jnp.bfloat16), FS),
        nested_sum(gram_of(out_basis).astype(jnp.bfloat16), FS),
        nested_sum(gram_of(value_basis).astype(jnp.bfloat16), FS),
    )
    mean_o, square_o, direction_o = moments(proj_o, out_mean, out_square)
    mean_v, square_v, direction_v = moments(proj_v, value_mean, value_square)
    local_o = jnp.sum(direction_o * jnp.dot(gram_o, direction_o, precision=lax.Precision.HIGHEST))
    local_v = jnp.sum(direction_v * jnp.dot(gram_v, direction_v, precision=lax.Precision.HIGHEST))
    total_o, total_v = (by_axis(local_o, TP), by_axis(local_v, TP))
    update_o = jnp.dot(out_basis.astype(jnp.float32), direction_o, precision=lax.Precision.HIGHEST)
    update_v = jnp.dot(
        value_basis.astype(jnp.float32), direction_v, precision=lax.Precision.HIGHEST
    )
    step_o = LEARN_RATE * update_o * lax.rsqrt(total_o / count_o + EPS_RMS)
    step_v = LEARN_RATE * update_v * lax.rsqrt(total_v / count_v + EPS_RMS)
    new_o = out_weight - step_o
    new_v = value_up_matrix - step_v
    copy_o, copy_v = gather_packed(
        (new_o.astype(jnp.bfloat16), new_v.astype(jnp.bfloat16)), FS, (0, 0)
    )
    return (step_o, new_o, copy_o, mean_o, square_o, step_v, new_v, copy_v, mean_v, square_v)


def solution(mesh):
    torus = Mesh(mesh.devices.reshape(16, 2, 4, 4), ("fs_0", "fs_1", "tp_0", "tp_1"))
    return jax.shard_map(
        per_device,
        mesh=torus,
        in_specs=(
            P(FS, TP),
            P(FS, TP),
            P(FS, TP),
            P(FS, TP),
            P(FS, TP),
            P(FS, TP),
            P(FS, None),
            P(FS, None),
            P(None, TP),
            P(None, TP),
            P(None, TP),
            P(None, TP),
        ),
        out_specs=(
            P(FS, TP),
            P(FS, TP),
            P(None, TP),
            P(None, TP),
            P(None, TP),
            P(FS, TP),
            P(FS, TP),
            P(None, TP),
            P(None, TP),
            P(None, TP),
        ),
        check_vma=False,
    )
```

profile of v0, /device:TPU:1, one launch (start us, length us, event | category | flops | bytes accessed | tf_op | source)
XLA Modules:
  0.0 401.0 jit_solution(75111885679601764)
XLA Ops:
  7.2 1.2 copy.27
  8.7 1.9 pad_maximum_fusion
  10.8 32.4 %all_to_all.60 = bf16[32,8,256]{2,1,0:T(8,128)(2,1)S(1)} all-to-all(bf16[32,8,256]{2,1,0:T(8,128)(2,1)S(1)} %fusion.2), channel_id=1, replica_groups=mesh['fs_0'=16,'fs_1'=2,'tp_0'=4,'tp_1'=4] {'fs_0','fs_1'}, dimensions={0} | all-to-all | bytes 262144 | tf_op jit(solution)/shard_map/all_to_all | solution.py:53
  43.2 15.3 %all_to_all.61 = bf16[16,32,256]{2,1,0:T(8,128)(2,1)S(1)} all-to-all(bf16[16,32,256]{2,1,0:T(8,128)(2,1)S(1)} %broadcast_in_dim.20), channel_id=1, replica_groups=mesh['fs_0'=16,'fs_1'=2,'tp_0'=4,'tp_1'=4] {'fs_0'}, dimensions={0} | all-to-all | bytes 524288 | tf_op jit(solution)/shard_map/all_to_all | solution.py:35
  58.6 10.8 %all_to_all.62 = bf16[2,16,32,256]{3,2,1,0:T(8,128)(2,1)S(1)} all-to-all(bf16[2,16,32,256]{3,2,1,0:T(8,128)(2,1)S(1)} %broadcast_in_dim.21), channel_id=1, replica_groups=mesh['fs_0'=16,'fs_1'=2,'tp_0'=4,'tp_1'=4] {'fs_1'}, dimensions={0} | all-to-all | bytes 1048576 | tf_op jit(solution)/shard_map/all_to_all | solution.py:35
  69.5 0.8 broadcast_in_dim.16
  70.3 5.0 %all-to-all-start = ((bf16[16,64,256]{2,1,0:T(8,128)(2,1)}), bf16[16,64,256]{2,1,0:T(8,128)(2,1)S(1)}, u32[]{:S(2)}, u32[]{:S(2)}) async-start(bf16[16,64,256]{2,1,0:T(8,128)(2,1)} %broadcast_in_dim.16), calls=%async_computation | async-start | bytes 1048576 | tf_op jit(solution)/shard_map/all_to_all | solution.py:35
  75.3 0.9 fusion.1
  76.3 21.8 %all-to-all-done = bf16[16,64,256]{2,1,0:T(8,128)(2,1)S(1)} async-done(((bf16[16,64,256]{2,1,0:T(8,128)(2,1)}), bf16[16,64,256]{2,1,0:T(8,128)(2,1)S(1)}, u32[]{:S(2)}, u32[]{:S(2)}) %all-to-all-start) | async-done | bytes 524320 | tf_op jit(solution)/shard_map/all_to_all | solution.py:35
  98.2 11.3 %all_to_all.63 = bf16[2,16,64,256]{3,2,1,0:T(8,128)(2,1)S(1)} all-to-all(bf16[2,16,64,256]{3,2,1,0:T(8,128)(2,1)S(1)} %broadcast_in_dim.17), channel_id=1, replica_groups=mesh['fs_0'=16,'fs_1'=2,'tp_0'=4,'tp_1'=4] {'fs_1'}, dimensions={0} | all-to-all | bytes 2097152 | tf_op jit(solution)/shard_map/all_to_all | solution.py:35
  109.5 6.9 %all-to-all-start.4 = ((bf16[32,8,256]{2,1,0:T(8,128)(2,1)}), bf16[32,8,256]{2,1,0:T(8,128)(2,1)S(1)}, u32[]{:S(2)}, u32[]{:S(2)}) async-start(bf16[32,8,256]{2,1,0:T(8,128)(2,1)} %fusion.1), calls=%async_computation.4 | async-start | bytes 262144 | tf_op jit(solution)/shard_map/all_to_all | solution.py:53
  116.4 1.0 copy.29
  117.4 12.9 %reshape.92 = bf16[16,294912]{1,0:T(8,128)(2,1)} reshape(bf16[4718592]{0:T(1024)(128)(2,1)} %all-gather.5.cloned.1.call-done) | data formatting | bytes 18874368 | tf_op jit(solution)/shard_map/all_gather | solution.py:25
  130.4 3.7 slice.17
  134.1 6.4 %slice_bitcast_fusion = bf16[2,8,1536,128]{3,1,2,0:T(8,128)(2,1)} fusion(bf16[16,294912]{1,0:T(8,128)(2,1)} %reshape.92), kind=kLoop, calls=%fused_computation | loop fusion | bytes 12582912
  140.6 8.8 %reshape.84 = bf16[16,1536,64]{2,1,0:T(8,128)(2,1)} reshape(bf16[16,98304]{1,0:T(8,128)(2,1)} %slice.17) | data formatting | bytes 6291456 | tf_op jit(solution)/shard_map/reshape | solution.py:27
  149.4 6.8 %copy.30 = bf16[1536,16,64]{0,2,1:T(8,128)(2,1)} copy(bf16[1536,16,64]{2,0,1:T(8,128)(2,1)} %bitcast.60) | data formatting | bytes 6291456 | tf_op jit(solution)/shard_map/transpose | solution.py:18
  156.2 3.1 fusion.23
  159.2 0.7 copy-done.1
  159.9 3.8 copy.32
  163.7 8.7 %copy.28 = bf16[1536,16,128]{0,2,1:T(8,128)(2,1)} copy(bf16[1536,16,128]{2,0,1:T(8,128)(2,1)} %bitcast.61) | data formatting | bytes 12582912 | tf_op jit(solution)/shard_map/transpose | solution.py:18
  172.8 1.0 fusion.5
  173.9 0.7 broadcast_in_dim.23
  174.5 12.2 %all-to-all-start.11 = ((bf16[32,8,256]{2,1,0:T(8,128)(2,1)}), bf16[32,8,256]{2,1,0:T(8,128)(2,1)S(1)}, u32[]{:S(2)}, u32[]{:S(2)}) async-start(bf16[32,8,256]{2,1,0:T(8,128)(2,1)} %broadcast_in_dim.23), calls=%async_computation.11 | async-start | bytes 262144 | tf_op jit(solution)/shard_map/all_to_all | solution.py:35
  186.7 4.9 %fusion.22 = f32[1536,256]{1,0:T(8,128)S(1)} fusion(bf16[1536,2048]{0,1:T(8,128)(2,1)} %bitcast.62, bf16[2048,256]{1,0:T(8,128)(2,1)} %bitcast.64), kind=kOutput, calls=%fused_computation.45 | convolution fusion | flops 1610612736 | bytes 8912896 | tf_op jit(solution)/shard_map/dot_general | solution.py:120
  191.6 11.0 %all-to-all-done.11 = bf16[32,8,256]{2,1,0:T(8,128)(2,1)S(1)} async-done(((bf16[32,8,256]{2,1,0:T(8,128)(2,1)}), bf16[32,8,256]{2,1,0:T(8,128)(2,1)S(1)}, u32[]{:S(2)}, u32[]{:S(2)}) %all-to-all-start.11) | async-done | bytes 131104 | tf_op jit(solution)/shard_map/all_to_all | solution.py:35
  202.6 5.1 %all-to-all-start.8 = ((bf16[32,8,128]{2,1,0:T(8,128)(2,1)}), bf16[32,8,128]{2,1,0:T(8,128)(2,1)S(1)}, u32[]{:S(2)}, u32[]{:S(2)}) async-start(bf16[32,8,128]{2,1,0:T(8,128)(2,1)} %fusion.5), calls=%async_computation.8 | async-start | bytes 131072 | tf_op jit(solution)/shard_map/all_to_all | solution.py:53
  208.1 1.1 fusion.3
  209.2 11.5 %all-to-all-done.8 = bf16[32,8,128]{2,1,0:T(8,128)(2,1)S(1)} async-done(((bf16[32,8,128]{2,1,0:T(8,128)(2,1)}), bf16[32,8,128]{2,1,0:T(8,128)(2,1)S(1)}, u32[]{:S(2)}, u32[]{:S(2)}) %all-to-all-start.8) | async-done | bytes 65568 | tf_op jit(solution)/shard_map/all_to_all | solution.py:53
  220.7 5.2 %all-to-all-start.2 = ((bf16[32,8,256]{2,1,0:T(8,128)(2,1)}), bf16[32,8,256]{2,1,0:T(8,128)(2,1)S(1)}, u32[]{:S(2)}, u32[]{:S(2)}) async-start(bf16[32,8,256]{2,1,0:T(8,128)(2,1)} %fusion.3), calls=%async_computation.2 | async-start | bytes 262144 | tf_op jit(solution)/shard_map/all_to_all | solution.py:53
  225.9 16.2 %all-to-all-done.2 = bf16[32,8,256]{2,1,0:T(8,128)(2,1)S(1)} async-done(((bf16[32,8,256]{2,1,0:T(8,128)(2,1)}), bf16[32,8,256]{2,1,0:T(8,128)(2,1)S(1)}, u32[]{:S(2)}, u32[]{:S(2)}) %all-to-all-start.2) | async-done | bytes 131104 | tf_op jit(solution)/shard_map/all_to_all | solution.py:53
  242.7 4.8 %all-to-all-start.9 = ((bf16[32,8,128]{2,1,0:T(8,128)(2,1)}), bf16[32,8,128]{2,1,0:T(8,128)(2,1)S(1)}, u32[]{:S(2)}, u32[]{:S(2)}) async-start(bf16[32,8,128]{2,1,0:T(8,128)(2,1)} %broadcast_in_dim.22), calls=%async_computation.9 | async-start | bytes 131072 | tf_op jit(solution)/shard_map/all_to_all | solution.py:35
  247.6 13.0 %all-to-all-done.9 = bf16[32,8,128]{2,1,0:T(8,128)(2,1)S(1)} async-done(((bf16[32,8,128]{2,1,0:T(8,128)(2,1)}), bf16[32,8,128]{2,1,0:T(8,128)(2,1)S(1)}, u32[]{:S(2)}, u32[]{:S(2)}) %all-to-all-start.9) | async-done | bytes 65568 | tf_op jit(solution)/shard_map/all_to_all | solution.py:35
  260.5 0.7 broadcast_in_dim.18
  261.2 5.2 %all-to-all-start.3 = ((bf16[32,8,256]{2,1,0:T(8,128)(2,1)}), bf16[32,8,256]{2,1,0:T(8,128)(2,1)S(1)}, u32[]{:S(2)}, u32[]{:S(2)}) async-start(bf16[32,8,256]{2,1,0:T(8,128)(2,1)} %broadcast_in_dim.18), calls=%async_computation.3 | async-start | bytes 262144 | tf_op jit(solution)/shard_map/all_to_all | solution.py:35
  266.4 16.1 %all-to-all-done.3 = bf16[32,8,256]{2,1,0:T(8,128)(2,1)S(1)} async-done(((bf16[32,8,256]{2,1,0:T(8,128)(2,1)}), bf16[32,8,256]{2,1,0:T(8,128)(2,1)S(1)}, u32[]{:S(2)}, u32[]{:S(2)}) %all-to-all-start.3) | async-done | bytes 131104 | tf_op jit(solution)/shard_map/all_to_all | solution.py:35
  282.6 0.7 broadcast_in_dim.19
  283.3 4.8 %all-to-all-start.5 = ((bf16[32,8,256]{2,1,0:T(8,128)(2,1)}), bf16[32,8,256]{2,1,0:T(8,128)(2,1)S(1)}, u32[]{:S(2)}, u32[]{:S(2)}) async-start(bf16[32,8,256]{2,1,0:T(8,128)(2,1)} %broadcast_in_dim.19), calls=%async_computation.5 | async-start | bytes 262144 | tf_op jit(solution)/shard_map/all_to_all | solution.py:35
  288.2 0.9 fusion.9
  289.3 15.0 %all-to-all-done.5 = bf16[32,8,256]{2,1,0:T(8,128)(2,1)S(1)} async-done(((bf16[32,8,256]{2,1,0:T(8,128)(2,1)}), bf16[32,8,256]{2,1,0:T(8,128)(2,1)S(1)}, u32[]{:S(2)}, u32[]{:S(2)}) %all-to-all-start.5) | async-done | bytes 131104 | tf_op jit(solution)/shard_map/all_to_all | solution.py:35
  304.3 0.9 fusion.8
  305.2 9.3 %all-reduce.1 = (f32[]{:T(128)}, f32[]{:T(128)}) all-reduce(f32[]{:T(128)} %fusion.8, f32[]{:T(128)} %fusion.9), channel_id=1, replica_groups=mesh['fs_0'=16,'fs_1'=2,'tp_0'=4,'tp_1'=4] {'tp_0'}, use_global_device_ids=true, to_apply=%region_3.4 | all-reduce | flops 2 | bytes 16 | tf_op jit(solution)/shard_map/psum | solution.py:76
  314.6 9.1 %all-reduce = (f32[]{:T(128)}, f32[]{:T(128)}) all-reduce(f32[]{:T(128)} %get-tuple-element.12, f32[]{:T(128)} %get-tuple-element.13), channel_id=1, replica_groups=mesh['fs_0'=16,'fs_1'=2,'tp_0'=4,'tp_1'=4] {'tp_1'}, use_global_device_ids=true, to_apply=%region_4.5 | all-reduce | flops 2 | bytes 16 | tf_op jit(solution)/shard_map/psum | solution.py:76
  325.5 0.7 convert_bitcast_fusion
  327.5 62.8 %all-gather.7.cloned.1.call-done = bf16[655360]{0:T(1024)(128)(2,1)} async-done(((bf16[20480]{0:T(1024)(128)(2,1)}), bf16[655360]{0:T(1024)(128)(2,1)}) %all-gather.7.cloned.1.call-update) | async-done | bytes 1310736 | tf_op jit(solution)/shard_map/all_gather | solution.py:25
  390.3 1.7 reshape.93
  392.1 1.3 reshape_reshape.14
  393.4 0.8 reshape_reshape.15
  (61 shorter events, 4.4 us)
Async XLA Ops:
  7.2 200.5 %copy-start = (bf16[1536,256]{1,0:T(8,128)(2,1)S(1)}, bf16[1536,256]{1,0:T(8,128)(2,1)}, u32[]{:S(2)}) copy-start(bf16[1536,256]{1,0:T(8,128)(2,1)} %param.13) | copy-start | bytes 2359300
  7.2 3.4 copy-start.8
  7.2 110.2 %all-gather.5.cloned.1.call-start = ((), (), s32[]{:S(2)}) async-start(), calls=%async_computation.12 | async-start | bytes 10027008 | tf_op jit(solution)/shard_map/all_gather | solution.py:25
  10.6 58.9 %copy-start.7 = (bf16[64,256]{1,0:T(8,128)(2,1)S(1)}, bf16[64,256]{1,0:T(8,128)(2,1)}, u32[]{:S(2)}) copy-start(bf16[64,256]{1,0:T(8,128)(2,1)} %param.18) | copy-start | bytes 98308
  70.3 27.7 %all-to-all-start = ((bf16[16,64,256]{2,1,0:T(8,128)(2,1)}), bf16[16,64,256]{2,1,0:T(8,128)(2,1)S(1)}, u32[]{:S(2)}, u32[]{:S(2)}) async-start(bf16[16,64,256]{2,1,0:T(8,128)(2,1)} %broadcast_in_dim.16), calls=%async_computation | async-start | bytes 1048576 | tf_op jit(solution)/shard_map/all_to_all | solution.py:35
  109.5 64.4 %all-to-all-start.4 = ((bf16[32,8,256]{2,1,0:T(8,128)(2,1)}), bf16[32,8,256]{2,1,0:T(8,128)(2,1)S(1)}, u32[]{:S(2)}, u32[]{:S(2)}) async-start(bf16[32,8,256]{2,1,0:T(8,128)(2,1)} %fusion.1), calls=%async_computation.4 | async-start | bytes 262144 | tf_op jit(solution)/shard_map/all_to_all | solution.py:53
  156.2 3.7 copy-start.1
  163.7 8.7 %copy-start.4 = (bf16[1536,128]{1,0:T(8,128)(2,1)S(1)}, bf16[1536,128]{1,0:T(8,128)(2,1)}, u32[]{:S(2)}) copy-start(bf16[1536,128]{1,0:T(8,128)(2,1)} %param.15) | copy-start | bytes 1179652
  174.5 28.0 %all-to-all-start.11 = ((bf16[32,8,256]{2,1,0:T(8,128)(2,1)}), bf16[32,8,256]{2,1,0:T(8,128)(2,1)S(1)}, u32[]{:S(2)}, u32[]{:S(2)}) async-start(bf16[32,8,256]{2,1,0:T(8,128)(2,1)} %broadcast_in_dim.23), calls=%async_computation.11 | async-start | bytes 262144 | tf_op jit(solution)/shard_map/all_to_all | solution.py:35
  202.6 18.1 %all-to-all-start.8 = ((bf16[32,8,128]{2,1,0:T(8,128)(2,1)}), bf16[32,8,128]{2,1,0:T(8,128)(2,1)S(1)}, u32[]{:S(2)}, u32[]{:S(2)}) async-start(bf16[32,8,128]{2,1,0:T(8,128)(2,1)} %fusion.5), calls=%async_computation.8 | async-start | bytes 131072 | tf_op jit(solution)/shard_map/all_to_all | solution.py:53
  208.1 80.1 %copy-start.12 = (f32[256,128]{1,0:T(8,128)S(1)}, f32[256,128]{1,0:T(8,128)}, u32[]{:S(2)}) copy-start(f32[256,128]{1,0:T(8,128)} %param.23) | copy-start | bytes 393220
  208.1 80.1 %copy-start.13 = (f32[256,128]{1,0:T(8,128)S(1)}, f32[256,128]{1,0:T(8,128)}, u32[]{:S(2)}) copy-start(f32[256,128]{1,0:T(8,128)} %param.22) | copy-start | bytes 393220
  209.2 80.0 %copy-start.9 = (f32[256,256]{1,0:T(8,128)S(1)}, f32[256,256]{1,0:T(8,128)}, u32[]{:S(2)}) copy-start(f32[256,256]{1,0:T(8,128)} %param.21) | copy-start | bytes 786436
  209.2 80.0 %copy-start.10 = (f32[256,256]{1,0:T(8,128)S(1)}, f32[256,256]{1,0:T(8,128)}, u32[]{:S(2)}) copy-start(f32[256,256]{1,0:T(8,128)} %param.20) | copy-start | bytes 786436
  220.7 21.4 %all-to-all-start.2 = ((bf16[32,8,256]{2,1,0:T(8,128)(2,1)}), bf16[32,8,256]{2,1,0:T(8,128)(2,1)S(1)}, u32[]{:S(2)}, u32[]{:S(2)}) async-start(bf16[32,8,256]{2,1,0:T(8,128)(2,1)} %fusion.3), calls=%async_computation.2 | async-start | bytes 262144 | tf_op jit(solution)/shard_map/all_to_all | solution.py:53
  242.7 17.9 %all-to-all-start.9 = ((bf16[32,8,128]{2,1,0:T(8,128)(2,1)}), bf16[32,8,128]{2,1,0:T(8,128)(2,1)S(1)}, u32[]{:S(2)}, u32[]{:S(2)}) async-start(bf16[32,8,128]{2,1,0:T(8,128)(2,1)} %broadcast_in_dim.22), calls=%async_computation.9 | async-start | bytes 131072 | tf_op jit(solution)/shard_map/all_to_all | solution.py:35
  261.2 21.4 %all-to-all-start.3 = ((bf16[32,8,256]{2,1,0:T(8,128)(2,1)}), bf16[32,8,256]{2,1,0:T(8,128)(2,1)S(1)}, u32[]{:S(2)}, u32[]{:S(2)}) async-start(bf16[32,8,256]{2,1,0:T(8,128)(2,1)} %broadcast_in_dim.18), calls=%async_computation.3 | async-start | bytes 262144 | tf_op jit(solution)/shard_map/all_to_all | solution.py:35
  283.3 21.0 %all-to-all-start.5 = ((bf16[32,8,256]{2,1,0:T(8,128)(2,1)}), bf16[32,8,256]{2,1,0:T(8,128)(2,1)S(1)}, u32[]{:S(2)}, u32[]{:S(2)}) async-start(bf16[32,8,256]{2,1,0:T(8,128)(2,1)} %broadcast_in_dim.19), calls=%async_computation.5 | async-start | bytes 262144 | tf_op jit(solution)/shard_map/all_to_all | solution.py:35
  288.1 102.2 %all-gather.7.cloned.1.call-start = ((), (), s32[]{:S(2)}) async-start(), calls=%async_computation.13 | async-start | bytes 1351680 | tf_op jit(solution)/shard_map/all_gather | solution.py:25
  288.2 37.3 %copy-start.5 = (f32[256,128]{1,0:T(8,128)}, f32[256,128]{1,0:T(8,128)S(1)}, u32[]{:S(2)}) copy-start(f32[256,128]{1,0:T(8,128)S(1)} %get-tuple-element.20) | copy-start | bytes 393220
  288.2 37.3 %copy-start.6 = (f32[256,128]{1,0:T(8,128)}, f32[256,128]{1,0:T(8,128)S(1)}, u32[]{:S(2)}) copy-start(f32[256,128]{1,0:T(8,128)S(1)} %get-tuple-element.21) | copy-start | bytes 393220
  288.2 37.3 %copy-start.14 = (f32[64,256]{1,0:T(8,128)S(1)}, f32[64,256]{1,0:T(8,128)}, u32[]{:S(2)}) copy-start(f32[64,256]{1,0:T(8,128)} %param.16) | copy-start | bytes 196612
  289.1 37.1 %copy-start.16 = (f32[32,128]{1,0:T(8,128)S(1)}, f32[32,128]{1,0:T(8,128)}, u32[]{:S(2)}) copy-start(f32[32,128]{1,0:T(8,128)} %param.17) | copy-start | bytes 49156
  289.2 38.3 %copy-start.3 = (f32[256,256]{1,0:T(8,128)}, f32[256,256]{1,0:T(8,128)S(1)}, u32[]{:S(2)}) copy-start(f32[256,256]{1,0:T(8,128)S(1)} %get-tuple-element.19) | copy-start | bytes 786436
  289.2 102.7 %copy-start.2 = (f32[256,256]{1,0:T(8,128)}, f32[256,256]{1,0:T(8,128)S(1)}, u32[]{:S(2)}) copy-start(f32[256,256]{1,0:T(8,128)S(1)} %get-tuple-element.18) | copy-start | bytes 786436
  324.5 65.8 %copy-start.15 = (f32[32,128]{1,0:T(8,128)}, f32[32,128]{1,0:T(8,128)S(1)}, u32[]{:S(2)}) copy-start(f32[32,128]{1,0:T(8,128)S(1)} %fusion.7) | copy-start | bytes 49156
  325.5 64.7 %copy-start.11 = (f32[64,256]{1,0:T(8,128)}, f32[64,256]{1,0:T(8,128)S(1)}, u32[]{:S(2)}) copy-start(f32[64,256]{1,0:T(8,128)S(1)} %fusion.6) | copy-start | bytes 196612
Sparse Core Ops, SparseCore 0:
  11.0 95.9 all-gather.4
  327.6 62.6 all-gather.6
where the time goes:
time: 402 us; the launch traced here: 401 us
  waiting for transfers between devices  167 us (42%)
  blocking collectives  88.3 us (22%)
  local copies, waits for them, and re-layouts  62 us (15%)
  starting transfers between devices  49.2 us (12%)
  between operations  15.8 us (4%)
  matrix products  14.2 us (4%)
    all_to_all x5, waiting for transfers between devices, from_everyone(): lax.all_to_all(jnp.broadcast_to(value[None], (devices, *value.shape)), ax...  76.9 us
    all_gather x2, waiting for transfers between devices, gather_packed(): lines, at, done = (lax.all_gather(ravelled, axis), 0, [])  62.8 us
    all_to_all x3, blocking collectives, from_everyone(): lax.all_to_all(jnp.broadcast_to(value[None], (devices, *value.shape)), ax...  37.5 us
    all_to_all x1, blocking collectives, summed_on_arrival(): lax.all_to_all(pieces, axis, split_axis=0, concat_axis=0, tiled=True)  32.4 us
    all_to_all x5, starting transfers between devices, from_everyone(): lax.all_to_all(jnp.broadcast_to(value[None], (devices, *value.shape)), ax...  32 us
    all_to_all x3, waiting for transfers between devices, summed_on_arrival(): lax.all_to_all(pieces, axis, split_axis=0, concat_axis=0, tiled=True)  27.7 us
    psum x2, blocking collectives, by_axis(): value = lax.psum(value, axis)  18.4 us
    all_to_all x3, starting transfers between devices, summed_on_arrival(): lax.all_to_all(pieces, axis, split_axis=0, concat_axis=0, tiled=True)  17.1 us
  transfers between devices with their start and end apart: 10, of which 8 were waited for; matrix products, arithmetic and copies ran while one was open for 17% of the time, Pallas kernels for 0%

commit v1 on v0

v1 whole, which is shorter than its diff:
```python
import jax
import jax.numpy as jnp
from jax import lax
from jax.sharding import Mesh
from jax.sharding import PartitionSpec as P


TP = ("y", "x")
FS = ("zh", "zl", "c")
PLANE = ("c", "y", "x")
ALL = ("zh", "zl", "c", "y", "x")

LEARN_RATE = 0.01
MEAN_DECAY = 0.8
BETA_SQUARE = 0.9
EPS_RMS = 1e-06

BF = jnp.bfloat16
F32 = jnp.float32


def exchange(value, axes):
    return lax.all_to_all(value, axes, 0, 0, tiled=True)


def from_everyone(value, axes):
    devices = lax.axis_size(axes)
    return exchange(jnp.broadcast_to(value[None], (devices, *value.shape)), axes)


def swapped_blocks(value):
    pairs = []
    for j in range(16):
        for b in range(2):
            for t in range(16):
                pairs.append(((2 * j + b) * 16 + t, (2 * t + b) * 16 + j))
    return lax.ppermute(value, ALL, pairs)


def moments(proj, mean_in, square_in):
    mean_new = MEAN_DECAY * mean_in + (1.0 - MEAN_DECAY) * proj
    square_new = BETA_SQUARE * square_in + (1.0 - BETA_SQUARE) * proj * proj
    return (mean_new, square_new, mean_new / jnp.sqrt(square_new))


def split_dot(basis, direction):
    upper = direction.astype(BF)
    lower = (direction - upper.astype(F32)).astype(BF)
    return jnp.dot(basis, upper, preferred_element_type=F32) + jnp.dot(
        basis, lower, preferred_element_type=F32
    )


def per_device(
    attn_out,
    out_cot,
    latent,
    value_cot,
    out_weight,
    value_up_matrix,
    out_basis,
    value_basis,
    out_mean,
    out_square,
    value_mean,
    value_square,
):
    tokens, heads = attn_out.shape
    lat = latent.shape[1]
    cols_o = out_cot.shape[1]
    cols_v = value_cot.shape[1]
    rows_o, rank = out_basis.shape
    rows_v = value_basis.shape[0]
    tp = lax.axis_size(TP)
    fs = lax.axis_size(FS)
    mine = tokens // tp

    early_o, early_v = lax.optimization_barrier((out_weight, value_up_matrix))
    w_o = early_o.astype(BF).reshape(-1, 128)
    w_v = early_v.astype(BF)
    packed = lax.optimization_barrier(jnp.concatenate([w_o, w_v], 0))
    held = lax.all_gather(packed, FS)

    block = jnp.concatenate([out_basis, value_basis], 0)
    block = swapped_blocks(block)

    lat3 = latent.reshape(tp, 2, mine // 2, lat)
    lat_packed = jnp.concatenate([lat3[:, 0], lat3[:, 1]], -1)
    sent = jnp.concatenate([attn_out.reshape(tp, mine, heads), lat_packed], 1)
    got = exchange(sent, TP)

    blocks = from_everyone(block, PLANE).reshape(2, tp, rows_o + rows_v, rank)
    whole_o = blocks[:, :, :rows_o].swapaxes(0, 1).reshape(-1, rank)
    whole_v = blocks[:, :, rows_o:].swapaxes(0, 1).reshape(-1, rank)

    heads_all = got[:, :mine].swapaxes(0, 1).reshape(mine, -1)
    lat_got = got[:, mine:]
    lat_all = jnp.concatenate(
        [
            lat_got[:, :, :lat].swapaxes(0, 1).reshape(mine // 2, -1),
            lat_got[:, :, lat:].swapaxes(0, 1).reshape(mine // 2, -1),
        ],
        0,
    )
    lifted_o = jnp.dot(heads_all, whole_o, preferred_element_type=F32)
    lifted_v = jnp.dot(lat_all, whole_v, preferred_element_type=F32)
    lifted = jnp.concatenate([lifted_o.astype(BF), lifted_v.astype(BF)], 1)
    lifted = from_everyone(lifted, TP).reshape(tokens, 2 * rank)

    part_o = jnp.dot(lifted[:, :rank].T, out_cot, preferred_element_type=F32)
    part_v = jnp.dot(lifted[:, rank:].T, value_cot, preferred_element_type=F32)
    part = jnp.concatenate([part_o.astype(BF), part_v.astype(BF)], 1)
    near = lax.axis_size(("zl", "c"))
    part = exchange(part.reshape(near, rank // near, -1), ("zl", "c"))
    part = part.astype(F32).sum(0)
    part = from_everyone(part, "zh").sum(0)
    proj = from_everyone(part.astype(BF), ("zl", "c")).reshape(rank, -1).astype(F32)

    mean_o, square_o, direction_o = moments(proj[:, :cols_o], out_mean, out_square)
    mean_v, square_v, direction_v = moments(proj[:, cols_o:], value_mean, value_square)
    update_o = jnp.dot(whole_o, direction_o.astype(BF), preferred_element_type=F32)
    update_v = jnp.dot(whole_v, direction_v.astype(BF), preferred_element_type=F32)
    totals = jnp.stack([jnp.sum(update_o * update_o), jnp.sum(update_v * update_v)])
    totals = jnp.broadcast_to(totals[:, None], (2, 128))
    totals = from_everyone(totals, TP).sum(0)
    count_o = rows_o * fs * cols_o * tp
    count_v = rows_v * fs * cols_v * tp
    scale_o = LEARN_RATE * lax.rsqrt(totals[0, 0] / count_o + EPS_RMS)
    scale_v = LEARN_RATE * lax.rsqrt(totals[1, 0] / count_v + EPS_RMS)
    step_o = split_dot(out_basis, direction_o) * scale_o
    step_v = split_dot(value_basis, direction_v) * scale_v
    new_o = out_weight - step_o
    new_v = value_up_matrix - step_v

    split = w_o.shape[0]
    held_o = held[:, :split].reshape(rows_o * fs, cols_o)
    held_v = held[:, split:].reshape(rows_v * fs, cols_v)
    copy_o = (held_o.astype(F32) - scale_o * update_o).astype(BF)
    copy_v = (held_v.astype(F32) - scale_v * update_v).astype(BF)
    return (step_o, new_o, copy_o, mean_o, square_o, step_v, new_v, copy_v, mean_v, square_v)


def solution(mesh):
    torus = Mesh(mesh.devices.reshape(4, 4, 2, 4, 4), ALL)
    both = P(FS, TP)
    cols = P(None, TP)
    rows = P(FS, None)

    return jax.shard_map(
        per_device,
        mesh=torus,
        in_specs=(both, both, both, both, both, both, rows, rows, cols, cols, cols, cols),
        out_specs=(both, both, cols, cols, cols, both, both, cols, cols, cols),
        check_vma=False,
    )
```

time: 402 us -> 202 us (0.50)
  waiting for transfers between devices: 167 us -> 67.1 us
  blocking collectives: 88.3 us -> 38.2 us
  local copies, waits for them, and re-layouts: 62 us -> 12.8 us
  other arithmetic: 4.02 us -> 11.8 us
  matrix products: 14.2 us -> 10.1 us
    all_gather x2 -> x1, waiting for transfers between devices: 62.8 us -> 9.35 us  [per_device(): held = lax.all_gather(packed, FS)]
    all_to_all x8 -> x5, waiting for transfers between devices: 105 us -> 57.7 us  [exchange(): return lax.all_to_all(value, axes, 0, 0, tiled=True)]
    all_to_all x4 -> x2, blocking collectives: 69.9 us -> 38.2 us  [exchange(): return lax.all_to_all(value, axes, 0, 0, tiled=True)]
    psum x2 -> x0, blocking collectives: 18.4 us -> none  [by_axis(): value = lax.psum(value, axis)]
    transpose x2 -> x7, local copies, waits for them, and re-layouts: 15.5 us -> 0.47 us  [the longest x2 0.18 us: per_device(): whole_o = blocks[:, :, :rows_o].swapaxes(0, 1).reshape(-1, rank)]
    all_gather x2 -> x0, local copies, waits for them, and re-layouts: 14.6 us -> none  [gather_packed(): lines, at, done = (lax.all_gather(ravelled, axis), 0, [])]
    unnamed x38, local copies, waits for them, and re-layouts: 12.2 us -> 0.48 us
    convert_element_type x0 -> x6, other arithmetic: none -> 7.63 us  [the longest x2 5.78 us: per_device(): copy_o = (held_o.astype(F32) - scale_o * update_o).astype(BF)]
  transfers between devices with their start and end apart: 10 -> 7, of which waited for: 8 -> 5; matrix products, arithmetic and copies ran while one was open for 17% -> 5% of each run, Pallas kernels for 0% -> 0%
where the time goes in v1:
time: 202 us; the launch traced here: 201 us
  waiting for transfers between devices  67.1 us (33%)
  starting transfers between devices  45.6 us (23%)
  blocking collectives  38.2 us (19%)
  between operations  15.8 us (8%)
  local copies, waits for them, and re-layouts  12.8 us (6%)
  other arithmetic  11.8 us (6%)
  matrix products  10.1 us (5%)
    all_to_all x5, waiting for transfers between devices, exchange(): return lax.all_to_all(value, axes, 0, 0, tiled=True)  57.7 us
    all_to_all x5, starting transfers between devices, exchange(): return lax.all_to_all(value, axes, 0, 0, tiled=True)  44.9 us
    all_to_all x2, blocking collectives, exchange(): return lax.all_to_all(value, axes, 0, 0, tiled=True)  38.2 us
    all_gather x1, waiting for transfers between devices, per_device(): held = lax.all_gather(packed, FS)  9.35 us
    convert_element_type x2, other arithmetic, per_device(): copy_o = (held_o.astype(F32) - scale_o * update_o).astype(BF)  5.78 us
  transfers between devices with their start and end apart: 7, of which 5 were waited for; matrix products, arithmetic and copies ran while one was open for 5% of the time, Pallas kernels for 0%

profile of v1, /device:TPU:1, one launch (start us, length us, event | category | flops | bytes accessed | tf_op | source)
XLA Modules:
  0.0 201.3 jit_solution(14610107357451122183)
XLA Ops:
  7.2 1.5 reshape.83
  8.7 0.7 fusion.27
  9.5 0.4 copy.52
  9.9 0.4 copy.53
  10.4 0.9 maximum_maximum_fusion
  11.3 7.6 %all-to-all-start = ((bf16[16,144,128]{2,1,0:T(8,128)(2,1)}), bf16[16,144,128]{2,1,0:T(8,128)(2,1)S(1)}, u32[]{:S(2)}, u32[]{:S(2)}) async-start(bf16[16,144,128]{2,1,0:T(8,128)(2,1)} %maximum_maximum_fusion), calls=%async_computation | async-start | bytes 1179648 | tf_op jit(solution)/shard_map/all_to_all | solution.py:23
  19.0 0.7 collective-permute-start
  19.6 8.9 %all-to-all-done = bf16[16,144,128]{2,1,0:T(8,128)(2,1)S(1)} async-done(((bf16[16,144,128]{2,1,0:T(8,128)(2,1)}), bf16[16,144,128]{2,1,0:T(8,128)(2,1)S(1)}, u32[]{:S(2)}, u32[]{:S(2)}) %all-to-all-start) | async-done | bytes 589856 | tf_op jit(solution)/shard_map/all_to_all | solution.py:23
  28.6 1.4 broadcast_in_dim.8
  29.9 18.6 %all-to-all-start.1 = ((bf16[32,96,256]{2,1,0:T(8,128)(2,1)}), bf16[32,96,256]{2,1,0:T(8,128)(2,1)S(1)}, u32[]{:S(2)}, u32[]{:S(2)}) async-start(bf16[32,96,256]{2,1,0:T(8,128)(2,1)} %broadcast_in_dim.8), calls=%async_computation.1 | async-start | bytes 3145728 | tf_op jit(solution)/shard_map/all_to_all | solution.py:23
  48.5 0.1 slice_bitcast_fusion.4
  48.7 0.2 reshape.87
  49.0 0.2 reshape.88
  49.1 21.8 %all-to-all-done.1 = bf16[32,96,256]{2,1,0:T(8,128)(2,1)S(1)} async-done(((bf16[32,96,256]{2,1,0:T(8,128)(2,1)}), bf16[32,96,256]{2,1,0:T(8,128)(2,1)S(1)}, u32[]{:S(2)}, u32[]{:S(2)}) %all-to-all-start.1) | async-done | bytes 1572896 | tf_op jit(solution)/shard_map/all_to_all | solution.py:23
  71.1 0.1 copy.55
  71.2 0.2 convolution_convert_fusion.3
  71.5 0.3 convolution_convert_fusion.2
  71.8 0.4 copy-done.1
  72.2 1.3 broadcast_in_dim.9
  73.5 3.8 %all-to-all-start.2 = ((bf16[16,96,512]{2,1,0:T(8,128)(2,1)}), bf16[16,96,512]{2,1,0:T(8,128)(2,1)S(1)}, u32[]{:S(2)}, u32[]{:S(2)}) async-start(bf16[16,96,512]{2,1,0:T(8,128)(2,1)} %broadcast_in_dim.9), calls=%async_computation.2 | async-start | bytes 3145728 | tf_op jit(solution)/shard_map/all_to_all | solution.py:23
  77.5 0.6 pad_maximum_fusion.3
  78.1 21.6 %all-to-all-done.2 = bf16[16,96,512]{2,1,0:T(8,128)(2,1)S(1)} async-done(((bf16[16,96,512]{2,1,0:T(8,128)(2,1)}), bf16[16,96,512]{2,1,0:T(8,128)(2,1)S(1)}, u32[]{:S(2)}, u32[]{:S(2)}) %all-to-all-start.2) | async-done | bytes 1572896 | tf_op jit(solution)/shard_map/all_to_all | solution.py:23
  99.7 0.3 convolution_convert_fusion.1
  100.0 0.4 convolution_convert_fusion
  100.5 0.2 copy.59
  100.6 12.6 %all_to_all.35 = bf16[8,32,384]{2,1,0:T(8,128)(2,1)S(1)} all-to-all(bf16[8,32,384]{2,1,0:T(8,128)(2,1)S(1)} %bitcast.61), channel_id=1, replica_groups=mesh['zh'=4,'zl'=4,'c'=2,'y'=4,'x'=4] {'zl','c'}, dimensions={0} | all-to-all | bytes 393216 | tf_op jit(solution)/shard_map/all_to_all | solution.py:23
  113.3 25.5 %all_to_all.36 = f32[4,32,384]{2,1,0:T(8,128)S(1)} all-to-all(f32[4,32,384]{2,1,0:T(8,128)S(1)} %broadcast_in_dim.10), channel_id=1, replica_groups=mesh['zh'=4,'zl'=4,'c'=2,'y'=4,'x'=4] {'zh'}, dimensions={0} | all-to-all | bytes 393216 | tf_op jit(solution)/shard_map/all_to_all | solution.py:23
  138.9 0.7 broadcast_in_dim.11
  139.6 8.4 %all-to-all-start.5 = ((bf16[8,32,384]{2,1,0:T(8,128)(2,1)}), bf16[8,32,384]{2,1,0:T(8,128)(2,1)}, u32[]{:S(2)}, u32[]{:S(2)}) async-start(bf16[8,32,384]{2,1,0:T(8,128)(2,1)} %broadcast_in_dim.11), calls=%async_computation.5 | async-start | bytes 393216 | tf_op jit(solution)/shard_map/all_to_all | solution.py:23
  148.0 9.3 %all-gather.3.cloned.1.call-done = bf16[5120,128]{1,0:T(8,128)(2,1)} async-done(((bf16[160,128]{1,0:T(8,128)(2,1)}), bf16[5120,128]{1,0:T(8,128)(2,1)}) %all-gather.3.cloned.1.call-update) | async-done | bytes 1310736 | tf_op jit(solution)/shard_map/all_gather | solution.py:82
  157.4 1.7 slice.75
  159.0 2.8 %slice_convert_fusion = f32[32,128,128]{2,1,0:T(8,128)} fusion(bf16[32,160,128]{2,1,0:T(8,128)(2,1)} %bitcast.60), kind=kLoop, calls=%fused_computation.12 | loop fusion | flops 524288 | bytes 3145728 | tf_op jit(solution)/shard_map/convert_element_type | solution.py:138
  161.8 1.9 reshape.94
  163.7 1.0 bitcast_convert_fusion
  164.8 1.1 fusion.9
  165.9 0.8 fusion.25
  166.8 2.6 %multiply_reduce_fusion = (f32[]{:T(128)}, f32[2048,256]{1,0:T(8,128)}) fusion(bf16[2048,256]{1,0:T(8,128)(2,1)S(1)} %bitcast.56, f32[256,256]{1,0:T(8,128)S(1)} %get-tuple-element.21, f32[256,256]{1,0:T(8,128)S(1)} %get-tuple-element.20), kind=kOutput, calls=%fused_computation.1 | convolution fusion | flops 269615104 | bytes 3670020 | tf_op jit(solution)/shard_map/dot_general | solution.py:121
  169.4 1.7 multiply_reduce_fusion.1
  171.1 1.4 pad_maximum_fusion.4
  172.5 0.7 broadcast_in_dim_broadcast_in_dim_broadcast_in_dim.2
  173.2 6.4 %all-to-all-start.6 = ((f32[16,2,128]{2,1,0:T(2,128)}), f32[16,2,128]{2,1,0:T(2,128)S(1)}, u32[]{:S(2)}, u32[]{:S(2)}) async-start(f32[16,2,128]{2,1,0:T(2,128)} %broadcast_in_dim_broadcast_in_dim_broadcast_in_dim.2), calls=%async_computation.6 | async-start | bytes 32768 | tf_op jit(solution)/shard_map/all_to_all | solution.py:23
  179.6 1.0 fusion.18
  180.6 5.4 %all-to-all-done.6 = f32[16,2,128]{2,1,0:T(2,128)S(1)} async-done(((f32[16,2,128]{2,1,0:T(2,128)}), f32[16,2,128]{2,1,0:T(2,128)S(1)}, u32[]{:S(2)}, u32[]{:S(2)}) %all-to-all-start.6) | async-done | bytes 16416 | tf_op jit(solution)/shard_map/all_to_all | solution.py:23
  186.1 0.5 fusion.28
  188.0 1.9 fusion.29
  189.9 3.0 %subtract_convert_fusion = bf16[2048,256]{1,0:T(8,128)(2,1)} fusion(f32[2048,256]{1,0:T(8,128)S(1)} %reshape.94, f32[2048,256]{1,0:T(8,128)} %get-tuple-element.27, f32[]{:T(128)} %bitcast.17), kind=kLoop, calls=%fused_computation | loop fusion | flops 1572864 | bytes 5242884 | tf_op jit(solution)/shard_map/convert_element_type | solution.py:138
  192.9 0.8 fusion.30
  193.7 0.8 fusion.6
  (57 shorter events, 0.6 us)
Async XLA Ops:
  7.2 92.8 %copy-start = (bf16[1536,256]{1,0:T(8,128)(2,1)S(1)}, bf16[1536,256]{1,0:T(8,128)(2,1)}, u32[]{:S(2)}) copy-start(bf16[1536,256]{1,0:T(8,128)(2,1)} %param.13) | copy-start | bytes 2359300
  8.7 1.7 copy-start.10
  9.9 9.0 %copy-start.11 = (bf16[64,256]{1,0:T(8,128)(2,1)S(1)}, bf16[64,256]{1,0:T(8,128)(2,1)}, u32[]{:S(2)}) copy-start(bf16[64,256]{1,0:T(8,128)(2,1)} %param.18) | copy-start | bytes 98308
  9.9 9.0 %copy-start.13 = (bf16[32,256]{1,0:T(8,128)(2,1)S(1)}, bf16[32,256]{1,0:T(8,128)(2,1)}, u32[]{:S(2)}) copy-start(bf16[32,256]{1,0:T(8,128)(2,1)} %param.19) | copy-start | bytes 49156
  11.3 17.2 %all-to-all-start = ((bf16[16,144,128]{2,1,0:T(8,128)(2,1)}), bf16[16,144,128]{2,1,0:T(8,128)(2,1)S(1)}, u32[]{:S(2)}, u32[]{:S(2)}) async-start(bf16[16,144,128]{2,1,0:T(8,128)(2,1)} %maximum_maximum_fusion), calls=%async_computation | async-start | bytes 1179648 | tf_op jit(solution)/shard_map/all_to_all | solution.py:23
  19.0 0.7 collective-permute-start
  29.9 41.0 %all-to-all-start.1 = ((bf16[32,96,256]{2,1,0:T(8,128)(2,1)}), bf16[32,96,256]{2,1,0:T(8,128)(2,1)S(1)}, u32[]{:S(2)}, u32[]{:S(2)}) async-start(bf16[32,96,256]{2,1,0:T(8,128)(2,1)} %broadcast_in_dim.8), calls=%async_computation.1 | async-start | bytes 3145728 | tf_op jit(solution)/shard_map/all_to_all | solution.py:23
  71.2 1.0 copy-start.1
  73.5 3.9 %copy-start.16 = (f32[32,128]{1,0:T(8,128)S(1)}, f32[32,128]{1,0:T(8,128)}, u32[]{:S(2)}) copy-start(f32[32,128]{1,0:T(8,128)} %param.17) | copy-start | bytes 49156
  73.5 3.9 %copy-start.12 = (f32[64,256]{1,0:T(8,128)S(1)}, f32[64,256]{1,0:T(8,128)}, u32[]{:S(2)}) copy-start(f32[64,256]{1,0:T(8,128)} %param.16) | copy-start | bytes 196612
  73.5 26.2 %copy-start.18 = (bf16[1536,128]{1,0:T(8,128)(2,1)S(1)}, bf16[1536,128]{1,0:T(8,128)(2,1)}, u32[]{:S(2)}) copy-start(bf16[1536,128]{1,0:T(8,128)(2,1)} %param.15) | copy-start | bytes 1179652
  73.5 26.2 %all-to-all-start.2 = ((bf16[16,96,512]{2,1,0:T(8,128)(2,1)}), bf16[16,96,512]{2,1,0:T(8,128)(2,1)S(1)}, u32[]{:S(2)}, u32[]{:S(2)}) async-start(bf16[16,96,512]{2,1,0:T(8,128)(2,1)} %broadcast_in_dim.9), calls=%async_computation.2 | async-start | bytes 3145728 | tf_op jit(solution)/shard_map/all_to_all | solution.py:23
  77.3 80.0 %all-gather.3.cloned.1.call-start = ((), (), s32[]{:S(2)}) async-start(), calls=%async_computation.7 | async-start | bytes 1351680 | tf_op jit(solution)/shard_map/all_gather | solution.py:82
  139.6 24.1 %all-to-all-start.5 = ((bf16[8,32,384]{2,1,0:T(8,128)(2,1)}), bf16[8,32,384]{2,1,0:T(8,128)(2,1)}, u32[]{:S(2)}, u32[]{:S(2)}) async-start(bf16[8,32,384]{2,1,0:T(8,128)(2,1)} %broadcast_in_dim.11), calls=%async_computation.5 | async-start | bytes 393216 | tf_op jit(solution)/shard_map/all_to_all | solution.py:23
  163.7 3.0 %copy-start.2 = (bf16[16,2,64,256]{3,2,1,0:T(8,128)(2,1)S(1)}, bf16[16,2,64,256]{3,2,1,0:T(8,128)(2,1)}, u32[]{:S(2)}) copy-start(bf16[16,2,64,256]{3,2,1,0:T(8,128)(2,1)} %copy-done.1) | copy-start | bytes 3145732
  165.9 3.4 %copy-start.3 = (f32[256,256]{1,0:T(8,128)}, f32[256,256]{1,0:T(8,128)S(1)}, u32[]{:S(2)}) copy-start(f32[256,256]{1,0:T(8,128)S(1)} %get-tuple-element.20) | copy-start | bytes 786436
  165.9 3.4 %copy-start.4 = (f32[256,256]{1,0:T(8,128)}, f32[256,256]{1,0:T(8,128)S(1)}, u32[]{:S(2)}) copy-start(f32[256,256]{1,0:T(8,128)S(1)} %get-tuple-element.21) | copy-start | bytes 786436
  166.7 2.6 %copy-start.14 = (f32[256,128]{1,0:T(8,128)S(1)}, f32[256,128]{1,0:T(8,128)}, u32[]{:S(2)}) copy-start(f32[256,128]{1,0:T(8,128)} %param.23) | copy-start | bytes 393220
  166.7 2.6 %copy-start.15 = (f32[256,128]{1,0:T(8,128)S(1)}, f32[256,128]{1,0:T(8,128)}, u32[]{:S(2)}) copy-start(f32[256,128]{1,0:T(8,128)} %param.22) | copy-start | bytes 393220
  169.4 1.7 copy-start.6
  169.4 23.5 %copy-start.5 = (f32[256,128]{1,0:T(8,128)}, f32[256,128]{1,0:T(8,128)S(1)}, u32[]{:S(2)}) copy-start(f32[256,128]{1,0:T(8,128)S(1)} %get-tuple-element.18) | copy-start | bytes 393220
  173.2 12.9 %all-to-all-start.6 = ((f32[16,2,128]{2,1,0:T(2,128)}), f32[16,2,128]{2,1,0:T(2,128)S(1)}, u32[]{:S(2)}, u32[]{:S(2)}) async-start(f32[16,2,128]{2,1,0:T(2,128)} %broadcast_in_dim_broadcast_in_dim_broadcast_in_dim.2), calls=%async_computation.6 | async-start | bytes 32768 | tf_op jit(solution)/shard_map/all_to_all | solution.py:23
  189.9 3.0 %copy-start.7 = (f32[256,128]{1,0:T(8,128)S(1)}, f32[256,128]{1,0:T(8,128)}, u32[]{:S(2)}) copy-start(f32[256,128]{1,0:T(8,128)} %copy-done.6) | copy-start | bytes 393220
  189.9 3.0 %copy-start.17 = (f32[32,128]{1,0:T(8,128)S(1)}, f32[32,128]{1,0:T(8,128)}, u32[]{:S(2)}) copy-start(f32[32,128]{1,0:T(8,128)} %param.17) | copy-start | bytes 49156
  189.9 3.8 %copy-start.8 = (f32[1024,128]{1,0:T(8,128)S(1)}, f32[1024,128]{1,0:T(8,128)}, u32[]{:S(2)}) copy-start(f32[1024,128]{1,0:T(8,128)} %get-tuple-element.25) | copy-start | bytes 1572868
  189.9 3.8 %copy-start.9 = (bf16[32,32,128]{2,1,0:T(8,128)(2,1)S(1)}, bf16[32,32,128]{2,1,0:T(8,128)(2,1)}, u32[]{:S(2)}) copy-start(bf16[32,32,128]{2,1,0:T(8,128)(2,1)} %slice.75) | copy-start | bytes 786436
Sparse Core Ops, SparseCore 0:
  80.9 76.4 all-gather.2

commit v2 on v1

v2 whole, which is shorter than its diff:
```python
import functools

import jax
import jax.numpy as jnp
from jax import lax
from jax.experimental import pallas as pl
from jax.experimental.pallas import tpu as pltpu
from jax.sharding import Mesh
from jax.sharding import PartitionSpec as P


TP = ("y", "x")
FS = ("zh", "zl", "c")
NEAR = ("zl", "c")
ALL = ("zh", "zl", "c", "y", "x")

LEARN_RATE = 0.01
MEAN_DECAY = 0.8
BETA_SQUARE = 0.9
EPS_RMS = 1e-06

BF = jnp.bfloat16
ROOM = 20 * 2**20
F32 = jnp.float32


def exchange(value, axes):
    return lax.all_to_all(value, axes, 0, 0, tiled=True)


def from_everyone(value, axes):
    devices = lax.axis_size(axes)
    return exchange(jnp.broadcast_to(value[None], (devices, *value.shape)), axes)


def swapped_blocks(value):
    pairs = []
    for j in range(16):
        for b in range(2):
            for t in range(16):
                pairs.append(((2 * j + b) * 16 + t, (2 * t + b) * 16 + j))
    return lax.ppermute(value, ALL, pairs)


def shifted(value, axis, by):
    devices = lax.axis_size(axis)
    return lax.ppermute(value, axis, [(i, (i + by) % devices) for i in range(devices)])


def dot(a, b):
    return jnp.dot(a, b, preferred_element_type=F32)


def pack_kernel(attn_ref, lat_ref, out_ref):
    groups = out_ref.shape[0]
    tokens = attn_ref.shape[0] // groups
    each = tokens // groups
    turned = lat_ref[...].T
    for g in range(groups):
        pieces = []
        for p in range(groups):
            at = (p * groups + g) * each
            out_ref[g, p * each : (p + 1) * each, :] = attn_ref[at : at + each, :]
            pieces.append(turned[at : at + each])
        half = groups // 2
        for p in range(half):
            at = tokens + p * each
            out_ref[g, at : at + each, :] = jnp.concatenate([pieces[p], pieces[half + p]], axis=1)


def pack(attn_out, lat_turned, groups):
    tokens, heads = attn_out.shape
    rows = tokens // groups
    return pl.pallas_call(
        pack_kernel,
        out_shape=jax.ShapeDtypeStruct((groups, rows + rows // 2, heads), BF),
        cost_estimate=pl.CostEstimate(flops=10**7, bytes_accessed=10**6, transcendentals=0),
        compiler_params=pltpu.CompilerParams(vmem_limit_bytes=ROOM),
        name="pack",
    )(attn_out, lat_turned)


def lift_kernel(rows_o, tokens, got_ref, blocks_ref, out_ref):
    groups = got_ref.shape[0]
    rank = blocks_ref.shape[2]
    half = tokens // 2
    first = jnp.zeros((tokens, rank), F32)
    second = jnp.zeros((half, 2 * rank), F32)
    for g in range(groups):
        low, high = blocks_ref[g], blocks_ref[groups + g]
        basis_o = jnp.concatenate([low[:rows_o], high[:rows_o]], 0)
        basis_v = jnp.concatenate([low[rows_o:], high[rows_o:]], 0)
        none = jnp.zeros_like(basis_v)
        pair = jnp.concatenate(
            [jnp.concatenate([basis_v, none], 0), jnp.concatenate([none, basis_v], 0)], 1
        )
        first = first + dot(got_ref[g, :tokens, :], basis_o)
        second = second + dot(got_ref[g, tokens:, :], pair)
    parts, each = out_ref.shape[:2]
    for p in range(parts):
        at = p * each
        out_ref[p, :, :rank] = first[at : at + each].astype(BF)
        row, side = at % half, at // half
        out_ref[p, :, rank:] = second[row : row + each, side * rank : (side + 1) * rank].astype(BF)


def lift(got, blocks, rows_o, tokens, parts):
    rank = blocks.shape[2]
    return pl.pallas_call(
        functools.partial(lift_kernel, rows_o, tokens),
        out_shape=jax.ShapeDtypeStruct((parts, tokens // parts, 2 * rank), BF),
        cost_estimate=pl.CostEstimate(flops=2 * 10**8, bytes_accessed=10**6, transcendentals=0),
        compiler_params=pltpu.CompilerParams(vmem_limit_bytes=ROOM),
        name="lift",
    )(got, blocks)


def spread_kernel(got_ref, out_ref):
    total = got_ref[0].astype(F32)
    for i in range(1, got_ref.shape[0]):
        total = total + got_ref[i].astype(F32)
    total = total.astype(out_ref.dtype)
    for i in range(out_ref.shape[0]):
        out_ref[i] = total


def summed_for(got, copies, kind):
    return pl.pallas_call(
        spread_kernel,
        out_shape=jax.ShapeDtypeStruct((copies, *got.shape[1:]), kind),
        cost_estimate=pl.CostEstimate(flops=10**7, bytes_accessed=10**6, transcendentals=0),
        compiler_params=pltpu.CompilerParams(vmem_limit_bytes=ROOM),
    )(got)


def direction_kernel(
    rows_o, got_ref, mean_o, square_o, mean_v, square_v, b0, b1, b2, b3,
    mean_o_out, square_o_out, mean_v_out, square_v_out, way_out, total_out,
):
    cols_o = mean_o.shape[1]
    near, _, _ = got_ref.shape
    proj = jnp.concatenate([got_ref[i] for i in range(near)], 0).astype(F32)
    ways = []
    for p, mean, square, mean_out, square_out in (
        (proj[:, :cols_o], mean_o, square_o, mean_o_out, square_o_out),
        (proj[:, cols_o:], mean_v, square_v, mean_v_out, square_v_out),
    ):
        mean_new = MEAN_DECAY * mean[...] + (1.0 - MEAN_DECAY) * p
        square_new = BETA_SQUARE * square[...] + (1.0 - BETA_SQUARE) * p * p
        mean_out[...] = mean_new
        square_out[...] = square_new
        ways.append(mean_new / jnp.sqrt(square_new))
    way_out[:, :cols_o] = ways[0]
    way_out[:, cols_o:] = ways[1]
    upper_o, upper_v = ways[0].astype(BF), ways[1].astype(BF)
    total_o = jnp.zeros((8, cols_o), F32)
    total_v = jnp.zeros((8, ways[1].shape[1]), F32)
    for ref in (b0, b1, b2, b3):
        count, _, _ = ref.shape
        basis_o = jnp.concatenate([ref[i, :rows_o, :] for i in range(count)], 0)
        basis_v = jnp.concatenate([ref[i, rows_o:, :] for i in range(count)], 0)
        update = dot(basis_o, upper_o)
        total_o = total_o + jnp.sum((update * update).reshape(-1, 8, cols_o), 0)
        update = dot(basis_v, upper_v)
        total_v = total_v + jnp.sum((update * update).reshape(-1, 8, update.shape[1]), 0)
    sums = [
        jnp.broadcast_to(jnp.sum(t, keepdims=True), (4, 128)) for t in (total_o, total_v)
    ]
    tile = jnp.concatenate(sums, 0)
    for i in range(total_out.shape[0]):
        total_out[i] = tile


def directions(rows_o, copies, got, mean_o, square_o, mean_v, square_v, segments):
    rank = mean_o.shape[0]
    shape = jax.ShapeDtypeStruct
    return pl.pallas_call(
        functools.partial(direction_kernel, rows_o),
        out_shape=(
            shape(mean_o.shape, F32),
            shape(mean_o.shape, F32),
            shape(mean_v.shape, F32),
            shape(mean_v.shape, F32),
            shape((rank, mean_o.shape[1] + mean_v.shape[1]), F32),
            shape((copies, 8, 128), F32),
        ),
        cost_estimate=pl.CostEstimate(flops=4 * 10**8, bytes_accessed=4 * 10**6, transcendentals=10**5),
        compiler_params=pltpu.CompilerParams(vmem_limit_bytes=ROOM),
        name="directions",
    )(got, mean_o, square_o, mean_v, square_v, *segments)


def output_kernel(
    rows_o, rows_v, counts, y_ref, total_ref, way_ref, weight_o, weight_v, local_o, local_v, held_ref,
    b0, b1, b2, b3,
    step_o_out, new_o_out, copy_o_out, step_v_out, new_v_out, copy_v_out,
):
    cols_o = weight_o.shape[1]
    total = total_ref[0]
    for i in range(1, total_ref.shape[0]):
        total = total + total_ref[i]
    scale = LEARN_RATE * lax.rsqrt(total[0:1, 0:1] / counts[0] + EPS_RMS)
    scale_o = scale
    scale_v = LEARN_RATE * lax.rsqrt(total[4:5, 0:1] / counts[1] + EPS_RMS)
    way_o, way_v = way_ref[:, :cols_o], way_ref[:, cols_o:]
    for way, local, scale, weight, step_out, new_out in (
        (way_o, local_o, scale_o, weight_o, step_o_out, new_o_out),
        (way_v, local_v, scale_v, weight_v, step_v_out, new_v_out),
    ):
        upper = way.astype(BF)
        lower = (way - upper.astype(F32)).astype(BF)
        step = (dot(local[...], upper) + dot(local[...], lower)) * scale
        step_out[...] = step
        new_out[...] = weight[...] - step
    scaled_o = (way_o * scale_o).astype(BF)
    scaled_v = (way_v * scale_v).astype(BF)
    y = y_ref[0]
    for k, ref in enumerate((b0, b1, b2, b3)):
        origin = lax.rem(y + 4 - k, 4)
        count = ref.shape[0]
        basis_o = jnp.concatenate([ref[i, :rows_o, :] for i in range(count)], 0)
        basis_v = jnp.concatenate([ref[i, rows_o:, :] for i in range(count)], 0)
        update_o = dot(basis_o, scaled_o)
        update_v = dot(basis_v, scaled_v)
        for i in range(count):
            c, x = divmod(i, count // 2)
            index = 8 * origin + 2 * x + c
            held = held_ref[index].astype(F32)
            old_o = jnp.concatenate([held[:rows_o], held[rows_o : 2 * rows_o]], 1)
            at = pl.multiple_of(index * rows_o, rows_o)
            copy_o_out[pl.ds(at, rows_o), :] = (old_o - update_o[i * rows_o : (i + 1) * rows_o]).astype(BF)
            at = pl.multiple_of(index * rows_v, rows_v)
            copy_v_out[pl.ds(at, rows_v), :] = (
                held[2 * rows_o :] - update_v[i * rows_v : (i + 1) * rows_v]
            ).astype(BF)


def outputs(counts, y, total, way, weight_o, weight_v, local_o, local_v, held, segments):
    rows_o, rows_v = local_o.shape[0], local_v.shape[0]
    fs = held.shape[0]
    shape = jax.ShapeDtypeStruct
    vmem = pl.BlockSpec(memory_space=pltpu.VMEM)
    return pl.pallas_call(
        functools.partial(output_kernel, rows_o, rows_v, counts),
        in_specs=[pl.BlockSpec(memory_space=pltpu.SMEM)] + [vmem] * 11,
        out_shape=(
            shape(weight_o.shape, F32),
            shape(weight_o.shape, F32),
            shape((rows_o * fs, weight_o.shape[1]), BF),
            shape(weight_v.shape, F32),
            shape(weight_v.shape, F32),
            shape((rows_v * fs, weight_v.shape[1]), BF),
        ),
        cost_estimate=pl.CostEstimate(flops=4 * 10**8, bytes_accessed=4 * 10**6, transcendentals=10),
        compiler_params=pltpu.CompilerParams(vmem_limit_bytes=ROOM),
        name="outputs",
    )(y, total, way, weight_o, weight_v, local_o, local_v, held, *segments)


def per_device(
    attn_out,
    out_cot,
    latent,
    value_cot,
    out_weight,
    value_up_matrix,
    out_basis,
    value_basis,
    out_mean,
    out_square,
    value_mean,
    value_square,
):
    tokens = attn_out.shape[0]
    cols_o = out_cot.shape[1]
    cols_v = value_cot.shape[1]
    rows_o, rank = out_basis.shape
    rows_v = value_basis.shape[0]
    tp = lax.axis_size(TP)
    fs = lax.axis_size(FS)
    xs, ys = lax.axis_size("x"), lax.axis_size("y")

    early_o, early_v = lax.optimization_barrier((out_weight, value_up_matrix))
    early_o, early_v = early_o.astype(BF), early_v.astype(BF)
    packed = jnp.concatenate([early_o[:, :128], early_o[:, 128:], early_v], 0)
    packed = lax.optimization_barrier(packed)
    held = lax.all_gather(packed, FS)

    block = swapped_blocks(jnp.concatenate([out_basis, value_basis], 0))

    sent = pack(attn_out, latent.T, xs)
    got = exchange(sent, "x")
    blocks = from_everyone(block, ("c", "x"))
    partial = lift(got, blocks, rows_o, tokens // xs, ys)
    partial = exchange(partial, "y")
    lifted = summed_for(partial, tp, BF)
    lifted = exchange(lifted, TP).reshape(tokens, 2 * rank)

    part_o = dot(lifted[:, :rank].T, out_cot)
    part_v = dot(lifted[:, rank:].T, value_cot)
    part = jnp.concatenate([part_o.astype(BF), part_v.astype(BF)], 1)
    near = lax.axis_size(NEAR)
    part = exchange(part.reshape(near, rank // near, -1), NEAR)
    part = exchange(summed_for(part, lax.axis_size("zh"), F32), "zh")
    proj = exchange(summed_for(part, near, BF), NEAR)

    segments = [blocks]
    for k in range(1, ys):
        segments.append(shifted(blocks, "y", k))

    mean_o, square_o, mean_v, square_v, way, total = directions(
        rows_o, tp, proj, out_mean, out_square, value_mean, value_square, segments
    )
    total = exchange(total, TP)
    counts = (rows_o * fs * cols_o * tp, rows_v * fs * cols_v * tp)
    y = lax.axis_index("y").astype(jnp.int32).reshape(1)
    step_o, new_o, copy_o, step_v, new_v, copy_v = outputs(
        counts, y, total, way, out_weight, value_up_matrix, out_basis, value_basis, held, segments
    )
    return (step_o, new_o, copy_o, mean_o, square_o, step_v, new_v, copy_v, mean_v, square_v)


def solution(mesh):
    torus = Mesh(mesh.devices.reshape(4, 4, 2, 4, 4), ALL)
    both = P(FS, TP)
    cols = P(None, TP)
    rows = P(FS, None)

    return jax.shard_map(
        per_device,
        mesh=torus,
        in_specs=(both, both, both, both, both, both, rows, rows, cols, cols, cols, cols),
        out_specs=(both, both, cols, cols, cols, both, both, cols, cols, cols),
        check_vma=False,
    )
```

time: 202 us -> 193 us (0.955)
  blocking collectives: 38.2 us -> 72.4 us
  waiting for transfers between devices: 67.1 us -> 48.1 us
  other arithmetic: 11.8 us -> 1.52 us
  matrix products: 10.1 us -> 0.73 us
  Pallas kernels: 0 us -> 5.99 us
  local copies, waits for them, and re-layouts: 12.8 us -> 7.13 us
  starting transfers between devices: 45.6 us -> 41.6 us
    all_to_all x2 -> x4, blocking collectives: 38.2 us -> 72.4 us  [exchange(): return lax.all_to_all(value, axes, 0, 0, tiled=True)]
    all_to_all x5 -> x4, waiting for transfers between devices: 57.7 us -> 32.1 us  [exchange(): return lax.all_to_all(value, axes, 0, 0, tiled=True)]
    ppermute x0 -> x3, waiting for transfers between devices: none -> 16 us  [shifted(): lax.ppermute(value, axis, [(i, (i + by) % devices) for i in range(devices)])]
    all_to_all x5 -> x4, starting transfers between devices: 44.9 us -> 32.5 us  [exchange(): return lax.all_to_all(value, axes, 0, 0, tiled=True)]
    dot_general x10 -> x2, matrix products: 10.1 us -> 0.73 us  [dot(): return jnp.dot(a, b, preferred_element_type=F32)]
    all_gather x1, waiting for transfers between devices: 9.35 us -> 0.02 us  [per_device(): held = lax.all_gather(packed, FS)]
    ppermute x0 -> x3, starting transfers between devices: none -> 8.4 us  [shifted(): lax.ppermute(value, axis, [(i, (i + by) % devices) for i in range(devices)])]
    convert_element_type x6 -> x2, other arithmetic: 7.63 us -> 0.01 us  [per_device(): early_o, early_v = (early_o.astype(BF), early_v.astype(BF))]
  transfers between devices with their start and end apart: 7 -> 9, of which waited for: 5 -> 5; matrix products, arithmetic and copies ran while one was open for 5% -> 1% of each run, Pallas kernels for 0% -> 1%
where the time goes in v2:
time: 193 us; the launch traced here: 192 us
  blocking collectives  72.4 us (38%)
  waiting for transfers between devices  48.1 us (25%)
  starting transfers between devices  41.6 us (22%)
  between operations  14.3 us (7%)
  local copies, waits for them, and re-layouts  7.13 us (4%)
  Pallas kernels  5.99 us (3%)
    all_to_all x4, blocking collectives, exchange(): return lax.all_to_all(value, axes, 0, 0, tiled=True)  72.4 us
    all_to_all x4, starting transfers between devices, exchange(): return lax.all_to_all(value, axes, 0, 0, tiled=True)  32.5 us
    all_to_all x4, waiting for transfers between devices, exchange(): return lax.all_to_all(value, axes, 0, 0, tiled=True)  32.1 us
    ppermute x3, waiting for transfers between devices, shifted(): lax.ppermute(value, axis, [(i, (i + by) % devices) for i in range(devices)])  16 us
    ppermute x3, starting transfers between devices, shifted(): lax.ppermute(value, axis, [(i, (i + by) % devices) for i in range(devices)])  8.4 us
    unnamed x28, local copies, waits for them, and re-layouts  6.19 us
  transfers between devices with their start and end apart: 9, of which 5 were waited for; matrix products, arithmetic and copies ran while one was open for 1% of the time, Pallas kernels for 1%

profile of v2, /device:TPU:1, one launch (start us, length us, event | category | flops | bytes accessed | tf_op | source)
XLA Modules:
  0.0 191.8 jit_solution(1180530193155379978)
XLA Ops:
  7.2 0.0 copy-start
  7.2 0.0 copy-start.2
  7.2 0.9 pad_maximum_fusion.1
  8.1 0.7 collective-permute-start
  8.7 0.0 collective-permute-done
  8.7 0.8 broadcast_in_dim.2
  9.5 15.3 %all-to-all-start.1 = ((bf16[8,96,256]{2,1,0:T(8,128)(2,1)}), bf16[8,96,256]{2,1,0:T(8,128)(2,1)S(1)}, u32[]{:S(2)}, u32[]{:S(2)}) async-start(bf16[8,96,256]{2,1,0:T(8,128)(2,1)} %broadcast_in_dim.2), calls=%async_computation.1 | async-start | bytes 786432 | tf_op jit(solution)/shard_map/all_to_all | solution.py:28
  24.8 0.9 copy-done.6
  25.7 0.2 pack.1
  26.0 6.8 %all-to-all-done.1.blocks_ref.b0 = bf16[8,96,256]{2,1,0:T(8,128)(2,1)S(1)} async-done(((bf16[8,96,256]{2,1,0:T(8,128)(2,1)}), bf16[8,96,256]{2,1,0:T(8,128)(2,1)S(1)}, u32[]{:S(2)}, u32[]{:S(2)}) %all-to-all-start.1) | async-done | bytes 393248 | tf_op jit(solution)/shard_map/all_to_all | solution.py:28
  32.7 12.3 %all_to_all.40.got_ref = bf16[4,576,128]{2,1,0:T(8,128)(2,1)S(1)} all-to-all(bf16[4,576,128]{2,1,0:T(8,128)(2,1)S(1)} %pack.1), channel_id=1, replica_groups=mesh['zh'=4,'zl'=4,'c'=2,'y'=4,'x'=4] {'x'}, dimensions={0} | all-to-all | bytes 1179648 | tf_op jit(solution)/shard_map/all_to_all | solution.py:28
  45.0 0.5 lift.1
  45.6 19.5 %all_to_all.41.got_ref = bf16[4,96,512]{2,1,0:T(8,128)(2,1)S(1)} all-to-all(bf16[4,96,512]{2,1,0:T(8,128)(2,1)S(1)} %lift.1), channel_id=1, replica_groups=mesh['zh'=4,'zl'=4,'c'=2,'y'=4,'x'=4] {'y'}, dimensions={0} | all-to-all | bytes 786432 | tf_op jit(solution)/shard_map/all_to_all | solution.py:28
  65.0 1.4 shard_map.195
  66.4 3.8 %all-to-all-start.3 = ((bf16[16,96,512]{2,1,0:T(8,128)(2,1)}), bf16[16,96,512]{2,1,0:T(8,128)(2,1)S(1)}, u32[]{:S(2)}, u32[]{:S(2)}) async-start(bf16[16,96,512]{2,1,0:T(8,128)(2,1)} %shard_map.195), calls=%async_computation.3 | async-start | bytes 3145728 | tf_op jit(solution)/shard_map/all_to_all | solution.py:28
  70.3 0.0 all-gather.3.cloned.1.call-start
  70.4 0.6 pad_maximum_fusion.2
  71.0 0.0 all-gather.3.cloned.1.call-update
  71.0 18.8 %all-to-all-done.3 = bf16[16,96,512]{2,1,0:T(8,128)(2,1)S(1)} async-done(((bf16[16,96,512]{2,1,0:T(8,128)(2,1)}), bf16[16,96,512]{2,1,0:T(8,128)(2,1)S(1)}, u32[]{:S(2)}, u32[]{:S(2)}) %all-to-all-start.3) | async-done | bytes 1572896 | tf_op jit(solution)/shard_map/all_to_all | solution.py:28
  89.8 0.0 copy-done.13
  89.8 0.3 convolution_convert_fusion.1
  90.2 0.4 convolution_convert_fusion
  90.6 0.0 copy-start.3
  90.6 0.0 copy-start.4
  90.6 0.2 copy.22
  90.8 15.5 %all_to_all.42.got_ref = bf16[8,32,384]{2,1,0:T(8,128)(2,1)S(1)} all-to-all(bf16[8,32,384]{2,1,0:T(8,128)(2,1)S(1)} %bitcast.11), channel_id=1, replica_groups=mesh['zh'=4,'zl'=4,'c'=2,'y'=4,'x'=4] {'zl','c'}, dimensions={0} | all-to-all | bytes 393216 | tf_op jit(solution)/shard_map/all_to_all | solution.py:28
  106.3 25.2 %all_to_all.43.got_ref = f32[4,32,384]{2,1,0:T(8,128)S(1)} all-to-all(f32[4,32,384]{2,1,0:T(8,128)S(1)} %shard_map.196), channel_id=1, replica_groups=mesh['zh'=4,'zl'=4,'c'=2,'y'=4,'x'=4] {'zh'}, dimensions={0} | all-to-all | bytes 393216 | tf_op jit(solution)/shard_map/all_to_all | solution.py:28
  131.5 0.7 shard_map.197
  132.2 9.0 %all-to-all-start.6 = ((bf16[8,32,384]{2,1,0:T(8,128)(2,1)}), bf16[8,32,384]{2,1,0:T(8,128)(2,1)S(1)}, u32[]{:S(2)}, u32[]{:S(2)}) async-start(bf16[8,32,384]{2,1,0:T(8,128)(2,1)} %shard_map.197), calls=%async_computation.6 | async-start | bytes 393216 | tf_op jit(solution)/shard_map/all_to_all | solution.py:28
  141.2 1.9 collective-permute-start.1
  143.1 3.1 %collective-permute-start.2 = (bf16[8,96,256]{2,1,0:T(8,128)(2,1)S(1)}, bf16[8,96,256]{2,1,0:T(8,128)(2,1)S(1)}, u32[]{:S(2)}, u32[]{:S(2)}) collective-permute-start(bf16[8,96,256]{2,1,0:T(8,128)(2,1)S(1)} %all-to-all-done.1.blocks_ref.b0), channel_id=1, source_target_pairs={{0,8},{4,12},{8,0},{12,4},{1,9},{5,13},{9,1},{13,5},{2,10},{6,14},... | collective-permute-start | bytes 1179656 | tf_op jit(solution)/shard_map/ppermute | solution.py:47
  146.2 3.4 %collective-permute-start.3 = (bf16[8,96,256]{2,1,0:T(8,128)(2,1)S(1)}, bf16[8,96,256]{2,1,0:T(8,128)(2,1)S(1)}, u32[]{:S(2)}, u32[]{:S(2)}) collective-permute-start(bf16[8,96,256]{2,1,0:T(8,128)(2,1)S(1)} %all-to-all-done.1.blocks_ref.b0), channel_id=1, source_target_pairs={{0,12},{4,0},{8,4},{12,8},{1,13},{5,1},{9,5},{13,9},{2,14},{6,2},{... | collective-permute-start | bytes 1179656 | tf_op jit(solution)/shard_map/ppermute | solution.py:47
  149.7 13.8 %collective-permute-done.1.b1 = bf16[8,96,256]{2,1,0:T(8,128)(2,1)S(1)} collective-permute-done((bf16[8,96,256]{2,1,0:T(8,128)(2,1)S(1)}, bf16[8,96,256]{2,1,0:T(8,128)(2,1)S(1)}, u32[]{:S(2)}, u32[]{:S(2)}) %collective-permute-start.1) | collective-permute-done | bytes 393248 | tf_op jit(solution)/shard_map/ppermute | solution.py:47
  163.4 0.0 collective-permute-done.2.b2
  163.4 2.3 %collective-permute-done.3.b3 = bf16[8,96,256]{2,1,0:T(8,128)(2,1)S(1)} collective-permute-done((bf16[8,96,256]{2,1,0:T(8,128)(2,1)S(1)}, bf16[8,96,256]{2,1,0:T(8,128)(2,1)S(1)}, u32[]{:S(2)}, u32[]{:S(2)}) %collective-permute-start.3) | collective-permute-done | bytes 393248 | tf_op jit(solution)/shard_map/ppermute | solution.py:47
  165.7 0.0 all-to-all-done.6.got_ref
  165.7 0.0 copy-start.8
  165.7 0.9 copy-done.8
  166.6 0.9 copy-done.9
  167.5 1.4 directions.1
  168.9 0.6 copy-done.12
  169.5 4.4 %all-to-all-start.7 = ((f32[16,8,128]{2,1,0:T(8,128)}), f32[16,8,128]{2,1,0:T(8,128)S(1)}, u32[]{:S(2)}, u32[]{:S(2)}) async-start(f32[16,8,128]{2,1,0:T(8,128)} %copy-done.12), calls=%async_computation.7 | async-start | bytes 131072 | tf_op jit(solution)/shard_map/all_to_all | solution.py:28
  173.9 0.0 all-gather.3.cloned.1.call-done
  174.0 6.5 %all-to-all-done.7.total_ref = f32[16,8,128]{2,1,0:T(8,128)S(1)} async-done(((f32[16,8,128]{2,1,0:T(8,128)}), f32[16,8,128]{2,1,0:T(8,128)S(1)}, u32[]{:S(2)}, u32[]{:S(2)}) %all-to-all-start.7) | async-done | bytes 65568 | tf_op jit(solution)/shard_map/all_to_all | solution.py:28
  180.4 1.3 copy-done.1
  181.8 0.8 copy-done.7
  182.5 0.7 copy-done.11
  183.2 1.7 outputs.1
  (20 shorter events, 0.1 us)
Async XLA Ops:
  7.2 83.0 %copy-start = (bf16[1536,256]{1,0:T(8,128)(2,1)S(1)}, bf16[1536,256]{1,0:T(8,128)(2,1)}, u32[]{:S(2)}) copy-start(bf16[1536,256]{1,0:T(8,128)(2,1)} %param.13) | copy-start | bytes 2359300
  7.2 17.6 %copy-start.2 = (bf16[1536,128]{1,0:T(8,128)(2,1)S(1)}, bf16[1536,128]{1,0:T(8,128)(2,1)}, u32[]{:S(2)}) copy-start(bf16[1536,128]{1,0:T(8,128)(2,1)} %attn_ref.1) | copy-start | bytes 1179652
  8.1 0.7 collective-permute-start
  9.5 23.2 %all-to-all-start.1 = ((bf16[8,96,256]{2,1,0:T(8,128)(2,1)}), bf16[8,96,256]{2,1,0:T(8,128)(2,1)S(1)}, u32[]{:S(2)}, u32[]{:S(2)}) async-start(bf16[8,96,256]{2,1,0:T(8,128)(2,1)} %broadcast_in_dim.2), calls=%async_computation.1 | async-start | bytes 786432 | tf_op jit(solution)/shard_map/all_to_all | solution.py:28
  24.8 0.9 copy-start.6
  66.4 3.9 %copy-start.5 = (f32[64,256]{1,0:T(8,128)S(1)}, f32[64,256]{1,0:T(8,128)}, u32[]{:S(2)}) copy-start(f32[64,256]{1,0:T(8,128)} %weight_o.1) | copy-start | bytes 196612
  66.4 3.9 %copy-start.10 = (f32[32,128]{1,0:T(8,128)S(1)}, f32[32,128]{1,0:T(8,128)}, u32[]{:S(2)}) copy-start(f32[32,128]{1,0:T(8,128)} %weight_v.1) | copy-start | bytes 49156
  66.4 23.4 %copy-start.13 = (bf16[1536,128]{1,0:T(8,128)(2,1)S(1)}, bf16[1536,128]{1,0:T(8,128)(2,1)}, u32[]{:S(2)}) copy-start(bf16[1536,128]{1,0:T(8,128)(2,1)} %param.15) | copy-start | bytes 1179652
  66.4 23.4 %all-to-all-start.3 = ((bf16[16,96,512]{2,1,0:T(8,128)(2,1)}), bf16[16,96,512]{2,1,0:T(8,128)(2,1)S(1)}, u32[]{:S(2)}, u32[]{:S(2)}) async-start(bf16[16,96,512]{2,1,0:T(8,128)(2,1)} %shard_map.195), calls=%async_computation.3 | async-start | bytes 3145728 | tf_op jit(solution)/shard_map/all_to_all | solution.py:28
  70.3 103.7 %all-gather.3.cloned.1.call-start = ((), (), s32[]{:S(2)}) async-start(), calls=%async_computation.8 | async-start | bytes 1351680 | tf_op jit(solution)/shard_map/all_gather | solution.py:287
  90.6 75.1 %copy-start.3 = (f32[256,256]{1,0:T(8,128)S(1)}, f32[256,256]{1,0:T(8,128)}, u32[]{:S(2)}) copy-start(f32[256,256]{1,0:T(8,128)} %mean_o.1) | copy-start | bytes 786436
  90.6 75.1 %copy-start.4 = (f32[256,256]{1,0:T(8,128)S(1)}, f32[256,256]{1,0:T(8,128)}, u32[]{:S(2)}) copy-start(f32[256,256]{1,0:T(8,128)} %square_o.1) | copy-start | bytes 786436
  132.2 33.5 %all-to-all-start.6 = ((bf16[8,32,384]{2,1,0:T(8,128)(2,1)}), bf16[8,32,384]{2,1,0:T(8,128)(2,1)S(1)}, u32[]{:S(2)}, u32[]{:S(2)}) async-start(bf16[8,32,384]{2,1,0:T(8,128)(2,1)} %shard_map.197), calls=%async_computation.6 | async-start | bytes 393216 | tf_op jit(solution)/shard_map/all_to_all | solution.py:28
  141.2 22.2 %collective-permute-start.1 = (bf16[8,96,256]{2,1,0:T(8,128)(2,1)S(1)}, bf16[8,96,256]{2,1,0:T(8,128)(2,1)S(1)}, u32[]{:S(2)}, u32[]{:S(2)}) collective-permute-start(bf16[8,96,256]{2,1,0:T(8,128)(2,1)S(1)} %all-to-all-done.1.blocks_ref.b0), channel_id=1, source_target_pairs={{0,4},{4,8},{8,12},{12,0},{1,5},{5,9},{9,13},{13,1},{2,6},{6,10},{... | collective-permute-start | bytes 1179656 | tf_op jit(solution)/shard_map/ppermute | solution.py:47
  143.1 20.3 %collective-permute-start.2 = (bf16[8,96,256]{2,1,0:T(8,128)(2,1)S(1)}, bf16[8,96,256]{2,1,0:T(8,128)(2,1)S(1)}, u32[]{:S(2)}, u32[]{:S(2)}) collective-permute-start(bf16[8,96,256]{2,1,0:T(8,128)(2,1)S(1)} %all-to-all-done.1.blocks_ref.b0), channel_id=1, source_target_pairs={{0,8},{4,12},{8,0},{12,4},{1,9},{5,13},{9,1},{13,5},{2,10},{6,14},... | collective-permute-start | bytes 1179656 | tf_op jit(solution)/shard_map/ppermute | solution.py:47
  146.2 19.4 %collective-permute-start.3 = (bf16[8,96,256]{2,1,0:T(8,128)(2,1)S(1)}, bf16[8,96,256]{2,1,0:T(8,128)(2,1)S(1)}, u32[]{:S(2)}, u32[]{:S(2)}) collective-permute-start(bf16[8,96,256]{2,1,0:T(8,128)(2,1)S(1)} %all-to-all-done.1.blocks_ref.b0), channel_id=1, source_target_pairs={{0,12},{4,0},{8,4},{12,8},{1,13},{5,1},{9,5},{13,9},{2,14},{6,2},{... | collective-permute-start | bytes 1179656 | tf_op jit(solution)/shard_map/ppermute | solution.py:47
  165.7 0.9 copy-start.8
  166.6 0.9 copy-start.9
  168.9 0.6 copy-start.12
  169.5 10.9 %all-to-all-start.7 = ((f32[16,8,128]{2,1,0:T(8,128)}), f32[16,8,128]{2,1,0:T(8,128)S(1)}, u32[]{:S(2)}, u32[]{:S(2)}) async-start(f32[16,8,128]{2,1,0:T(8,128)} %copy-done.12), calls=%async_computation.7 | async-start | bytes 131072 | tf_op jit(solution)/shard_map/all_to_all | solution.py:28
  180.4 1.3 copy-start.1
  181.8 0.8 copy-start.7
  182.5 0.7 copy-start.11
Sparse Core Ops, SparseCore 0:
  73.8 80.2 all-gather.2

commit v3 on v2

v3 whole, which is shorter than its diff:
```python
import functools

import jax
import jax.numpy as jnp
from jax import lax
from jax.experimental import pallas as pl
from jax.experimental.pallas import tpu as pltpu
from jax.sharding import Mesh
from jax.sharding import PartitionSpec as P


TP = ("y", "x")
FS = ("zh", "zl", "c")
NEAR = ("zl", "c")
Z = ("zh", "zl")
ALL = ("zh", "zl", "c", "y", "x")

LEARN_RATE = 0.01
MEAN_DECAY = 0.8
BETA_SQUARE = 0.9
EPS_RMS = 1e-06

BF = jnp.bfloat16
ROOM = 12 * 2**20
F32 = jnp.float32


def exchange(value, axes):
    return lax.all_to_all(value, axes, 0, 0, tiled=True)


def from_everyone(value, axes):
    devices = lax.axis_size(axes)
    return exchange(jnp.broadcast_to(value[None], (devices, *value.shape)), axes)


def swapped_blocks(value):
    pairs = []
    for j in range(16):
        for b in range(2):
            for t in range(16):
                pairs.append(((2 * j + b) * 16 + t, (2 * t + b) * 16 + j))
    return lax.ppermute(value, ALL, pairs)


def shifted(value, axis, by):
    devices = lax.axis_size(axis)
    return lax.ppermute(value, axis, [(i, (i + by) % devices) for i in range(devices)])


def dot(a, b):
    return jnp.dot(a, b, preferred_element_type=F32)


def pack_kernel(at_ref, attn_ref, lat_ref, *refs):
    outs, turned = refs[:-1], refs[-1]
    groups = len(outs)
    each = attn_ref.shape[0] // groups**2
    turned[...] = lat_ref[...].T
    for k in range(groups):
        g = lax.rem(at_ref[0] + k, groups)
        pieces = []
        for p in range(groups):
            at = pl.multiple_of((p * groups + g) * each, each)
            outs[k][p * each : (p + 1) * each, :] = attn_ref[pl.ds(at, each), :]
            pieces.append(turned[pl.ds(at, each), :])
        half = groups // 2
        for p in range(half):
            at = (groups + p) * each
            outs[k][at : at + each, :] = jnp.concatenate([pieces[p], pieces[half + p]], axis=1)


def pack(at, attn_out, lat_turned, groups):
    tokens, heads = attn_out.shape
    rows = tokens // groups
    vmem = pl.BlockSpec(memory_space=pltpu.VMEM)
    return pl.pallas_call(
        pack_kernel,
        in_specs=[pl.BlockSpec(memory_space=pltpu.SMEM), vmem, vmem],
        out_shape=tuple(jax.ShapeDtypeStruct((rows + rows // 2, heads), BF) for _ in range(groups)),
        scratch_shapes=[pltpu.VMEM(lat_turned.shape[::-1], BF)],
        cost_estimate=pl.CostEstimate(flops=10**7, bytes_accessed=10**6, transcendentals=0),
        compiler_params=pltpu.CompilerParams(vmem_limit_bytes=ROOM),
        name="pack",
    )(at, attn_out, lat_turned)


def old_kernel(weight_o, weight_v, out_ref):
    rows_o = weight_o.shape[0]
    out_ref[:rows_o] = weight_o[:, :128].astype(BF)
    out_ref[rows_o : 2 * rows_o] = weight_o[:, 128:].astype(BF)
    out_ref[2 * rows_o :] = weight_v[...].astype(BF)


def old_rows(weight_o, weight_v):
    rows = 2 * weight_o.shape[0] + weight_v.shape[0]
    return pl.pallas_call(
        old_kernel,
        out_shape=jax.ShapeDtypeStruct((rows, 128), BF),
        cost_estimate=pl.CostEstimate(flops=10**6, bytes_accessed=10**5, transcendentals=0),
        compiler_params=pltpu.CompilerParams(vmem_limit_bytes=ROOM),
        name="old",
    )(weight_o, weight_v)


def lift_kernel(rows_o, tokens, at_ref, blocks_ref, *refs):
    gots, out_ref = refs[:-1], refs[-1]
    groups = len(gots)
    rank = blocks_ref.shape[2]
    half = tokens // 2
    first = jnp.zeros((tokens, rank), F32)
    second = jnp.zeros((half, 2 * rank), F32)
    for k, got_ref in enumerate(gots):
        g = lax.rem(at_ref[0] + groups - k, groups)
        low, high = blocks_ref[g], blocks_ref[groups + g]
        basis_o = jnp.concatenate([low[:rows_o], high[:rows_o]], 0)
        basis_v = jnp.concatenate([low[rows_o:], high[rows_o:]], 0)
        none = jnp.zeros_like(basis_v)
        pair = jnp.concatenate(
            [jnp.concatenate([basis_v, none], 0), jnp.concatenate([none, basis_v], 0)], 1
        )
        first = first + dot(got_ref[:tokens, :], basis_o)
        second = second + dot(got_ref[tokens:, :], pair)
    parts, each = out_ref.shape[:2]
    for p in range(parts):
        at = p * each
        out_ref[p, :, :rank] = first[at : at + each].astype(BF)
        row, side = at % half, at // half
        out_ref[p, :, rank:] = second[row : row + each, side * rank : (side + 1) * rank].astype(BF)


def lift(at, blocks, gots, rows_o, tokens, parts):
    rank = blocks.shape[2]
    vmem = pl.BlockSpec(memory_space=pltpu.VMEM)
    return pl.pallas_call(
        functools.partial(lift_kernel, rows_o, tokens),
        in_specs=[pl.BlockSpec(memory_space=pltpu.SMEM)] + [vmem] * (1 + len(gots)),
        out_shape=jax.ShapeDtypeStruct((parts, tokens // parts, 2 * rank), BF),
        cost_estimate=pl.CostEstimate(flops=2 * 10**8, bytes_accessed=10**6, transcendentals=0),
        compiler_params=pltpu.CompilerParams(vmem_limit_bytes=ROOM),
        name="lift",
    )(at, blocks, *gots)


def spread_kernel(got_ref, out_ref):
    total = got_ref[0].astype(F32)
    for i in range(1, got_ref.shape[0]):
        total = total + got_ref[i].astype(F32)
    total = total.astype(out_ref.dtype)
    for i in range(out_ref.shape[0]):
        out_ref[i] = total


def summed_for(got, copies, kind):
    return pl.pallas_call(
        spread_kernel,
        out_shape=jax.ShapeDtypeStruct((copies, *got.shape[1:]), kind),
        cost_estimate=pl.CostEstimate(flops=10**7, bytes_accessed=10**6, transcendentals=0),
        compiler_params=pltpu.CompilerParams(vmem_limit_bytes=ROOM),
    )(got)


def decay_kernel(mean_o, square_o, mean_v, square_v, mean_out, square_out):
    cols_o = mean_o.shape[1]
    mean_out[:, :cols_o] = MEAN_DECAY * mean_o[...]
    mean_out[:, cols_o:] = MEAN_DECAY * mean_v[...]
    square_out[:, :cols_o] = BETA_SQUARE * square_o[...]
    square_out[:, cols_o:] = BETA_SQUARE * square_v[...]


def decayed(mean_o, square_o, mean_v, square_v):
    shape = jax.ShapeDtypeStruct((mean_o.shape[0], mean_o.shape[1] + mean_v.shape[1]), F32)
    return pl.pallas_call(
        decay_kernel,
        out_shape=(shape, shape),
        cost_estimate=pl.CostEstimate(flops=10**6, bytes_accessed=10**6, transcendentals=0),
        compiler_params=pltpu.CompilerParams(vmem_limit_bytes=ROOM),
        name="decay",
    )(mean_o, square_o, mean_v, square_v)


def direction_kernel(
    rows_o, cols_o, got_ref, mean_ref, square_ref, b0, b1, b2, b3,
    mean_o_out, square_o_out, mean_v_out, square_v_out, way_out, total_out,
):
    near = got_ref.shape[0]
    proj = jnp.concatenate([got_ref[i] for i in range(near)], 0).astype(F32)
    mean = mean_ref[...] + (1.0 - MEAN_DECAY) * proj
    square = square_ref[...] + (1.0 - BETA_SQUARE) * proj * proj
    mean_o_out[...] = mean[:, :cols_o]
    mean_v_out[...] = mean[:, cols_o:]
    square_o_out[...] = square[:, :cols_o]
    square_v_out[...] = square[:, cols_o:]
    way = mean / jnp.sqrt(square)
    way_out[...] = way
    upper = way.astype(BF)
    upper_o, upper_v = upper[:, :cols_o], upper[:, cols_o:]
    total_o = jnp.zeros((8, cols_o), F32)
    total_v = jnp.zeros((8, upper_v.shape[1]), F32)
    for ref in (b0, b1, b2, b3):
        count = ref.shape[0]
        basis_o = jnp.concatenate([ref[i, :rows_o, :] for i in range(count)], 0)
        basis_v = jnp.concatenate([ref[i, rows_o:, :] for i in range(count)], 0)
        update = dot(basis_o, upper_o)
        total_o = total_o + jnp.sum((update * update).reshape(-1, 8, cols_o), 0)
        update = dot(basis_v, upper_v)
        total_v = total_v + jnp.sum((update * update).reshape(-1, 8, update.shape[1]), 0)
    sums = [
        jnp.broadcast_to(jnp.sum(t, keepdims=True), (4, 128)) for t in (total_o, total_v)
    ]
    tile = jnp.concatenate(sums, 0)
    for i in range(total_out.shape[0]):
        total_out[i] = tile


def directions(rows_o, cols_o, copies, got, mean, square, segments):
    rank, cols = mean.shape
    shape = jax.ShapeDtypeStruct
    return pl.pallas_call(
        functools.partial(direction_kernel, rows_o, cols_o),
        out_shape=(
            shape((rank, cols_o), F32),
            shape((rank, cols_o), F32),
            shape((rank, cols - cols_o), F32),
            shape((rank, cols - cols_o), F32),
            shape((rank, cols), F32),
            shape((copies, 8, 128), F32),
        ),
        cost_estimate=pl.CostEstimate(flops=4 * 10**8, bytes_accessed=4 * 10**6, transcendentals=10**5),
        compiler_params=pltpu.CompilerParams(vmem_limit_bytes=ROOM),
        name="directions",
    )(got, mean, square, *segments)


def ready_kernel(
    rows_o, rows_v, cols_o, at_ref, way_ref, local_o, local_v, h0, h1, h2, h3, b0, b1, b2, b3,
    step_o_out, step_v_out, update_o_out, update_v_out, old_o_out, old_v_out,
):
    way = way_ref[...]
    upper = way.astype(BF)
    lower = (way - upper.astype(F32)).astype(BF)
    upper_o, upper_v = upper[:, :cols_o], upper[:, cols_o:]
    step_o_out[...] = dot(local_o[...], upper_o) + dot(local_o[...], lower[:, :cols_o])
    step_v_out[...] = dot(local_v[...], upper_v) + dot(local_v[...], lower[:, cols_o:])
    y, z, c = at_ref[1], at_ref[2], at_ref[3]
    for k, ref in enumerate((b0, b1, b2, b3)):
        origin = lax.rem(y + 4 - k, 4)
        count = ref.shape[0]
        basis_o = jnp.concatenate([ref[i, :rows_o, :] for i in range(count)], 0)
        basis_v = jnp.concatenate([ref[i, rows_o:, :] for i in range(count)], 0)
        update_o = dot(basis_o, upper_o).astype(BF)
        update_v = dot(basis_v, upper_v).astype(BF)
        for i in range(count):
            core, x = divmod(i, count // 2)
            index = 8 * origin + 2 * x + core
            at = pl.multiple_of(index * rows_o, rows_o)
            update_o_out[pl.ds(at, rows_o), :] = update_o[i * rows_o : (i + 1) * rows_o]
            at = pl.multiple_of(index * rows_v, rows_v)
            update_v_out[pl.ds(at, rows_v), :] = update_v[i * rows_v : (i + 1) * rows_v]
    for ref, core, last in ((h0, c, 0), (h1, c, 1), (h2, 1 - c, 0), (h3, 1 - c, 1)):
        for p in range(ref.shape[0]):
            behind = (p & 1) * 8 + (p >> 1 & 1) * 4 + (p >> 2) * 2 + last
            index = 2 * lax.rem(z + 16 - behind, 16) + core
            at = pl.multiple_of(index * rows_o, rows_o)
            old_o_out[pl.ds(at, rows_o), :128] = ref[p, :rows_o]
            old_o_out[pl.ds(at, rows_o), 128:] = ref[p, rows_o : 2 * rows_o]
            at = pl.multiple_of(index * rows_v, rows_v)
            old_v_out[pl.ds(at, rows_v), :] = ref[p, 2 * rows_o :]


def ready(cols_o, at, way, local_o, local_v, held, segments):
    rows_o, rows_v = local_o.shape[0], local_v.shape[0]
    cols_v = way.shape[1] - cols_o
    fs = 4 * held[0].shape[0]
    shape = jax.ShapeDtypeStruct
    vmem = pl.BlockSpec(memory_space=pltpu.VMEM)
    return pl.pallas_call(
        functools.partial(ready_kernel, rows_o, rows_v, cols_o),
        in_specs=[pl.BlockSpec(memory_space=pltpu.SMEM)] + [vmem] * 11,
        out_shape=(
            shape((rows_o, cols_o), F32),
            shape((rows_v, cols_v), F32),
            shape((rows_o * fs, cols_o), BF),
            shape((rows_v * fs, cols_v), BF),
            shape((rows_o * fs, cols_o), BF),
            shape((rows_v * fs, cols_v), BF),
        ),
        cost_estimate=pl.CostEstimate(flops=4 * 10**8, bytes_accessed=4 * 10**6, transcendentals=0),
        compiler_params=pltpu.CompilerParams(vmem_limit_bytes=ROOM),
        name="ready",
    )(at, way, local_o, local_v, *held, *segments)


def output_kernel(
    counts, total_ref, weight_o, weight_v, step_o, step_v, update_o, update_v, old_o, old_v,
    step_o_out, new_o_out, copy_o_out, step_v_out, new_v_out, copy_v_out,
):
    total = total_ref[0]
    for i in range(1, total_ref.shape[0]):
        total = total + total_ref[i]
    for row, count, weight, step, update, old, step_out, new_out, copy_out in (
        (0, counts[0], weight_o, step_o, update_o, old_o, step_o_out, new_o_out, copy_o_out),
        (4, counts[1], weight_v, step_v, update_v, old_v, step_v_out, new_v_out, copy_v_out),
    ):
        scale = LEARN_RATE * lax.rsqrt(total[row : row + 1, 0:1] / count + EPS_RMS)
        mine = step[...] * scale
        step_out[...] = mine
        new_out[...] = weight[...] - mine
        copy_out[...] = (old[...].astype(F32) - update[...].astype(F32) * scale).astype(BF)


def outputs(counts, total, weight_o, weight_v, step_o, step_v, update_o, update_v, old_o, old_v):
    shape = jax.ShapeDtypeStruct
    return pl.pallas_call(
        functools.partial(output_kernel, counts),
        out_shape=(
            shape(weight_o.shape, F32),
            shape(weight_o.shape, F32),
            shape(old_o.shape, BF),
            shape(weight_v.shape, F32),
            shape(weight_v.shape, F32),
            shape(old_v.shape, BF),
        ),
        cost_estimate=pl.CostEstimate(flops=10**7, bytes_accessed=4 * 10**6, transcendentals=10),
        compiler_params=pltpu.CompilerParams(vmem_limit_bytes=ROOM),
        name="outputs",
    )(total, weight_o, weight_v, step_o, step_v, update_o, update_v, old_o, old_v)


def per_device(
    attn_out,
    out_cot,
    latent,
    value_cot,
    out_weight,
    value_up_matrix,
    out_basis,
    value_basis,
    out_mean,
    out_square,
    value_mean,
    value_square,
):
    tokens = attn_out.shape[0]
    cols_o = out_cot.shape[1]
    cols_v = value_cot.shape[1]
    rows_o, rank = out_basis.shape
    rows_v = value_basis.shape[0]
    tp = lax.axis_size(TP)
    fs = lax.axis_size(FS)
    xs, ys = lax.axis_size("x"), lax.axis_size("y")

    x = lax.axis_index("x").astype(jnp.int32)
    y = lax.axis_index("y").astype(jnp.int32)
    z = lax.axis_index(Z).astype(jnp.int32)
    c = lax.axis_index("c").astype(jnp.int32)
    at = jnp.stack([x, y, z, c])

    block = swapped_blocks(jnp.concatenate([out_basis, value_basis], 0))

    gots = list(pack(at, attn_out, latent.T, xs))
    for k in range(1, xs):
        gots[k] = shifted(gots[k], "x", k)

    own = old_rows(out_weight, value_up_matrix)[None]
    for k in (8, 4, 2):
        more = shifted(own, Z, k)
        own = lax.optimization_barrier(jnp.concatenate([own, more], 0))
    more = shifted(own, Z, 1)
    held = [own, more, shifted(own, "c", 1)]
    held.append(shifted(more, "c", 1))

    blocks = from_everyone(block, ("c", "x"))
    partial = lift(at, blocks, gots, rows_o, tokens // xs, ys)
    partial = exchange(partial, "y")
    lifted = summed_for(partial, tp, BF)
    lifted = exchange(lifted, TP).reshape(tokens, 2 * rank)

    part_o = dot(lifted[:, :rank].T, out_cot)
    part_v = dot(lifted[:, rank:].T, value_cot)
    part = jnp.concatenate([part_o.astype(BF), part_v.astype(BF)], 1)
    near = lax.axis_size(NEAR)
    part = exchange(part.reshape(near, rank // near, -1), NEAR)
    part = exchange(summed_for(part, lax.axis_size("zh"), F32), "zh")
    proj = exchange(summed_for(part, near, BF), NEAR)

    segments = [blocks]
    for k in range(1, ys):
        segments.append(shifted(blocks, "y", k))

    mean, square = decayed(out_mean, out_square, value_mean, value_square)
    mean_o, square_o, mean_v, square_v, way, total = directions(
        rows_o, cols_o, tp, proj, mean, square, segments
    )
    total = exchange(total, TP)
    prepared = ready(cols_o, at, way, out_basis, value_basis, held, segments)
    counts = (rows_o * fs * cols_o * tp, rows_v * fs * cols_v * tp)
    step_o, new_o, copy_o, step_v, new_v, copy_v = outputs(
        counts, total, out_weight, value_up_matrix, *prepared
    )
    return (step_o, new_o, copy_o, mean_o, square_o, step_v, new_v, copy_v, mean_v, square_v)


def solution(mesh):
    torus = Mesh(mesh.devices.reshape(4, 4, 2, 4, 4), ALL)
    both = P(FS, TP)
    cols = P(None, TP)
    rows = P(FS, None)

    return jax.shard_map(
        per_device,
        mesh=torus,
        in_specs=(both, both, both, both, both, both, rows, rows, cols, cols, cols, cols),
        out_specs=(both, both, cols, cols, cols, both, both, cols, cols, cols),
        check_vma=False,
    )
```

time: 193 us -> 201 us (1.041)
  starting transfers between devices: 41.6 us -> 92.7 us
  waiting for transfers between devices: 48.1 us -> 21 us
  between operations: 14.3 us -> 1.01 us
  blocking collectives: 72.4 us -> 60 us
  local copies, waits for them, and re-layouts: 7.13 us -> 14.7 us
  Pallas kernels: 5.99 us -> 8.8 us
    ppermute x3 -> x12, starting transfers between devices: 8.4 us -> 46.6 us  [shifted(): lax.ppermute(value, axis, [(i, (i + by) % devices) for i in range(devices)])]
    all_to_all x4, waiting for transfers between devices: 32.1 us -> 0.01 us  [exchange(): return lax.all_to_all(value, axes, 0, 0, tiled=True)]
    all_to_all x4, starting transfers between devices: 32.5 us -> 45.4 us  [exchange(): return lax.all_to_all(value, axes, 0, 0, tiled=True)]
    all_to_all x4 -> x3, blocking collectives: 72.4 us -> 60 us  [exchange(): return lax.all_to_all(value, axes, 0, 0, tiled=True)]
    unnamed x28 -> x46, local copies, waits for them, and re-layouts: 6.19 us -> 13.7 us
    ppermute x3 -> x12, waiting for transfers between devices: 16 us -> 21 us  [shifted(): lax.ppermute(value, axis, [(i, (i + by) % devices) for i in range(devices)])]
    pallas_call x4 -> x7, Pallas kernels: 3.89 us -> 7.25 us  [the longest x1 1.99 us: ready(): pl.pallas_call(functools.partial(ready_kernel, rows_o, rows_v, cols_o), i...]
  transfers between devices with their start and end apart: 9 -> 17, of which waited for: 5 -> 5; matrix products, arithmetic and copies ran while one was open for 1% -> 0% of each run, Pallas kernels for 1% -> 3%
where the time goes in v3:
time: 201 us; the launch traced here: 200 us
  starting transfers between devices  92.7 us (46%)
  blocking collectives  60 us (30%)
  waiting for transfers between devices  21 us (10%)
  local copies, waits for them, and re-layouts  14.7 us (7%)
  Pallas kernels  8.8 us (4%)
    all_to_all x3, blocking collectives, exchange(): return lax.all_to_all(value, axes, 0, 0, tiled=True)  60 us
    ppermute x12, starting transfers between devices, shifted(): lax.ppermute(value, axis, [(i, (i + by) % devices) for i in range(devices)])  46.6 us
    all_to_all x4, starting transfers between devices, exchange(): return lax.all_to_all(value, axes, 0, 0, tiled=True)  45.4 us
    ppermute x12, waiting for transfers between devices, shifted(): lax.ppermute(value, axis, [(i, (i + by) % devices) for i in range(devices)])  21 us
    unnamed x46, local copies, waits for them, and re-layouts  13.7 us
  transfers between devices with their start and end apart: 17, of which 5 were waited for; matrix products, arithmetic and copies ran while one was open for 0% of the time, Pallas kernels for 3%

profile of v3, /device:TPU:1, one launch (start us, length us, event | category | flops | bytes accessed | tf_op | source)
XLA Modules:
  0.0 199.9 jit_solution(18182939416539409753)
XLA Ops:
  0.7 0.9 pad_maximum_fusion.4
  2.2 0.8 broadcast_in_dim.4
  3.0 15.3 %all-to-all-start = ((bf16[8,96,256]{2,1,0:T(8,128)(2,1)}), bf16[8,96,256]{2,1,0:T(8,128)(2,1)S(1)}, u32[]{:S(2)}, u32[]{:S(2)}) async-start(bf16[8,96,256]{2,1,0:T(8,128)(2,1)} %broadcast_in_dim.4), calls=%async_computation | async-start | bytes 786432 | tf_op jit(solution)/shard_map/all_to_all | solution.py:29
  18.3 0.9 copy-done.14
  19.3 0.8 pack.1
  20.1 3.3 %collective-permute-start.1 = (bf16[576,128]{1,0:T(8,128)(2,1)S(1)}, bf16[576,128]{1,0:T(8,128)(2,1)S(1)}, u32[]{:S(2)}, u32[]{:S(2)}) collective-permute-start(bf16[576,128]{1,0:T(8,128)(2,1)S(1)} %get-tuple-element.35), channel_id=1, source_target_pairs={{0,1},{1,2},{2,3},{3,0},{4,5},{5,6},{6,7},{7,4},{8,9},{9,10},{10,1... | collective-permute-start | bytes 442376 | tf_op jit(solution)/shard_map/ppermute | solution.py:48
  23.4 4.3 %collective-permute-start.2 = (bf16[576,128]{1,0:T(8,128)(2,1)S(1)}, bf16[576,128]{1,0:T(8,128)(2,1)S(1)}, u32[]{:S(2)}, u32[]{:S(2)}) collective-permute-start(bf16[576,128]{1,0:T(8,128)(2,1)S(1)} %get-tuple-element.36), channel_id=1, source_target_pairs={{0,2},{1,3},{2,0},{3,1},{4,6},{5,7},{6,4},{7,5},{8,10},{9,11},{10,... | collective-permute-start | bytes 442376 | tf_op jit(solution)/shard_map/ppermute | solution.py:48
  27.7 3.1 %collective-permute-start.3 = (bf16[576,128]{1,0:T(8,128)(2,1)S(1)}, bf16[576,128]{1,0:T(8,128)(2,1)S(1)}, u32[]{:S(2)}, u32[]{:S(2)}) collective-permute-start(bf16[576,128]{1,0:T(8,128)(2,1)S(1)} %get-tuple-element.37), channel_id=1, source_target_pairs={{0,3},{1,0},{2,1},{3,2},{4,7},{5,4},{6,5},{7,6},{8,11},{9,8},{10,9... | collective-permute-start | bytes 442376 | tf_op jit(solution)/shard_map/ppermute | solution.py:48
  30.8 1.8 collective-permute-done.2.refs_2_
  32.6 1.4 collective-permute-done.3.refs_3_
  34.0 1.1 lift.1
  35.1 20.0 %all_to_all.35.got_ref = bf16[4,96,512]{2,1,0:T(8,128)(2,1)S(1)} all-to-all(bf16[4,96,512]{2,1,0:T(8,128)(2,1)S(1)} %lift.1), channel_id=1, replica_groups=mesh['zh'=4,'zl'=4,'c'=2,'y'=4,'x'=4] {'y'}, dimensions={0} | all-to-all | bytes 786432 | tf_op jit(solution)/shard_map/all_to_all | solution.py:29
  55.3 26.9 %all_to_all.36 = bf16[16,96,512]{2,1,0:T(8,128)(2,1)S(1)} all-to-all(bf16[16,96,512]{2,1,0:T(8,128)(2,1)S(1)} %shard_map.195), channel_id=1, replica_groups=mesh['zh'=4,'zl'=4,'c'=2,'y'=4,'x'=4] {'y','x'}, dimensions={0} | all-to-all | bytes 3145728 | tf_op jit(solution)/shard_map/all_to_all | solution.py:29
  83.2 13.1 %all_to_all.37.got_ref = bf16[8,32,384]{2,1,0:T(8,128)(2,1)S(1)} all-to-all(bf16[8,32,384]{2,1,0:T(8,128)(2,1)S(1)} %bitcast.15), channel_id=1, replica_groups=mesh['zh'=4,'zl'=4,'c'=2,'y'=4,'x'=4] {'zl','c'}, dimensions={0} | all-to-all | bytes 393216 | tf_op jit(solution)/shard_map/all_to_all | solution.py:29
  96.3 0.7 shard_map.196
  97.0 11.3 %all-to-all-start.4 = ((f32[4,32,384]{2,1,0:T(8,128)}), f32[4,32,384]{2,1,0:T(8,128)S(1)}, u32[]{:S(2)}, u32[]{:S(2)}) async-start(f32[4,32,384]{2,1,0:T(8,128)} %shard_map.196), calls=%async_computation.4 | async-start | bytes 393216 | tf_op jit(solution)/shard_map/all_to_all | solution.py:29
  108.3 12.1 %collective-permute-start.7 = (bf16[1,160,128]{2,1,0:T(8,128)(2,1)S(1)}, bf16[1,160,128]{2,1,0:T(8,128)(2,1)S(1)}, u32[]{:S(2)}, u32[]{:S(2)}) collective-permute-start(bf16[1,160,128]{2,1,0:T(8,128)(2,1)S(1)} %bitcast.11), channel_id=1, source_target_pairs={{0,256},{32,288},{64,320},{96,352},{128,384},{160,416},{192,448},{... | collective-permute-start | bytes 122888 | tf_op jit(solution)/shard_map/ppermute | solution.py:48
  120.4 4.7 %collective-permute-done.7 = bf16[1,160,128]{2,1,0:T(8,128)(2,1)S(1)} collective-permute-done((bf16[1,160,128]{2,1,0:T(8,128)(2,1)S(1)}, bf16[1,160,128]{2,1,0:T(8,128)(2,1)S(1)}, u32[]{:S(2)}, u32[]{:S(2)}) %collective-permute-start.7) | collective-permute-done | bytes 40992 | tf_op jit(solution)/shard_map/ppermute | solution.py:48
  125.1 4.5 %collective-permute-start.8 = (bf16[2,160,128]{2,1,0:T(8,128)(2,1)S(1)}, bf16[2,160,128]{2,1,0:T(8,128)(2,1)S(1)}, u32[]{:S(2)}, u32[]{:S(2)}) collective-permute-start(bf16[2,160,128]{2,1,0:T(8,128)(2,1)S(1)} %pad_maximum_fusion.3), channel_id=1, source_target_pairs={{0,128},{32,160},{64,192},{96,224},{128,256},{160,288},{192,320},{... | collective-permute-start | bytes 245768 | tf_op jit(solution)/shard_map/ppermute | solution.py:48
  129.7 4.6 %collective-permute-done.8 = bf16[2,160,128]{2,1,0:T(8,128)(2,1)S(1)} collective-permute-done((bf16[2,160,128]{2,1,0:T(8,128)(2,1)S(1)}, bf16[2,160,128]{2,1,0:T(8,128)(2,1)S(1)}, u32[]{:S(2)}, u32[]{:S(2)}) %collective-permute-start.8) | collective-permute-done | bytes 81952 | tf_op jit(solution)/shard_map/ppermute | solution.py:48
  134.3 2.7 %collective-permute-start.9 = (bf16[4,160,128]{2,1,0:T(8,128)(2,1)S(1)}, bf16[4,160,128]{2,1,0:T(8,128)(2,1)S(1)}, u32[]{:S(2)}, u32[]{:S(2)}) collective-permute-start(bf16[4,160,128]{2,1,0:T(8,128)(2,1)S(1)} %pad_maximum_fusion.2), channel_id=1, source_target_pairs={{0,64},{32,96},{64,128},{96,160},{128,192},{160,224},{192,256},{22... | collective-permute-start | bytes 491528 | tf_op jit(solution)/shard_map/ppermute | solution.py:48
  137.0 0.7 shard_map.197
  137.7 15.4 %all-to-all-start.5 = ((bf16[8,32,384]{2,1,0:T(8,128)(2,1)}), bf16[8,32,384]{2,1,0:T(8,128)(2,1)S(1)}, u32[]{:S(2)}, u32[]{:S(2)}) async-start(bf16[8,32,384]{2,1,0:T(8,128)(2,1)} %shard_map.197), calls=%async_computation.5 | async-start | bytes 393216 | tf_op jit(solution)/shard_map/all_to_all | solution.py:29
  153.2 3.3 %collective-permute-start.10 = (bf16[8,160,128]{2,1,0:T(8,128)(2,1)S(1)}, bf16[8,160,128]{2,1,0:T(8,128)(2,1)}, u32[]{:S(2)}, u32[]{:S(2)}) collective-permute-start(bf16[8,160,128]{2,1,0:T(8,128)(2,1)S(1)} %pad_maximum_fusion.h0), channel_id=1, source_target_pairs={{0,32},{32,64},{64,96},{96,128},{128,160},{160,192},{192,224},{224... | collective-permute-start | bytes 983048 | tf_op jit(solution)/shard_map/ppermute | solution.py:48
  156.5 2.5 %collective-permute-start.6 = (bf16[8,96,256]{2,1,0:T(8,128)(2,1)S(1)}, bf16[8,96,256]{2,1,0:T(8,128)(2,1)S(1)}, u32[]{:S(2)}, u32[]{:S(2)}) collective-permute-start(bf16[8,96,256]{2,1,0:T(8,128)(2,1)S(1)} %all-to-all-done.blocks_ref.b0), channel_id=1, source_target_pairs={{0,12},{4,0},{8,4},{12,8},{1,13},{5,1},{9,5},{13,9},{2,14},{6,2},{... | collective-permute-start | bytes 1179656 | tf_op jit(solution)/shard_map/ppermute | solution.py:48
  159.0 2.3 %collective-permute-start.5 = (bf16[8,96,256]{2,1,0:T(8,128)(2,1)S(1)}, bf16[8,96,256]{2,1,0:T(8,128)(2,1)S(1)}, u32[]{:S(2)}, u32[]{:S(2)}) collective-permute-start(bf16[8,96,256]{2,1,0:T(8,128)(2,1)S(1)} %all-to-all-done.blocks_ref.b0), channel_id=1, source_target_pairs={{0,8},{4,12},{8,0},{12,4},{1,9},{5,13},{9,1},{13,5},{2,10},{6,14},... | collective-permute-start | bytes 1179656 | tf_op jit(solution)/shard_map/ppermute | solution.py:48
  161.3 2.4 %collective-permute-start.4 = (bf16[8,96,256]{2,1,0:T(8,128)(2,1)S(1)}, bf16[8,96,256]{2,1,0:T(8,128)(2,1)S(1)}, u32[]{:S(2)}, u32[]{:S(2)}) collective-permute-start(bf16[8,96,256]{2,1,0:T(8,128)(2,1)S(1)} %all-to-all-done.blocks_ref.b0), channel_id=1, source_target_pairs={{0,4},{4,8},{8,12},{12,0},{1,5},{5,9},{9,13},{13,1},{2,6},{6,10},{... | collective-permute-start | bytes 1179656 | tf_op jit(solution)/shard_map/ppermute | solution.py:48
  163.7 4.2 %collective-permute-start.11 = (bf16[8,160,128]{2,1,0:T(8,128)(2,1)S(1)}, bf16[8,160,128]{2,1,0:T(8,128)(2,1)}, u32[]{:S(2)}, u32[]{:S(2)}) collective-permute-start(bf16[8,160,128]{2,1,0:T(8,128)(2,1)S(1)} %pad_maximum_fusion.h0), channel_id=1, source_target_pairs={{0,16},{16,0},{1,17},{17,1},{2,18},{18,2},{3,19},{19,3},{4,20},{20... | collective-permute-start | bytes 983048 | tf_op jit(solution)/shard_map/ppermute | solution.py:48
  167.9 1.9 collective-permute-start.12
  169.8 0.9 copy-done.11
  170.8 0.9 copy-done.16
  171.7 0.9 copy-done.17
  172.7 0.7 copy-done.5
  173.4 8.4 %collective-permute-done.4.b1 = bf16[8,96,256]{2,1,0:T(8,128)(2,1)S(1)} collective-permute-done((bf16[8,96,256]{2,1,0:T(8,128)(2,1)S(1)}, bf16[8,96,256]{2,1,0:T(8,128)(2,1)S(1)}, u32[]{:S(2)}, u32[]{:S(2)}) %collective-permute-start.4) | collective-permute-done | bytes 393248 | tf_op jit(solution)/shard_map/ppermute | solution.py:48
  181.8 1.0 copy-done.6
  182.8 1.5 directions.1
  184.3 0.7 copy-done.8
  185.1 3.5 %all-to-all-start.6 = ((f32[16,8,128]{2,1,0:T(8,128)}), f32[16,8,128]{2,1,0:T(8,128)S(1)}, u32[]{:S(2)}, u32[]{:S(2)}) async-start(f32[16,8,128]{2,1,0:T(8,128)} %get-tuple-element.40), calls=%async_computation.6 | async-start | bytes 131072 | tf_op jit(solution)/shard_map/all_to_all | solution.py:29
  188.6 1.0 copy-done.9
  189.6 0.8 copy-done.15
  190.4 0.7 copy-done.19
  191.1 0.7 copy-done.21
  191.7 2.0 ready.1
  193.7 1.0 copy-done.1
  194.7 1.0 copy-done.3
  195.7 1.2 copy-done.2
  196.9 1.2 copy-done.4
  198.2 1.8 outputs.1
  (55 shorter events, 2.1 us)
Async XLA Ops:
  0.6 81.9 %copy-start = (bf16[1536,256]{1,0:T(8,128)(2,1)S(1)}, bf16[1536,256]{1,0:T(8,128)(2,1)}, u32[]{:S(2)}) copy-start(bf16[1536,256]{1,0:T(8,128)(2,1)} %param.13) | copy-start | bytes 2359300
  0.7 17.7 %copy-start.7 = (bf16[1536,128]{1,0:T(8,128)(2,1)S(1)}, bf16[1536,128]{1,0:T(8,128)(2,1)}, u32[]{:S(2)}) copy-start(bf16[1536,128]{1,0:T(8,128)(2,1)} %attn_ref.1) | copy-start | bytes 1179652
  1.5 0.7 collective-permute-start
  3.0 31.0 %all-to-all-start = ((bf16[8,96,256]{2,1,0:T(8,128)(2,1)}), bf16[8,96,256]{2,1,0:T(8,128)(2,1)S(1)}, u32[]{:S(2)}, u32[]{:S(2)}) async-start(bf16[8,96,256]{2,1,0:T(8,128)(2,1)} %broadcast_in_dim.4), calls=%async_computation | async-start | bytes 786432 | tf_op jit(solution)/shard_map/all_to_all | solution.py:29
  18.3 36.9 %copy-start.20 = (s32[4]{0:T(128)}, s32[4]{0:T(128)S(1)}, u32[]{:S(2)}) copy-start(s32[4]{0:T(128)S(1)} %pad_add_fusion.at_ref) | copy-start | bytes 52
  18.3 0.9 copy-start.14
  20.1 10.7 %collective-permute-start.1 = (bf16[576,128]{1,0:T(8,128)(2,1)S(1)}, bf16[576,128]{1,0:T(8,128)(2,1)S(1)}, u32[]{:S(2)}, u32[]{:S(2)}) collective-permute-start(bf16[576,128]{1,0:T(8,128)(2,1)S(1)} %get-tuple-element.35), channel_id=1, source_target_pairs={{0,1},{1,2},{2,3},{3,0},{4,5},{5,6},{6,7},{7,4},{8,9},{9,10},{10,1... | collective-permute-start | bytes 442376 | tf_op jit(solution)/shard_map/ppermute | solution.py:48
  23.4 9.3 %collective-permute-start.2 = (bf16[576,128]{1,0:T(8,128)(2,1)S(1)}, bf16[576,128]{1,0:T(8,128)(2,1)S(1)}, u32[]{:S(2)}, u32[]{:S(2)}) collective-permute-start(bf16[576,128]{1,0:T(8,128)(2,1)S(1)} %get-tuple-element.36), channel_id=1, source_target_pairs={{0,2},{1,3},{2,0},{3,1},{4,6},{5,7},{6,4},{7,5},{8,10},{9,11},{10,... | collective-permute-start | bytes 442376 | tf_op jit(solution)/shard_map/ppermute | solution.py:48
  27.7 6.3 %collective-permute-start.3 = (bf16[576,128]{1,0:T(8,128)(2,1)S(1)}, bf16[576,128]{1,0:T(8,128)(2,1)S(1)}, u32[]{:S(2)}, u32[]{:S(2)}) collective-permute-start(bf16[576,128]{1,0:T(8,128)(2,1)S(1)} %get-tuple-element.37), channel_id=1, source_target_pairs={{0,3},{1,0},{2,1},{3,2},{4,7},{5,4},{6,5},{7,6},{8,11},{9,8},{10,9... | collective-permute-start | bytes 442376 | tf_op jit(solution)/shard_map/ppermute | solution.py:48
  55.3 26.9 %copy-start.22 = (bf16[1536,128]{1,0:T(8,128)(2,1)S(1)}, bf16[1536,128]{1,0:T(8,128)(2,1)}, u32[]{:S(2)}) copy-start(bf16[1536,128]{1,0:T(8,128)(2,1)} %param.15) | copy-start | bytes 1179652
  82.5 25.8 %copy-start.12 = (f32[64,256]{1,0:T(8,128)S(1)}, f32[64,256]{1,0:T(8,128)}, u32[]{:S(2)}) copy-start(f32[64,256]{1,0:T(8,128)} %weight_o.3) | copy-start | bytes 196612
  82.6 25.7 %copy-start.18 = (f32[32,128]{1,0:T(8,128)S(1)}, f32[32,128]{1,0:T(8,128)}, u32[]{:S(2)}) copy-start(f32[32,128]{1,0:T(8,128)} %weight_v.3) | copy-start | bytes 49156
  83.2 86.6 %copy-start.10 = (f32[256,256]{1,0:T(8,128)S(1)}, f32[256,256]{1,0:T(8,128)}, u32[]{:S(2)}) copy-start(f32[256,256]{1,0:T(8,128)} %mean_o.1) | copy-start | bytes 786436
  97.0 40.0 %all-to-all-start.4 = ((f32[4,32,384]{2,1,0:T(8,128)}), f32[4,32,384]{2,1,0:T(8,128)S(1)}, u32[]{:S(2)}, u32[]{:S(2)}) async-start(f32[4,32,384]{2,1,0:T(8,128)} %shard_map.196), calls=%async_computation.4 | async-start | bytes 393216 | tf_op jit(solution)/shard_map/all_to_all | solution.py:29
  108.3 16.8 %collective-permute-start.7 = (bf16[1,160,128]{2,1,0:T(8,128)(2,1)S(1)}, bf16[1,160,128]{2,1,0:T(8,128)(2,1)S(1)}, u32[]{:S(2)}, u32[]{:S(2)}) collective-permute-start(bf16[1,160,128]{2,1,0:T(8,128)(2,1)S(1)} %bitcast.11), channel_id=1, source_target_pairs={{0,256},{32,288},{64,320},{96,352},{128,384},{160,416},{192,448},{... | collective-permute-start | bytes 122888 | tf_op jit(solution)/shard_map/ppermute | solution.py:48
  125.1 9.1 %collective-permute-start.8 = (bf16[2,160,128]{2,1,0:T(8,128)(2,1)S(1)}, bf16[2,160,128]{2,1,0:T(8,128)(2,1)S(1)}, u32[]{:S(2)}, u32[]{:S(2)}) collective-permute-start(bf16[2,160,128]{2,1,0:T(8,128)(2,1)S(1)} %pad_maximum_fusion.3), channel_id=1, source_target_pairs={{0,128},{32,160},{64,192},{96,224},{128,256},{160,288},{192,320},{... | collective-permute-start | bytes 245768 | tf_op jit(solution)/shard_map/ppermute | solution.py:48
  134.3 18.9 %collective-permute-start.9 = (bf16[4,160,128]{2,1,0:T(8,128)(2,1)S(1)}, bf16[4,160,128]{2,1,0:T(8,128)(2,1)S(1)}, u32[]{:S(2)}, u32[]{:S(2)}) collective-permute-start(bf16[4,160,128]{2,1,0:T(8,128)(2,1)S(1)} %pad_maximum_fusion.2), channel_id=1, source_target_pairs={{0,64},{32,96},{64,128},{96,160},{128,192},{160,224},{192,256},{22... | collective-permute-start | bytes 491528 | tf_op jit(solution)/shard_map/ppermute | solution.py:48
  137.7 44.1 %all-to-all-start.5 = ((bf16[8,32,384]{2,1,0:T(8,128)(2,1)}), bf16[8,32,384]{2,1,0:T(8,128)(2,1)S(1)}, u32[]{:S(2)}, u32[]{:S(2)}) async-start(bf16[8,32,384]{2,1,0:T(8,128)(2,1)} %shard_map.197), calls=%async_computation.5 | async-start | bytes 393216 | tf_op jit(solution)/shard_map/all_to_all | solution.py:29
  153.2 14.7 %collective-permute-start.10 = (bf16[8,160,128]{2,1,0:T(8,128)(2,1)S(1)}, bf16[8,160,128]{2,1,0:T(8,128)(2,1)}, u32[]{:S(2)}, u32[]{:S(2)}) collective-permute-start(bf16[8,160,128]{2,1,0:T(8,128)(2,1)S(1)} %pad_maximum_fusion.h0), channel_id=1, source_target_pairs={{0,32},{32,64},{64,96},{96,128},{128,160},{160,192},{192,224},{224... | collective-permute-start | bytes 983048 | tf_op jit(solution)/shard_map/ppermute | solution.py:48
  156.5 16.9 %collective-permute-start.6 = (bf16[8,96,256]{2,1,0:T(8,128)(2,1)S(1)}, bf16[8,96,256]{2,1,0:T(8,128)(2,1)S(1)}, u32[]{:S(2)}, u32[]{:S(2)}) collective-permute-start(bf16[8,96,256]{2,1,0:T(8,128)(2,1)S(1)} %all-to-all-done.blocks_ref.b0), channel_id=1, source_target_pairs={{0,12},{4,0},{8,4},{12,8},{1,13},{5,1},{9,5},{13,9},{2,14},{6,2},{... | collective-permute-start | bytes 1179656 | tf_op jit(solution)/shard_map/ppermute | solution.py:48
  159.0 14.4 %collective-permute-start.5 = (bf16[8,96,256]{2,1,0:T(8,128)(2,1)S(1)}, bf16[8,96,256]{2,1,0:T(8,128)(2,1)S(1)}, u32[]{:S(2)}, u32[]{:S(2)}) collective-permute-start(bf16[8,96,256]{2,1,0:T(8,128)(2,1)S(1)} %all-to-all-done.blocks_ref.b0), channel_id=1, source_target_pairs={{0,8},{4,12},{8,0},{12,4},{1,9},{5,13},{9,1},{13,5},{2,10},{6,14},... | collective-permute-start | bytes 1179656 | tf_op jit(solution)/shard_map/ppermute | solution.py:48
  161.3 20.6 %collective-permute-start.4 = (bf16[8,96,256]{2,1,0:T(8,128)(2,1)S(1)}, bf16[8,96,256]{2,1,0:T(8,128)(2,1)S(1)}, u32[]{:S(2)}, u32[]{:S(2)}) collective-permute-start(bf16[8,96,256]{2,1,0:T(8,128)(2,1)S(1)} %all-to-all-done.blocks_ref.b0), channel_id=1, source_target_pairs={{0,4},{4,8},{8,12},{12,0},{1,5},{5,9},{9,13},{13,1},{2,6},{6,10},{... | collective-permute-start | bytes 1179656 | tf_op jit(solution)/shard_map/ppermute | solution.py:48
  163.7 24.9 %collective-permute-start.11 = (bf16[8,160,128]{2,1,0:T(8,128)(2,1)S(1)}, bf16[8,160,128]{2,1,0:T(8,128)(2,1)}, u32[]{:S(2)}, u32[]{:S(2)}) collective-permute-start(bf16[8,160,128]{2,1,0:T(8,128)(2,1)S(1)} %pad_maximum_fusion.h0), channel_id=1, source_target_pairs={{0,16},{16,0},{1,17},{17,1},{2,18},{18,2},{3,19},{19,3},{4,20},{20... | collective-permute-start | bytes 983048 | tf_op jit(solution)/shard_map/ppermute | solution.py:48
  167.9 20.7 %collective-permute-start.12 = (bf16[8,160,128]{2,1,0:T(8,128)(2,1)}, bf16[8,160,128]{2,1,0:T(8,128)(2,1)}, u32[]{:S(2)}, u32[]{:S(2)}) collective-permute-start(bf16[8,160,128]{2,1,0:T(8,128)(2,1)} %collective-permute-done.10.h1), channel_id=1, source_target_pairs={{0,16},{16,0},{1,17},{17,1},{2,18},{18,2},{3,19},{19,3},{4,20},{20... | collective-permute-start | bytes 983048 | tf_op jit(solution)/shard_map/ppermute | solution.py:48
  169.8 1.0 copy-start.11
  170.8 0.9 copy-start.16
  171.7 0.9 copy-start.17
  172.7 0.7 copy-start.5
  181.8 1.0 copy-start.6
  184.3 0.7 copy-start.8
  185.1 10.6 %all-to-all-start.6 = ((f32[16,8,128]{2,1,0:T(8,128)}), f32[16,8,128]{2,1,0:T(8,128)S(1)}, u32[]{:S(2)}, u32[]{:S(2)}) async-start(f32[16,8,128]{2,1,0:T(8,128)} %get-tuple-element.40), calls=%async_computation.6 | async-start | bytes 131072 | tf_op jit(solution)/shard_map/all_to_all | solution.py:29
  188.6 1.0 copy-start.9
  189.6 0.8 copy-start.15
  190.4 0.7 copy-start.19
  191.1 0.7 copy-start.21
  191.7 4.0 %copy-start.13 = (f32[64,256]{1,0:T(8,128)S(1)}, f32[64,256]{1,0:T(8,128)}, u32[]{:S(2)}) copy-start(f32[64,256]{1,0:T(8,128)} %weight_o.3) | copy-start | bytes 196612
  193.7 1.0 copy-start.1
  194.7 1.0 copy-start.3
  195.7 1.2 copy-start.2
  196.9 1.2 copy-start.4

commit v4 on v3

--- a/solution.py
+++ b/solution.py
@@ -22,6 +22,7 @@
 
 BF = jnp.bfloat16
 ROOM = 12 * 2**20
+WHOLE = 67043328
 F32 = jnp.float32
 
 
@@ -53,16 +54,24 @@
 
 
 def pack_kernel(at_ref, attn_ref, lat_ref, *refs):
-    outs, turned = refs[:-1], refs[-1]
+    outs, (attn_here, lat_here, turned, sems) = refs[:-4], refs[-4:]
     groups = len(outs)
     each = attn_ref.shape[0] // groups**2
-    turned[...] = lat_ref[...].T
+    copies = [
+        pltpu.make_async_copy(lat_ref, lat_here, sems.at[0]),
+        pltpu.make_async_copy(attn_ref, attn_here, sems.at[1]),
+    ]
+    for copy in copies:
+        copy.start()
+    copies[0].wait()
+    turned[...] = lat_here[...].T
+    copies[1].wait()
     for k in range(groups):
         g = lax.rem(at_ref[0] + k, groups)
         pieces = []
         for p in range(groups):
             at = pl.multiple_of((p * groups + g) * each, each)
-            outs[k][p * each : (p + 1) * each, :] = attn_ref[pl.ds(at, each), :]
+            outs[k][p * each : (p + 1) * each, :] = attn_here[pl.ds(at, each), :]
             pieces.append(turned[pl.ds(at, each), :])
         half = groups // 2
         for p in range(half):
@@ -73,14 +82,19 @@
 def pack(at, attn_out, lat_turned, groups):
     tokens, heads = attn_out.shape
     rows = tokens // groups
-    vmem = pl.BlockSpec(memory_space=pltpu.VMEM)
+    hbm = pl.BlockSpec(memory_space=pltpu.HBM)
     return pl.pallas_call(
         pack_kernel,
-        in_specs=[pl.BlockSpec(memory_space=pltpu.SMEM), vmem, vmem],
+        in_specs=[pl.BlockSpec(memory_space=pltpu.SMEM), hbm, hbm],
         out_shape=tuple(jax.ShapeDtypeStruct((rows + rows // 2, heads), BF) for _ in range(groups)),
-        scratch_shapes=[pltpu.VMEM(lat_turned.shape[::-1], BF)],
+        scratch_shapes=[
+            pltpu.VMEM(attn_out.shape, BF),
+            pltpu.VMEM(lat_turned.shape, BF),
+            pltpu.VMEM(lat_turned.shape[::-1], BF),
+            pltpu.SemaphoreType.DMA((2,)),
+        ],
         cost_estimate=pl.CostEstimate(flops=10**7, bytes_accessed=10**6, transcendentals=0),
-        compiler_params=pltpu.CompilerParams(vmem_limit_bytes=ROOM),
+        compiler_params=pltpu.CompilerParams(vmem_limit_bytes=WHOLE),
         name="pack",
     )(at, attn_out, lat_turned)
 
@@ -160,33 +174,66 @@
     )(got)
 
 
-def decay_kernel(mean_o, square_o, mean_v, square_v, mean_out, square_out):
-    cols_o = mean_o.shape[1]
-    mean_out[:, :cols_o] = MEAN_DECAY * mean_o[...]
-    mean_out[:, cols_o:] = MEAN_DECAY * mean_v[...]
-    square_out[:, :cols_o] = BETA_SQUARE * square_o[...]
-    square_out[:, cols_o:] = BETA_SQUARE * square_v[...]
-
-
-def decayed(mean_o, square_o, mean_v, square_v):
-    shape = jax.ShapeDtypeStruct((mean_o.shape[0], mean_o.shape[1] + mean_v.shape[1]), F32)
-    return pl.pallas_call(
-        decay_kernel,
-        out_shape=(shape, shape),
-        cost_estimate=pl.CostEstimate(flops=10**6, bytes_accessed=10**6, transcendentals=0),
+def contract_kernel(lifted_ref, cot_o, cot_v, out_ref, total_o, total_v):
+    step = pl.program_id(0)
+    rank = total_o.shape[0]
+    dims = (((0,), (0,)), ((), ()))
+
+    def term(side, cot):
+        rows = lifted_ref[:, side * rank : (side + 1) * rank]
+        return lax.dot_general(rows, cot[...], dims, preferred_element_type=F32)
+
+    @pl.when(step == 0)
+    def _():
+        total_o[...] = term(0, cot_o)
+        total_v[...] = term(1, cot_v)
+
+    @pl.when(step > 0)
+    def _():
+        total_o[...] += term(0, cot_o)
+        total_v[...] += term(1, cot_v)
+
+    @pl.when(step == pl.num_programs(0) - 1)
+    def _():
+        cols_o = total_o.shape[1]
+        parts, each, _ = out_ref.shape
+        for p in range(parts):
+            out_ref[p, :, :cols_o] = total_o[p * each : (p + 1) * each].astype(BF)
+            out_ref[p, :, cols_o:] = total_v[p * each : (p + 1) * each].astype(BF)
+
+
+def contract(lifted, cot_o, cot_v, parts, steps):
+    tokens, both = lifted.shape
+    rank, cols_o, cols_v = both // 2, cot_o.shape[1], cot_v.shape[1]
+    rows = tokens // steps
+    shape = (parts, rank // parts, cols_o + cols_v)
+    return pl.pallas_call(
+        contract_kernel,
+        grid=(steps,),
+        in_specs=[
+            pl.BlockSpec((rows, both), lambda i: (i, 0)),
+            pl.BlockSpec((rows, cols_o), lambda i: (i, 0)),
+            pl.BlockSpec((rows, cols_v), lambda i: (i, 0)),
+        ],
+        out_specs=pl.BlockSpec(shape, lambda i: (0, 0, 0)),
+        out_shape=jax.ShapeDtypeStruct(shape, BF),
+        scratch_shapes=[pltpu.VMEM((rank, cols_o), F32), pltpu.VMEM((rank, cols_v), F32)],
+        cost_estimate=pl.CostEstimate(flops=3 * 10**8, bytes_accessed=3 * 10**6, transcendentals=0),
         compiler_params=pltpu.CompilerParams(vmem_limit_bytes=ROOM),
-        name="decay",
-    )(mean_o, square_o, mean_v, square_v)
+        name="contract",
+    )(lifted, cot_o, cot_v)
 
 
 def direction_kernel(
-    rows_o, cols_o, got_ref, mean_ref, square_ref, b0, b1, b2, b3,
+    rows_o, cols_o, got_ref, mean_o, square_o, mean_v, square_v, b0, b1, b2, b3,
     mean_o_out, square_o_out, mean_v_out, square_v_out, way_out, total_out,
 ):
     near = got_ref.shape[0]
     proj = jnp.concatenate([got_ref[i] for i in range(near)], 0).astype(F32)
-    mean = mean_ref[...] + (1.0 - MEAN_DECAY) * proj
-    square = square_ref[...] + (1.0 - BETA_SQUARE) * proj * proj
+    mean = jnp.concatenate([mean_o[...], mean_v[...]], 1)
+    square = jnp.concatenate([square_o[...], square_v[...]], 1)
+    mean = MEAN_DECAY * mean + (1.0 - MEAN_DECAY) * proj
+    square = BETA_SQUARE * square + (1.0 - BETA_SQUARE) * proj * proj
     mean_o_out[...] = mean[:, :cols_o]
     mean_v_out[...] = mean[:, cols_o:]
     square_o_out[...] = square[:, :cols_o]
@@ -213,23 +260,24 @@
         total_out[i] = tile
 
 
-def directions(rows_o, cols_o, copies, got, mean, square, segments):
-    rank, cols = mean.shape
+def directions(rows_o, copies, got, mean_o, square_o, mean_v, square_v, segments):
+    rank, cols_o = mean_o.shape
+    cols = cols_o + mean_v.shape[1]
     shape = jax.ShapeDtypeStruct
     return pl.pallas_call(
         functools.partial(direction_kernel, rows_o, cols_o),
         out_shape=(
-            shape((rank, cols_o), F32),
-            shape((rank, cols_o), F32),
-            shape((rank, cols - cols_o), F32),
-            shape((rank, cols - cols_o), F32),
+            shape(mean_o.shape, F32),
+            shape(mean_o.shape, F32),
+            shape(mean_v.shape, F32),
+            shape(mean_v.shape, F32),
             shape((rank, cols), F32),
             shape((copies, 8, 128), F32),
         ),
         cost_estimate=pl.CostEstimate(flops=4 * 10**8, bytes_accessed=4 * 10**6, transcendentals=10**5),
         compiler_params=pltpu.CompilerParams(vmem_limit_bytes=ROOM),
         name="directions",
-    )(got, mean, square, *segments)
+    )(got, mean_o, square_o, mean_v, square_v, *segments)
 
 
 def ready_kernel(
@@ -286,33 +334,61 @@
             shape((rows_v * fs, cols_v), BF),
         ),
         cost_estimate=pl.CostEstimate(flops=4 * 10**8, bytes_accessed=4 * 10**6, transcendentals=0),
-        compiler_params=pltpu.CompilerParams(vmem_limit_bytes=ROOM),
+        compiler_params=pltpu.CompilerParams(vmem_limit_bytes=WHOLE),
         name="ready",
     )(at, way, local_o, local_v, *held, *segments)
 
 
 def output_kernel(
-    counts, total_ref, weight_o, weight_v, step_o, step_v, update_o, update_v, old_o, old_v,
+    counts, pieces, total_ref, weight_o, weight_v, step_o, step_v, update_o, update_v, old_o, old_v,
     step_o_out, new_o_out, copy_o_out, step_v_out, new_v_out, copy_v_out,
+    update_o_here, update_v_here, old_o_here, old_v_here, sems,
 ):
+    copies = []
+    for n, (source, here) in enumerate(
+        ((update_o, update_o_here), (old_o, old_o_here), (update_v, update_v_here), (old_v, old_v_here))
+    ):
+        rows = source.shape[0] // pieces
+        for p in range(pieces):
+            part = pl.ds(p * rows, rows)
+            copies.append(pltpu.make_async_copy(source.at[part], here.at[part], sems.at[n, p]))
+    for copy in copies:
+        copy.start()
     total = total_ref[0]
     for i in range(1, total_ref.shape[0]):
         total = total + total_ref[i]
-    for row, count, weight, step, update, old, step_out, new_out, copy_out in (
-        (0, counts[0], weight_o, step_o, update_o, old_o, step_o_out, new_o_out, copy_o_out),
-        (4, counts[1], weight_v, step_v, update_v, old_v, step_v_out, new_v_out, copy_v_out),
+    scales = []
+    for row, count, weight, step, step_out, new_out in (
+        (0, counts[0], weight_o, step_o, step_o_out, new_o_out),
+        (4, counts[1], weight_v, step_v, step_v_out, new_v_out),
     ):
         scale = LEARN_RATE * lax.rsqrt(total[row : row + 1, 0:1] / count + EPS_RMS)
         mine = step[...] * scale
         step_out[...] = mine
         new_out[...] = weight[...] - mine
-        copy_out[...] = (old[...].astype(F32) - update[...].astype(F32) * scale).astype(BF)
+        scales.append(scale)
+    for n, (scale, update, old, copy_out) in enumerate(
+        (
+            (scales[0], update_o_here, old_o_here, copy_o_out),
+            (scales[1], update_v_here, old_v_here, copy_v_out),
+        )
+    ):
+        rows = old.shape[0] // pieces
+        for p in range(pieces):
+            copies[2 * n * pieces + p].wait()
+            copies[(2 * n + 1) * pieces + p].wait()
+            part = pl.ds(p * rows, rows)
+            copy_out[part, :] = (old[part, :].astype(F32) - update[part, :].astype(F32) * scale).astype(BF)
 
 
 def outputs(counts, total, weight_o, weight_v, step_o, step_v, update_o, update_v, old_o, old_v):
     shape = jax.ShapeDtypeStruct
-    return pl.pallas_call(
-        functools.partial(output_kernel, counts),
+    vmem = pl.BlockSpec(memory_space=pltpu.VMEM)
+    hbm = pl.BlockSpec(memory_space=pltpu.HBM)
+    pieces = 4
+    return pl.pallas_call(
+        functools.partial(output_kernel, counts, pieces),
+        in_specs=[vmem] * 5 + [hbm] * 4,
         out_shape=(
             shape(weight_o.shape, F32),
             shape(weight_o.shape, F32),
@@ -321,8 +397,10 @@
             shape(weight_v.shape, F32),
             shape(old_v.shape, BF),
         ),
+        scratch_shapes=[pltpu.VMEM(a.shape, BF) for a in (update_o, update_v, old_o, old_v)]
+        + [pltpu.SemaphoreType.DMA((4, pieces))],
         cost_estimate=pl.CostEstimate(flops=10**7, bytes_accessed=4 * 10**6, transcendentals=10),
-        compiler_params=pltpu.CompilerParams(vmem_limit_bytes=ROOM),
+        compiler_params=pltpu.CompilerParams(vmem_limit_bytes=WHOLE),
         name="outputs",
     )(total, weight_o, weight_v, step_o, step_v, update_o, update_v, old_o, old_v)
 
@@ -376,11 +454,9 @@
     lifted = summed_for(partial, tp, BF)
     lifted = exchange(lifted, TP).reshape(tokens, 2 * rank)
 
-    part_o = dot(lifted[:, :rank].T, out_cot)
-    part_v = dot(lifted[:, rank:].T, value_cot)
-    part = jnp.concatenate([part_o.astype(BF), part_v.astype(BF)], 1)
     near = lax.axis_size(NEAR)
-    part = exchange(part.reshape(near, rank // near, -1), NEAR)
+    part = contract(lifted, out_cot, value_cot, near, 4)
+    part = exchange(part, NEAR)
     part = exchange(summed_for(part, lax.axis_size("zh"), F32), "zh")
     proj = exchange(summed_for(part, near, BF), NEAR)
 
@@ -388,9 +464,8 @@
     for k in range(1, ys):
         segments.append(shifted(blocks, "y", k))
 
-    mean, square = decayed(out_mean, out_square, value_mean, value_square)
     mean_o, square_o, mean_v, square_v, way, total = directions(
-        rows_o, cols_o, tp, proj, mean, square, segments
+        rows_o, tp, proj, out_mean, out_square, value_mean, value_square, segments
     )
     total = exchange(total, TP)
     prepared = ready(cols_o, at, way, out_basis, value_basis, held, segments)

time: 201 us -> 206 us (1.025)
  local copies, waits for them, and re-layouts: 14.7 us -> 5.28 us
  Pallas kernels: 8.8 us -> 17.7 us
  waiting for transfers between devices: 21 us -> 25.9 us
    unnamed x46 -> x36, local copies, waits for them, and re-layouts: 13.7 us -> 4.5 us
    ppermute x12, waiting for transfers between devices: 21 us -> 25 us  [shifted(): lax.ppermute(value, axis, [(i, (i + by) % devices) for i in range(devices)])]
    pallas_call x2, Pallas kernels: 1.83 us -> 5.17 us  [the longest x1 3.82 us: outputs(): pl.pallas_call(functools.partial(output_kernel, counts, pieces), in_specs...]
    pallas_call x1, Pallas kernels: 1.99 us -> 4.09 us  [ready(): pl.pallas_call(functools.partial(ready_kernel, rows_o, rows_v, cols_o), i...]
  transfers between devices with their start and end apart: 17 -> 17, of which waited for: 5 -> 7; matrix products, arithmetic and copies ran while one was open for 0% -> 0% of each run, Pallas kernels for 3% -> 5%
where the time goes in v4:
time: 206 us; the launch traced here: 205 us
  starting transfers between devices  93.2 us (45%)
  blocking collectives  60.1 us (29%)
  waiting for transfers between devices  25.9 us (13%)
  Pallas kernels  17.7 us (9%)
  local copies, waits for them, and re-layouts  5.28 us (3%)
    all_to_all x3, blocking collectives, exchange(): return lax.all_to_all(value, axes, 0, 0, tiled=True)  60.1 us
    ppermute x12, starting transfers between devices, shifted(): lax.ppermute(value, axis, [(i, (i + by) % devices) for i in range(devices)])  46.6 us
    all_to_all x4, starting transfers between devices, exchange(): return lax.all_to_all(value, axes, 0, 0, tiled=True)  46 us
    ppermute x12, waiting for transfers between devices, shifted(): lax.ppermute(value, axis, [(i, (i + by) % devices) for i in range(devices)])  25 us
    unnamed x36, local copies, waits for them, and re-layouts  4.5 us
  transfers between devices with their start and end apart: 17, of which 7 were waited for; matrix products, arithmetic and copies ran while one was open for 0% of the time, Pallas kernels for 5%

profile of v4, /device:TPU:1, one launch (start us, length us, event | category | flops | bytes accessed | tf_op | source)
XLA Modules:
  0.0 204.6 jit_solution(13322418956558893405)
XLA Ops:
  0.6 0.8 pad_maximum_fusion.3
  1.4 0.7 collective-permute-start
  2.1 0.8 broadcast_in_dim.4
  2.9 15.3 %all-to-all-start = ((bf16[8,96,256]{2,1,0:T(8,128)(2,1)}), bf16[8,96,256]{2,1,0:T(8,128)(2,1)}, u32[]{:S(2)}, u32[]{:S(2)}) async-start(bf16[8,96,256]{2,1,0:T(8,128)(2,1)} %broadcast_in_dim.4), calls=%async_computation | async-start | bytes 786432 | tf_op jit(solution)/shard_map/all_to_all | solution.py:30
  18.1 0.6 pad_add_fusion.at_ref
  18.7 2.7 %pack.1 = (bf16[576,128]{1,0:T(8,128)(2,1)}, bf16[576,128]{1,0:T(8,128)(2,1)}, bf16[576,128]{1,0:T(8,128)(2,1)}, bf16[576,128]{1,0:T(8,128)(2,1)}) custom-call(s32[4]{0:T(128)} %pad_add_fusion.at_ref, bf16[1536,128]{1,0:T(8,128)(2,1)} %attn_ref.1, bf16[64,1536]{1,0:T(8,128)(2,1)} %bitcast.10), custom_call_target="tpu_custom_call" | custom-call | flops 10000000 | bytes 1000000 | tf_op jit(solution)/shard_map/pack/pallas_call | solution.py:86
  21.4 3.3 %collective-permute-start.1 = (bf16[576,128]{1,0:T(8,128)(2,1)}, bf16[576,128]{1,0:T(8,128)(2,1)S(1)}, u32[]{:S(2)}, u32[]{:S(2)}) collective-permute-start(bf16[576,128]{1,0:T(8,128)(2,1)} %get-tuple-element.33), channel_id=1, source_target_pairs={{0,1},{1,2},{2,3},{3,0},{4,5},{5,6},{6,7},{7,4},{8,9},{9,10},{10,1... | collective-permute-start | bytes 442376 | tf_op jit(solution)/shard_map/ppermute | solution.py:49
  24.6 4.3 %collective-permute-start.2 = (bf16[576,128]{1,0:T(8,128)(2,1)}, bf16[576,128]{1,0:T(8,128)(2,1)S(1)}, u32[]{:S(2)}, u32[]{:S(2)}) collective-permute-start(bf16[576,128]{1,0:T(8,128)(2,1)} %get-tuple-element.34), channel_id=1, source_target_pairs={{0,2},{1,3},{2,0},{3,1},{4,6},{5,7},{6,4},{7,5},{8,10},{9,11},{10,... | collective-permute-start | bytes 442376 | tf_op jit(solution)/shard_map/ppermute | solution.py:49
  28.9 3.1 %collective-permute-start.3 = (bf16[576,128]{1,0:T(8,128)(2,1)}, bf16[576,128]{1,0:T(8,128)(2,1)S(1)}, u32[]{:S(2)}, u32[]{:S(2)}) collective-permute-start(bf16[576,128]{1,0:T(8,128)(2,1)} %get-tuple-element.35), channel_id=1, source_target_pairs={{0,3},{1,0},{2,1},{3,2},{4,7},{5,4},{6,5},{7,6},{8,11},{9,8},{10,9... | collective-permute-start | bytes 442376 | tf_op jit(solution)/shard_map/ppermute | solution.py:49
  32.1 2.1 %collective-permute-done.2.refs_2_ = bf16[576,128]{1,0:T(8,128)(2,1)S(1)} collective-permute-done((bf16[576,128]{1,0:T(8,128)(2,1)}, bf16[576,128]{1,0:T(8,128)(2,1)S(1)}, u32[]{:S(2)}, u32[]{:S(2)}) %collective-permute-start.2) | collective-permute-done | bytes 147488 | tf_op jit(solution)/shard_map/ppermute | solution.py:49
  34.1 1.4 collective-permute-done.3.refs_3_
  35.5 0.9 copy-done.9
  36.4 0.6 copy-done.13
  37.0 1.6 lift.1
  38.6 20.0 %all_to_all.35.got_ref = bf16[4,96,512]{2,1,0:T(8,128)(2,1)S(1)} all-to-all(bf16[4,96,512]{2,1,0:T(8,128)(2,1)S(1)} %lift.1), channel_id=1, replica_groups=mesh['zh'=4,'zl'=4,'c'=2,'y'=4,'x'=4] {'y'}, dimensions={0} | all-to-all | bytes 786432 | tf_op jit(solution)/shard_map/all_to_all | solution.py:30
  58.5 0.2 shard_map.195
  58.7 0.0 copy-start.4
  58.7 26.9 %all_to_all.36 = bf16[16,96,512]{2,1,0:T(8,128)(2,1)S(1)} all-to-all(bf16[16,96,512]{2,1,0:T(8,128)(2,1)S(1)} %shard_map.195), channel_id=1, replica_groups=mesh['zh'=4,'zl'=4,'c'=2,'y'=4,'x'=4] {'y','x'}, dimensions={0} | all-to-all | bytes 3145728 | tf_op jit(solution)/shard_map/all_to_all | solution.py:30
  85.7 1.4 contract.1
  87.0 0.0 copy-start.6
  87.0 0.0 copy-start.7
  87.1 13.2 %all_to_all.37.got_ref = bf16[8,32,384]{2,1,0:T(8,128)(2,1)S(1)} all-to-all(bf16[8,32,384]{2,1,0:T(8,128)(2,1)S(1)} %contract.1), channel_id=1, replica_groups=mesh['zh'=4,'zl'=4,'c'=2,'y'=4,'x'=4] {'zl','c'}, dimensions={0} | all-to-all | bytes 393216 | tf_op jit(solution)/shard_map/all_to_all | solution.py:30
  100.3 0.7 shard_map.196
  101.0 11.1 %all-to-all-start.4 = ((f32[4,32,384]{2,1,0:T(8,128)}), f32[4,32,384]{2,1,0:T(8,128)S(1)}, u32[]{:S(2)}, u32[]{:S(2)}) async-start(f32[4,32,384]{2,1,0:T(8,128)} %shard_map.196), calls=%async_computation.4 | async-start | bytes 393216 | tf_op jit(solution)/shard_map/all_to_all | solution.py:30
  112.2 12.1 %collective-permute-start.7 = (bf16[1,160,128]{2,1,0:T(8,128)(2,1)S(1)}, bf16[1,160,128]{2,1,0:T(8,128)(2,1)S(1)}, u32[]{:S(2)}, u32[]{:S(2)}) collective-permute-start(bf16[1,160,128]{2,1,0:T(8,128)(2,1)S(1)} %bitcast.8), channel_id=1, source_target_pairs={{0,256},{32,288},{64,320},{96,352},{128,384},{160,416},{192,448},{... | collective-permute-start | bytes 122888 | tf_op jit(solution)/shard_map/ppermute | solution.py:49
  124.3 4.7 %collective-permute-done.7 = bf16[1,160,128]{2,1,0:T(8,128)(2,1)S(1)} collective-permute-done((bf16[1,160,128]{2,1,0:T(8,128)(2,1)S(1)}, bf16[1,160,128]{2,1,0:T(8,128)(2,1)S(1)}, u32[]{:S(2)}, u32[]{:S(2)}) %collective-permute-start.7) | collective-permute-done | bytes 40992 | tf_op jit(solution)/shard_map/ppermute | solution.py:49
  129.0 4.5 %collective-permute-start.8 = (bf16[2,160,128]{2,1,0:T(8,128)(2,1)S(1)}, bf16[2,160,128]{2,1,0:T(8,128)(2,1)S(1)}, u32[]{:S(2)}, u32[]{:S(2)}) collective-permute-start(bf16[2,160,128]{2,1,0:T(8,128)(2,1)S(1)} %pad_maximum_fusion.2), channel_id=1, source_target_pairs={{0,128},{32,160},{64,192},{96,224},{128,256},{160,288},{192,320},{... | collective-permute-start | bytes 245768 | tf_op jit(solution)/shard_map/ppermute | solution.py:49
  133.5 4.6 %collective-permute-done.8 = bf16[2,160,128]{2,1,0:T(8,128)(2,1)S(1)} collective-permute-done((bf16[2,160,128]{2,1,0:T(8,128)(2,1)S(1)}, bf16[2,160,128]{2,1,0:T(8,128)(2,1)S(1)}, u32[]{:S(2)}, u32[]{:S(2)}) %collective-permute-start.8) | collective-permute-done | bytes 81952 | tf_op jit(solution)/shard_map/ppermute | solution.py:49
  138.2 2.7 %collective-permute-start.9 = (bf16[4,160,128]{2,1,0:T(8,128)(2,1)S(1)}, bf16[4,160,128]{2,1,0:T(8,128)(2,1)S(1)}, u32[]{:S(2)}, u32[]{:S(2)}) collective-permute-start(bf16[4,160,128]{2,1,0:T(8,128)(2,1)S(1)} %pad_maximum_fusion.1), channel_id=1, source_target_pairs={{0,64},{32,96},{64,128},{96,160},{128,192},{160,224},{192,256},{22... | collective-permute-start | bytes 491528 | tf_op jit(solution)/shard_map/ppermute | solution.py:49
  140.9 0.7 shard_map.197
  141.6 15.4 %all-to-all-start.5 = ((bf16[8,32,384]{2,1,0:T(8,128)(2,1)}), bf16[8,32,384]{2,1,0:T(8,128)(2,1)S(1)}, u32[]{:S(2)}, u32[]{:S(2)}) async-start(bf16[8,32,384]{2,1,0:T(8,128)(2,1)} %shard_map.197), calls=%async_computation.5 | async-start | bytes 393216 | tf_op jit(solution)/shard_map/all_to_all | solution.py:30
  157.1 3.3 %collective-permute-start.10 = (bf16[8,160,128]{2,1,0:T(8,128)(2,1)S(1)}, bf16[8,160,128]{2,1,0:T(8,128)(2,1)S(1)}, u32[]{:S(2)}, u32[]{:S(2)}) collective-permute-start(bf16[8,160,128]{2,1,0:T(8,128)(2,1)S(1)} %pad_maximum_fusion.h0), channel_id=1, source_target_pairs={{0,32},{32,64},{64,96},{96,128},{128,160},{160,192},{192,224},{224... | collective-permute-start | bytes 983048 | tf_op jit(solution)/shard_map/ppermute | solution.py:49
  160.4 2.5 %collective-permute-start.6 = (bf16[8,96,256]{2,1,0:T(8,128)(2,1)}, bf16[8,96,256]{2,1,0:T(8,128)(2,1)S(1)}, u32[]{:S(2)}, u32[]{:S(2)}) collective-permute-start(bf16[8,96,256]{2,1,0:T(8,128)(2,1)} %all-to-all-done.blocks_ref.b0), channel_id=1, source_target_pairs={{0,12},{4,0},{8,4},{12,8},{1,13},{5,1},{9,5},{13,9},{2,14},{6,2},{... | collective-permute-start | bytes 1179656 | tf_op jit(solution)/shard_map/ppermute | solution.py:49
  162.8 2.3 %collective-permute-start.5 = (bf16[8,96,256]{2,1,0:T(8,128)(2,1)}, bf16[8,96,256]{2,1,0:T(8,128)(2,1)S(1)}, u32[]{:S(2)}, u32[]{:S(2)}) collective-permute-start(bf16[8,96,256]{2,1,0:T(8,128)(2,1)} %all-to-all-done.blocks_ref.b0), channel_id=1, source_target_pairs={{0,8},{4,12},{8,0},{12,4},{1,9},{5,13},{9,1},{13,5},{2,10},{6,14},... | collective-permute-start | bytes 1179656 | tf_op jit(solution)/shard_map/ppermute | solution.py:49
  165.1 2.4 %collective-permute-start.4 = (bf16[8,96,256]{2,1,0:T(8,128)(2,1)}, bf16[8,96,256]{2,1,0:T(8,128)(2,1)S(1)}, u32[]{:S(2)}, u32[]{:S(2)}) collective-permute-start(bf16[8,96,256]{2,1,0:T(8,128)(2,1)} %all-to-all-done.blocks_ref.b0), channel_id=1, source_target_pairs={{0,4},{4,8},{8,12},{12,0},{1,5},{5,9},{9,13},{13,1},{2,6},{6,10},{... | collective-permute-start | bytes 1179656 | tf_op jit(solution)/shard_map/ppermute | solution.py:49
  167.6 4.2 %collective-permute-start.11 = (bf16[8,160,128]{2,1,0:T(8,128)(2,1)S(1)}, bf16[8,160,128]{2,1,0:T(8,128)(2,1)S(1)}, u32[]{:S(2)}, u32[]{:S(2)}) collective-permute-start(bf16[8,160,128]{2,1,0:T(8,128)(2,1)S(1)} %pad_maximum_fusion.h0), channel_id=1, source_target_pairs={{0,16},{16,0},{1,17},{17,1},{2,18},{18,2},{3,19},{19,3},{4,20},{20... | collective-permute-start | bytes 983048 | tf_op jit(solution)/shard_map/ppermute | solution.py:49
  171.8 1.9 collective-permute-start.12
  173.7 1.7 collective-permute-done.5.b2
  175.4 10.5 %collective-permute-done.4.b1 = bf16[8,96,256]{2,1,0:T(8,128)(2,1)S(1)} collective-permute-done((bf16[8,96,256]{2,1,0:T(8,128)(2,1)}, bf16[8,96,256]{2,1,0:T(8,128)(2,1)S(1)}, u32[]{:S(2)}, u32[]{:S(2)}) %collective-permute-start.4) | collective-permute-done | bytes 393248 | tf_op jit(solution)/shard_map/ppermute | solution.py:49
  186.0 2.6 %directions.1 = (f32[256,256]{1,0:T(8,128)}, f32[256,256]{1,0:T(8,128)}, f32[256,128]{1,0:T(8,128)}, f32[256,128]{1,0:T(8,128)}, f32[256,384]{1,0:T(8,128)S(1)}, /*index=5*/f32[16,8,128]{2,1,0:T(8,128)}) custom-call(bf16[8,32,384]{2,1,0:T(8,128)(2,1)S(1)} %all-to-all-done.5.got_ref, f32[256,256]{1,0:T(8,128)S(1)} %copy-done.6, f32[256,256]{1,0:T(8,128)S(1)} %copy-done.7, ...), custom_call_target="tpu_custom_call" | custom-call | flops 400000000 | bytes 4000000 | tf_op jit(solution)/shard_map/directions/pallas_call | solution.py:267
  188.6 0.7 copy-done
  189.3 0.7 copy-done.5
  190.1 4.1 %all-to-all-start.6 = ((f32[16,8,128]{2,1,0:T(8,128)}), f32[16,8,128]{2,1,0:T(8,128)}, u32[]{:S(2)}, u32[]{:S(2)}) async-start(f32[16,8,128]{2,1,0:T(8,128)} %get-tuple-element.36), calls=%async_computation.6 | async-start | bytes 131072 | tf_op jit(solution)/shard_map/all_to_all | solution.py:30
  194.3 0.7 copy-done.16
  195.0 0.7 copy-done.17
  195.7 4.1 %ready.1 = (f32[64,256]{1,0:T(8,128)}, f32[32,128]{1,0:T(8,128)}, bf16[2048,256]{1,0:T(8,128)(2,1)}, bf16[1024,128]{1,0:T(8,128)(2,1)}, bf16[2048,256]{1,0:T(8,128)(2,1)}, /*index=5*/bf16[1024,128]{1,0:T(8,128)(2,1)}) custom-call(s32[4]{0:T(128)} %pad_add_fusion.at_ref, f32[256,384]{1,0:T(8,128)} %copy-done.5, bf16[64,256]{1,0:T(8,128)(2,1)} %local_o.1, ...), custom_call_target="tpu_custom_call" | custom-call | flops 400000000 | bytes 4000000 | tf_op jit(solution)/shard_map/ready/pallas_call | solution.py:325
  199.8 0.9 all-to-all-done.6.total_ref
  200.8 3.8 %outputs.1 = (f32[64,256]{1,0:T(8,128)}, f32[64,256]{1,0:T(8,128)}, bf16[2048,256]{1,0:T(8,128)(2,1)}, f32[32,128]{1,0:T(8,128)}, f32[32,128]{1,0:T(8,128)}, /*index=5*/bf16[1024,128]{1,0:T(8,128)(2,1)}) custom-call(f32[16,8,128]{2,1,0:T(8,128)} %all-to-all-done.6.total_ref, f32[64,256]{1,0:T(8,128)} %weight_o.3, f32[32,128]{1,0:T(8,128)} %weight_v.3, ...), custom_call_target="tpu_custom_call" | custom-call | flops 10000000 | bytes 4000000 | tf_op jit(solution)/shard_map/outputs/pallas_call | solution.py:389
  (41 shorter events, 0.1 us)
Async XLA Ops:
  1.4 0.7 collective-permute-start
  2.9 32.6 %all-to-all-start = ((bf16[8,96,256]{2,1,0:T(8,128)(2,1)}), bf16[8,96,256]{2,1,0:T(8,128)(2,1)}, u32[]{:S(2)}, u32[]{:S(2)}) async-start(bf16[8,96,256]{2,1,0:T(8,128)(2,1)} %broadcast_in_dim.4), calls=%async_computation | async-start | bytes 786432 | tf_op jit(solution)/shard_map/all_to_all | solution.py:30
  21.4 10.7 %collective-permute-start.1 = (bf16[576,128]{1,0:T(8,128)(2,1)}, bf16[576,128]{1,0:T(8,128)(2,1)S(1)}, u32[]{:S(2)}, u32[]{:S(2)}) collective-permute-start(bf16[576,128]{1,0:T(8,128)(2,1)} %get-tuple-element.33), channel_id=1, source_target_pairs={{0,1},{1,2},{2,3},{3,0},{4,5},{5,6},{6,7},{7,4},{8,9},{9,10},{10,1... | collective-permute-start | bytes 442376 | tf_op jit(solution)/shard_map/ppermute | solution.py:49
  24.6 9.5 %collective-permute-start.2 = (bf16[576,128]{1,0:T(8,128)(2,1)}, bf16[576,128]{1,0:T(8,128)(2,1)S(1)}, u32[]{:S(2)}, u32[]{:S(2)}) collective-permute-start(bf16[576,128]{1,0:T(8,128)(2,1)} %get-tuple-element.34), channel_id=1, source_target_pairs={{0,2},{1,3},{2,0},{3,1},{4,6},{5,7},{6,4},{7,5},{8,10},{9,11},{10,... | collective-permute-start | bytes 442376 | tf_op jit(solution)/shard_map/ppermute | solution.py:49
  28.9 6.6 %collective-permute-start.3 = (bf16[576,128]{1,0:T(8,128)(2,1)}, bf16[576,128]{1,0:T(8,128)(2,1)S(1)}, u32[]{:S(2)}, u32[]{:S(2)}) collective-permute-start(bf16[576,128]{1,0:T(8,128)(2,1)} %get-tuple-element.35), channel_id=1, source_target_pairs={{0,3},{1,0},{2,1},{3,2},{4,7},{5,4},{6,5},{7,6},{8,11},{9,8},{10,9... | collective-permute-start | bytes 442376 | tf_op jit(solution)/shard_map/ppermute | solution.py:49
  35.5 0.9 copy-start.9
  36.4 0.6 copy-start.13
  58.7 27.0 %copy-start.3 = (bf16[1536,256]{1,0:T(8,128)(2,1)S(1)}, bf16[1536,256]{1,0:T(8,128)(2,1)}, u32[]{:S(2)}) copy-start(bf16[1536,256]{1,0:T(8,128)(2,1)} %cot_o.1) | copy-start | bytes 2359300
  58.7 26.9 %copy-start.4 = (bf16[1536,128]{1,0:T(8,128)(2,1)S(1)}, bf16[1536,128]{1,0:T(8,128)(2,1)}, u32[]{:S(2)}) copy-start(bf16[1536,128]{1,0:T(8,128)(2,1)} %cot_v.1) | copy-start | bytes 1179652
  85.7 26.5 %copy-start.8 = (f32[64,256]{1,0:T(8,128)S(1)}, f32[64,256]{1,0:T(8,128)}, u32[]{:S(2)}) copy-start(f32[64,256]{1,0:T(8,128)} %weight_o.3) | copy-start | bytes 196612
  85.7 26.5 %copy-start.12 = (f32[32,128]{1,0:T(8,128)S(1)}, f32[32,128]{1,0:T(8,128)}, u32[]{:S(2)}) copy-start(f32[32,128]{1,0:T(8,128)} %weight_v.3) | copy-start | bytes 49156
  87.0 98.9 %copy-start.6 = (f32[256,256]{1,0:T(8,128)S(1)}, f32[256,256]{1,0:T(8,128)}, u32[]{:S(2)}) copy-start(f32[256,256]{1,0:T(8,128)} %mean_o.1) | copy-start | bytes 786436
  87.0 98.9 %copy-start.7 = (f32[256,256]{1,0:T(8,128)S(1)}, f32[256,256]{1,0:T(8,128)}, u32[]{:S(2)}) copy-start(f32[256,256]{1,0:T(8,128)} %square_o.1) | copy-start | bytes 786436
  87.1 98.9 %copy-start.10 = (f32[256,128]{1,0:T(8,128)S(1)}, f32[256,128]{1,0:T(8,128)}, u32[]{:S(2)}) copy-start(f32[256,128]{1,0:T(8,128)} %mean_v.1) | copy-start | bytes 393220
  87.1 98.9 %copy-start.11 = (f32[256,128]{1,0:T(8,128)S(1)}, f32[256,128]{1,0:T(8,128)}, u32[]{:S(2)}) copy-start(f32[256,128]{1,0:T(8,128)} %square_v.1) | copy-start | bytes 393220
  101.0 39.9 %all-to-all-start.4 = ((f32[4,32,384]{2,1,0:T(8,128)}), f32[4,32,384]{2,1,0:T(8,128)S(1)}, u32[]{:S(2)}, u32[]{:S(2)}) async-start(f32[4,32,384]{2,1,0:T(8,128)} %shard_map.196), calls=%async_computation.4 | async-start | bytes 393216 | tf_op jit(solution)/shard_map/all_to_all | solution.py:30
  112.2 16.8 %collective-permute-start.7 = (bf16[1,160,128]{2,1,0:T(8,128)(2,1)S(1)}, bf16[1,160,128]{2,1,0:T(8,128)(2,1)S(1)}, u32[]{:S(2)}, u32[]{:S(2)}) collective-permute-start(bf16[1,160,128]{2,1,0:T(8,128)(2,1)S(1)} %bitcast.8), channel_id=1, source_target_pairs={{0,256},{32,288},{64,320},{96,352},{128,384},{160,416},{192,448},{... | collective-permute-start | bytes 122888 | tf_op jit(solution)/shard_map/ppermute | solution.py:49
  129.0 9.1 %collective-permute-start.8 = (bf16[2,160,128]{2,1,0:T(8,128)(2,1)S(1)}, bf16[2,160,128]{2,1,0:T(8,128)(2,1)S(1)}, u32[]{:S(2)}, u32[]{:S(2)}) collective-permute-start(bf16[2,160,128]{2,1,0:T(8,128)(2,1)S(1)} %pad_maximum_fusion.2), channel_id=1, source_target_pairs={{0,128},{32,160},{64,192},{96,224},{128,256},{160,288},{192,320},{... | collective-permute-start | bytes 245768 | tf_op jit(solution)/shard_map/ppermute | solution.py:49
  138.2 18.9 %collective-permute-start.9 = (bf16[4,160,128]{2,1,0:T(8,128)(2,1)S(1)}, bf16[4,160,128]{2,1,0:T(8,128)(2,1)S(1)}, u32[]{:S(2)}, u32[]{:S(2)}) collective-permute-start(bf16[4,160,128]{2,1,0:T(8,128)(2,1)S(1)} %pad_maximum_fusion.1), channel_id=1, source_target_pairs={{0,64},{32,96},{64,128},{96,160},{128,192},{160,224},{192,256},{22... | collective-permute-start | bytes 491528 | tf_op jit(solution)/shard_map/ppermute | solution.py:49
  141.6 44.3 %all-to-all-start.5 = ((bf16[8,32,384]{2,1,0:T(8,128)(2,1)}), bf16[8,32,384]{2,1,0:T(8,128)(2,1)S(1)}, u32[]{:S(2)}, u32[]{:S(2)}) async-start(bf16[8,32,384]{2,1,0:T(8,128)(2,1)} %shard_map.197), calls=%async_computation.5 | async-start | bytes 393216 | tf_op jit(solution)/shard_map/all_to_all | solution.py:30
  157.1 33.0 %copy-start.14 = (bf16[8,160,128]{2,1,0:T(8,128)(2,1)}, bf16[8,160,128]{2,1,0:T(8,128)(2,1)S(1)}, u32[]{:S(2)}) copy-start(bf16[8,160,128]{2,1,0:T(8,128)(2,1)S(1)} %pad_maximum_fusion.h0) | copy-start | bytes 983044
  157.1 14.7 %collective-permute-start.10 = (bf16[8,160,128]{2,1,0:T(8,128)(2,1)S(1)}, bf16[8,160,128]{2,1,0:T(8,128)(2,1)S(1)}, u32[]{:S(2)}, u32[]{:S(2)}) collective-permute-start(bf16[8,160,128]{2,1,0:T(8,128)(2,1)S(1)} %pad_maximum_fusion.h0), channel_id=1, source_target_pairs={{0,32},{32,64},{64,96},{96,128},{128,160},{160,192},{192,224},{224... | collective-permute-start | bytes 983048 | tf_op jit(solution)/shard_map/ppermute | solution.py:49
  160.4 13.3 %collective-permute-start.6 = (bf16[8,96,256]{2,1,0:T(8,128)(2,1)}, bf16[8,96,256]{2,1,0:T(8,128)(2,1)S(1)}, u32[]{:S(2)}, u32[]{:S(2)}) collective-permute-start(bf16[8,96,256]{2,1,0:T(8,128)(2,1)} %all-to-all-done.blocks_ref.b0), channel_id=1, source_target_pairs={{0,12},{4,0},{8,4},{12,8},{1,13},{5,1},{9,5},{13,9},{2,14},{6,2},{... | collective-permute-start | bytes 1179656 | tf_op jit(solution)/shard_map/ppermute | solution.py:49
  162.8 12.6 %collective-permute-start.5 = (bf16[8,96,256]{2,1,0:T(8,128)(2,1)}, bf16[8,96,256]{2,1,0:T(8,128)(2,1)S(1)}, u32[]{:S(2)}, u32[]{:S(2)}) collective-permute-start(bf16[8,96,256]{2,1,0:T(8,128)(2,1)} %all-to-all-done.blocks_ref.b0), channel_id=1, source_target_pairs={{0,8},{4,12},{8,0},{12,4},{1,9},{5,13},{9,1},{13,5},{2,10},{6,14},... | collective-permute-start | bytes 1179656 | tf_op jit(solution)/shard_map/ppermute | solution.py:49
  165.1 20.8 %collective-permute-start.4 = (bf16[8,96,256]{2,1,0:T(8,128)(2,1)}, bf16[8,96,256]{2,1,0:T(8,128)(2,1)S(1)}, u32[]{:S(2)}, u32[]{:S(2)}) collective-permute-start(bf16[8,96,256]{2,1,0:T(8,128)(2,1)} %all-to-all-done.blocks_ref.b0), channel_id=1, source_target_pairs={{0,4},{4,8},{8,12},{12,0},{1,5},{5,9},{9,13},{13,1},{2,6},{6,10},{... | collective-permute-start | bytes 1179656 | tf_op jit(solution)/shard_map/ppermute | solution.py:49
  167.6 26.7 %collective-permute-start.11 = (bf16[8,160,128]{2,1,0:T(8,128)(2,1)S(1)}, bf16[8,160,128]{2,1,0:T(8,128)(2,1)S(1)}, u32[]{:S(2)}, u32[]{:S(2)}) collective-permute-start(bf16[8,160,128]{2,1,0:T(8,128)(2,1)S(1)} %pad_maximum_fusion.h0), channel_id=1, source_target_pairs={{0,16},{16,0},{1,17},{17,1},{2,18},{18,2},{3,19},{19,3},{4,20},{20... | collective-permute-start | bytes 983048 | tf_op jit(solution)/shard_map/ppermute | solution.py:49
  171.8 22.5 %copy-start.15 = (bf16[8,160,128]{2,1,0:T(8,128)(2,1)}, bf16[8,160,128]{2,1,0:T(8,128)(2,1)S(1)}, u32[]{:S(2)}) copy-start(bf16[8,160,128]{2,1,0:T(8,128)(2,1)S(1)} %collective-permute-done.10.h1) | copy-start | bytes 983044
  171.8 22.5 %collective-permute-start.12 = (bf16[8,160,128]{2,1,0:T(8,128)(2,1)S(1)}, bf16[8,160,128]{2,1,0:T(8,128)(2,1)S(1)}, u32[]{:S(2)}, u32[]{:S(2)}) collective-permute-start(bf16[8,160,128]{2,1,0:T(8,128)(2,1)S(1)} %collective-permute-done.10.h1), channel_id=1, source_target_pairs={{0,16},{16,0},{1,17},{17,1},{2,18},{18,2},{3,19},{19,3},{4,20},{20... | collective-permute-start | bytes 983048 | tf_op jit(solution)/shard_map/ppermute | solution.py:49
  175.4 13.2 %copy-start.1 = (bf16[8,96,256]{2,1,0:T(8,128)(2,1)}, bf16[8,96,256]{2,1,0:T(8,128)(2,1)S(1)}, u32[]{:S(2)}) copy-start(bf16[8,96,256]{2,1,0:T(8,128)(2,1)S(1)} %collective-permute-done.5.b2) | copy-start | bytes 1179652
  185.9 4.2 %copy-start.2 = (bf16[8,96,256]{2,1,0:T(8,128)(2,1)}, bf16[8,96,256]{2,1,0:T(8,128)(2,1)S(1)}, u32[]{:S(2)}) copy-start(bf16[8,96,256]{2,1,0:T(8,128)(2,1)S(1)} %collective-permute-done.4.b1) | copy-start | bytes 1179652
  188.6 0.7 copy-start
  189.3 0.7 copy-start.5
  190.1 10.7 %all-to-all-start.6 = ((f32[16,8,128]{2,1,0:T(8,128)}), f32[16,8,128]{2,1,0:T(8,128)}, u32[]{:S(2)}, u32[]{:S(2)}) async-start(f32[16,8,128]{2,1,0:T(8,128)} %get-tuple-element.36), calls=%async_computation.6 | async-start | bytes 131072 | tf_op jit(solution)/shard_map/all_to_all | solution.py:30
  194.3 0.7 copy-start.16
  195.0 0.7 copy-start.17

commit v5 on v4

--- a/solution.py
+++ b/solution.py
@@ -23,6 +23,7 @@
 BF = jnp.bfloat16
 ROOM = 12 * 2**20
 WHOLE = 67043328
+STEPS = (0, 1, 2, -1)
 F32 = jnp.float32
 
 
@@ -53,7 +54,7 @@
     return jnp.dot(a, b, preferred_element_type=F32)
 
 
-def pack_kernel(at_ref, attn_ref, lat_ref, *refs):
+def pack_kernel( attn_ref, lat_ref, *refs):
     outs, (attn_here, lat_here, turned, sems) = refs[:-4], refs[-4:]
     groups = len(outs)
     each = attn_ref.shape[0] // groups**2
@@ -67,7 +68,7 @@
     turned[...] = lat_here[...].T
     copies[1].wait()
     for k in range(groups):
-        g = lax.rem(at_ref[0] + k, groups)
+        g = lax.rem(lax.axis_index("x") + k, groups)
         pieces = []
         for p in range(groups):
             at = pl.multiple_of((p * groups + g) * each, each)
@@ -79,13 +80,13 @@
             outs[k][at : at + each, :] = jnp.concatenate([pieces[p], pieces[half + p]], axis=1)
 
 
-def pack(at, attn_out, lat_turned, groups):
+def pack(attn_out, lat_turned, groups):
     tokens, heads = attn_out.shape
     rows = tokens // groups
     hbm = pl.BlockSpec(memory_space=pltpu.HBM)
     return pl.pallas_call(
         pack_kernel,
-        in_specs=[pl.BlockSpec(memory_space=pltpu.SMEM), hbm, hbm],
+        in_specs=[hbm, hbm],
         out_shape=tuple(jax.ShapeDtypeStruct((rows + rows // 2, heads), BF) for _ in range(groups)),
         scratch_shapes=[
             pltpu.VMEM(attn_out.shape, BF),
@@ -96,7 +97,7 @@
         cost_estimate=pl.CostEstimate(flops=10**7, bytes_accessed=10**6, transcendentals=0),
         compiler_params=pltpu.CompilerParams(vmem_limit_bytes=WHOLE),
         name="pack",
-    )(at, attn_out, lat_turned)
+    )(attn_out, lat_turned)
 
 
 def old_kernel(weight_o, weight_v, out_ref):
@@ -117,7 +118,7 @@
     )(weight_o, weight_v)
 
 
-def lift_kernel(rows_o, tokens, at_ref, blocks_ref, *refs):
+def lift_kernel(rows_o, tokens, blocks_ref, *refs):
     gots, out_ref = refs[:-1], refs[-1]
     groups = len(gots)
     rank = blocks_ref.shape[2]
@@ -125,7 +126,7 @@
     first = jnp.zeros((tokens, rank), F32)
     second = jnp.zeros((half, 2 * rank), F32)
     for k, got_ref in enumerate(gots):
-        g = lax.rem(at_ref[0] + groups - k, groups)
+        g = lax.rem(lax.axis_index("x") + groups - k, groups)
         low, high = blocks_ref[g], blocks_ref[groups + g]
         basis_o = jnp.concatenate([low[:rows_o], high[:rows_o]], 0)
         basis_v = jnp.concatenate([low[rows_o:], high[rows_o:]], 0)
@@ -143,17 +144,15 @@
         out_ref[p, :, rank:] = second[row : row + each, side * rank : (side + 1) * rank].astype(BF)
 
 
-def lift(at, blocks, gots, rows_o, tokens, parts):
+def lift(blocks, gots, rows_o, tokens, parts):
     rank = blocks.shape[2]
-    vmem = pl.BlockSpec(memory_space=pltpu.VMEM)
     return pl.pallas_call(
         functools.partial(lift_kernel, rows_o, tokens),
-        in_specs=[pl.BlockSpec(memory_space=pltpu.SMEM)] + [vmem] * (1 + len(gots)),
         out_shape=jax.ShapeDtypeStruct((parts, tokens // parts, 2 * rank), BF),
         cost_estimate=pl.CostEstimate(flops=2 * 10**8, bytes_accessed=10**6, transcendentals=0),
         compiler_params=pltpu.CompilerParams(vmem_limit_bytes=ROOM),
         name="lift",
-    )(at, blocks, *gots)
+    )(blocks, *gots)
 
 
 def spread_kernel(got_ref, out_ref):
@@ -281,7 +280,7 @@
 
 
 def ready_kernel(
-    rows_o, rows_v, cols_o, at_ref, way_ref, local_o, local_v, h0, h1, h2, h3, b0, b1, b2, b3,
+    rows_o, rows_v, cols_o, way_ref, local_o, local_v, own_ref, other_ref, b0, b1, b2, b3,
     step_o_out, step_v_out, update_o_out, update_v_out, old_o_out, old_v_out,
 ):
     way = way_ref[...]
@@ -290,7 +289,8 @@
     upper_o, upper_v = upper[:, :cols_o], upper[:, cols_o:]
     step_o_out[...] = dot(local_o[...], upper_o) + dot(local_o[...], lower[:, :cols_o])
     step_v_out[...] = dot(local_v[...], upper_v) + dot(local_v[...], lower[:, cols_o:])
-    y, z, c = at_ref[1], at_ref[2], at_ref[3]
+    y, c = lax.axis_index("y"), lax.axis_index("c")
+    z = 4 * lax.axis_index("zh") + lax.axis_index("zl")
     for k, ref in enumerate((b0, b1, b2, b3)):
         origin = lax.rem(y + 4 - k, 4)
         count = ref.shape[0]
@@ -305,9 +305,9 @@
             update_o_out[pl.ds(at, rows_o), :] = update_o[i * rows_o : (i + 1) * rows_o]
             at = pl.multiple_of(index * rows_v, rows_v)
             update_v_out[pl.ds(at, rows_v), :] = update_v[i * rows_v : (i + 1) * rows_v]
-    for ref, core, last in ((h0, c, 0), (h1, c, 1), (h2, 1 - c, 0), (h3, 1 - c, 1)):
+    for ref, core in ((own_ref, c), (other_ref, 1 - c)):
         for p in range(ref.shape[0]):
-            behind = (p & 1) * 8 + (p >> 1 & 1) * 4 + (p >> 2) * 2 + last
+            behind = (p & 1) * 8 + (p >> 1 & 1) * 4 + STEPS[p >> 2]
             index = 2 * lax.rem(z + 16 - behind, 16) + core
             at = pl.multiple_of(index * rows_o, rows_o)
             old_o_out[pl.ds(at, rows_o), :128] = ref[p, :rows_o]
@@ -316,15 +316,13 @@
             old_v_out[pl.ds(at, rows_v), :] = ref[p, 2 * rows_o :]
 
 
-def ready(cols_o, at, way, local_o, local_v, held, segments):
+def ready(cols_o, way, local_o, local_v, own, other, segments):
     rows_o, rows_v = local_o.shape[0], local_v.shape[0]
     cols_v = way.shape[1] - cols_o
-    fs = 4 * held[0].shape[0]
+    fs = 2 * own.shape[0]
     shape = jax.ShapeDtypeStruct
-    vmem = pl.BlockSpec(memory_space=pltpu.VMEM)
     return pl.pallas_call(
         functools.partial(ready_kernel, rows_o, rows_v, cols_o),
-        in_specs=[pl.BlockSpec(memory_space=pltpu.SMEM)] + [vmem] * 11,
         out_shape=(
             shape((rows_o, cols_o), F32),
             shape((rows_v, cols_v), F32),
@@ -336,7 +334,7 @@
         cost_estimate=pl.CostEstimate(flops=4 * 10**8, bytes_accessed=4 * 10**6, transcendentals=0),
         compiler_params=pltpu.CompilerParams(vmem_limit_bytes=WHOLE),
         name="ready",
-    )(at, way, local_o, local_v, *held, *segments)
+    )(way, local_o, local_v, own, other, *segments)
 
 
 def output_kernel(
@@ -428,28 +426,25 @@
     fs = lax.axis_size(FS)
     xs, ys = lax.axis_size("x"), lax.axis_size("y")
 
-    x = lax.axis_index("x").astype(jnp.int32)
-    y = lax.axis_index("y").astype(jnp.int32)
-    z = lax.axis_index(Z).astype(jnp.int32)
-    c = lax.axis_index("c").astype(jnp.int32)
-    at = jnp.stack([x, y, z, c])
 
     block = swapped_blocks(jnp.concatenate([out_basis, value_basis], 0))
 
-    gots = list(pack(at, attn_out, latent.T, xs))
+    gots = list(pack(attn_out, latent.T, xs))
     for k in range(1, xs):
         gots[k] = shifted(gots[k], "x", k)
 
     own = old_rows(out_weight, value_up_matrix)[None]
-    for k in (8, 4, 2):
+    for k in (8, 4):
         more = shifted(own, Z, k)
         own = lax.optimization_barrier(jnp.concatenate([own, more], 0))
-    more = shifted(own, Z, 1)
-    held = [own, more, shifted(own, "c", 1)]
-    held.append(shifted(more, "c", 1))
+    rows = [own]
+    for k in STEPS[1:]:
+        rows.append(shifted(own, Z, k))
+    own = lax.optimization_barrier(jnp.concatenate(rows, 0))
+    other = shifted(own, "c", 1)
 
     blocks = from_everyone(block, ("c", "x"))
-    partial = lift(at, blocks, gots, rows_o, tokens // xs, ys)
+    partial = lift(blocks, gots, rows_o, tokens // xs, ys)
     partial = exchange(partial, "y")
     lifted = summed_for(partial, tp, BF)
     lifted = exchange(lifted, TP).reshape(tokens, 2 * rank)
@@ -457,7 +452,7 @@
     near = lax.axis_size(NEAR)
     part = contract(lifted, out_cot, value_cot, near, 4)
     part = exchange(part, NEAR)
-    part = exchange(summed_for(part, lax.axis_size("zh"), F32), "zh")
+    part = exchange(summed_for(part, lax.axis_size("zh"), BF), "zh")
     proj = exchange(summed_for(part, near, BF), NEAR)
 
     segments = [blocks]
@@ -468,7 +463,7 @@
         rows_o, tp, proj, out_mean, out_square, value_mean, value_square, segments
     )
     total = exchange(total, TP)
-    prepared = ready(cols_o, at, way, out_basis, value_basis, held, segments)
+    prepared = ready(cols_o, way, out_basis, value_basis, own, other, segments)
     counts = (rows_o * fs * cols_o * tp, rows_v * fs * cols_v * tp)
     step_o, new_o, copy_o, step_v, new_v, copy_v = outputs(
         counts, total, out_weight, value_up_matrix, *prepared

time: 206 us -> 194 us (0.942)
  blocking collectives: 60.1 us -> 46.9 us
    all_to_all x3 -> x2, blocking collectives: 60.1 us -> 46.9 us  [exchange(): return lax.all_to_all(value, axes, 0, 0, tiled=True)]
    ppermute x12, starting transfers between devices: 46.6 us -> 54.4 us  [shifted(): lax.ppermute(value, axis, [(i, (i + by) % devices) for i in range(devices)])]
    all_to_all x4 -> x5, starting transfers between devices: 46 us -> 39.6 us  [exchange(): return lax.all_to_all(value, axes, 0, 0, tiled=True)]
    unnamed x36 -> x30, local copies, waits for them, and re-layouts: 4.5 us -> 3.3 us
  transfers between devices with their start and end apart: 17 -> 18, of which waited for: 7 -> 8; matrix products, arithmetic and copies ran while one was open for 0% -> 0% of each run, Pallas kernels for 5% -> 5%
where the time goes in v5:
time: 194 us; the launch traced here: 193 us
  starting transfers between devices  94.7 us (49%)
  blocking collectives  46.9 us (24%)
  waiting for transfers between devices  27.4 us (14%)
  Pallas kernels  17.7 us (9%)
  local copies, waits for them, and re-layouts  4.07 us (2%)
    ppermute x12, starting transfers between devices, shifted(): lax.ppermute(value, axis, [(i, (i + by) % devices) for i in range(devices)])  54.4 us
    all_to_all x2, blocking collectives, exchange(): return lax.all_to_all(value, axes, 0, 0, tiled=True)  46.9 us
    all_to_all x5, starting transfers between devices, exchange(): return lax.all_to_all(value, axes, 0, 0, tiled=True)  39.6 us
    ppermute x12, waiting for transfers between devices, shifted(): lax.ppermute(value, axis, [(i, (i + by) % devices) for i in range(devices)])  26 us
    pallas_call x1, Pallas kernels, ready(): pl.pallas_call(functools.partial(ready_kernel, rows_o, rows_v, cols_o), o...  4.19 us
  transfers between devices with their start and end apart: 18, of which 8 were waited for; matrix products, arithmetic and copies ran while one was open for 0% of the time, Pallas kernels for 5%

profile of v5, /device:TPU:1, one launch (start us, length us, event | category | flops | bytes accessed | tf_op | source)
XLA Modules:
  0.0 192.7 jit_solution(1328267057205512590)
XLA Ops:
  0.6 0.8 pad_maximum_fusion.3
  1.4 0.7 collective-permute-start
  2.1 0.8 broadcast_in_dim.4
  2.9 15.3 %all-to-all-start = ((bf16[8,96,256]{2,1,0:T(8,128)(2,1)}), bf16[8,96,256]{2,1,0:T(8,128)(2,1)}, u32[]{:S(2)}, u32[]{:S(2)}) async-start(bf16[8,96,256]{2,1,0:T(8,128)(2,1)} %broadcast_in_dim.4), calls=%async_computation | async-start | bytes 786432 | tf_op jit(solution)/shard_map/all_to_all | solution.py:31
  18.1 2.0 %pack.1 = (bf16[576,128]{1,0:T(8,128)(2,1)}, bf16[576,128]{1,0:T(8,128)(2,1)}, bf16[576,128]{1,0:T(8,128)(2,1)}, bf16[576,128]{1,0:T(8,128)(2,1)}) custom-call(bf16[1536,128]{1,0:T(8,128)(2,1)} %attn_ref.1, bf16[64,1536]{1,0:T(8,128)(2,1)} %bitcast.6), custom_call_target="tpu_custom_call" | custom-call | flops 10000000 | bytes 1000000 | tf_op jit(solution)/shard_map/pack/pallas_call | solution.py:87
  20.1 3.3 %collective-permute-start.1 = (bf16[576,128]{1,0:T(8,128)(2,1)}, bf16[576,128]{1,0:T(8,128)(2,1)S(1)}, u32[]{:S(2)}, u32[]{:S(2)}) collective-permute-start(bf16[576,128]{1,0:T(8,128)(2,1)} %get-tuple-element.33), channel_id=1, source_target_pairs={{0,1},{1,2},{2,3},{3,0},{4,5},{5,6},{6,7},{7,4},{8,9},{9,10},{10,1... | collective-permute-start | bytes 442376 | tf_op jit(solution)/shard_map/ppermute | solution.py:50
  23.4 4.3 %collective-permute-start.2 = (bf16[576,128]{1,0:T(8,128)(2,1)}, bf16[576,128]{1,0:T(8,128)(2,1)S(1)}, u32[]{:S(2)}, u32[]{:S(2)}) collective-permute-start(bf16[576,128]{1,0:T(8,128)(2,1)} %get-tuple-element.34), channel_id=1, source_target_pairs={{0,2},{1,3},{2,0},{3,1},{4,6},{5,7},{6,4},{7,5},{8,10},{9,11},{10,... | collective-permute-start | bytes 442376 | tf_op jit(solution)/shard_map/ppermute | solution.py:50
  27.7 3.1 %collective-permute-start.3 = (bf16[576,128]{1,0:T(8,128)(2,1)}, bf16[576,128]{1,0:T(8,128)(2,1)S(1)}, u32[]{:S(2)}, u32[]{:S(2)}) collective-permute-start(bf16[576,128]{1,0:T(8,128)(2,1)} %get-tuple-element.35), channel_id=1, source_target_pairs={{0,3},{1,0},{2,1},{3,2},{4,7},{5,4},{6,5},{7,6},{8,11},{9,8},{10,9... | collective-permute-start | bytes 442376 | tf_op jit(solution)/shard_map/ppermute | solution.py:50
  30.8 2.1 %collective-permute-done.2.refs_2_ = bf16[576,128]{1,0:T(8,128)(2,1)S(1)} collective-permute-done((bf16[576,128]{1,0:T(8,128)(2,1)}, bf16[576,128]{1,0:T(8,128)(2,1)S(1)}, u32[]{:S(2)}, u32[]{:S(2)}) %collective-permute-start.2) | collective-permute-done | bytes 147488 | tf_op jit(solution)/shard_map/ppermute | solution.py:50
  32.9 1.4 collective-permute-done.3.refs_3_
  34.3 0.9 copy-done.9
  35.2 1.5 lift.1
  36.7 20.0 %all_to_all.35.got_ref = bf16[4,96,512]{2,1,0:T(8,128)(2,1)S(1)} all-to-all(bf16[4,96,512]{2,1,0:T(8,128)(2,1)S(1)} %lift.1), channel_id=1, replica_groups=mesh['zh'=4,'zl'=4,'c'=2,'y'=4,'x'=4] {'y'}, dimensions={0} | all-to-all | bytes 786432 | tf_op jit(solution)/shard_map/all_to_all | solution.py:31
  56.7 0.2 shard_map.195
  56.9 0.0 copy-start.3
  56.9 0.0 copy-start.5
  56.9 26.9 %all_to_all.36 = bf16[16,96,512]{2,1,0:T(8,128)(2,1)S(1)} all-to-all(bf16[16,96,512]{2,1,0:T(8,128)(2,1)S(1)} %shard_map.195), channel_id=1, replica_groups=mesh['zh'=4,'zl'=4,'c'=2,'y'=4,'x'=4] {'y','x'}, dimensions={0} | all-to-all | bytes 3145728 | tf_op jit(solution)/shard_map/all_to_all | solution.py:31
  83.8 2.0 %contract.1 = bf16[8,32,384]{2,1,0:T(8,128)(2,1)} custom-call(bf16[1536,512]{1,0:T(8,128)(2,1)S(1)} %bitcast.3, bf16[1536,256]{1,0:T(8,128)(2,1)S(1)} %copy-done.3, bf16[1536,128]{1,0:T(8,128)(2,1)S(1)} %copy-done.5), custom_call_target="tpu_custom_call" | custom-call | flops 300000000 | bytes 3000000 | tf_op jit(solution)/shard_map/contract/pallas_call | solution.py:209
  85.8 6.8 %all-to-all-start.3 = ((bf16[8,32,384]{2,1,0:T(8,128)(2,1)}), bf16[8,32,384]{2,1,0:T(8,128)(2,1)S(1)}, u32[]{:S(2)}, u32[]{:S(2)}) async-start(bf16[8,32,384]{2,1,0:T(8,128)(2,1)} %contract.1), calls=%async_computation.3 | async-start | bytes 393216 | tf_op jit(solution)/shard_map/all_to_all | solution.py:31
  92.6 0.0 copy-start.6
  92.7 0.0 copy-start.11
  92.7 12.6 %collective-permute-start.7 = (bf16[1,160,128]{2,1,0:T(8,128)(2,1)S(1)}, bf16[1,160,128]{2,1,0:T(8,128)(2,1)S(1)}, u32[]{:S(2)}, u32[]{:S(2)}) collective-permute-start(bf16[1,160,128]{2,1,0:T(8,128)(2,1)S(1)} %bitcast.4), channel_id=1, source_target_pairs={{0,256},{32,288},{64,320},{96,352},{128,384},{160,416},{192,448},{... | collective-permute-start | bytes 122888 | tf_op jit(solution)/shard_map/ppermute | solution.py:50
  105.3 3.2 %collective-permute-done.7 = bf16[1,160,128]{2,1,0:T(8,128)(2,1)S(1)} collective-permute-done((bf16[1,160,128]{2,1,0:T(8,128)(2,1)S(1)}, bf16[1,160,128]{2,1,0:T(8,128)(2,1)S(1)}, u32[]{:S(2)}, u32[]{:S(2)}) %collective-permute-start.7) | collective-permute-done | bytes 40992 | tf_op jit(solution)/shard_map/ppermute | solution.py:50
  108.6 8.3 %collective-permute-start.8 = (bf16[2,160,128]{2,1,0:T(8,128)(2,1)S(1)}, bf16[2,160,128]{2,1,0:T(8,128)(2,1)S(1)}, u32[]{:S(2)}, u32[]{:S(2)}) collective-permute-start(bf16[2,160,128]{2,1,0:T(8,128)(2,1)S(1)} %pad_maximum_fusion.2), channel_id=1, source_target_pairs={{0,128},{32,160},{64,192},{96,224},{128,256},{160,288},{192,320},{... | collective-permute-start | bytes 245768 | tf_op jit(solution)/shard_map/ppermute | solution.py:50
  116.9 0.7 shard_map.196
  117.5 5.1 %all-to-all-start.4 = ((bf16[4,32,384]{2,1,0:T(8,128)(2,1)}), bf16[4,32,384]{2,1,0:T(8,128)(2,1)S(1)}, u32[]{:S(2)}, u32[]{:S(2)}) async-start(bf16[4,32,384]{2,1,0:T(8,128)(2,1)} %shard_map.196), calls=%async_computation.4 | async-start | bytes 196608 | tf_op jit(solution)/shard_map/all_to_all | solution.py:31
  122.6 8.4 %collective-permute-start.11 = (bf16[4,160,128]{2,1,0:T(8,128)(2,1)S(1)}, bf16[4,160,128]{2,1,0:T(8,128)(2,1)S(1)}, u32[]{:S(2)}, u32[]{:S(2)}) collective-permute-start(bf16[4,160,128]{2,1,0:T(8,128)(2,1)S(1)} %pad_maximum_fusion.1), channel_id=1, source_target_pairs={{0,480},{32,0},{64,32},{96,64},{128,96},{160,128},{192,160},{224,1... | collective-permute-start | bytes 491528 | tf_op jit(solution)/shard_map/ppermute | solution.py:50
  131.0 1.9 collective-permute-start.10
  133.0 1.9 collective-permute-start.9
  134.9 0.7 shard_map.197
  135.6 8.3 %all-to-all-start.5 = ((bf16[8,32,384]{2,1,0:T(8,128)(2,1)}), bf16[8,32,384]{2,1,0:T(8,128)(2,1)S(1)}, u32[]{:S(2)}, u32[]{:S(2)}) async-start(bf16[8,32,384]{2,1,0:T(8,128)(2,1)} %shard_map.197), calls=%async_computation.5 | async-start | bytes 393216 | tf_op jit(solution)/shard_map/all_to_all | solution.py:31
  143.9 1.2 collective-permute-done.9
  145.1 0.1 pad_maximum_fusion.own_ref
  145.2 3.4 %collective-permute-start.12 = (bf16[16,160,128]{2,1,0:T(8,128)(2,1)S(1)}, bf16[16,160,128]{2,1,0:T(8,128)(2,1)S(1)}, u32[]{:S(2)}, u32[]{:S(2)}) collective-permute-start(bf16[16,160,128]{2,1,0:T(8,128)(2,1)S(1)} %pad_maximum_fusion.own_ref), channel_id=1, source_target_pairs={{0,16},{16,0},{1,17},{17,1},{2,18},{18,2},{3,19},{19,3},{4,20},{20... | collective-permute-start | bytes 1966088 | tf_op jit(solution)/shard_map/ppermute | solution.py:50
  148.7 2.2 %collective-permute-start.6 = (bf16[8,96,256]{2,1,0:T(8,128)(2,1)}, bf16[8,96,256]{2,1,0:T(8,128)(2,1)S(1)}, u32[]{:S(2)}, u32[]{:S(2)}) collective-permute-start(bf16[8,96,256]{2,1,0:T(8,128)(2,1)} %all-to-all-done.blocks_ref.b0), channel_id=1, source_target_pairs={{0,12},{4,0},{8,4},{12,8},{1,13},{5,1},{9,5},{13,9},{2,14},{6,2},{... | collective-permute-start | bytes 1179656 | tf_op jit(solution)/shard_map/ppermute | solution.py:50
  150.9 2.4 %collective-permute-start.5 = (bf16[8,96,256]{2,1,0:T(8,128)(2,1)}, bf16[8,96,256]{2,1,0:T(8,128)(2,1)S(1)}, u32[]{:S(2)}, u32[]{:S(2)}) collective-permute-start(bf16[8,96,256]{2,1,0:T(8,128)(2,1)} %all-to-all-done.blocks_ref.b0), channel_id=1, source_target_pairs={{0,8},{4,12},{8,0},{12,4},{1,9},{5,13},{9,1},{13,5},{2,10},{6,14},... | collective-permute-start | bytes 1179656 | tf_op jit(solution)/shard_map/ppermute | solution.py:50
  153.3 2.6 %collective-permute-start.4 = (bf16[8,96,256]{2,1,0:T(8,128)(2,1)}, bf16[8,96,256]{2,1,0:T(8,128)(2,1)S(1)}, u32[]{:S(2)}, u32[]{:S(2)}) collective-permute-start(bf16[8,96,256]{2,1,0:T(8,128)(2,1)} %all-to-all-done.blocks_ref.b0), channel_id=1, source_target_pairs={{0,4},{4,8},{8,12},{12,0},{1,5},{5,9},{9,13},{13,1},{2,6},{6,10},{... | collective-permute-start | bytes 1179656 | tf_op jit(solution)/shard_map/ppermute | solution.py:50
  155.9 5.5 %collective-permute-done.6.b3 = bf16[8,96,256]{2,1,0:T(8,128)(2,1)S(1)} collective-permute-done((bf16[8,96,256]{2,1,0:T(8,128)(2,1)}, bf16[8,96,256]{2,1,0:T(8,128)(2,1)S(1)}, u32[]{:S(2)}, u32[]{:S(2)}) %collective-permute-start.6) | collective-permute-done | bytes 393248 | tf_op jit(solution)/shard_map/ppermute | solution.py:50
  161.4 3.5 %collective-permute-done.5.b2 = bf16[8,96,256]{2,1,0:T(8,128)(2,1)S(1)} collective-permute-done((bf16[8,96,256]{2,1,0:T(8,128)(2,1)}, bf16[8,96,256]{2,1,0:T(8,128)(2,1)S(1)}, u32[]{:S(2)}, u32[]{:S(2)}) %collective-permute-start.5) | collective-permute-done | bytes 393248 | tf_op jit(solution)/shard_map/ppermute | solution.py:50
  164.9 9.1 %collective-permute-done.4.b1 = bf16[8,96,256]{2,1,0:T(8,128)(2,1)S(1)} collective-permute-done((bf16[8,96,256]{2,1,0:T(8,128)(2,1)}, bf16[8,96,256]{2,1,0:T(8,128)(2,1)S(1)}, u32[]{:S(2)}, u32[]{:S(2)}) %collective-permute-start.4) | collective-permute-done | bytes 393248 | tf_op jit(solution)/shard_map/ppermute | solution.py:50
  174.0 2.6 %directions.1 = (f32[256,256]{1,0:T(8,128)}, f32[256,256]{1,0:T(8,128)}, f32[256,128]{1,0:T(8,128)}, f32[256,128]{1,0:T(8,128)}, f32[256,384]{1,0:T(8,128)S(1)}, /*index=5*/f32[16,8,128]{2,1,0:T(8,128)}) custom-call(bf16[8,32,384]{2,1,0:T(8,128)(2,1)S(1)} %all-to-all-done.5.got_ref, f32[256,256]{1,0:T(8,128)S(1)} %copy-done.6, f32[256,256]{1,0:T(8,128)S(1)} %copy-done.7, ...), custom_call_target="tpu_custom_call" | custom-call | flops 400000000 | bytes 4000000 | tf_op jit(solution)/shard_map/directions/pallas_call | solution.py:266
  176.7 0.7 copy-done
  177.4 0.8 copy-done.4
  178.2 4.2 %all-to-all-start.6 = ((f32[16,8,128]{2,1,0:T(8,128)}), f32[16,8,128]{2,1,0:T(8,128)}, u32[]{:S(2)}, u32[]{:S(2)}) async-start(f32[16,8,128]{2,1,0:T(8,128)} %get-tuple-element.36), calls=%async_computation.6 | async-start | bytes 131072 | tf_op jit(solution)/shard_map/all_to_all | solution.py:31
  182.4 0.8 copy-done.14
  183.2 4.2 %ready.1 = (f32[64,256]{1,0:T(8,128)}, f32[32,128]{1,0:T(8,128)}, bf16[2048,256]{1,0:T(8,128)(2,1)}, bf16[1024,128]{1,0:T(8,128)(2,1)}, bf16[2048,256]{1,0:T(8,128)(2,1)}, /*index=5*/bf16[1024,128]{1,0:T(8,128)(2,1)}) custom-call(f32[256,384]{1,0:T(8,128)} %copy-done.4, bf16[64,256]{1,0:T(8,128)(2,1)} %local_o.1, bf16[32,256]{1,0:T(8,128)(2,1)} %local_v.1, ...), custom_call_target="tpu_custom_call" | custom-call | flops 400000000 | bytes 4000000 | tf_op jit(solution)/shard_map/ready/pallas_call | solution.py:324
  187.4 1.5 all-to-all-done.6.total_ref
  188.8 3.8 %outputs.1 = (f32[64,256]{1,0:T(8,128)}, f32[64,256]{1,0:T(8,128)}, bf16[2048,256]{1,0:T(8,128)(2,1)}, f32[32,128]{1,0:T(8,128)}, f32[32,128]{1,0:T(8,128)}, /*index=5*/bf16[1024,128]{1,0:T(8,128)(2,1)}) custom-call(f32[16,8,128]{2,1,0:T(8,128)} %all-to-all-done.6.total_ref, f32[64,256]{1,0:T(8,128)} %weight_o.3, f32[32,128]{1,0:T(8,128)} %weight_v.3, ...), custom_call_target="tpu_custom_call" | custom-call | flops 10000000 | bytes 4000000 | tf_op jit(solution)/shard_map/outputs/pallas_call | solution.py:387
  (35 shorter events, 0.1 us)
Async XLA Ops:
  1.4 0.7 collective-permute-start
  2.9 31.4 %all-to-all-start = ((bf16[8,96,256]{2,1,0:T(8,128)(2,1)}), bf16[8,96,256]{2,1,0:T(8,128)(2,1)}, u32[]{:S(2)}, u32[]{:S(2)}) async-start(bf16[8,96,256]{2,1,0:T(8,128)(2,1)} %broadcast_in_dim.4), calls=%async_computation | async-start | bytes 786432 | tf_op jit(solution)/shard_map/all_to_all | solution.py:31
  20.1 10.7 %collective-permute-start.1 = (bf16[576,128]{1,0:T(8,128)(2,1)}, bf16[576,128]{1,0:T(8,128)(2,1)S(1)}, u32[]{:S(2)}, u32[]{:S(2)}) collective-permute-start(bf16[576,128]{1,0:T(8,128)(2,1)} %get-tuple-element.33), channel_id=1, source_target_pairs={{0,1},{1,2},{2,3},{3,0},{4,5},{5,6},{6,7},{7,4},{8,9},{9,10},{10,1... | collective-permute-start | bytes 442376 | tf_op jit(solution)/shard_map/ppermute | solution.py:50
  23.4 9.5 %collective-permute-start.2 = (bf16[576,128]{1,0:T(8,128)(2,1)}, bf16[576,128]{1,0:T(8,128)(2,1)S(1)}, u32[]{:S(2)}, u32[]{:S(2)}) collective-permute-start(bf16[576,128]{1,0:T(8,128)(2,1)} %get-tuple-element.34), channel_id=1, source_target_pairs={{0,2},{1,3},{2,0},{3,1},{4,6},{5,7},{6,4},{7,5},{8,10},{9,11},{10,... | collective-permute-start | bytes 442376 | tf_op jit(solution)/shard_map/ppermute | solution.py:50
  27.7 6.6 %collective-permute-start.3 = (bf16[576,128]{1,0:T(8,128)(2,1)}, bf16[576,128]{1,0:T(8,128)(2,1)S(1)}, u32[]{:S(2)}, u32[]{:S(2)}) collective-permute-start(bf16[576,128]{1,0:T(8,128)(2,1)} %get-tuple-element.35), channel_id=1, source_target_pairs={{0,3},{1,0},{2,1},{3,2},{4,7},{5,4},{6,5},{7,6},{8,11},{9,8},{10,9... | collective-permute-start | bytes 442376 | tf_op jit(solution)/shard_map/ppermute | solution.py:50
  34.3 0.9 copy-start.9
  56.9 27.0 %copy-start.3 = (bf16[1536,256]{1,0:T(8,128)(2,1)S(1)}, bf16[1536,256]{1,0:T(8,128)(2,1)}, u32[]{:S(2)}) copy-start(bf16[1536,256]{1,0:T(8,128)(2,1)} %cot_o.1) | copy-start | bytes 2359300
  56.9 26.9 %copy-start.5 = (bf16[1536,128]{1,0:T(8,128)(2,1)S(1)}, bf16[1536,128]{1,0:T(8,128)(2,1)}, u32[]{:S(2)}) copy-start(bf16[1536,128]{1,0:T(8,128)(2,1)} %cot_v.1) | copy-start | bytes 1179652
  83.8 8.8 %copy-start.8 = (f32[64,256]{1,0:T(8,128)S(1)}, f32[64,256]{1,0:T(8,128)}, u32[]{:S(2)}) copy-start(f32[64,256]{1,0:T(8,128)} %weight_o.3) | copy-start | bytes 196612
  83.8 8.8 %copy-start.12 = (f32[32,128]{1,0:T(8,128)S(1)}, f32[32,128]{1,0:T(8,128)}, u32[]{:S(2)}) copy-start(f32[32,128]{1,0:T(8,128)} %weight_v.3) | copy-start | bytes 49156
  85.8 31.0 %all-to-all-start.3 = ((bf16[8,32,384]{2,1,0:T(8,128)(2,1)}), bf16[8,32,384]{2,1,0:T(8,128)(2,1)S(1)}, u32[]{:S(2)}, u32[]{:S(2)}) async-start(bf16[8,32,384]{2,1,0:T(8,128)(2,1)} %contract.1), calls=%async_computation.3 | async-start | bytes 393216 | tf_op jit(solution)/shard_map/all_to_all | solution.py:31
  92.6 81.3 %copy-start.6 = (f32[256,256]{1,0:T(8,128)S(1)}, f32[256,256]{1,0:T(8,128)}, u32[]{:S(2)}) copy-start(f32[256,256]{1,0:T(8,128)} %mean_o.1) | copy-start | bytes 786436
  92.7 81.3 %copy-start.7 = (f32[256,256]{1,0:T(8,128)S(1)}, f32[256,256]{1,0:T(8,128)}, u32[]{:S(2)}) copy-start(f32[256,256]{1,0:T(8,128)} %square_o.1) | copy-start | bytes 786436
  92.7 81.3 %copy-start.10 = (f32[256,128]{1,0:T(8,128)S(1)}, f32[256,128]{1,0:T(8,128)}, u32[]{:S(2)}) copy-start(f32[256,128]{1,0:T(8,128)} %mean_v.1) | copy-start | bytes 393220
  92.7 81.3 %copy-start.11 = (f32[256,128]{1,0:T(8,128)S(1)}, f32[256,128]{1,0:T(8,128)}, u32[]{:S(2)}) copy-start(f32[256,128]{1,0:T(8,128)} %square_v.1) | copy-start | bytes 393220
  92.7 15.9 %collective-permute-start.7 = (bf16[1,160,128]{2,1,0:T(8,128)(2,1)S(1)}, bf16[1,160,128]{2,1,0:T(8,128)(2,1)S(1)}, u32[]{:S(2)}, u32[]{:S(2)}) collective-permute-start(bf16[1,160,128]{2,1,0:T(8,128)(2,1)S(1)} %bitcast.4), channel_id=1, source_target_pairs={{0,256},{32,288},{64,320},{96,352},{128,384},{160,416},{192,448},{... | collective-permute-start | bytes 122888 | tf_op jit(solution)/shard_map/ppermute | solution.py:50
  108.6 14.0 %collective-permute-start.8 = (bf16[2,160,128]{2,1,0:T(8,128)(2,1)S(1)}, bf16[2,160,128]{2,1,0:T(8,128)(2,1)S(1)}, u32[]{:S(2)}, u32[]{:S(2)}) collective-permute-start(bf16[2,160,128]{2,1,0:T(8,128)(2,1)S(1)} %pad_maximum_fusion.2), channel_id=1, source_target_pairs={{0,128},{32,160},{64,192},{96,224},{128,256},{160,288},{192,320},{... | collective-permute-start | bytes 245768 | tf_op jit(solution)/shard_map/ppermute | solution.py:50
  117.5 17.4 %all-to-all-start.4 = ((bf16[4,32,384]{2,1,0:T(8,128)(2,1)}), bf16[4,32,384]{2,1,0:T(8,128)(2,1)S(1)}, u32[]{:S(2)}, u32[]{:S(2)}) async-start(bf16[4,32,384]{2,1,0:T(8,128)(2,1)} %shard_map.196), calls=%async_computation.4 | async-start | bytes 196608 | tf_op jit(solution)/shard_map/all_to_all | solution.py:31
  122.6 21.2 %collective-permute-start.11 = (bf16[4,160,128]{2,1,0:T(8,128)(2,1)S(1)}, bf16[4,160,128]{2,1,0:T(8,128)(2,1)S(1)}, u32[]{:S(2)}, u32[]{:S(2)}) collective-permute-start(bf16[4,160,128]{2,1,0:T(8,128)(2,1)S(1)} %pad_maximum_fusion.1), channel_id=1, source_target_pairs={{0,480},{32,0},{64,32},{96,64},{128,96},{160,128},{192,160},{224,1... | collective-permute-start | bytes 491528 | tf_op jit(solution)/shard_map/ppermute | solution.py:50
  131.0 12.9 %collective-permute-start.10 = (bf16[4,160,128]{2,1,0:T(8,128)(2,1)S(1)}, bf16[4,160,128]{2,1,0:T(8,128)(2,1)S(1)}, u32[]{:S(2)}, u32[]{:S(2)}) collective-permute-start(bf16[4,160,128]{2,1,0:T(8,128)(2,1)S(1)} %pad_maximum_fusion.1), channel_id=1, source_target_pairs={{0,64},{32,96},{64,128},{96,160},{128,192},{160,224},{192,256},{22... | collective-permute-start | bytes 491528 | tf_op jit(solution)/shard_map/ppermute | solution.py:50
  133.0 12.2 %collective-permute-start.9 = (bf16[4,160,128]{2,1,0:T(8,128)(2,1)S(1)}, bf16[4,160,128]{2,1,0:T(8,128)(2,1)S(1)}, u32[]{:S(2)}, u32[]{:S(2)}) collective-permute-start(bf16[4,160,128]{2,1,0:T(8,128)(2,1)S(1)} %pad_maximum_fusion.1), channel_id=1, source_target_pairs={{0,32},{32,64},{64,96},{96,128},{128,160},{160,192},{192,224},{224... | collective-permute-start | bytes 491528 | tf_op jit(solution)/shard_map/ppermute | solution.py:50
  135.6 38.4 %all-to-all-start.5 = ((bf16[8,32,384]{2,1,0:T(8,128)(2,1)}), bf16[8,32,384]{2,1,0:T(8,128)(2,1)S(1)}, u32[]{:S(2)}, u32[]{:S(2)}) async-start(bf16[8,32,384]{2,1,0:T(8,128)(2,1)} %shard_map.197), calls=%async_computation.5 | async-start | bytes 393216 | tf_op jit(solution)/shard_map/all_to_all | solution.py:31
  145.2 32.9 %copy-start.13 = (bf16[16,160,128]{2,1,0:T(8,128)(2,1)}, bf16[16,160,128]{2,1,0:T(8,128)(2,1)S(1)}, u32[]{:S(2)}) copy-start(bf16[16,160,128]{2,1,0:T(8,128)(2,1)S(1)} %pad_maximum_fusion.own_ref) | copy-start | bytes 1966084
  145.2 37.1 %collective-permute-start.12 = (bf16[16,160,128]{2,1,0:T(8,128)(2,1)S(1)}, bf16[16,160,128]{2,1,0:T(8,128)(2,1)S(1)}, u32[]{:S(2)}, u32[]{:S(2)}) collective-permute-start(bf16[16,160,128]{2,1,0:T(8,128)(2,1)S(1)} %pad_maximum_fusion.own_ref), channel_id=1, source_target_pairs={{0,16},{16,0},{1,17},{17,1},{2,18},{18,2},{3,19},{19,3},{4,20},{20... | collective-permute-start | bytes 1966088 | tf_op jit(solution)/shard_map/ppermute | solution.py:50
  148.7 12.8 %collective-permute-start.6 = (bf16[8,96,256]{2,1,0:T(8,128)(2,1)}, bf16[8,96,256]{2,1,0:T(8,128)(2,1)S(1)}, u32[]{:S(2)}, u32[]{:S(2)}) collective-permute-start(bf16[8,96,256]{2,1,0:T(8,128)(2,1)} %all-to-all-done.blocks_ref.b0), channel_id=1, source_target_pairs={{0,12},{4,0},{8,4},{12,8},{1,13},{5,1},{9,5},{13,9},{2,14},{6,2},{... | collective-permute-start | bytes 1179656 | tf_op jit(solution)/shard_map/ppermute | solution.py:50
  150.9 14.0 %collective-permute-start.5 = (bf16[8,96,256]{2,1,0:T(8,128)(2,1)}, bf16[8,96,256]{2,1,0:T(8,128)(2,1)S(1)}, u32[]{:S(2)}, u32[]{:S(2)}) collective-permute-start(bf16[8,96,256]{2,1,0:T(8,128)(2,1)} %all-to-all-done.blocks_ref.b0), channel_id=1, source_target_pairs={{0,8},{4,12},{8,0},{12,4},{1,9},{5,13},{9,1},{13,5},{2,10},{6,14},... | collective-permute-start | bytes 1179656 | tf_op jit(solution)/shard_map/ppermute | solution.py:50
  153.3 20.7 %collective-permute-start.4 = (bf16[8,96,256]{2,1,0:T(8,128)(2,1)}, bf16[8,96,256]{2,1,0:T(8,128)(2,1)S(1)}, u32[]{:S(2)}, u32[]{:S(2)}) collective-permute-start(bf16[8,96,256]{2,1,0:T(8,128)(2,1)} %all-to-all-done.blocks_ref.b0), channel_id=1, source_target_pairs={{0,4},{4,8},{8,12},{12,0},{1,5},{5,9},{9,13},{13,1},{2,6},{6,10},{... | collective-permute-start | bytes 1179656 | tf_op jit(solution)/shard_map/ppermute | solution.py:50
  164.9 11.8 %copy-start.1 = (bf16[8,96,256]{2,1,0:T(8,128)(2,1)}, bf16[8,96,256]{2,1,0:T(8,128)(2,1)S(1)}, u32[]{:S(2)}) copy-start(bf16[8,96,256]{2,1,0:T(8,128)(2,1)S(1)} %collective-permute-done.5.b2) | copy-start | bytes 1179652
  174.0 4.2 %copy-start.2 = (bf16[8,96,256]{2,1,0:T(8,128)(2,1)}, bf16[8,96,256]{2,1,0:T(8,128)(2,1)S(1)}, u32[]{:S(2)}) copy-start(bf16[8,96,256]{2,1,0:T(8,128)(2,1)S(1)} %collective-permute-done.4.b1) | copy-start | bytes 1179652
  176.7 0.7 copy-start
  177.4 0.8 copy-start.4
  178.2 10.7 %all-to-all-start.6 = ((f32[16,8,128]{2,1,0:T(8,128)}), f32[16,8,128]{2,1,0:T(8,128)}, u32[]{:S(2)}, u32[]{:S(2)}) async-start(f32[16,8,128]{2,1,0:T(8,128)} %get-tuple-element.36), calls=%async_computation.6 | async-start | bytes 131072 | tf_op jit(solution)/shard_map/all_to_all | solution.py:31
  182.3 0.8 copy-start.14

commit v6 on v5

--- a/solution.py
+++ b/solution.py
@@ -225,7 +225,7 @@
 
 def direction_kernel(
     rows_o, cols_o, got_ref, mean_o, square_o, mean_v, square_v, b0, b1, b2, b3,
-    mean_o_out, square_o_out, mean_v_out, square_v_out, way_out, total_out,
+    mean_o_out, square_o_out, mean_v_out, square_v_out, total_out,
 ):
     near = got_ref.shape[0]
     proj = jnp.concatenate([got_ref[i] for i in range(near)], 0).astype(F32)
@@ -237,9 +237,7 @@
     mean_v_out[...] = mean[:, cols_o:]
     square_o_out[...] = square[:, :cols_o]
     square_v_out[...] = square[:, cols_o:]
-    way = mean / jnp.sqrt(square)
-    way_out[...] = way
-    upper = way.astype(BF)
+    upper = (mean / jnp.sqrt(square)).astype(BF)
     upper_o, upper_v = upper[:, :cols_o], upper[:, cols_o:]
     total_o = jnp.zeros((8, cols_o), F32)
     total_v = jnp.zeros((8, upper_v.shape[1]), F32)
@@ -260,8 +258,7 @@
 
 
 def directions(rows_o, copies, got, mean_o, square_o, mean_v, square_v, segments):
-    rank, cols_o = mean_o.shape
-    cols = cols_o + mean_v.shape[1]
+    cols_o = mean_o.shape[1]
     shape = jax.ShapeDtypeStruct
     return pl.pallas_call(
         functools.partial(direction_kernel, rows_o, cols_o),
@@ -270,7 +267,6 @@
             shape(mean_o.shape, F32),
             shape(mean_v.shape, F32),
             shape(mean_v.shape, F32),
-            shape((rank, cols), F32),
             shape((copies, 8, 128), F32),
         ),
         cost_estimate=pl.CostEstimate(flops=4 * 10**8, bytes_accessed=4 * 10**6, transcendentals=10**5),
@@ -280,15 +276,20 @@
 
 
 def ready_kernel(
-    rows_o, rows_v, cols_o, way_ref, local_o, local_v, own_ref, other_ref, b0, b1, b2, b3,
+    rows_o, rows_v, mean_o, square_o, mean_v, square_v, local_o, local_v, own_ref, other_ref, b0, b1, b2, b3,
     step_o_out, step_v_out, update_o_out, update_v_out, old_o_out, old_v_out,
 ):
-    way = way_ref[...]
-    upper = way.astype(BF)
-    lower = (way - upper.astype(F32)).astype(BF)
-    upper_o, upper_v = upper[:, :cols_o], upper[:, cols_o:]
-    step_o_out[...] = dot(local_o[...], upper_o) + dot(local_o[...], lower[:, :cols_o])
-    step_v_out[...] = dot(local_v[...], upper_v) + dot(local_v[...], lower[:, cols_o:])
+    uppers = []
+    for mean, square, local, step_out in (
+        (mean_o, square_o, local_o, step_o_out),
+        (mean_v, square_v, local_v, step_v_out),
+    ):
+        way = mean[...] / jnp.sqrt(square[...])
+        upper = way.astype(BF)
+        lower = (way - upper.astype(F32)).astype(BF)
+        step_out[...] = dot(local[...], upper) + dot(local[...], lower)
+        uppers.append(upper)
+    upper_o, upper_v = uppers
     y, c = lax.axis_index("y"), lax.axis_index("c")
     z = 4 * lax.axis_index("zh") + lax.axis_index("zl")
     for k, ref in enumerate((b0, b1, b2, b3)):
@@ -316,13 +317,13 @@
             old_v_out[pl.ds(at, rows_v), :] = ref[p, 2 * rows_o :]
 
 
-def ready(cols_o, way, local_o, local_v, own, other, segments):
+def ready(moments, local_o, local_v, own, other, segments):
     rows_o, rows_v = local_o.shape[0], local_v.shape[0]
-    cols_v = way.shape[1] - cols_o
+    cols_o, cols_v = moments[0].shape[1], moments[2].shape[1]
     fs = 2 * own.shape[0]
     shape = jax.ShapeDtypeStruct
     return pl.pallas_call(
-        functools.partial(ready_kernel, rows_o, rows_v, cols_o),
+        functools.partial(ready_kernel, rows_o, rows_v),
         out_shape=(
             shape((rows_o, cols_o), F32),
             shape((rows_v, cols_v), F32),
@@ -334,7 +335,7 @@
         cost_estimate=pl.CostEstimate(flops=4 * 10**8, bytes_accessed=4 * 10**6, transcendentals=0),
         compiler_params=pltpu.CompilerParams(vmem_limit_bytes=WHOLE),
         name="ready",
-    )(way, local_o, local_v, own, other, *segments)
+    )(*moments, local_o, local_v, own, other, *segments)
 
 
 def output_kernel(
@@ -459,11 +460,12 @@
     for k in range(1, ys):
         segments.append(shifted(blocks, "y", k))
 
-    mean_o, square_o, mean_v, square_v, way, total = directions(
+    mean_o, square_o, mean_v, square_v, total = directions(
         rows_o, tp, proj, out_mean, out_square, value_mean, value_square, segments
     )
     total = exchange(total, TP)
-    prepared = ready(cols_o, way, out_basis, value_basis, own, other, segments)
+    moments = (mean_o, square_o, mean_v, square_v)
+    prepared = ready(moments, out_basis, value_basis, own, other, segments)
     counts = (rows_o * fs * cols_o * tp, rows_v * fs * cols_v * tp)
     step_o, new_o, copy_o, step_v, new_v, copy_v = outputs(
         counts, total, out_weight, value_up_matrix, *prepared

time: 194 us -> 193 us (level)
  waiting for transfers between devices: 27.4 us -> 25.2 us
    ppermute x12, waiting for transfers between devices: 26 us -> 24 us  [shifted(): lax.ppermute(value, axis, [(i, (i + by) % devices) for i in range(devices)])]
  transfers between devices with their start and end apart: 18 -> 18, of which waited for: 8 -> 7; matrix products, arithmetic and copies ran while one was open for 0% -> 0% of each run, Pallas kernels for 5% -> 5%
where the time goes in v6:
time: 193 us; the launch traced here: 192 us
  starting transfers between devices  96.5 us (50%)
  blocking collectives  46.9 us (24%)
  waiting for transfers between devices  25.2 us (13%)
  Pallas kernels  18 us (9%)
  local copies, waits for them, and re-layouts  3.35 us (2%)
    ppermute x12, starting transfers between devices, shifted(): lax.ppermute(value, axis, [(i, (i + by) % devices) for i in range(devices)])  55.7 us
    all_to_all x2, blocking collectives, exchange(): return lax.all_to_all(value, axes, 0, 0, tiled=True)  46.9 us
    all_to_all x5, starting transfers between devices, exchange(): return lax.all_to_all(value, axes, 0, 0, tiled=True)  40.1 us
    ppermute x12, waiting for transfers between devices, shifted(): lax.ppermute(value, axis, [(i, (i + by) % devices) for i in range(devices)])  24 us
    pallas_call x1, Pallas kernels, ready(): pl.pallas_call(functools.partial(ready_kernel, rows_o, rows_v), out_shape...  4.46 us
  transfers between devices with their start and end apart: 18, of which 7 were waited for; matrix products, arithmetic and copies ran while one was open for 0% of the time, Pallas kernels for 5%

profile of v6, /device:TPU:1, one launch (start us, length us, event | category | flops | bytes accessed | tf_op | source)
XLA Modules:
  0.0 191.8 jit_solution(2869276489258426535)
XLA Ops:
  0.6 0.8 pad_maximum_fusion.3
  1.4 0.7 collective-permute-start
  2.1 0.8 broadcast_in_dim.4
  2.9 15.3 %all-to-all-start = ((bf16[8,96,256]{2,1,0:T(8,128)(2,1)}), bf16[8,96,256]{2,1,0:T(8,128)(2,1)}, u32[]{:S(2)}, u32[]{:S(2)}) async-start(bf16[8,96,256]{2,1,0:T(8,128)(2,1)} %broadcast_in_dim.4), calls=%async_computation | async-start | bytes 786432 | tf_op jit(solution)/shard_map/all_to_all | solution.py:31
  18.1 2.0 %pack.1 = (bf16[576,128]{1,0:T(8,128)(2,1)}, bf16[576,128]{1,0:T(8,128)(2,1)}, bf16[576,128]{1,0:T(8,128)(2,1)}, bf16[576,128]{1,0:T(8,128)(2,1)}) custom-call(bf16[1536,128]{1,0:T(8,128)(2,1)} %attn_ref.1, bf16[64,1536]{1,0:T(8,128)(2,1)} %bitcast.6), custom_call_target="tpu_custom_call" | custom-call | flops 10000000 | bytes 1000000 | tf_op jit(solution)/shard_map/pack/pallas_call | solution.py:87
  20.1 3.3 %collective-permute-start.1 = (bf16[576,128]{1,0:T(8,128)(2,1)}, bf16[576,128]{1,0:T(8,128)(2,1)S(1)}, u32[]{:S(2)}, u32[]{:S(2)}) collective-permute-start(bf16[576,128]{1,0:T(8,128)(2,1)} %get-tuple-element.32), channel_id=1, source_target_pairs={{0,1},{1,2},{2,3},{3,0},{4,5},{5,6},{6,7},{7,4},{8,9},{9,10},{10,1... | collective-permute-start | bytes 442376 | tf_op jit(solution)/shard_map/ppermute | solution.py:50
  23.4 4.3 %collective-permute-start.2 = (bf16[576,128]{1,0:T(8,128)(2,1)}, bf16[576,128]{1,0:T(8,128)(2,1)S(1)}, u32[]{:S(2)}, u32[]{:S(2)}) collective-permute-start(bf16[576,128]{1,0:T(8,128)(2,1)} %get-tuple-element.33), channel_id=1, source_target_pairs={{0,2},{1,3},{2,0},{3,1},{4,6},{5,7},{6,4},{7,5},{8,10},{9,11},{10,... | collective-permute-start | bytes 442376 | tf_op jit(solution)/shard_map/ppermute | solution.py:50
  27.7 3.1 %collective-permute-start.3 = (bf16[576,128]{1,0:T(8,128)(2,1)}, bf16[576,128]{1,0:T(8,128)(2,1)S(1)}, u32[]{:S(2)}, u32[]{:S(2)}) collective-permute-start(bf16[576,128]{1,0:T(8,128)(2,1)} %get-tuple-element.34), channel_id=1, source_target_pairs={{0,3},{1,0},{2,1},{3,2},{4,7},{5,4},{6,5},{7,6},{8,11},{9,8},{10,9... | collective-permute-start | bytes 442376 | tf_op jit(solution)/shard_map/ppermute | solution.py:50
  30.8 2.1 %collective-permute-done.2.refs_2_ = bf16[576,128]{1,0:T(8,128)(2,1)S(1)} collective-permute-done((bf16[576,128]{1,0:T(8,128)(2,1)}, bf16[576,128]{1,0:T(8,128)(2,1)S(1)}, u32[]{:S(2)}, u32[]{:S(2)}) %collective-permute-start.2) | collective-permute-done | bytes 147488 | tf_op jit(solution)/shard_map/ppermute | solution.py:50
  32.9 1.4 collective-permute-done.3.refs_3_
  34.3 0.9 copy-done.8
  35.2 1.5 lift.1
  36.7 20.0 %all_to_all.35.got_ref = bf16[4,96,512]{2,1,0:T(8,128)(2,1)S(1)} all-to-all(bf16[4,96,512]{2,1,0:T(8,128)(2,1)S(1)} %lift.1), channel_id=1, replica_groups=mesh['zh'=4,'zl'=4,'c'=2,'y'=4,'x'=4] {'y'}, dimensions={0} | all-to-all | bytes 786432 | tf_op jit(solution)/shard_map/all_to_all | solution.py:31
  56.7 0.2 shard_map.195
  56.9 0.0 copy-start.3
  56.9 0.0 copy-start.4
  56.9 26.9 %all_to_all.36 = bf16[16,96,512]{2,1,0:T(8,128)(2,1)S(1)} all-to-all(bf16[16,96,512]{2,1,0:T(8,128)(2,1)S(1)} %shard_map.195), channel_id=1, replica_groups=mesh['zh'=4,'zl'=4,'c'=2,'y'=4,'x'=4] {'y','x'}, dimensions={0} | all-to-all | bytes 3145728 | tf_op jit(solution)/shard_map/all_to_all | solution.py:31
  83.8 2.0 %contract.1 = bf16[8,32,384]{2,1,0:T(8,128)(2,1)} custom-call(bf16[1536,512]{1,0:T(8,128)(2,1)S(1)} %bitcast.3, bf16[1536,256]{1,0:T(8,128)(2,1)S(1)} %copy-done.3, bf16[1536,128]{1,0:T(8,128)(2,1)S(1)} %copy-done.4), custom_call_target="tpu_custom_call" | custom-call | flops 300000000 | bytes 3000000 | tf_op jit(solution)/shard_map/contract/pallas_call | solution.py:209
  85.9 6.8 %all-to-all-start.3 = ((bf16[8,32,384]{2,1,0:T(8,128)(2,1)}), bf16[8,32,384]{2,1,0:T(8,128)(2,1)S(1)}, u32[]{:S(2)}, u32[]{:S(2)}) async-start(bf16[8,32,384]{2,1,0:T(8,128)(2,1)} %contract.1), calls=%async_computation.3 | async-start | bytes 393216 | tf_op jit(solution)/shard_map/all_to_all | solution.py:31
  92.6 0.0 copy-start.5
  92.6 0.0 copy-start.6
  92.7 0.0 copy-start.9
  92.7 0.0 copy-start.10
  92.7 12.6 %collective-permute-start.7 = (bf16[1,160,128]{2,1,0:T(8,128)(2,1)S(1)}, bf16[1,160,128]{2,1,0:T(8,128)(2,1)S(1)}, u32[]{:S(2)}, u32[]{:S(2)}) collective-permute-start(bf16[1,160,128]{2,1,0:T(8,128)(2,1)S(1)} %bitcast.4), channel_id=1, source_target_pairs={{0,256},{32,288},{64,320},{96,352},{128,384},{160,416},{192,448},{... | collective-permute-start | bytes 122888 | tf_op jit(solution)/shard_map/ppermute | solution.py:50
  105.3 3.2 %collective-permute-done.7 = bf16[1,160,128]{2,1,0:T(8,128)(2,1)S(1)} collective-permute-done((bf16[1,160,128]{2,1,0:T(8,128)(2,1)S(1)}, bf16[1,160,128]{2,1,0:T(8,128)(2,1)S(1)}, u32[]{:S(2)}, u32[]{:S(2)}) %collective-permute-start.7) | collective-permute-done | bytes 40992 | tf_op jit(solution)/shard_map/ppermute | solution.py:50
  108.6 8.3 %collective-permute-start.8 = (bf16[2,160,128]{2,1,0:T(8,128)(2,1)S(1)}, bf16[2,160,128]{2,1,0:T(8,128)(2,1)S(1)}, u32[]{:S(2)}, u32[]{:S(2)}) collective-permute-start(bf16[2,160,128]{2,1,0:T(8,128)(2,1)S(1)} %pad_maximum_fusion.2), channel_id=1, source_target_pairs={{0,128},{32,160},{64,192},{96,224},{128,256},{160,288},{192,320},{... | collective-permute-start | bytes 245768 | tf_op jit(solution)/shard_map/ppermute | solution.py:50
  116.9 0.7 shard_map.196
  117.5 5.1 %all-to-all-start.4 = ((bf16[4,32,384]{2,1,0:T(8,128)(2,1)}), bf16[4,32,384]{2,1,0:T(8,128)(2,1)S(1)}, u32[]{:S(2)}, u32[]{:S(2)}) async-start(bf16[4,32,384]{2,1,0:T(8,128)(2,1)} %shard_map.196), calls=%async_computation.4 | async-start | bytes 196608 | tf_op jit(solution)/shard_map/all_to_all | solution.py:31
  122.7 8.4 %collective-permute-start.11 = (bf16[4,160,128]{2,1,0:T(8,128)(2,1)S(1)}, bf16[4,160,128]{2,1,0:T(8,128)(2,1)S(1)}, u32[]{:S(2)}, u32[]{:S(2)}) collective-permute-start(bf16[4,160,128]{2,1,0:T(8,128)(2,1)S(1)} %pad_maximum_fusion.1), channel_id=1, source_target_pairs={{0,480},{32,0},{64,32},{96,64},{128,96},{160,128},{192,160},{224,1... | collective-permute-start | bytes 491528 | tf_op jit(solution)/shard_map/ppermute | solution.py:50
  131.0 1.9 %collective-permute-start.10 = (bf16[4,160,128]{2,1,0:T(8,128)(2,1)S(1)}, bf16[4,160,128]{2,1,0:T(8,128)(2,1)S(1)}, u32[]{:S(2)}, u32[]{:S(2)}) collective-permute-start(bf16[4,160,128]{2,1,0:T(8,128)(2,1)S(1)} %pad_maximum_fusion.1), channel_id=1, source_target_pairs={{0,64},{32,96},{64,128},{96,160},{128,192},{160,224},{192,256},{22... | collective-permute-start | bytes 491528 | tf_op jit(solution)/shard_map/ppermute | solution.py:50
  133.0 1.9 %collective-permute-start.9 = (bf16[4,160,128]{2,1,0:T(8,128)(2,1)S(1)}, bf16[4,160,128]{2,1,0:T(8,128)(2,1)S(1)}, u32[]{:S(2)}, u32[]{:S(2)}) collective-permute-start(bf16[4,160,128]{2,1,0:T(8,128)(2,1)S(1)} %pad_maximum_fusion.1), channel_id=1, source_target_pairs={{0,32},{32,64},{64,96},{96,128},{128,160},{160,192},{192,224},{224... | collective-permute-start | bytes 491528 | tf_op jit(solution)/shard_map/ppermute | solution.py:50
  134.9 0.7 shard_map.197
  135.6 8.3 %all-to-all-start.5 = ((bf16[8,32,384]{2,1,0:T(8,128)(2,1)}), bf16[8,32,384]{2,1,0:T(8,128)(2,1)S(1)}, u32[]{:S(2)}, u32[]{:S(2)}) async-start(bf16[8,32,384]{2,1,0:T(8,128)(2,1)} %shard_map.197), calls=%async_computation.5 | async-start | bytes 393216 | tf_op jit(solution)/shard_map/all_to_all | solution.py:31
  143.9 1.2 collective-permute-done.9
  145.0 0.1 pad_maximum_fusion.own_ref
  145.1 3.5 %collective-permute-start.12 = (bf16[16,160,128]{2,1,0:T(8,128)(2,1)S(1)}, bf16[16,160,128]{2,1,0:T(8,128)(2,1)S(1)}, u32[]{:S(2)}, u32[]{:S(2)}) collective-permute-start(bf16[16,160,128]{2,1,0:T(8,128)(2,1)S(1)} %pad_maximum_fusion.own_ref), channel_id=1, source_target_pairs={{0,16},{16,0},{1,17},{17,1},{2,18},{18,2},{3,19},{19,3},{4,20},{20... | collective-permute-start | bytes 1966088 | tf_op jit(solution)/shard_map/ppermute | solution.py:50
  148.6 1.9 %collective-permute-start.4 = (bf16[8,96,256]{2,1,0:T(8,128)(2,1)}, bf16[8,96,256]{2,1,0:T(8,128)(2,1)S(1)}, u32[]{:S(2)}, u32[]{:S(2)}) collective-permute-start(bf16[8,96,256]{2,1,0:T(8,128)(2,1)} %all-to-all-done.blocks_ref.b0), channel_id=1, source_target_pairs={{0,4},{4,8},{8,12},{12,0},{1,5},{5,9},{9,13},{13,1},{2,6},{6,10},{... | collective-permute-start | bytes 1179656 | tf_op jit(solution)/shard_map/ppermute | solution.py:50
  150.6 3.5 %collective-permute-start.5 = (bf16[8,96,256]{2,1,0:T(8,128)(2,1)}, bf16[8,96,256]{2,1,0:T(8,128)(2,1)S(1)}, u32[]{:S(2)}, u32[]{:S(2)}) collective-permute-start(bf16[8,96,256]{2,1,0:T(8,128)(2,1)} %all-to-all-done.blocks_ref.b0), channel_id=1, source_target_pairs={{0,8},{4,12},{8,0},{12,4},{1,9},{5,13},{9,1},{13,5},{2,10},{6,14},... | collective-permute-start | bytes 1179656 | tf_op jit(solution)/shard_map/ppermute | solution.py:50
  154.0 3.1 %collective-permute-start.6 = (bf16[8,96,256]{2,1,0:T(8,128)(2,1)}, bf16[8,96,256]{2,1,0:T(8,128)(2,1)S(1)}, u32[]{:S(2)}, u32[]{:S(2)}) collective-permute-start(bf16[8,96,256]{2,1,0:T(8,128)(2,1)} %all-to-all-done.blocks_ref.b0), channel_id=1, source_target_pairs={{0,12},{4,0},{8,4},{12,8},{1,13},{5,1},{9,5},{13,9},{2,14},{6,2},{... | collective-permute-start | bytes 1179656 | tf_op jit(solution)/shard_map/ppermute | solution.py:50
  157.2 13.9 %collective-permute-done.4.b1 = bf16[8,96,256]{2,1,0:T(8,128)(2,1)S(1)} collective-permute-done((bf16[8,96,256]{2,1,0:T(8,128)(2,1)}, bf16[8,96,256]{2,1,0:T(8,128)(2,1)S(1)}, u32[]{:S(2)}, u32[]{:S(2)}) %collective-permute-start.4) | collective-permute-done | bytes 393248 | tf_op jit(solution)/shard_map/ppermute | solution.py:50
  171.0 2.3 %collective-permute-done.6.b3 = bf16[8,96,256]{2,1,0:T(8,128)(2,1)S(1)} collective-permute-done((bf16[8,96,256]{2,1,0:T(8,128)(2,1)}, bf16[8,96,256]{2,1,0:T(8,128)(2,1)S(1)}, u32[]{:S(2)}, u32[]{:S(2)}) %collective-permute-start.6) | collective-permute-done | bytes 393248 | tf_op jit(solution)/shard_map/ppermute | solution.py:50
  173.3 2.6 %directions.1 = (f32[256,256]{1,0:T(8,128)}, f32[256,256]{1,0:T(8,128)}, f32[256,128]{1,0:T(8,128)}, f32[256,128]{1,0:T(8,128)}, f32[16,8,128]{2,1,0:T(8,128)}) custom-call(bf16[8,32,384]{2,1,0:T(8,128)(2,1)S(1)} %all-to-all-done.5.got_ref, f32[256,256]{1,0:T(8,128)S(1)} %copy-done.5, f32[256,256]{1,0:T(8,128)S(1)} %copy-done.6, f32[256,128]{1,0:T(8,128)S(1)} %copy-done.9, ...), custom_call_target="tpu_custom_call" | custom-call | flops 400000000 | bytes 4000000 | tf_op jit(solution)/shard_map/directions/pallas_call | solution.py:263
  176.0 0.8 copy-done
  176.7 4.7 %all-to-all-start.6 = ((f32[16,8,128]{2,1,0:T(8,128)}), f32[16,8,128]{2,1,0:T(8,128)}, u32[]{:S(2)}, u32[]{:S(2)}) async-start(f32[16,8,128]{2,1,0:T(8,128)} %get-tuple-element.35), calls=%async_computation.6 | async-start | bytes 131072 | tf_op jit(solution)/shard_map/all_to_all | solution.py:31
  181.5 0.8 copy-done.13
  182.3 4.5 %ready.1 = (f32[64,256]{1,0:T(8,128)}, f32[32,128]{1,0:T(8,128)}, bf16[2048,256]{1,0:T(8,128)(2,1)}, bf16[1024,128]{1,0:T(8,128)(2,1)}, bf16[2048,256]{1,0:T(8,128)(2,1)}, /*index=5*/bf16[1024,128]{1,0:T(8,128)(2,1)}) custom-call(f32[256,256]{1,0:T(8,128)} %get-tuple-element.24.mean_o, f32[256,256]{1,0:T(8,128)} %get-tuple-element.25.square_o, ...), custom_call_target="tpu_custom_call" | custom-call | flops 400000000 | bytes 4000000 | tf_op jit(solution)/shard_map/ready/pallas_call | solution.py:325
  186.8 1.3 all-to-all-done.6.total_ref
  188.0 3.8 %outputs.1 = (f32[64,256]{1,0:T(8,128)}, f32[64,256]{1,0:T(8,128)}, bf16[2048,256]{1,0:T(8,128)(2,1)}, f32[32,128]{1,0:T(8,128)}, f32[32,128]{1,0:T(8,128)}, /*index=5*/bf16[1024,128]{1,0:T(8,128)(2,1)}) custom-call(f32[16,8,128]{2,1,0:T(8,128)} %all-to-all-done.6.total_ref, f32[64,256]{1,0:T(8,128)} %weight_o.3, f32[32,128]{1,0:T(8,128)} %weight_v.3, ...), custom_call_target="tpu_custom_call" | custom-call | flops 10000000 | bytes 4000000 | tf_op jit(solution)/shard_map/outputs/pallas_call | solution.py:388
  (33 shorter events, 0.1 us)
Async XLA Ops:
  1.4 0.7 collective-permute-start
  2.9 31.4 %all-to-all-start = ((bf16[8,96,256]{2,1,0:T(8,128)(2,1)}), bf16[8,96,256]{2,1,0:T(8,128)(2,1)}, u32[]{:S(2)}, u32[]{:S(2)}) async-start(bf16[8,96,256]{2,1,0:T(8,128)(2,1)} %broadcast_in_dim.4), calls=%async_computation | async-start | bytes 786432 | tf_op jit(solution)/shard_map/all_to_all | solution.py:31
  20.1 10.7 %collective-permute-start.1 = (bf16[576,128]{1,0:T(8,128)(2,1)}, bf16[576,128]{1,0:T(8,128)(2,1)S(1)}, u32[]{:S(2)}, u32[]{:S(2)}) collective-permute-start(bf16[576,128]{1,0:T(8,128)(2,1)} %get-tuple-element.32), channel_id=1, source_target_pairs={{0,1},{1,2},{2,3},{3,0},{4,5},{5,6},{6,7},{7,4},{8,9},{9,10},{10,1... | collective-permute-start | bytes 442376 | tf_op jit(solution)/shard_map/ppermute | solution.py:50
  23.4 9.5 %collective-permute-start.2 = (bf16[576,128]{1,0:T(8,128)(2,1)}, bf16[576,128]{1,0:T(8,128)(2,1)S(1)}, u32[]{:S(2)}, u32[]{:S(2)}) collective-permute-start(bf16[576,128]{1,0:T(8,128)(2,1)} %get-tuple-element.33), channel_id=1, source_target_pairs={{0,2},{1,3},{2,0},{3,1},{4,6},{5,7},{6,4},{7,5},{8,10},{9,11},{10,... | collective-permute-start | bytes 442376 | tf_op jit(solution)/shard_map/ppermute | solution.py:50
  27.7 6.6 %collective-permute-start.3 = (bf16[576,128]{1,0:T(8,128)(2,1)}, bf16[576,128]{1,0:T(8,128)(2,1)S(1)}, u32[]{:S(2)}, u32[]{:S(2)}) collective-permute-start(bf16[576,128]{1,0:T(8,128)(2,1)} %get-tuple-element.34), channel_id=1, source_target_pairs={{0,3},{1,0},{2,1},{3,2},{4,7},{5,4},{6,5},{7,6},{8,11},{9,8},{10,9... | collective-permute-start | bytes 442376 | tf_op jit(solution)/shard_map/ppermute | solution.py:50
  34.3 0.9 copy-start.8
  56.9 27.0 %copy-start.3 = (bf16[1536,256]{1,0:T(8,128)(2,1)S(1)}, bf16[1536,256]{1,0:T(8,128)(2,1)}, u32[]{:S(2)}) copy-start(bf16[1536,256]{1,0:T(8,128)(2,1)} %cot_o.1) | copy-start | bytes 2359300
  56.9 27.0 %copy-start.4 = (bf16[1536,128]{1,0:T(8,128)(2,1)S(1)}, bf16[1536,128]{1,0:T(8,128)(2,1)}, u32[]{:S(2)}) copy-start(bf16[1536,128]{1,0:T(8,128)(2,1)} %cot_v.1) | copy-start | bytes 1179652
  83.8 8.8 %copy-start.7 = (f32[64,256]{1,0:T(8,128)S(1)}, f32[64,256]{1,0:T(8,128)}, u32[]{:S(2)}) copy-start(f32[64,256]{1,0:T(8,128)} %weight_o.3) | copy-start | bytes 196612
  83.8 8.8 %copy-start.11 = (f32[32,128]{1,0:T(8,128)S(1)}, f32[32,128]{1,0:T(8,128)}, u32[]{:S(2)}) copy-start(f32[32,128]{1,0:T(8,128)} %weight_v.3) | copy-start | bytes 49156
  85.9 31.0 %all-to-all-start.3 = ((bf16[8,32,384]{2,1,0:T(8,128)(2,1)}), bf16[8,32,384]{2,1,0:T(8,128)(2,1)S(1)}, u32[]{:S(2)}, u32[]{:S(2)}) async-start(bf16[8,32,384]{2,1,0:T(8,128)(2,1)} %contract.1), calls=%async_computation.3 | async-start | bytes 393216 | tf_op jit(solution)/shard_map/all_to_all | solution.py:31
  92.6 80.7 %copy-start.5 = (f32[256,256]{1,0:T(8,128)S(1)}, f32[256,256]{1,0:T(8,128)}, u32[]{:S(2)}) copy-start(f32[256,256]{1,0:T(8,128)} %mean_o.1) | copy-start | bytes 786436
  92.6 80.7 %copy-start.6 = (f32[256,256]{1,0:T(8,128)S(1)}, f32[256,256]{1,0:T(8,128)}, u32[]{:S(2)}) copy-start(f32[256,256]{1,0:T(8,128)} %square_o.1) | copy-start | bytes 786436
  92.7 80.7 %copy-start.9 = (f32[256,128]{1,0:T(8,128)S(1)}, f32[256,128]{1,0:T(8,128)}, u32[]{:S(2)}) copy-start(f32[256,128]{1,0:T(8,128)} %mean_v.1) | copy-start | bytes 393220
  92.7 80.6 %copy-start.10 = (f32[256,128]{1,0:T(8,128)S(1)}, f32[256,128]{1,0:T(8,128)}, u32[]{:S(2)}) copy-start(f32[256,128]{1,0:T(8,128)} %square_v.1) | copy-start | bytes 393220
  92.7 15.9 %collective-permute-start.7 = (bf16[1,160,128]{2,1,0:T(8,128)(2,1)S(1)}, bf16[1,160,128]{2,1,0:T(8,128)(2,1)S(1)}, u32[]{:S(2)}, u32[]{:S(2)}) collective-permute-start(bf16[1,160,128]{2,1,0:T(8,128)(2,1)S(1)} %bitcast.4), channel_id=1, source_target_pairs={{0,256},{32,288},{64,320},{96,352},{128,384},{160,416},{192,448},{... | collective-permute-start | bytes 122888 | tf_op jit(solution)/shard_map/ppermute | solution.py:50
  108.6 14.1 %collective-permute-start.8 = (bf16[2,160,128]{2,1,0:T(8,128)(2,1)S(1)}, bf16[2,160,128]{2,1,0:T(8,128)(2,1)S(1)}, u32[]{:S(2)}, u32[]{:S(2)}) collective-permute-start(bf16[2,160,128]{2,1,0:T(8,128)(2,1)S(1)} %pad_maximum_fusion.2), channel_id=1, source_target_pairs={{0,128},{32,160},{64,192},{96,224},{128,256},{160,288},{192,320},{... | collective-permute-start | bytes 245768 | tf_op jit(solution)/shard_map/ppermute | solution.py:50
  117.5 17.4 %all-to-all-start.4 = ((bf16[4,32,384]{2,1,0:T(8,128)(2,1)}), bf16[4,32,384]{2,1,0:T(8,128)(2,1)S(1)}, u32[]{:S(2)}, u32[]{:S(2)}) async-start(bf16[4,32,384]{2,1,0:T(8,128)(2,1)} %shard_map.196), calls=%async_computation.4 | async-start | bytes 196608 | tf_op jit(solution)/shard_map/all_to_all | solution.py:31
  122.7 21.2 %collective-permute-start.11 = (bf16[4,160,128]{2,1,0:T(8,128)(2,1)S(1)}, bf16[4,160,128]{2,1,0:T(8,128)(2,1)S(1)}, u32[]{:S(2)}, u32[]{:S(2)}) collective-permute-start(bf16[4,160,128]{2,1,0:T(8,128)(2,1)S(1)} %pad_maximum_fusion.1), channel_id=1, source_target_pairs={{0,480},{32,0},{64,32},{96,64},{128,96},{160,128},{192,160},{224,1... | collective-permute-start | bytes 491528 | tf_op jit(solution)/shard_map/ppermute | solution.py:50
  131.0 12.9 %collective-permute-start.10 = (bf16[4,160,128]{2,1,0:T(8,128)(2,1)S(1)}, bf16[4,160,128]{2,1,0:T(8,128)(2,1)S(1)}, u32[]{:S(2)}, u32[]{:S(2)}) collective-permute-start(bf16[4,160,128]{2,1,0:T(8,128)(2,1)S(1)} %pad_maximum_fusion.1), channel_id=1, source_target_pairs={{0,64},{32,96},{64,128},{96,160},{128,192},{160,224},{192,256},{22... | collective-permute-start | bytes 491528 | tf_op jit(solution)/shard_map/ppermute | solution.py:50
  133.0 12.1 %collective-permute-start.9 = (bf16[4,160,128]{2,1,0:T(8,128)(2,1)S(1)}, bf16[4,160,128]{2,1,0:T(8,128)(2,1)S(1)}, u32[]{:S(2)}, u32[]{:S(2)}) collective-permute-start(bf16[4,160,128]{2,1,0:T(8,128)(2,1)S(1)} %pad_maximum_fusion.1), channel_id=1, source_target_pairs={{0,32},{32,64},{64,96},{96,128},{128,160},{160,192},{192,224},{224... | collective-permute-start | bytes 491528 | tf_op jit(solution)/shard_map/ppermute | solution.py:50
  135.6 37.7 %all-to-all-start.5 = ((bf16[8,32,384]{2,1,0:T(8,128)(2,1)}), bf16[8,32,384]{2,1,0:T(8,128)(2,1)S(1)}, u32[]{:S(2)}, u32[]{:S(2)}) async-start(bf16[8,32,384]{2,1,0:T(8,128)(2,1)} %shard_map.197), calls=%async_computation.5 | async-start | bytes 393216 | tf_op jit(solution)/shard_map/all_to_all | solution.py:31
  145.1 31.6 %copy-start.12 = (bf16[16,160,128]{2,1,0:T(8,128)(2,1)}, bf16[16,160,128]{2,1,0:T(8,128)(2,1)S(1)}, u32[]{:S(2)}) copy-start(bf16[16,160,128]{2,1,0:T(8,128)(2,1)S(1)} %pad_maximum_fusion.own_ref) | copy-start | bytes 1966084
  145.1 36.3 %collective-permute-start.12 = (bf16[16,160,128]{2,1,0:T(8,128)(2,1)S(1)}, bf16[16,160,128]{2,1,0:T(8,128)(2,1)S(1)}, u32[]{:S(2)}, u32[]{:S(2)}) collective-permute-start(bf16[16,160,128]{2,1,0:T(8,128)(2,1)S(1)} %pad_maximum_fusion.own_ref), channel_id=1, source_target_pairs={{0,16},{16,0},{1,17},{17,1},{2,18},{18,2},{3,19},{19,3},{4,20},{20... | collective-permute-start | bytes 1966088 | tf_op jit(solution)/shard_map/ppermute | solution.py:50
  148.6 22.4 %collective-permute-start.4 = (bf16[8,96,256]{2,1,0:T(8,128)(2,1)}, bf16[8,96,256]{2,1,0:T(8,128)(2,1)S(1)}, u32[]{:S(2)}, u32[]{:S(2)}) collective-permute-start(bf16[8,96,256]{2,1,0:T(8,128)(2,1)} %all-to-all-done.blocks_ref.b0), channel_id=1, source_target_pairs={{0,4},{4,8},{8,12},{12,0},{1,5},{5,9},{9,13},{13,1},{2,6},{6,10},{... | collective-permute-start | bytes 1179656 | tf_op jit(solution)/shard_map/ppermute | solution.py:50
  150.6 20.5 %collective-permute-start.5 = (bf16[8,96,256]{2,1,0:T(8,128)(2,1)}, bf16[8,96,256]{2,1,0:T(8,128)(2,1)S(1)}, u32[]{:S(2)}, u32[]{:S(2)}) collective-permute-start(bf16[8,96,256]{2,1,0:T(8,128)(2,1)} %all-to-all-done.blocks_ref.b0), channel_id=1, source_target_pairs={{0,8},{4,12},{8,0},{12,4},{1,9},{5,13},{9,1},{13,5},{2,10},{6,14},... | collective-permute-start | bytes 1179656 | tf_op jit(solution)/shard_map/ppermute | solution.py:50
  154.0 19.3 %collective-permute-start.6 = (bf16[8,96,256]{2,1,0:T(8,128)(2,1)}, bf16[8,96,256]{2,1,0:T(8,128)(2,1)S(1)}, u32[]{:S(2)}, u32[]{:S(2)}) collective-permute-start(bf16[8,96,256]{2,1,0:T(8,128)(2,1)} %all-to-all-done.blocks_ref.b0), channel_id=1, source_target_pairs={{0,12},{4,0},{8,4},{12,8},{1,13},{5,1},{9,5},{13,9},{2,14},{6,2},{... | collective-permute-start | bytes 1179656 | tf_op jit(solution)/shard_map/ppermute | solution.py:50
  171.0 4.9 %copy-start.1 = (bf16[8,96,256]{2,1,0:T(8,128)(2,1)}, bf16[8,96,256]{2,1,0:T(8,128)(2,1)S(1)}, u32[]{:S(2)}) copy-start(bf16[8,96,256]{2,1,0:T(8,128)(2,1)S(1)} %collective-permute-done.5.b2) | copy-start | bytes 1179652
  173.3 3.5 %copy-start.2 = (bf16[8,96,256]{2,1,0:T(8,128)(2,1)}, bf16[8,96,256]{2,1,0:T(8,128)(2,1)S(1)}, u32[]{:S(2)}) copy-start(bf16[8,96,256]{2,1,0:T(8,128)(2,1)S(1)} %collective-permute-done.6.b3) | copy-start | bytes 1179652
  176.0 0.8 copy-start
  176.7 11.3 %all-to-all-start.6 = ((f32[16,8,128]{2,1,0:T(8,128)}), f32[16,8,128]{2,1,0:T(8,128)}, u32[]{:S(2)}, u32[]{:S(2)}) async-start(f32[16,8,128]{2,1,0:T(8,128)} %get-tuple-element.35), calls=%async_computation.6 | async-start | bytes 131072 | tf_op jit(solution)/shard_map/all_to_all | solution.py:31
  181.5 0.8 copy-start.13

commit v7 on v6

--- a/solution.py
+++ b/solution.py
@@ -71,7 +71,7 @@
         g = lax.rem(lax.axis_index("x") + k, groups)
         pieces = []
         for p in range(groups):
-            at = pl.multiple_of((p * groups + g) * each, each)
+            at = pl.multiple_of((g * groups + p) * each, each)
             outs[k][p * each : (p + 1) * each, :] = attn_here[pl.ds(at, each), :]
             pieces.append(turned[pl.ds(at, each), :])
         half = groups // 2
@@ -95,7 +95,7 @@
             pltpu.SemaphoreType.DMA((2,)),
         ],
         cost_estimate=pl.CostEstimate(flops=10**7, bytes_accessed=10**6, transcendentals=0),
-        compiler_params=pltpu.CompilerParams(vmem_limit_bytes=WHOLE),
+        compiler_params=pltpu.CompilerParams(vmem_limit_bytes=WHOLE - 2**18),
         name="pack",
     )(attn_out, lat_turned)
 
@@ -150,7 +150,7 @@
         functools.partial(lift_kernel, rows_o, tokens),
         out_shape=jax.ShapeDtypeStruct((parts, tokens // parts, 2 * rank), BF),
         cost_estimate=pl.CostEstimate(flops=2 * 10**8, bytes_accessed=10**6, transcendentals=0),
-        compiler_params=pltpu.CompilerParams(vmem_limit_bytes=ROOM),
+        compiler_params=pltpu.CompilerParams(vmem_limit_bytes=WHOLE),
         name="lift",
     )(blocks, *gots)
 
@@ -308,8 +308,8 @@
             update_v_out[pl.ds(at, rows_v), :] = update_v[i * rows_v : (i + 1) * rows_v]
     for ref, core in ((own_ref, c), (other_ref, 1 - c)):
         for p in range(ref.shape[0]):
-            behind = (p & 1) * 8 + (p >> 1 & 1) * 4 + STEPS[p >> 2]
-            index = 2 * lax.rem(z + 16 - behind, 16) + core
+            behind = (0, 8, 4, 12)[p & 3] + STEPS[p >> 2]
+            index = 2 * lax.rem(z + 32 - behind, 16) + core
             at = pl.multiple_of(index * rows_o, rows_o)
             old_o_out[pl.ds(at, rows_o), :128] = ref[p, :rows_o]
             old_o_out[pl.ds(at, rows_o), 128:] = ref[p, rows_o : 2 * rows_o]
@@ -341,7 +341,7 @@
 def output_kernel(
     counts, pieces, total_ref, weight_o, weight_v, step_o, step_v, update_o, update_v, old_o, old_v,
     step_o_out, new_o_out, copy_o_out, step_v_out, new_v_out, copy_v_out,
-    update_o_here, update_v_here, old_o_here, old_v_here, sems,
+    update_o_here, update_v_here, old_o_here, old_v_here, copy_o_here, copy_v_here, sems, out_sems,
 ):
     copies = []
     for n, (source, here) in enumerate(
@@ -366,10 +366,11 @@
         step_out[...] = mine
         new_out[...] = weight[...] - mine
         scales.append(scale)
-    for n, (scale, update, old, copy_out) in enumerate(
+    leaving = []
+    for n, (scale, update, old, here, copy_out) in enumerate(
         (
-            (scales[0], update_o_here, old_o_here, copy_o_out),
-            (scales[1], update_v_here, old_v_here, copy_v_out),
+            (scales[0], update_o_here, old_o_here, copy_o_here, copy_o_out),
+            (scales[1], update_v_here, old_v_here, copy_v_here, copy_v_out),
         )
     ):
         rows = old.shape[0] // pieces
@@ -377,7 +378,11 @@
             copies[2 * n * pieces + p].wait()
             copies[(2 * n + 1) * pieces + p].wait()
             part = pl.ds(p * rows, rows)
-            copy_out[part, :] = (old[part, :].astype(F32) - update[part, :].astype(F32) * scale).astype(BF)
+            here[part, :] = (old[part, :].astype(F32) - update[part, :].astype(F32) * scale).astype(BF)
+            leaving.append(pltpu.make_async_copy(here.at[part], copy_out.at[part], out_sems.at[n, p]))
+            leaving[-1].start()
+    for copy in leaving:
+        copy.wait()
 
 
 def outputs(counts, total, weight_o, weight_v, step_o, step_v, update_o, update_v, old_o, old_v):
@@ -388,6 +393,7 @@
     return pl.pallas_call(
         functools.partial(output_kernel, counts, pieces),
         in_specs=[vmem] * 5 + [hbm] * 4,
+        out_specs=(vmem, vmem, hbm, vmem, vmem, hbm),
         out_shape=(
             shape(weight_o.shape, F32),
             shape(weight_o.shape, F32),
@@ -396,8 +402,8 @@
             shape(weight_v.shape, F32),
             shape(old_v.shape, BF),
         ),
-        scratch_shapes=[pltpu.VMEM(a.shape, BF) for a in (update_o, update_v, old_o, old_v)]
-        + [pltpu.SemaphoreType.DMA((4, pieces))],
+        scratch_shapes=[pltpu.VMEM(a.shape, BF) for a in (update_o, update_v, old_o, old_v, old_o, old_v)]
+        + [pltpu.SemaphoreType.DMA((4, pieces)), pltpu.SemaphoreType.DMA((2, pieces))],
         cost_estimate=pl.CostEstimate(flops=10**7, bytes_accessed=4 * 10**6, transcendentals=10),
         compiler_params=pltpu.CompilerParams(vmem_limit_bytes=WHOLE),
         name="outputs",
@@ -435,9 +441,10 @@
         gots[k] = shifted(gots[k], "x", k)
 
     own = old_rows(out_weight, value_up_matrix)[None]
-    for k in (8, 4):
-        more = shifted(own, Z, k)
-        own = lax.optimization_barrier(jnp.concatenate([own, more], 0))
+    rows = [own]
+    for k in (8, 4, 12):
+        rows.append(shifted(own, Z, k))
+    own = lax.optimization_barrier(jnp.concatenate(rows, 0))
     rows = [own]
     for k in STEPS[1:]:
         rows.append(shifted(own, Z, k))
@@ -448,7 +455,7 @@
     partial = lift(blocks, gots, rows_o, tokens // xs, ys)
     partial = exchange(partial, "y")
     lifted = summed_for(partial, tp, BF)
-    lifted = exchange(lifted, TP).reshape(tokens, 2 * rank)
+    lifted = exchange(lifted, ("x", "y")).reshape(tokens, 2 * rank)
 
     near = lax.axis_size(NEAR)
     part = contract(lifted, out_cot, value_cot, near, 4)

time: 193 us -> 190 us (0.984)
  waiting for transfers between devices: 25.2 us -> 22.2 us
    ppermute x12 -> x13, waiting for transfers between devices: 24 us -> 19.6 us  [shifted(): lax.ppermute(value, axis, [(i, (i + by) % devices) for i in range(devices)])]
    all_to_all x5, starting transfers between devices: 40.1 us -> 38.1 us  [exchange(): return lax.all_to_all(value, axes, 0, 0, tiled=True)]
    ppermute x12 -> x13, starting transfers between devices: 55.7 us -> 57.4 us  [shifted(): lax.ppermute(value, axis, [(i, (i + by) % devices) for i in range(devices)])]
  transfers between devices with their start and end apart: 18 -> 19, of which waited for: 7 -> 6; matrix products, arithmetic and copies ran while one was open for 0% -> 0% of each run, Pallas kernels for 5% -> 6%
where the time goes in v7:
time: 190 us; the launch traced here: 188 us
  starting transfers between devices  96.2 us (51%)
  blocking collectives  46.5 us (24%)
  waiting for transfers between devices  22.2 us (12%)
  Pallas kernels  19.3 us (10%)
  local copies, waits for them, and re-layouts  2.42 us (1%)
    ppermute x13, starting transfers between devices, shifted(): lax.ppermute(value, axis, [(i, (i + by) % devices) for i in range(devices)])  57.4 us
    all_to_all x2, blocking collectives, exchange(): return lax.all_to_all(value, axes, 0, 0, tiled=True)  46.5 us
    all_to_all x5, starting transfers between devices, exchange(): return lax.all_to_all(value, axes, 0, 0, tiled=True)  38.1 us
    ppermute x13, waiting for transfers between devices, shifted(): lax.ppermute(value, axis, [(i, (i + by) % devices) for i in range(devices)])  19.6 us
    pallas_call x1, Pallas kernels, ready(): pl.pallas_call(functools.partial(ready_kernel, rows_o, rows_v), out_shape...  4.45 us
    pallas_call x1, Pallas kernels, outputs(): pl.pallas_call(functools.partial(output_kernel, counts, pieces), in_specs...  4.15 us
  transfers between devices with their start and end apart: 19, of which 6 were waited for; matrix products, arithmetic and copies ran while one was open for 0% of the time, Pallas kernels for 6%

profile of v7, /device:TPU:1, one launch (start us, length us, event | category | flops | bytes accessed | tf_op | source)
XLA Modules:
  0.0 188.4 jit_solution(15084360342165296408)
XLA Ops:
  0.6 0.8 pad_maximum_fusion.2
  1.4 0.7 collective-permute-start
  2.1 0.8 broadcast_in_dim.4
  2.9 15.3 %all-to-all-start = ((bf16[8,96,256]{2,1,0:T(8,128)(2,1)}), bf16[8,96,256]{2,1,0:T(8,128)(2,1)}, u32[]{:S(2)}, u32[]{:S(2)}) async-start(bf16[8,96,256]{2,1,0:T(8,128)(2,1)} %broadcast_in_dim.4), calls=%async_computation | async-start | bytes 786432 | tf_op jit(solution)/shard_map/all_to_all | solution.py:31
  18.1 2.0 %pack.1 = (bf16[576,128]{1,0:T(8,128)(2,1)}, bf16[576,128]{1,0:T(8,128)(2,1)}, bf16[576,128]{1,0:T(8,128)(2,1)}, bf16[576,128]{1,0:T(8,128)(2,1)}) custom-call(bf16[1536,128]{1,0:T(8,128)(2,1)} %attn_ref.1, bf16[64,1536]{1,0:T(8,128)(2,1)} %bitcast.8), custom_call_target="tpu_custom_call" | custom-call | flops 10000000 | bytes 1000000 | tf_op jit(solution)/shard_map/pack/pallas_call | solution.py:87
  20.1 3.3 %collective-permute-start.1 = (bf16[576,128]{1,0:T(8,128)(2,1)}, bf16[576,128]{1,0:T(8,128)(2,1)}, u32[]{:S(2)}, u32[]{:S(2)}) collective-permute-start(bf16[576,128]{1,0:T(8,128)(2,1)} %get-tuple-element.32), channel_id=1, source_target_pairs={{0,1},{1,2},{2,3},{3,0},{4,5},{5,6},{6,7},{7,4},{8,9},{9,10},{10,1... | collective-permute-start | bytes 442376 | tf_op jit(solution)/shard_map/ppermute | solution.py:50
  23.4 4.3 %collective-permute-start.2 = (bf16[576,128]{1,0:T(8,128)(2,1)}, bf16[576,128]{1,0:T(8,128)(2,1)}, u32[]{:S(2)}, u32[]{:S(2)}) collective-permute-start(bf16[576,128]{1,0:T(8,128)(2,1)} %get-tuple-element.33), channel_id=1, source_target_pairs={{0,2},{1,3},{2,0},{3,1},{4,6},{5,7},{6,4},{7,5},{8,10},{9,11},{10,... | collective-permute-start | bytes 442376 | tf_op jit(solution)/shard_map/ppermute | solution.py:50
  27.7 3.1 %collective-permute-start.3 = (bf16[576,128]{1,0:T(8,128)(2,1)}, bf16[576,128]{1,0:T(8,128)(2,1)}, u32[]{:S(2)}, u32[]{:S(2)}) collective-permute-start(bf16[576,128]{1,0:T(8,128)(2,1)} %get-tuple-element.34), channel_id=1, source_target_pairs={{0,3},{1,0},{2,1},{3,2},{4,7},{5,4},{6,5},{7,6},{8,11},{9,8},{10,9... | collective-permute-start | bytes 442376 | tf_op jit(solution)/shard_map/ppermute | solution.py:50
  30.8 0.0 collective-permute-done.1.refs_1_
  30.8 2.2 %collective-permute-done.2.refs_2_ = bf16[576,128]{1,0:T(8,128)(2,1)} collective-permute-done((bf16[576,128]{1,0:T(8,128)(2,1)}, bf16[576,128]{1,0:T(8,128)(2,1)}, u32[]{:S(2)}, u32[]{:S(2)}) %collective-permute-start.2) | collective-permute-done | bytes 147488 | tf_op jit(solution)/shard_map/ppermute | solution.py:50
  33.0 1.4 collective-permute-done.3.refs_3_
  34.4 0.0 all-to-all-done.blocks_ref.b0
  34.4 2.5 %lift.1 = bf16[4,96,512]{2,1,0:T(8,128)(2,1)} custom-call(bf16[8,96,256]{2,1,0:T(8,128)(2,1)} %all-to-all-done.blocks_ref.b0, bf16[576,128]{1,0:T(8,128)(2,1)} %get-tuple-element.31.refs_0_, bf16[576,128]{1,0:T(8,128)(2,1)} %collective-permute-done.1.refs_1_, bf16[576,128]{1,0:T(8,128)(2,1)} %collective-permute-done.2.refs_2_, ...), custom_call_target="tpu_custom_call" | custom-call | flops 200000000 | bytes 1000000 | tf_op jit(solution)/shard_map/lift/pallas_call | solution.py:149
  36.9 20.2 %all_to_all.35.got_ref = bf16[4,96,512]{2,1,0:T(8,128)(2,1)S(1)} all-to-all(bf16[4,96,512]{2,1,0:T(8,128)(2,1)} %lift.1), channel_id=1, replica_groups=mesh['zh'=4,'zl'=4,'c'=2,'y'=4,'x'=4] {'y'}, dimensions={0} | all-to-all | bytes 786432 | tf_op jit(solution)/shard_map/all_to_all | solution.py:31
  57.1 0.2 shard_map.195
  57.2 0.0 copy-start.3
  57.2 0.0 copy-start.4
  57.2 26.3 %all_to_all.36 = bf16[16,96,512]{2,1,0:T(8,128)(2,1)S(1)} all-to-all(bf16[16,96,512]{2,1,0:T(8,128)(2,1)S(1)} %shard_map.195), channel_id=1, replica_groups=mesh['zh'=4,'zl'=4,'c'=2,'y'=4,'x'=4] {'x','y'}, dimensions={0} | all-to-all | bytes 3145728 | tf_op jit(solution)/shard_map/all_to_all | solution.py:31
  83.6 2.0 %contract.1 = bf16[8,32,384]{2,1,0:T(8,128)(2,1)} custom-call(bf16[1536,512]{1,0:T(8,128)(2,1)S(1)} %bitcast.3, bf16[1536,256]{1,0:T(8,128)(2,1)S(1)} %copy-done.3, bf16[1536,128]{1,0:T(8,128)(2,1)S(1)} %copy-done.4), custom_call_target="tpu_custom_call" | custom-call | flops 300000000 | bytes 3000000 | tf_op jit(solution)/shard_map/contract/pallas_call | solution.py:209
  85.6 6.7 %all-to-all-start.3 = ((bf16[8,32,384]{2,1,0:T(8,128)(2,1)}), bf16[8,32,384]{2,1,0:T(8,128)(2,1)S(1)}, u32[]{:S(2)}, u32[]{:S(2)}) async-start(bf16[8,32,384]{2,1,0:T(8,128)(2,1)} %contract.1), calls=%async_computation.3 | async-start | bytes 393216 | tf_op jit(solution)/shard_map/all_to_all | solution.py:31
  92.3 11.0 %collective-permute-start.9 = (bf16[1,160,128]{2,1,0:T(8,128)(2,1)S(1)}, bf16[1,160,128]{2,1,0:T(8,128)(2,1)S(1)}, u32[]{:S(2)}, u32[]{:S(2)}) collective-permute-start(bf16[1,160,128]{2,1,0:T(8,128)(2,1)S(1)} %bitcast.4), channel_id=1, source_target_pairs={{0,384},{32,416},{64,448},{96,480},{128,0},{160,32},{192,64},{224,... | collective-permute-start | bytes 122888 | tf_op jit(solution)/shard_map/ppermute | solution.py:50
  103.3 1.9 %collective-permute-start.8 = (bf16[1,160,128]{2,1,0:T(8,128)(2,1)S(1)}, bf16[1,160,128]{2,1,0:T(8,128)(2,1)S(1)}, u32[]{:S(2)}, u32[]{:S(2)}) collective-permute-start(bf16[1,160,128]{2,1,0:T(8,128)(2,1)S(1)} %bitcast.5), channel_id=1, source_target_pairs={{0,128},{32,160},{64,192},{96,224},{128,256},{160,288},{192,320},{... | collective-permute-start | bytes 122888 | tf_op jit(solution)/shard_map/ppermute | solution.py:50
  105.3 10.3 %collective-permute-start.7 = (bf16[1,160,128]{2,1,0:T(8,128)(2,1)S(1)}, bf16[1,160,128]{2,1,0:T(8,128)(2,1)S(1)}, u32[]{:S(2)}, u32[]{:S(2)}) collective-permute-start(bf16[1,160,128]{2,1,0:T(8,128)(2,1)S(1)} %bitcast.6), channel_id=1, source_target_pairs={{0,256},{32,288},{64,320},{96,352},{128,384},{160,416},{192,448},{... | collective-permute-start | bytes 122888 | tf_op jit(solution)/shard_map/ppermute | solution.py:50
  115.6 0.7 shard_map.196
  116.3 3.3 %all-to-all-start.4 = ((bf16[4,32,384]{2,1,0:T(8,128)(2,1)}), bf16[4,32,384]{2,1,0:T(8,128)(2,1)S(1)}, u32[]{:S(2)}, u32[]{:S(2)}) async-start(bf16[4,32,384]{2,1,0:T(8,128)(2,1)} %shard_map.196), calls=%async_computation.4 | async-start | bytes 196608 | tf_op jit(solution)/shard_map/all_to_all | solution.py:31
  119.6 0.0 collective-permute-done.9
  119.6 0.0 collective-permute-done.7
  119.6 7.5 %collective-permute-start.12 = (bf16[4,160,128]{2,1,0:T(8,128)(2,1)S(1)}, bf16[4,160,128]{2,1,0:T(8,128)(2,1)S(1)}, u32[]{:S(2)}, u32[]{:S(2)}) collective-permute-start(bf16[4,160,128]{2,1,0:T(8,128)(2,1)S(1)} %pad_maximum_fusion.1), channel_id=1, source_target_pairs={{0,480},{32,0},{64,32},{96,64},{128,96},{160,128},{192,160},{224,1... | collective-permute-start | bytes 491528 | tf_op jit(solution)/shard_map/ppermute | solution.py:50
  127.1 1.9 %collective-permute-start.11 = (bf16[4,160,128]{2,1,0:T(8,128)(2,1)S(1)}, bf16[4,160,128]{2,1,0:T(8,128)(2,1)S(1)}, u32[]{:S(2)}, u32[]{:S(2)}) collective-permute-start(bf16[4,160,128]{2,1,0:T(8,128)(2,1)S(1)} %pad_maximum_fusion.1), channel_id=1, source_target_pairs={{0,64},{32,96},{64,128},{96,160},{128,192},{160,224},{192,256},{22... | collective-permute-start | bytes 491528 | tf_op jit(solution)/shard_map/ppermute | solution.py:50
  129.1 1.9 %collective-permute-start.10 = (bf16[4,160,128]{2,1,0:T(8,128)(2,1)S(1)}, bf16[4,160,128]{2,1,0:T(8,128)(2,1)S(1)}, u32[]{:S(2)}, u32[]{:S(2)}) collective-permute-start(bf16[4,160,128]{2,1,0:T(8,128)(2,1)S(1)} %pad_maximum_fusion.1), channel_id=1, source_target_pairs={{0,32},{32,64},{64,96},{96,128},{128,160},{160,192},{192,224},{224... | collective-permute-start | bytes 491528 | tf_op jit(solution)/shard_map/ppermute | solution.py:50
  131.0 1.3 all-to-all-done.4.got_ref
  132.3 0.7 shard_map.197
  133.0 7.9 %all-to-all-start.5 = ((bf16[8,32,384]{2,1,0:T(8,128)(2,1)}), bf16[8,32,384]{2,1,0:T(8,128)(2,1)S(1)}, u32[]{:S(2)}, u32[]{:S(2)}) async-start(bf16[8,32,384]{2,1,0:T(8,128)(2,1)} %shard_map.197), calls=%async_computation.5 | async-start | bytes 393216 | tf_op jit(solution)/shard_map/all_to_all | solution.py:31
  140.9 0.1 pad_maximum_fusion.own_ref
  141.0 0.0 copy-start.11
  141.0 3.6 %collective-permute-start.13 = (bf16[16,160,128]{2,1,0:T(8,128)(2,1)S(1)}, bf16[16,160,128]{2,1,0:T(8,128)(2,1)S(1)}, u32[]{:S(2)}, u32[]{:S(2)}) collective-permute-start(bf16[16,160,128]{2,1,0:T(8,128)(2,1)S(1)} %pad_maximum_fusion.own_ref), channel_id=1, source_target_pairs={{0,16},{16,0},{1,17},{17,1},{2,18},{18,2},{3,19},{19,3},{4,20},{20... | collective-permute-start | bytes 1966088 | tf_op jit(solution)/shard_map/ppermute | solution.py:50
  144.6 2.2 %collective-permute-start.4 = (bf16[8,96,256]{2,1,0:T(8,128)(2,1)}, bf16[8,96,256]{2,1,0:T(8,128)(2,1)S(1)}, u32[]{:S(2)}, u32[]{:S(2)}) collective-permute-start(bf16[8,96,256]{2,1,0:T(8,128)(2,1)} %all-to-all-done.blocks_ref.b0), channel_id=1, source_target_pairs={{0,4},{4,8},{8,12},{12,0},{1,5},{5,9},{9,13},{13,1},{2,6},{6,10},{... | collective-permute-start | bytes 1179656 | tf_op jit(solution)/shard_map/ppermute | solution.py:50
  146.8 3.1 %collective-permute-start.5 = (bf16[8,96,256]{2,1,0:T(8,128)(2,1)}, bf16[8,96,256]{2,1,0:T(8,128)(2,1)S(1)}, u32[]{:S(2)}, u32[]{:S(2)}) collective-permute-start(bf16[8,96,256]{2,1,0:T(8,128)(2,1)} %all-to-all-done.blocks_ref.b0), channel_id=1, source_target_pairs={{0,8},{4,12},{8,0},{12,4},{1,9},{5,13},{9,1},{13,5},{2,10},{6,14},... | collective-permute-start | bytes 1179656 | tf_op jit(solution)/shard_map/ppermute | solution.py:50
  149.8 3.4 %collective-permute-start.6 = (bf16[8,96,256]{2,1,0:T(8,128)(2,1)}, bf16[8,96,256]{2,1,0:T(8,128)(2,1)S(1)}, u32[]{:S(2)}, u32[]{:S(2)}) collective-permute-start(bf16[8,96,256]{2,1,0:T(8,128)(2,1)} %all-to-all-done.blocks_ref.b0), channel_id=1, source_target_pairs={{0,12},{4,0},{8,4},{12,8},{1,13},{5,1},{9,5},{13,9},{2,14},{6,2},{... | collective-permute-start | bytes 1179656 | tf_op jit(solution)/shard_map/ppermute | solution.py:50
  153.2 13.8 %collective-permute-done.4.b1 = bf16[8,96,256]{2,1,0:T(8,128)(2,1)S(1)} collective-permute-done((bf16[8,96,256]{2,1,0:T(8,128)(2,1)}, bf16[8,96,256]{2,1,0:T(8,128)(2,1)S(1)}, u32[]{:S(2)}, u32[]{:S(2)}) %collective-permute-start.4) | collective-permute-done | bytes 393248 | tf_op jit(solution)/shard_map/ppermute | solution.py:50
  167.0 2.3 %collective-permute-done.6.b3 = bf16[8,96,256]{2,1,0:T(8,128)(2,1)S(1)} collective-permute-done((bf16[8,96,256]{2,1,0:T(8,128)(2,1)}, bf16[8,96,256]{2,1,0:T(8,128)(2,1)S(1)}, u32[]{:S(2)}, u32[]{:S(2)}) %collective-permute-start.6) | collective-permute-done | bytes 393248 | tf_op jit(solution)/shard_map/ppermute | solution.py:50
  169.3 2.6 %directions.1 = (f32[256,256]{1,0:T(8,128)}, f32[256,256]{1,0:T(8,128)}, f32[256,128]{1,0:T(8,128)}, f32[256,128]{1,0:T(8,128)}, f32[16,8,128]{2,1,0:T(8,128)}) custom-call(bf16[8,32,384]{2,1,0:T(8,128)(2,1)S(1)} %all-to-all-done.5.got_ref, f32[256,256]{1,0:T(8,128)S(1)} %copy-done.5, f32[256,256]{1,0:T(8,128)S(1)} %copy-done.6, f32[256,128]{1,0:T(8,128)S(1)} %copy-done.8, ...), custom_call_target="tpu_custom_call" | custom-call | flops 400000000 | bytes 4000000 | tf_op jit(solution)/shard_map/directions/pallas_call | solution.py:263
  171.9 0.8 copy-done
  172.7 5.0 %all-to-all-start.6 = ((f32[16,8,128]{2,1,0:T(8,128)}), f32[16,8,128]{2,1,0:T(8,128)}, u32[]{:S(2)}, u32[]{:S(2)}) async-start(f32[16,8,128]{2,1,0:T(8,128)} %get-tuple-element.35), calls=%async_computation.6 | async-start | bytes 131072 | tf_op jit(solution)/shard_map/all_to_all | solution.py:31
  177.7 0.8 copy-done.12
  178.5 4.5 %ready.1 = (f32[64,256]{1,0:T(8,128)}, f32[32,128]{1,0:T(8,128)}, bf16[2048,256]{1,0:T(8,128)(2,1)}, bf16[1024,128]{1,0:T(8,128)(2,1)}, bf16[2048,256]{1,0:T(8,128)(2,1)}, /*index=5*/bf16[1024,128]{1,0:T(8,128)(2,1)}) custom-call(f32[256,256]{1,0:T(8,128)} %get-tuple-element.24.mean_o, f32[256,256]{1,0:T(8,128)} %get-tuple-element.25.square_o, ...), custom_call_target="tpu_custom_call" | custom-call | flops 400000000 | bytes 4000000 | tf_op jit(solution)/shard_map/ready/pallas_call | solution.py:325
  183.0 1.3 all-to-all-done.6.total_ref
  184.2 4.2 %outputs.1 = (f32[64,256]{1,0:T(8,128)}, f32[64,256]{1,0:T(8,128)}, bf16[2048,256]{1,0:T(8,128)(2,1)}, f32[32,128]{1,0:T(8,128)}, f32[32,128]{1,0:T(8,128)}, /*index=5*/bf16[1024,128]{1,0:T(8,128)(2,1)}) custom-call(f32[16,8,128]{2,1,0:T(8,128)} %all-to-all-done.6.total_ref, f32[64,256]{1,0:T(8,128)} %weight_o.3, f32[32,128]{1,0:T(8,128)} %weight_v.3, ...), custom_call_target="tpu_custom_call" | custom-call | flops 10000000 | bytes 4000000 | tf_op jit(solution)/shard_map/outputs/pallas_call | solution.py:393
  (32 shorter events, 0.1 us)
Async XLA Ops:
  1.4 0.7 collective-permute-start
  2.9 31.5 %all-to-all-start = ((bf16[8,96,256]{2,1,0:T(8,128)(2,1)}), bf16[8,96,256]{2,1,0:T(8,128)(2,1)}, u32[]{:S(2)}, u32[]{:S(2)}) async-start(bf16[8,96,256]{2,1,0:T(8,128)(2,1)} %broadcast_in_dim.4), calls=%async_computation | async-start | bytes 786432 | tf_op jit(solution)/shard_map/all_to_all | solution.py:31
  20.1 10.7 %collective-permute-start.1 = (bf16[576,128]{1,0:T(8,128)(2,1)}, bf16[576,128]{1,0:T(8,128)(2,1)}, u32[]{:S(2)}, u32[]{:S(2)}) collective-permute-start(bf16[576,128]{1,0:T(8,128)(2,1)} %get-tuple-element.32), channel_id=1, source_target_pairs={{0,1},{1,2},{2,3},{3,0},{4,5},{5,6},{6,7},{7,4},{8,9},{9,10},{10,1... | collective-permute-start | bytes 442376 | tf_op jit(solution)/shard_map/ppermute | solution.py:50
  23.4 9.6 %collective-permute-start.2 = (bf16[576,128]{1,0:T(8,128)(2,1)}, bf16[576,128]{1,0:T(8,128)(2,1)}, u32[]{:S(2)}, u32[]{:S(2)}) collective-permute-start(bf16[576,128]{1,0:T(8,128)(2,1)} %get-tuple-element.33), channel_id=1, source_target_pairs={{0,2},{1,3},{2,0},{3,1},{4,6},{5,7},{6,4},{7,5},{8,10},{9,11},{10,... | collective-permute-start | bytes 442376 | tf_op jit(solution)/shard_map/ppermute | solution.py:50
  27.7 6.7 %collective-permute-start.3 = (bf16[576,128]{1,0:T(8,128)(2,1)}, bf16[576,128]{1,0:T(8,128)(2,1)}, u32[]{:S(2)}, u32[]{:S(2)}) collective-permute-start(bf16[576,128]{1,0:T(8,128)(2,1)} %get-tuple-element.34), channel_id=1, source_target_pairs={{0,3},{1,0},{2,1},{3,2},{4,7},{5,4},{6,5},{7,6},{8,11},{9,8},{10,9... | collective-permute-start | bytes 442376 | tf_op jit(solution)/shard_map/ppermute | solution.py:50
  57.2 26.3 %copy-start.3 = (bf16[1536,256]{1,0:T(8,128)(2,1)S(1)}, bf16[1536,256]{1,0:T(8,128)(2,1)}, u32[]{:S(2)}) copy-start(bf16[1536,256]{1,0:T(8,128)(2,1)} %cot_o.1) | copy-start | bytes 2359300
  57.2 26.3 %copy-start.4 = (bf16[1536,128]{1,0:T(8,128)(2,1)S(1)}, bf16[1536,128]{1,0:T(8,128)(2,1)}, u32[]{:S(2)}) copy-start(bf16[1536,128]{1,0:T(8,128)(2,1)} %cot_v.1) | copy-start | bytes 1179652
  83.6 8.7 %copy-start.7 = (f32[64,256]{1,0:T(8,128)S(1)}, f32[64,256]{1,0:T(8,128)}, u32[]{:S(2)}) copy-start(f32[64,256]{1,0:T(8,128)} %weight_o.3) | copy-start | bytes 196612
  83.6 8.7 %copy-start.10 = (f32[32,128]{1,0:T(8,128)S(1)}, f32[32,128]{1,0:T(8,128)}, u32[]{:S(2)}) copy-start(f32[32,128]{1,0:T(8,128)} %weight_v.3) | copy-start | bytes 49156
  85.6 83.7 %copy-start.5 = (f32[256,256]{1,0:T(8,128)S(1)}, f32[256,256]{1,0:T(8,128)}, u32[]{:S(2)}) copy-start(f32[256,256]{1,0:T(8,128)} %mean_o.1) | copy-start | bytes 786436
  85.6 83.7 %copy-start.6 = (f32[256,256]{1,0:T(8,128)S(1)}, f32[256,256]{1,0:T(8,128)}, u32[]{:S(2)}) copy-start(f32[256,256]{1,0:T(8,128)} %square_o.1) | copy-start | bytes 786436
  85.6 83.7 %copy-start.8 = (f32[256,128]{1,0:T(8,128)S(1)}, f32[256,128]{1,0:T(8,128)}, u32[]{:S(2)}) copy-start(f32[256,128]{1,0:T(8,128)} %mean_v.1) | copy-start | bytes 393220
  85.6 83.7 %copy-start.9 = (f32[256,128]{1,0:T(8,128)S(1)}, f32[256,128]{1,0:T(8,128)}, u32[]{:S(2)}) copy-start(f32[256,128]{1,0:T(8,128)} %square_v.1) | copy-start | bytes 393220
  85.6 30.0 %all-to-all-start.3 = ((bf16[8,32,384]{2,1,0:T(8,128)(2,1)}), bf16[8,32,384]{2,1,0:T(8,128)(2,1)S(1)}, u32[]{:S(2)}, u32[]{:S(2)}) async-start(bf16[8,32,384]{2,1,0:T(8,128)(2,1)} %contract.1), calls=%async_computation.3 | async-start | bytes 393216 | tf_op jit(solution)/shard_map/all_to_all | solution.py:31
  92.3 27.3 %collective-permute-start.9 = (bf16[1,160,128]{2,1,0:T(8,128)(2,1)S(1)}, bf16[1,160,128]{2,1,0:T(8,128)(2,1)S(1)}, u32[]{:S(2)}, u32[]{:S(2)}) collective-permute-start(bf16[1,160,128]{2,1,0:T(8,128)(2,1)S(1)} %bitcast.4), channel_id=1, source_target_pairs={{0,384},{32,416},{64,448},{96,480},{128,0},{160,32},{192,64},{224,... | collective-permute-start | bytes 122888 | tf_op jit(solution)/shard_map/ppermute | solution.py:50
  103.3 16.3 %collective-permute-start.8 = (bf16[1,160,128]{2,1,0:T(8,128)(2,1)S(1)}, bf16[1,160,128]{2,1,0:T(8,128)(2,1)S(1)}, u32[]{:S(2)}, u32[]{:S(2)}) collective-permute-start(bf16[1,160,128]{2,1,0:T(8,128)(2,1)S(1)} %bitcast.5), channel_id=1, source_target_pairs={{0,128},{32,160},{64,192},{96,224},{128,256},{160,288},{192,320},{... | collective-permute-start | bytes 122888 | tf_op jit(solution)/shard_map/ppermute | solution.py:50
  105.3 14.3 %collective-permute-start.7 = (bf16[1,160,128]{2,1,0:T(8,128)(2,1)S(1)}, bf16[1,160,128]{2,1,0:T(8,128)(2,1)S(1)}, u32[]{:S(2)}, u32[]{:S(2)}) collective-permute-start(bf16[1,160,128]{2,1,0:T(8,128)(2,1)S(1)} %bitcast.6), channel_id=1, source_target_pairs={{0,256},{32,288},{64,320},{96,352},{128,384},{160,416},{192,448},{... | collective-permute-start | bytes 122888 | tf_op jit(solution)/shard_map/ppermute | solution.py:50
  116.3 16.0 %all-to-all-start.4 = ((bf16[4,32,384]{2,1,0:T(8,128)(2,1)}), bf16[4,32,384]{2,1,0:T(8,128)(2,1)S(1)}, u32[]{:S(2)}, u32[]{:S(2)}) async-start(bf16[4,32,384]{2,1,0:T(8,128)(2,1)} %shard_map.196), calls=%async_computation.4 | async-start | bytes 196608 | tf_op jit(solution)/shard_map/all_to_all | solution.py:31
  119.6 21.2 %collective-permute-start.12 = (bf16[4,160,128]{2,1,0:T(8,128)(2,1)S(1)}, bf16[4,160,128]{2,1,0:T(8,128)(2,1)S(1)}, u32[]{:S(2)}, u32[]{:S(2)}) collective-permute-start(bf16[4,160,128]{2,1,0:T(8,128)(2,1)S(1)} %pad_maximum_fusion.1), channel_id=1, source_target_pairs={{0,480},{32,0},{64,32},{96,64},{128,96},{160,128},{192,160},{224,1... | collective-permute-start | bytes 491528 | tf_op jit(solution)/shard_map/ppermute | solution.py:50
  127.1 13.7 %collective-permute-start.11 = (bf16[4,160,128]{2,1,0:T(8,128)(2,1)S(1)}, bf16[4,160,128]{2,1,0:T(8,128)(2,1)S(1)}, u32[]{:S(2)}, u32[]{:S(2)}) collective-permute-start(bf16[4,160,128]{2,1,0:T(8,128)(2,1)S(1)} %pad_maximum_fusion.1), channel_id=1, source_target_pairs={{0,64},{32,96},{64,128},{96,160},{128,192},{160,224},{192,256},{22... | collective-permute-start | bytes 491528 | tf_op jit(solution)/shard_map/ppermute | solution.py:50
  129.1 11.8 %collective-permute-start.10 = (bf16[4,160,128]{2,1,0:T(8,128)(2,1)S(1)}, bf16[4,160,128]{2,1,0:T(8,128)(2,1)S(1)}, u32[]{:S(2)}, u32[]{:S(2)}) collective-permute-start(bf16[4,160,128]{2,1,0:T(8,128)(2,1)S(1)} %pad_maximum_fusion.1), channel_id=1, source_target_pairs={{0,32},{32,64},{64,96},{96,128},{128,160},{160,192},{192,224},{224... | collective-permute-start | bytes 491528 | tf_op jit(solution)/shard_map/ppermute | solution.py:50
  133.0 36.2 %all-to-all-start.5 = ((bf16[8,32,384]{2,1,0:T(8,128)(2,1)}), bf16[8,32,384]{2,1,0:T(8,128)(2,1)S(1)}, u32[]{:S(2)}, u32[]{:S(2)}) async-start(bf16[8,32,384]{2,1,0:T(8,128)(2,1)} %shard_map.197), calls=%async_computation.5 | async-start | bytes 393216 | tf_op jit(solution)/shard_map/all_to_all | solution.py:31
  141.0 31.7 %copy-start.11 = (bf16[16,160,128]{2,1,0:T(8,128)(2,1)}, bf16[16,160,128]{2,1,0:T(8,128)(2,1)S(1)}, u32[]{:S(2)}) copy-start(bf16[16,160,128]{2,1,0:T(8,128)(2,1)S(1)} %pad_maximum_fusion.own_ref) | copy-start | bytes 1966084
  141.0 36.7 %collective-permute-start.13 = (bf16[16,160,128]{2,1,0:T(8,128)(2,1)S(1)}, bf16[16,160,128]{2,1,0:T(8,128)(2,1)S(1)}, u32[]{:S(2)}, u32[]{:S(2)}) collective-permute-start(bf16[16,160,128]{2,1,0:T(8,128)(2,1)S(1)} %pad_maximum_fusion.own_ref), channel_id=1, source_target_pairs={{0,16},{16,0},{1,17},{17,1},{2,18},{18,2},{3,19},{19,3},{4,20},{20... | collective-permute-start | bytes 1966088 | tf_op jit(solution)/shard_map/ppermute | solution.py:50
  144.6 22.4 %collective-permute-start.4 = (bf16[8,96,256]{2,1,0:T(8,128)(2,1)}, bf16[8,96,256]{2,1,0:T(8,128)(2,1)S(1)}, u32[]{:S(2)}, u32[]{:S(2)}) collective-permute-start(bf16[8,96,256]{2,1,0:T(8,128)(2,1)} %all-to-all-done.blocks_ref.b0), channel_id=1, source_target_pairs={{0,4},{4,8},{8,12},{12,0},{1,5},{5,9},{9,13},{13,1},{2,6},{6,10},{... | collective-permute-start | bytes 1179656 | tf_op jit(solution)/shard_map/ppermute | solution.py:50
  146.8 20.2 %collective-permute-start.5 = (bf16[8,96,256]{2,1,0:T(8,128)(2,1)}, bf16[8,96,256]{2,1,0:T(8,128)(2,1)S(1)}, u32[]{:S(2)}, u32[]{:S(2)}) collective-permute-start(bf16[8,96,256]{2,1,0:T(8,128)(2,1)} %all-to-all-done.blocks_ref.b0), channel_id=1, source_target_pairs={{0,8},{4,12},{8,0},{12,4},{1,9},{5,13},{9,1},{13,5},{2,10},{6,14},... | collective-permute-start | bytes 1179656 | tf_op jit(solution)/shard_map/ppermute | solution.py:50
  149.8 19.4 %collective-permute-start.6 = (bf16[8,96,256]{2,1,0:T(8,128)(2,1)}, bf16[8,96,256]{2,1,0:T(8,128)(2,1)S(1)}, u32[]{:S(2)}, u32[]{:S(2)}) collective-permute-start(bf16[8,96,256]{2,1,0:T(8,128)(2,1)} %all-to-all-done.blocks_ref.b0), channel_id=1, source_target_pairs={{0,12},{4,0},{8,4},{12,8},{1,13},{5,1},{9,5},{13,9},{2,14},{6,2},{... | collective-permute-start | bytes 1179656 | tf_op jit(solution)/shard_map/ppermute | solution.py:50
  167.0 4.9 %copy-start.1 = (bf16[8,96,256]{2,1,0:T(8,128)(2,1)}, bf16[8,96,256]{2,1,0:T(8,128)(2,1)S(1)}, u32[]{:S(2)}) copy-start(bf16[8,96,256]{2,1,0:T(8,128)(2,1)S(1)} %collective-permute-done.5.b2) | copy-start | bytes 1179652
  169.2 3.5 %copy-start.2 = (bf16[8,96,256]{2,1,0:T(8,128)(2,1)}, bf16[8,96,256]{2,1,0:T(8,128)(2,1)S(1)}, u32[]{:S(2)}) copy-start(bf16[8,96,256]{2,1,0:T(8,128)(2,1)S(1)} %collective-permute-done.6.b3) | copy-start | bytes 1179652
  171.9 0.8 copy-start
  172.7 11.6 %all-to-all-start.6 = ((f32[16,8,128]{2,1,0:T(8,128)}), f32[16,8,128]{2,1,0:T(8,128)}, u32[]{:S(2)}, u32[]{:S(2)}) async-start(f32[16,8,128]{2,1,0:T(8,128)} %get-tuple-element.35), calls=%async_computation.6 | async-start | bytes 131072 | tf_op jit(solution)/shard_map/all_to_all | solution.py:31
  177.7 0.8 copy-start.12

commit v8 on v6

--- a/solution.py
+++ b/solution.py
@@ -54,40 +54,35 @@
     return jnp.dot(a, b, preferred_element_type=F32)
 
 
-def pack_kernel( attn_ref, lat_ref, *refs):
-    outs, (attn_here, lat_here, turned, sems) = refs[:-4], refs[-4:]
-    groups = len(outs)
-    each = attn_ref.shape[0] // groups**2
+def pack_kernel(attn_ref, lat_ref, out_ref, attn_here, lat_here, turned, sems):
     copies = [
         pltpu.make_async_copy(lat_ref, lat_here, sems.at[0]),
         pltpu.make_async_copy(attn_ref, attn_here, sems.at[1]),
     ]
     for copy in copies:
         copy.start()
+    groups = out_ref.shape[0]
+    each = attn_ref.shape[0] // groups
+    half = each // 2
     copies[0].wait()
     turned[...] = lat_here[...].T
     copies[1].wait()
-    for k in range(groups):
-        g = lax.rem(lax.axis_index("x") + k, groups)
-        pieces = []
-        for p in range(groups):
-            at = pl.multiple_of((p * groups + g) * each, each)
-            outs[k][p * each : (p + 1) * each, :] = attn_here[pl.ds(at, each), :]
-            pieces.append(turned[pl.ds(at, each), :])
-        half = groups // 2
-        for p in range(half):
-            at = (groups + p) * each
-            outs[k][at : at + each, :] = jnp.concatenate([pieces[p], pieces[half + p]], axis=1)
+    for g in range(groups):
+        at = g * each
+        out_ref[g, :each, :] = attn_here[at : at + each, :]
+        out_ref[g, each:, :] = jnp.concatenate(
+            [turned[at : at + half, :], turned[at + half : at + each, :]], axis=1
+        )
 
 
 def pack(attn_out, lat_turned, groups):
     tokens, heads = attn_out.shape
-    rows = tokens // groups
+    each = tokens // groups
     hbm = pl.BlockSpec(memory_space=pltpu.HBM)
     return pl.pallas_call(
         pack_kernel,
         in_specs=[hbm, hbm],
-        out_shape=tuple(jax.ShapeDtypeStruct((rows + rows // 2, heads), BF) for _ in range(groups)),
+        out_shape=jax.ShapeDtypeStruct((groups, each + each // 2, heads), BF),
         scratch_shapes=[
             pltpu.VMEM(attn_out.shape, BF),
             pltpu.VMEM(lat_turned.shape, BF),
@@ -95,7 +90,7 @@
             pltpu.SemaphoreType.DMA((2,)),
         ],
         cost_estimate=pl.CostEstimate(flops=10**7, bytes_accessed=10**6, transcendentals=0),
-        compiler_params=pltpu.CompilerParams(vmem_limit_bytes=WHOLE),
+        compiler_params=pltpu.CompilerParams(vmem_limit_bytes=WHOLE - 2**18),
         name="pack",
     )(attn_out, lat_turned)
 
@@ -118,15 +113,14 @@
     )(weight_o, weight_v)
 
 
-def lift_kernel(rows_o, tokens, blocks_ref, *refs):
-    gots, out_ref = refs[:-1], refs[-1]
-    groups = len(gots)
+def lift_kernel(rows_o, got_ref, blocks_ref, out_ref):
+    groups, packed, _ = got_ref.shape
+    each = 2 * packed // 3
+    half = each // 2
     rank = blocks_ref.shape[2]
-    half = tokens // 2
-    first = jnp.zeros((tokens, rank), F32)
+    first = jnp.zeros((each, rank), F32)
     second = jnp.zeros((half, 2 * rank), F32)
-    for k, got_ref in enumerate(gots):
-        g = lax.rem(lax.axis_index("x") + groups - k, groups)
+    for g in range(groups):
         low, high = blocks_ref[g], blocks_ref[groups + g]
         basis_o = jnp.concatenate([low[:rows_o], high[:rows_o]], 0)
         basis_v = jnp.concatenate([low[rows_o:], high[rows_o:]], 0)
@@ -134,25 +128,24 @@
         pair = jnp.concatenate(
             [jnp.concatenate([basis_v, none], 0), jnp.concatenate([none, basis_v], 0)], 1
         )
-        first = first + dot(got_ref[:tokens, :], basis_o)
-        second = second + dot(got_ref[tokens:, :], pair)
-    parts, each = out_ref.shape[:2]
-    for p in range(parts):
-        at = p * each
-        out_ref[p, :, :rank] = first[at : at + each].astype(BF)
-        row, side = at % half, at // half
-        out_ref[p, :, rank:] = second[row : row + each, side * rank : (side + 1) * rank].astype(BF)
-
-
-def lift(blocks, gots, rows_o, tokens, parts):
-    rank = blocks.shape[2]
-    return pl.pallas_call(
-        functools.partial(lift_kernel, rows_o, tokens),
-        out_shape=jax.ShapeDtypeStruct((parts, tokens // parts, 2 * rank), BF),
-        cost_estimate=pl.CostEstimate(flops=2 * 10**8, bytes_accessed=10**6, transcendentals=0),
+        first = first + dot(got_ref[g, :each, :], basis_o)
+        second = second + dot(got_ref[g, each:, :], pair)
+    first, second = first.astype(BF), second.astype(BF)
+    for p in range(out_ref.shape[0]):
+        out_ref[p, :, :rank] = first
+        out_ref[p, :half, rank:] = second[:, :rank]
+        out_ref[p, half:, rank:] = second[:, rank:]
+
+
+def lift(got, blocks, rows_o):
+    groups, packed, _ = got.shape
+    return pl.pallas_call(
+        functools.partial(lift_kernel, rows_o),
+        out_shape=jax.ShapeDtypeStruct((groups, 2 * packed // 3, 2 * blocks.shape[2]), BF),
+        cost_estimate=pl.CostEstimate(flops=2 * 10**8, bytes_accessed=3 * 10**6, transcendentals=0),
         compiler_params=pltpu.CompilerParams(vmem_limit_bytes=ROOM),
         name="lift",
-    )(blocks, *gots)
+    )(got, blocks)
 
 
 def spread_kernel(got_ref, out_ref):
@@ -224,7 +217,7 @@
 
 
 def direction_kernel(
-    rows_o, cols_o, got_ref, mean_o, square_o, mean_v, square_v, b0, b1, b2, b3,
+    rows_o, cols_o, got_ref, mean_o, square_o, mean_v, square_v, blocks_ref,
     mean_o_out, square_o_out, mean_v_out, square_v_out, total_out,
 ):
     near = got_ref.shape[0]
@@ -241,10 +234,10 @@
     upper_o, upper_v = upper[:, :cols_o], upper[:, cols_o:]
     total_o = jnp.zeros((8, cols_o), F32)
     total_v = jnp.zeros((8, upper_v.shape[1]), F32)
-    for ref in (b0, b1, b2, b3):
-        count = ref.shape[0]
-        basis_o = jnp.concatenate([ref[i, :rows_o, :] for i in range(count)], 0)
-        basis_v = jnp.concatenate([ref[i, rows_o:, :] for i in range(count)], 0)
+    for group in range(4):
+        blocks = [blocks_ref[group * 8 + i] for i in range(8)]
+        basis_o = jnp.concatenate([b[:rows_o] for b in blocks], 0)
+        basis_v = jnp.concatenate([b[rows_o:] for b in blocks], 0)
         update = dot(basis_o, upper_o)
         total_o = total_o + jnp.sum((update * update).reshape(-1, 8, cols_o), 0)
         update = dot(basis_v, upper_v)
@@ -257,7 +250,7 @@
         total_out[i] = tile
 
 
-def directions(rows_o, copies, got, mean_o, square_o, mean_v, square_v, segments):
+def directions(rows_o, copies, got, mean_o, square_o, mean_v, square_v, blocks):
     cols_o = mean_o.shape[1]
     shape = jax.ShapeDtypeStruct
     return pl.pallas_call(
@@ -272,11 +265,11 @@
         cost_estimate=pl.CostEstimate(flops=4 * 10**8, bytes_accessed=4 * 10**6, transcendentals=10**5),
         compiler_params=pltpu.CompilerParams(vmem_limit_bytes=ROOM),
         name="directions",
-    )(got, mean_o, square_o, mean_v, square_v, *segments)
+    )(got, mean_o, square_o, mean_v, square_v, blocks)
 
 
 def ready_kernel(
-    rows_o, rows_v, mean_o, square_o, mean_v, square_v, local_o, local_v, own_ref, other_ref, b0, b1, b2, b3,
+    rows_o, rows_v, mean_o, square_o, mean_v, square_v, local_o, local_v, own_ref, other_ref, blocks_ref,
     step_o_out, step_v_out, update_o_out, update_v_out, old_o_out, old_v_out,
 ):
     uppers = []
@@ -290,22 +283,20 @@
         step_out[...] = dot(local[...], upper) + dot(local[...], lower)
         uppers.append(upper)
     upper_o, upper_v = uppers
-    y, c = lax.axis_index("y"), lax.axis_index("c")
+    c = lax.axis_index("c")
     z = 4 * lax.axis_index("zh") + lax.axis_index("zl")
-    for k, ref in enumerate((b0, b1, b2, b3)):
-        origin = lax.rem(y + 4 - k, 4)
-        count = ref.shape[0]
-        basis_o = jnp.concatenate([ref[i, :rows_o, :] for i in range(count)], 0)
-        basis_v = jnp.concatenate([ref[i, rows_o:, :] for i in range(count)], 0)
+    for group in range(4):
+        blocks = [blocks_ref[group * 8 + i] for i in range(8)]
+        basis_o = jnp.concatenate([b[:rows_o] for b in blocks], 0)
+        basis_v = jnp.concatenate([b[rows_o:] for b in blocks], 0)
         update_o = dot(basis_o, upper_o).astype(BF)
         update_v = dot(basis_v, upper_v).astype(BF)
-        for i in range(count):
-            core, x = divmod(i, count // 2)
-            index = 8 * origin + 2 * x + core
-            at = pl.multiple_of(index * rows_o, rows_o)
-            update_o_out[pl.ds(at, rows_o), :] = update_o[i * rows_o : (i + 1) * rows_o]
-            at = pl.multiple_of(index * rows_v, rows_v)
-            update_v_out[pl.ds(at, rows_v), :] = update_v[i * rows_v : (i + 1) * rows_v]
+        for i in range(8):
+            core, j = divmod(group * 8 + i, 16)
+            at = (2 * j + core) * rows_o
+            update_o_out[at : at + rows_o, :] = update_o[i * rows_o : (i + 1) * rows_o]
+            at = (2 * j + core) * rows_v
+            update_v_out[at : at + rows_v, :] = update_v[i * rows_v : (i + 1) * rows_v]
     for ref, core in ((own_ref, c), (other_ref, 1 - c)):
         for p in range(ref.shape[0]):
             behind = (p & 1) * 8 + (p >> 1 & 1) * 4 + STEPS[p >> 2]
@@ -317,7 +308,7 @@
             old_v_out[pl.ds(at, rows_v), :] = ref[p, 2 * rows_o :]
 
 
-def ready(moments, local_o, local_v, own, other, segments):
+def ready(moments, local_o, local_v, own, other, blocks):
     rows_o, rows_v = local_o.shape[0], local_v.shape[0]
     cols_o, cols_v = moments[0].shape[1], moments[2].shape[1]
     fs = 2 * own.shape[0]
@@ -335,7 +326,7 @@
         cost_estimate=pl.CostEstimate(flops=4 * 10**8, bytes_accessed=4 * 10**6, transcendentals=0),
         compiler_params=pltpu.CompilerParams(vmem_limit_bytes=WHOLE),
         name="ready",
-    )(*moments, local_o, local_v, own, other, *segments)
+    )(*moments, local_o, local_v, own, other, blocks)
 
 
 def output_kernel(
@@ -425,14 +416,12 @@
     rows_v = value_basis.shape[0]
     tp = lax.axis_size(TP)
     fs = lax.axis_size(FS)
-    xs, ys = lax.axis_size("x"), lax.axis_size("y")
 
 
     block = swapped_blocks(jnp.concatenate([out_basis, value_basis], 0))
 
-    gots = list(pack(attn_out, latent.T, xs))
-    for k in range(1, xs):
-        gots[k] = shifted(gots[k], "x", k)
+    sent = pack(attn_out, latent.T, tp)
+    got = exchange(sent, TP)
 
     own = old_rows(out_weight, value_up_matrix)[None]
     for k in (8, 4):
@@ -444,10 +433,8 @@
     own = lax.optimization_barrier(jnp.concatenate(rows, 0))
     other = shifted(own, "c", 1)
 
-    blocks = from_everyone(block, ("c", "x"))
-    partial = lift(blocks, gots, rows_o, tokens // xs, ys)
-    partial = exchange(partial, "y")
-    lifted = summed_for(partial, tp, BF)
+    blocks = from_everyone(block, ("c", "y", "x"))
+    lifted = lift(got, blocks, rows_o)
     lifted = exchange(lifted, TP).reshape(tokens, 2 * rank)
 
     near = lax.axis_size(NEAR)
@@ -456,16 +443,12 @@
     part = exchange(summed_for(part, lax.axis_size("zh"), BF), "zh")
     proj = exchange(summed_for(part, near, BF), NEAR)
 
-    segments = [blocks]
-    for k in range(1, ys):
-        segments.append(shifted(blocks, "y", k))
-
     mean_o, square_o, mean_v, square_v, total = directions(
-        rows_o, tp, proj, out_mean, out_square, value_mean, value_square, segments
+        rows_o, tp, proj, out_mean, out_square, value_mean, value_square, blocks
     )
     total = exchange(total, TP)
     moments = (mean_o, square_o, mean_v, square_v)
-    prepared = ready(moments, out_basis, value_basis, own, other, segments)
+    prepared = ready(moments, out_basis, value_basis, own, other, blocks)
     counts = (rows_o * fs * cols_o * tp, rows_v * fs * cols_v * tp)
     step_o, new_o, copy_o, step_v, new_v, copy_v = outputs(
         counts, total, out_weight, value_up_matrix, *prepared

time: 193 us -> 169 us (0.88)
  starting transfers between devices: 96.5 us -> 67.4 us
  blocking collectives: 46.9 us -> 66.2 us
  waiting for transfers between devices: 25.2 us -> 16.1 us
  local copies, waits for them, and re-layouts: 3.35 us -> 0.23 us
  Pallas kernels: 18 us -> 15.8 us
    ppermute x12 -> x6, starting transfers between devices: 55.7 us -> 35.4 us  [shifted(): lax.ppermute(value, axis, [(i, (i + by) % devices) for i in range(devices)])]
    ppermute x12 -> x6, waiting for transfers between devices: 24 us -> 4.08 us  [shifted(): lax.ppermute(value, axis, [(i, (i + by) % devices) for i in range(devices)])]
    all_to_all x2, blocking collectives: 46.9 us -> 66.2 us  [exchange(): return lax.all_to_all(value, axes, 0, 0, tiled=True)]
    all_to_all x5, waiting for transfers between devices: 1.27 us -> 12 us  [exchange(): return lax.all_to_all(value, axes, 0, 0, tiled=True)]
    all_to_all x5, starting transfers between devices: 40.1 us -> 31.3 us  [exchange(): return lax.all_to_all(value, axes, 0, 0, tiled=True)]
    unnamed x28 -> x24, local copies, waits for them, and re-layouts: 2.57 us -> 0.07 us
  transfers between devices with their start and end apart: 18 -> 12, of which waited for: 7 -> 6; matrix products, arithmetic and copies ran while one was open for 0% -> 1% of each run, Pallas kernels for 5% -> 4%
where the time goes in v8:
time: 169 us; the launch traced here: 168 us
  starting transfers between devices  67.4 us (40%)
  blocking collectives  66.2 us (39%)
  waiting for transfers between devices  16.1 us (10%)
  Pallas kernels  15.8 us (9%)
    all_to_all x2, blocking collectives, exchange(): return lax.all_to_all(value, axes, 0, 0, tiled=True)  66.2 us
    ppermute x6, starting transfers between devices, shifted(): lax.ppermute(value, axis, [(i, (i + by) % devices) for i in range(devices)])  35.4 us
    all_to_all x5, starting transfers between devices, exchange(): return lax.all_to_all(value, axes, 0, 0, tiled=True)  31.3 us
    all_to_all x5, waiting for transfers between devices, exchange(): return lax.all_to_all(value, axes, 0, 0, tiled=True)  12 us
    pallas_call x1, Pallas kernels, ready(): pl.pallas_call(functools.partial(ready_kernel, rows_o, rows_v), out_shape...  4.32 us
    ppermute x6, waiting for transfers between devices, shifted(): lax.ppermute(value, axis, [(i, (i + by) % devices) for i in range(devices)])  4.08 us
    pallas_call x1, Pallas kernels, outputs(): pl.pallas_call(functools.partial(output_kernel, counts, pieces), in_specs...  3.82 us
  transfers between devices with their start and end apart: 12, of which 6 were waited for; matrix products, arithmetic and copies ran while one was open for 1% of the time, Pallas kernels for 4%

profile of v8, /device:TPU:1, one launch (start us, length us, event | category | flops | bytes accessed | tf_op | source)
XLA Modules:
  0.0 167.9 jit_solution(6596524115109751970)
XLA Ops:
  0.6 0.0 copy-start.11
  0.7 0.0 copy-start.10
  0.7 2.1 %pack.1 = bf16[16,144,128]{2,1,0:T(8,128)(2,1)} custom-call(bf16[1536,128]{1,0:T(8,128)(2,1)} %attn_ref.1, bf16[64,1536]{1,0:T(8,128)(2,1)} %bitcast.6), custom_call_target="tpu_custom_call" | custom-call | flops 10000000 | bytes 1000000 | tf_op jit(solution)/shard_map/pack/pallas_call | solution.py:82
  2.7 7.6 %all-to-all-start = ((bf16[16,144,128]{2,1,0:T(8,128)(2,1)}), bf16[16,144,128]{2,1,0:T(8,128)(2,1)S(1)}, u32[]{:S(2)}, u32[]{:S(2)}) async-start(bf16[16,144,128]{2,1,0:T(8,128)(2,1)} %pack.1), calls=%async_computation | async-start | bytes 1179648 | tf_op jit(solution)/shard_map/all_to_all | solution.py:31
  10.3 0.0 copy-done.11
  10.3 0.0 copy-done.10
  10.4 0.7 collective-permute-start
  11.0 0.0 collective-permute-done
  11.0 8.9 %all-to-all-done.got_ref = bf16[16,144,128]{2,1,0:T(8,128)(2,1)S(1)} async-done(((bf16[16,144,128]{2,1,0:T(8,128)(2,1)}), bf16[16,144,128]{2,1,0:T(8,128)(2,1)S(1)}, u32[]{:S(2)}, u32[]{:S(2)}) %all-to-all-start) | async-done | bytes 589856 | tf_op jit(solution)/shard_map/all_to_all | solution.py:31
  20.0 0.2 broadcast_in_dim.4
  20.1 40.8 %all_to_all.35.blocks_ref = bf16[32,96,256]{2,1,0:T(8,128)(2,1)S(1)} all-to-all(bf16[32,96,256]{2,1,0:T(8,128)(2,1)S(1)} %broadcast_in_dim.4), channel_id=1, replica_groups=mesh['zh'=4,'zl'=4,'c'=2,'y'=4,'x'=4] {'c','y','x'}, dimensions={0} | all-to-all | bytes 3145728 | tf_op jit(solution)/shard_map/all_to_all | solution.py:31
  60.9 0.7 lift.1
  61.6 0.0 copy-start.1
  61.6 0.0 copy-start.2
  61.7 25.5 %all_to_all.36 = bf16[16,96,512]{2,1,0:T(8,128)(2,1)S(1)} all-to-all(bf16[16,96,512]{2,1,0:T(8,128)(2,1)S(1)} %lift.1), channel_id=1, replica_groups=mesh['zh'=4,'zl'=4,'c'=2,'y'=4,'x'=4] {'y','x'}, dimensions={0} | all-to-all | bytes 3145728 | tf_op jit(solution)/shard_map/all_to_all | solution.py:31
  87.1 2.0 %contract.1 = bf16[8,32,384]{2,1,0:T(8,128)(2,1)} custom-call(bf16[1536,512]{1,0:T(8,128)(2,1)S(1)} %bitcast.3, bf16[1536,256]{1,0:T(8,128)(2,1)S(1)} %copy-done.1, bf16[1536,128]{1,0:T(8,128)(2,1)S(1)} %copy-done.2), custom_call_target="tpu_custom_call" | custom-call | flops 300000000 | bytes 3000000 | tf_op jit(solution)/shard_map/contract/pallas_call | solution.py:202
  89.2 5.0 %all-to-all-start.3 = ((bf16[8,32,384]{2,1,0:T(8,128)(2,1)}), bf16[8,32,384]{2,1,0:T(8,128)(2,1)S(1)}, u32[]{:S(2)}, u32[]{:S(2)}) async-start(bf16[8,32,384]{2,1,0:T(8,128)(2,1)} %contract.1), calls=%async_computation.3 | async-start | bytes 393216 | tf_op jit(solution)/shard_map/all_to_all | solution.py:31
  94.1 0.0 copy-start.3
  94.2 0.0 copy-start.4
  94.2 0.0 copy-start.6
  94.2 0.0 copy-start.7
  94.2 11.6 %collective-permute-start.1 = (bf16[1,160,128]{2,1,0:T(8,128)(2,1)S(1)}, bf16[1,160,128]{2,1,0:T(8,128)(2,1)S(1)}, u32[]{:S(2)}, u32[]{:S(2)}) collective-permute-start(bf16[1,160,128]{2,1,0:T(8,128)(2,1)S(1)} %bitcast.4), channel_id=1, source_target_pairs={{0,256},{32,288},{64,320},{96,352},{128,384},{160,416},{192,448},{... | collective-permute-start | bytes 122888 | tf_op jit(solution)/shard_map/ppermute | solution.py:50
  105.8 3.2 %collective-permute-done.1 = bf16[1,160,128]{2,1,0:T(8,128)(2,1)S(1)} collective-permute-done((bf16[1,160,128]{2,1,0:T(8,128)(2,1)S(1)}, bf16[1,160,128]{2,1,0:T(8,128)(2,1)S(1)}, u32[]{:S(2)}, u32[]{:S(2)}) %collective-permute-start.1) | collective-permute-done | bytes 40992 | tf_op jit(solution)/shard_map/ppermute | solution.py:50
  109.0 8.2 %collective-permute-start.2 = (bf16[2,160,128]{2,1,0:T(8,128)(2,1)S(1)}, bf16[2,160,128]{2,1,0:T(8,128)(2,1)S(1)}, u32[]{:S(2)}, u32[]{:S(2)}) collective-permute-start(bf16[2,160,128]{2,1,0:T(8,128)(2,1)S(1)} %pad_maximum_fusion.2), channel_id=1, source_target_pairs={{0,128},{32,160},{64,192},{96,224},{128,256},{160,288},{192,320},{... | collective-permute-start | bytes 245768 | tf_op jit(solution)/shard_map/ppermute | solution.py:50
  117.2 0.0 all-to-all-done.3.got_ref
  117.2 0.7 shard_map.195
  117.9 6.3 %all-to-all-start.4 = ((bf16[4,32,384]{2,1,0:T(8,128)(2,1)}), bf16[4,32,384]{2,1,0:T(8,128)(2,1)S(1)}, u32[]{:S(2)}, u32[]{:S(2)}) async-start(bf16[4,32,384]{2,1,0:T(8,128)(2,1)} %shard_map.195), calls=%async_computation.4 | async-start | bytes 196608 | tf_op jit(solution)/shard_map/all_to_all | solution.py:31
  124.1 0.0 collective-permute-done.2
  124.2 7.9 %collective-permute-start.5 = (bf16[4,160,128]{2,1,0:T(8,128)(2,1)S(1)}, bf16[4,160,128]{2,1,0:T(8,128)(2,1)}, u32[]{:S(2)}, u32[]{:S(2)}) collective-permute-start(bf16[4,160,128]{2,1,0:T(8,128)(2,1)S(1)} %pad_maximum_fusion.1), channel_id=1, source_target_pairs={{0,480},{32,0},{64,32},{96,64},{128,96},{160,128},{192,160},{224,1... | collective-permute-start | bytes 491528 | tf_op jit(solution)/shard_map/ppermute | solution.py:50
  132.1 1.9 %collective-permute-start.4 = (bf16[4,160,128]{2,1,0:T(8,128)(2,1)S(1)}, bf16[4,160,128]{2,1,0:T(8,128)(2,1)}, u32[]{:S(2)}, u32[]{:S(2)}) collective-permute-start(bf16[4,160,128]{2,1,0:T(8,128)(2,1)S(1)} %pad_maximum_fusion.1), channel_id=1, source_target_pairs={{0,64},{32,96},{64,128},{96,160},{128,192},{160,224},{192,256},{22... | collective-permute-start | bytes 491528 | tf_op jit(solution)/shard_map/ppermute | solution.py:50
  134.0 1.9 %collective-permute-start.3 = (bf16[4,160,128]{2,1,0:T(8,128)(2,1)S(1)}, bf16[4,160,128]{2,1,0:T(8,128)(2,1)}, u32[]{:S(2)}, u32[]{:S(2)}) collective-permute-start(bf16[4,160,128]{2,1,0:T(8,128)(2,1)S(1)} %pad_maximum_fusion.1), channel_id=1, source_target_pairs={{0,32},{32,64},{64,96},{96,128},{128,160},{160,192},{192,224},{224... | collective-permute-start | bytes 491528 | tf_op jit(solution)/shard_map/ppermute | solution.py:50
  136.0 0.4 all-to-all-done.4.got_ref
  136.3 0.7 shard_map.196
  137.0 8.3 %all-to-all-start.5 = ((bf16[8,32,384]{2,1,0:T(8,128)(2,1)}), bf16[8,32,384]{2,1,0:T(8,128)(2,1)S(1)}, u32[]{:S(2)}, u32[]{:S(2)}) async-start(bf16[8,32,384]{2,1,0:T(8,128)(2,1)} %shard_map.196), calls=%async_computation.5 | async-start | bytes 393216 | tf_op jit(solution)/shard_map/all_to_all | solution.py:31
  145.4 0.0 collective-permute-done.5
  145.4 0.0 collective-permute-done.4
  145.4 0.9 collective-permute-done.3
  146.3 1.2 pad_maximum_fusion.own_ref
  147.4 0.0 copy-start.9
  147.4 3.9 %collective-permute-start.6 = (bf16[16,160,128]{2,1,0:T(8,128)(2,1)S(1)}, bf16[16,160,128]{2,1,0:T(8,128)(2,1)}, u32[]{:S(2)}, u32[]{:S(2)}) collective-permute-start(bf16[16,160,128]{2,1,0:T(8,128)(2,1)S(1)} %pad_maximum_fusion.own_ref), channel_id=1, source_target_pairs={{0,16},{16,0},{1,17},{17,1},{2,18},{18,2},{3,19},{19,3},{4,20},{20... | collective-permute-start | bytes 1966088 | tf_op jit(solution)/shard_map/ppermute | solution.py:50
  151.3 0.5 all-to-all-done.5.got_ref
  151.9 0.0 copy-done.3
  151.9 1.5 directions.1
  153.5 4.2 %all-to-all-start.6 = ((f32[16,8,128]{2,1,0:T(8,128)}), f32[16,8,128]{2,1,0:T(8,128)}, u32[]{:S(2)}, u32[]{:S(2)}) async-start(f32[16,8,128]{2,1,0:T(8,128)} %get-tuple-element.27), calls=%async_computation.6 | async-start | bytes 131072 | tf_op jit(solution)/shard_map/all_to_all | solution.py:31
  157.6 0.0 collective-permute-done.6.other_ref
  157.6 4.3 %ready.1 = (f32[64,256]{1,0:T(8,128)}, f32[32,128]{1,0:T(8,128)}, bf16[2048,256]{1,0:T(8,128)(2,1)}, bf16[1024,128]{1,0:T(8,128)(2,1)}, bf16[2048,256]{1,0:T(8,128)(2,1)}, /*index=5*/bf16[1024,128]{1,0:T(8,128)(2,1)}) custom-call(f32[256,256]{1,0:T(8,128)} %get-tuple-element.20.mean_o, f32[256,256]{1,0:T(8,128)} %get-tuple-element.21.square_o, ...), custom_call_target="tpu_custom_call" | custom-call | flops 400000000 | bytes 4000000 | tf_op jit(solution)/shard_map/ready/pallas_call | solution.py:316
  161.9 2.2 %all-to-all-done.6.total_ref = f32[16,8,128]{2,1,0:T(8,128)} async-done(((f32[16,8,128]{2,1,0:T(8,128)}), f32[16,8,128]{2,1,0:T(8,128)}, u32[]{:S(2)}, u32[]{:S(2)}) %all-to-all-start.6) | async-done | bytes 65568 | tf_op jit(solution)/shard_map/all_to_all | solution.py:31
  164.1 3.8 %outputs.1 = (f32[64,256]{1,0:T(8,128)}, f32[64,256]{1,0:T(8,128)}, bf16[2048,256]{1,0:T(8,128)(2,1)}, f32[32,128]{1,0:T(8,128)}, f32[32,128]{1,0:T(8,128)}, /*index=5*/bf16[1024,128]{1,0:T(8,128)(2,1)}) custom-call(f32[16,8,128]{2,1,0:T(8,128)} %all-to-all-done.6.total_ref, f32[64,256]{1,0:T(8,128)} %weight_o.3, f32[32,128]{1,0:T(8,128)} %weight_v.3, ...), custom_call_target="tpu_custom_call" | custom-call | flops 10000000 | bytes 4000000 | tf_op jit(solution)/shard_map/outputs/pallas_call | solution.py:379
  (16 shorter events, 0.1 us)
Async XLA Ops:
  0.6 9.7 %copy-start.11 = (bf16[32,256]{1,0:T(8,128)(2,1)S(1)}, bf16[32,256]{1,0:T(8,128)(2,1)}, u32[]{:S(2)}) copy-start(bf16[32,256]{1,0:T(8,128)(2,1)} %local_v.1) | copy-start | bytes 49156
  0.7 9.7 %copy-start.10 = (bf16[64,256]{1,0:T(8,128)(2,1)S(1)}, bf16[64,256]{1,0:T(8,128)(2,1)}, u32[]{:S(2)}) copy-start(bf16[64,256]{1,0:T(8,128)(2,1)} %local_o.1) | copy-start | bytes 98308
  2.7 17.2 %all-to-all-start = ((bf16[16,144,128]{2,1,0:T(8,128)(2,1)}), bf16[16,144,128]{2,1,0:T(8,128)(2,1)S(1)}, u32[]{:S(2)}, u32[]{:S(2)}) async-start(bf16[16,144,128]{2,1,0:T(8,128)(2,1)} %pack.1), calls=%async_computation | async-start | bytes 1179648 | tf_op jit(solution)/shard_map/all_to_all | solution.py:31
  10.4 0.7 collective-permute-start
  60.9 91.0 %copy-start = (bf16[32,96,256]{2,1,0:T(8,128)(2,1)}, bf16[32,96,256]{2,1,0:T(8,128)(2,1)S(1)}, u32[]{:S(2)}) copy-start(bf16[32,96,256]{2,1,0:T(8,128)(2,1)S(1)} %all_to_all.35.blocks_ref) | copy-start | bytes 4718596
  61.6 25.5 %copy-start.1 = (bf16[1536,256]{1,0:T(8,128)(2,1)S(1)}, bf16[1536,256]{1,0:T(8,128)(2,1)}, u32[]{:S(2)}) copy-start(bf16[1536,256]{1,0:T(8,128)(2,1)} %cot_o.1) | copy-start | bytes 2359300
  61.6 25.5 %copy-start.2 = (bf16[1536,128]{1,0:T(8,128)(2,1)S(1)}, bf16[1536,128]{1,0:T(8,128)(2,1)}, u32[]{:S(2)}) copy-start(bf16[1536,128]{1,0:T(8,128)(2,1)} %cot_v.1) | copy-start | bytes 1179652
  87.1 7.0 %copy-start.5 = (f32[64,256]{1,0:T(8,128)S(1)}, f32[64,256]{1,0:T(8,128)}, u32[]{:S(2)}) copy-start(f32[64,256]{1,0:T(8,128)} %weight_o.3) | copy-start | bytes 196612
  87.1 7.0 %copy-start.8 = (f32[32,128]{1,0:T(8,128)S(1)}, f32[32,128]{1,0:T(8,128)}, u32[]{:S(2)}) copy-start(f32[32,128]{1,0:T(8,128)} %weight_v.3) | copy-start | bytes 49156
  89.2 28.0 %all-to-all-start.3 = ((bf16[8,32,384]{2,1,0:T(8,128)(2,1)}), bf16[8,32,384]{2,1,0:T(8,128)(2,1)S(1)}, u32[]{:S(2)}, u32[]{:S(2)}) async-start(bf16[8,32,384]{2,1,0:T(8,128)(2,1)} %contract.1), calls=%async_computation.3 | async-start | bytes 393216 | tf_op jit(solution)/shard_map/all_to_all | solution.py:31
  94.1 57.8 %copy-start.3 = (f32[256,256]{1,0:T(8,128)S(1)}, f32[256,256]{1,0:T(8,128)}, u32[]{:S(2)}) copy-start(f32[256,256]{1,0:T(8,128)} %mean_o.1) | copy-start | bytes 786436
  94.2 57.7 %copy-start.4 = (f32[256,256]{1,0:T(8,128)S(1)}, f32[256,256]{1,0:T(8,128)}, u32[]{:S(2)}) copy-start(f32[256,256]{1,0:T(8,128)} %square_o.1) | copy-start | bytes 786436
  94.2 57.7 %copy-start.6 = (f32[256,128]{1,0:T(8,128)S(1)}, f32[256,128]{1,0:T(8,128)}, u32[]{:S(2)}) copy-start(f32[256,128]{1,0:T(8,128)} %mean_v.1) | copy-start | bytes 393220
  94.2 57.7 %copy-start.7 = (f32[256,128]{1,0:T(8,128)S(1)}, f32[256,128]{1,0:T(8,128)}, u32[]{:S(2)}) copy-start(f32[256,128]{1,0:T(8,128)} %square_v.1) | copy-start | bytes 393220
  94.2 14.7 %collective-permute-start.1 = (bf16[1,160,128]{2,1,0:T(8,128)(2,1)S(1)}, bf16[1,160,128]{2,1,0:T(8,128)(2,1)S(1)}, u32[]{:S(2)}, u32[]{:S(2)}) collective-permute-start(bf16[1,160,128]{2,1,0:T(8,128)(2,1)S(1)} %bitcast.4), channel_id=1, source_target_pairs={{0,256},{32,288},{64,320},{96,352},{128,384},{160,416},{192,448},{... | collective-permute-start | bytes 122888 | tf_op jit(solution)/shard_map/ppermute | solution.py:50
  109.0 15.2 %collective-permute-start.2 = (bf16[2,160,128]{2,1,0:T(8,128)(2,1)S(1)}, bf16[2,160,128]{2,1,0:T(8,128)(2,1)S(1)}, u32[]{:S(2)}, u32[]{:S(2)}) collective-permute-start(bf16[2,160,128]{2,1,0:T(8,128)(2,1)S(1)} %pad_maximum_fusion.2), channel_id=1, source_target_pairs={{0,128},{32,160},{64,192},{96,224},{128,256},{160,288},{192,320},{... | collective-permute-start | bytes 245768 | tf_op jit(solution)/shard_map/ppermute | solution.py:50
  117.9 18.5 %all-to-all-start.4 = ((bf16[4,32,384]{2,1,0:T(8,128)(2,1)}), bf16[4,32,384]{2,1,0:T(8,128)(2,1)S(1)}, u32[]{:S(2)}, u32[]{:S(2)}) async-start(bf16[4,32,384]{2,1,0:T(8,128)(2,1)} %shard_map.195), calls=%async_computation.4 | async-start | bytes 196608 | tf_op jit(solution)/shard_map/all_to_all | solution.py:31
  124.2 21.2 %collective-permute-start.5 = (bf16[4,160,128]{2,1,0:T(8,128)(2,1)S(1)}, bf16[4,160,128]{2,1,0:T(8,128)(2,1)}, u32[]{:S(2)}, u32[]{:S(2)}) collective-permute-start(bf16[4,160,128]{2,1,0:T(8,128)(2,1)S(1)} %pad_maximum_fusion.1), channel_id=1, source_target_pairs={{0,480},{32,0},{64,32},{96,64},{128,96},{160,128},{192,160},{224,1... | collective-permute-start | bytes 491528 | tf_op jit(solution)/shard_map/ppermute | solution.py:50
  132.1 13.3 %collective-permute-start.4 = (bf16[4,160,128]{2,1,0:T(8,128)(2,1)S(1)}, bf16[4,160,128]{2,1,0:T(8,128)(2,1)}, u32[]{:S(2)}, u32[]{:S(2)}) collective-permute-start(bf16[4,160,128]{2,1,0:T(8,128)(2,1)S(1)} %pad_maximum_fusion.1), channel_id=1, source_target_pairs={{0,64},{32,96},{64,128},{96,160},{128,192},{160,224},{192,256},{22... | collective-permute-start | bytes 491528 | tf_op jit(solution)/shard_map/ppermute | solution.py:50
  134.0 12.2 %collective-permute-start.3 = (bf16[4,160,128]{2,1,0:T(8,128)(2,1)S(1)}, bf16[4,160,128]{2,1,0:T(8,128)(2,1)}, u32[]{:S(2)}, u32[]{:S(2)}) collective-permute-start(bf16[4,160,128]{2,1,0:T(8,128)(2,1)S(1)} %pad_maximum_fusion.1), channel_id=1, source_target_pairs={{0,32},{32,64},{64,96},{96,128},{128,160},{160,192},{192,224},{224... | collective-permute-start | bytes 491528 | tf_op jit(solution)/shard_map/ppermute | solution.py:50
  137.0 14.9 %all-to-all-start.5 = ((bf16[8,32,384]{2,1,0:T(8,128)(2,1)}), bf16[8,32,384]{2,1,0:T(8,128)(2,1)S(1)}, u32[]{:S(2)}, u32[]{:S(2)}) async-start(bf16[8,32,384]{2,1,0:T(8,128)(2,1)} %shard_map.196), calls=%async_computation.5 | async-start | bytes 393216 | tf_op jit(solution)/shard_map/all_to_all | solution.py:31
  147.4 6.0 %copy-start.9 = (bf16[16,160,128]{2,1,0:T(8,128)(2,1)}, bf16[16,160,128]{2,1,0:T(8,128)(2,1)S(1)}, u32[]{:S(2)}) copy-start(bf16[16,160,128]{2,1,0:T(8,128)(2,1)S(1)} %pad_maximum_fusion.own_ref) | copy-start | bytes 1966084
  147.4 10.2 %collective-permute-start.6 = (bf16[16,160,128]{2,1,0:T(8,128)(2,1)S(1)}, bf16[16,160,128]{2,1,0:T(8,128)(2,1)}, u32[]{:S(2)}, u32[]{:S(2)}) collective-permute-start(bf16[16,160,128]{2,1,0:T(8,128)(2,1)S(1)} %pad_maximum_fusion.own_ref), channel_id=1, source_target_pairs={{0,16},{16,0},{1,17},{17,1},{2,18},{18,2},{3,19},{19,3},{4,20},{20... | collective-permute-start | bytes 1966088 | tf_op jit(solution)/shard_map/ppermute | solution.py:50
  153.5 10.7 %all-to-all-start.6 = ((f32[16,8,128]{2,1,0:T(8,128)}), f32[16,8,128]{2,1,0:T(8,128)}, u32[]{:S(2)}, u32[]{:S(2)}) async-start(f32[16,8,128]{2,1,0:T(8,128)} %get-tuple-element.27), calls=%async_computation.6 | async-start | bytes 131072 | tf_op jit(solution)/shard_map/all_to_all | solution.py:31

commit v9 on v6

--- a/solution.py
+++ b/solution.py
@@ -54,9 +54,8 @@
     return jnp.dot(a, b, preferred_element_type=F32)
 
 
-def pack_kernel( attn_ref, lat_ref, *refs):
+def pack_kernel(groups, first, attn_ref, lat_ref, *refs):
     outs, (attn_here, lat_here, turned, sems) = refs[:-4], refs[-4:]
-    groups = len(outs)
     each = attn_ref.shape[0] // groups**2
     copies = [
         pltpu.make_async_copy(lat_ref, lat_here, sems.at[0]),
@@ -67,27 +66,27 @@
     copies[0].wait()
     turned[...] = lat_here[...].T
     copies[1].wait()
-    for k in range(groups):
-        g = lax.rem(lax.axis_index("x") + k, groups)
+    for k, out in enumerate(outs):
+        g = lax.rem(lax.axis_index("x") + first + k, groups)
         pieces = []
         for p in range(groups):
             at = pl.multiple_of((p * groups + g) * each, each)
-            outs[k][p * each : (p + 1) * each, :] = attn_here[pl.ds(at, each), :]
+            out[p * each : (p + 1) * each, :] = attn_here[pl.ds(at, each), :]
             pieces.append(turned[pl.ds(at, each), :])
         half = groups // 2
         for p in range(half):
             at = (groups + p) * each
-            outs[k][at : at + each, :] = jnp.concatenate([pieces[p], pieces[half + p]], axis=1)
-
-
-def pack(attn_out, lat_turned, groups):
+            out[at : at + each, :] = jnp.concatenate([pieces[p], pieces[half + p]], axis=1)
+
+
+def pack(attn_out, lat_turned, groups, first, count, limit):
     tokens, heads = attn_out.shape
     rows = tokens // groups
     hbm = pl.BlockSpec(memory_space=pltpu.HBM)
     return pl.pallas_call(
-        pack_kernel,
+        functools.partial(pack_kernel, groups, first),
         in_specs=[hbm, hbm],
-        out_shape=tuple(jax.ShapeDtypeStruct((rows + rows // 2, heads), BF) for _ in range(groups)),
+        out_shape=tuple(jax.ShapeDtypeStruct((rows + rows // 2, heads), BF) for _ in range(count)),
         scratch_shapes=[
             pltpu.VMEM(attn_out.shape, BF),
             pltpu.VMEM(lat_turned.shape, BF),
@@ -95,8 +94,7 @@
             pltpu.SemaphoreType.DMA((2,)),
         ],
         cost_estimate=pl.CostEstimate(flops=10**7, bytes_accessed=10**6, transcendentals=0),
-        compiler_params=pltpu.CompilerParams(vmem_limit_bytes=WHOLE),
-        name="pack",
+        compiler_params=pltpu.CompilerParams(vmem_limit_bytes=limit),
     )(attn_out, lat_turned)
 
 
@@ -276,7 +274,7 @@
 
 
 def ready_kernel(
-    rows_o, rows_v, mean_o, square_o, mean_v, square_v, local_o, local_v, own_ref, other_ref, b0, b1, b2, b3,
+    rows_o, rows_v, mean_o, square_o, mean_v, square_v, local_o, local_v, h0, h1, h2, h3, b0, b1, b2, b3,
     step_o_out, step_v_out, update_o_out, update_v_out, old_o_out, old_v_out,
 ):
     uppers = []
@@ -306,10 +304,11 @@
             update_o_out[pl.ds(at, rows_o), :] = update_o[i * rows_o : (i + 1) * rows_o]
             at = pl.multiple_of(index * rows_v, rows_v)
             update_v_out[pl.ds(at, rows_v), :] = update_v[i * rows_v : (i + 1) * rows_v]
-    for ref, core in ((own_ref, c), (other_ref, 1 - c)):
-        for p in range(ref.shape[0]):
-            behind = (p & 1) * 8 + (p >> 1 & 1) * 4 + STEPS[p >> 2]
-            index = 2 * lax.rem(z + 16 - behind, 16) + core
+    for ref, step in zip((h0, h1, h2, h3), STEPS):
+        for p in range(8):
+            behind = (0, 8, 4, 12)[p & 3] + step
+            core = c if p < 4 else 1 - c
+            index = 2 * lax.rem(z + 32 - behind, 16) + core
             at = pl.multiple_of(index * rows_o, rows_o)
             old_o_out[pl.ds(at, rows_o), :128] = ref[p, :rows_o]
             old_o_out[pl.ds(at, rows_o), 128:] = ref[p, rows_o : 2 * rows_o]
@@ -317,10 +316,10 @@
             old_v_out[pl.ds(at, rows_v), :] = ref[p, 2 * rows_o :]
 
 
-def ready(moments, local_o, local_v, own, other, segments):
+def ready(moments, local_o, local_v, held, segments):
     rows_o, rows_v = local_o.shape[0], local_v.shape[0]
     cols_o, cols_v = moments[0].shape[1], moments[2].shape[1]
-    fs = 2 * own.shape[0]
+    fs = 4 * held[0].shape[0]
     shape = jax.ShapeDtypeStruct
     return pl.pallas_call(
         functools.partial(ready_kernel, rows_o, rows_v),
@@ -335,7 +334,7 @@
         cost_estimate=pl.CostEstimate(flops=4 * 10**8, bytes_accessed=4 * 10**6, transcendentals=0),
         compiler_params=pltpu.CompilerParams(vmem_limit_bytes=WHOLE),
         name="ready",
-    )(*moments, local_o, local_v, own, other, *segments)
+    )(*moments, local_o, local_v, *held, *segments)
 
 
 def output_kernel(
@@ -430,7 +429,8 @@
 
     block = swapped_blocks(jnp.concatenate([out_basis, value_basis], 0))
 
-    gots = list(pack(attn_out, latent.T, xs))
+    gots = [None, *pack(attn_out, latent.T, xs, 1, xs - 1, WHOLE - 380000)]
+    gots[:1] = pack(attn_out, latent.T, xs, 0, 1, ROOM)
     for k in range(1, xs):
         gots[k] = shifted(gots[k], "x", k)
 
@@ -438,11 +438,11 @@
     for k in (8, 4):
         more = shifted(own, Z, k)
         own = lax.optimization_barrier(jnp.concatenate([own, more], 0))
-    rows = [own]
+    other = shifted(own, "c", 1)
+    own = lax.optimization_barrier(jnp.concatenate([own, other], 0))
+    held = [own]
     for k in STEPS[1:]:
-        rows.append(shifted(own, Z, k))
-    own = lax.optimization_barrier(jnp.concatenate(rows, 0))
-    other = shifted(own, "c", 1)
+        held.append(shifted(own, Z, k))
 
     blocks = from_everyone(block, ("c", "x"))
     partial = lift(blocks, gots, rows_o, tokens // xs, ys)
@@ -465,7 +465,7 @@
     )
     total = exchange(total, TP)
     moments = (mean_o, square_o, mean_v, square_v)
-    prepared = ready(moments, out_basis, value_basis, own, other, segments)
+    prepared = ready(moments, out_basis, value_basis, held, segments)
     counts = (rows_o * fs * cols_o * tp, rows_v * fs * cols_v * tp)
     step_o, new_o, copy_o, step_v, new_v, copy_v = outputs(
         counts, total, out_weight, value_up_matrix, *prepared

time: 193 us -> 185 us (0.959)
  waiting for transfers between devices: 25.2 us -> 11.3 us
  blocking collectives: 46.9 us -> 60.1 us
  starting transfers between devices: 96.5 us -> 88.5 us
    ppermute x12, waiting for transfers between devices: 24 us -> 10.6 us  [shifted(): lax.ppermute(value, axis, [(i, (i + by) % devices) for i in range(devices)])]
    all_to_all x2 -> x3, blocking collectives: 46.9 us -> 60.1 us  [exchange(): return lax.all_to_all(value, axes, 0, 0, tiled=True)]
    ppermute x12, starting transfers between devices: 55.7 us -> 50.3 us  [shifted(): lax.ppermute(value, axis, [(i, (i + by) % devices) for i in range(devices)])]
    all_to_all x5 -> x4, starting transfers between devices: 40.1 us -> 37.6 us  [exchange(): return lax.all_to_all(value, axes, 0, 0, tiled=True)]
  transfers between devices with their start and end apart: 18 -> 17, of which waited for: 7 -> 6; matrix products, arithmetic and copies ran while one was open for 0% -> 0% of each run, Pallas kernels for 5% -> 6%
where the time goes in v9:
time: 185 us; the launch traced here: 184 us
  starting transfers between devices  88.5 us (48%)
  blocking collectives  60.1 us (32%)
  Pallas kernels  18 us (10%)
  waiting for transfers between devices  11.3 us (6%)
  local copies, waits for them, and re-layouts  3.98 us (2%)
    all_to_all x3, blocking collectives, exchange(): return lax.all_to_all(value, axes, 0, 0, tiled=True)  60.1 us
    ppermute x12, starting transfers between devices, shifted(): lax.ppermute(value, axis, [(i, (i + by) % devices) for i in range(devices)])  50.3 us
    all_to_all x4, starting transfers between devices, exchange(): return lax.all_to_all(value, axes, 0, 0, tiled=True)  37.6 us
    ppermute x12, waiting for transfers between devices, shifted(): lax.ppermute(value, axis, [(i, (i + by) % devices) for i in range(devices)])  10.6 us
    pallas_call x1, Pallas kernels, ready(): pl.pallas_call(functools.partial(ready_kernel, rows_o, rows_v), out_shape...  4.43 us
    pallas_call x1, Pallas kernels, outputs(): pl.pallas_call(functools.partial(output_kernel, counts, pieces), in_specs...  3.82 us
  transfers between devices with their start and end apart: 17, of which 6 were waited for; matrix products, arithmetic and copies ran while one was open for 0% of the time, Pallas kernels for 6%

profile of v9, /device:TPU:1, one launch (start us, length us, event | category | flops | bytes accessed | tf_op | source)
XLA Modules:
  0.0 183.8 jit_solution(6824630143868179105)
XLA Ops:
  0.6 0.0 copy-start.5
  0.7 0.8 pad_maximum_fusion.3
  1.5 0.7 collective-permute-start
  2.1 0.8 broadcast_in_dim.4
  2.9 15.3 %all-to-all-start = ((bf16[8,96,256]{2,1,0:T(8,128)(2,1)}), bf16[8,96,256]{2,1,0:T(8,128)(2,1)}, u32[]{:S(2)}, u32[]{:S(2)}) async-start(bf16[8,96,256]{2,1,0:T(8,128)(2,1)} %broadcast_in_dim.4), calls=%async_computation | async-start | bytes 786432 | tf_op jit(solution)/shard_map/all_to_all | solution.py:31
  18.2 2.0 %shard_map.196 = (bf16[576,128]{1,0:T(8,128)(2,1)}, bf16[576,128]{1,0:T(8,128)(2,1)}, bf16[576,128]{1,0:T(8,128)(2,1)}) custom-call(bf16[1536,128]{1,0:T(8,128)(2,1)} %attn_ref.3, bf16[64,1536]{1,0:T(8,128)(2,1)} %bitcast.4), custom_call_target="tpu_custom_call" | custom-call | flops 10000000 | bytes 1000000 | tf_op jit(solution)/shard_map/pallas_call | solution.py:86
  20.1 3.3 %collective-permute-start.1 = (bf16[576,128]{1,0:T(8,128)(2,1)}, bf16[576,128]{1,0:T(8,128)(2,1)S(1)}, u32[]{:S(2)}, u32[]{:S(2)}) collective-permute-start(bf16[576,128]{1,0:T(8,128)(2,1)} %get-tuple-element.30), channel_id=1, source_target_pairs={{0,1},{1,2},{2,3},{3,0},{4,5},{5,6},{6,7},{7,4},{8,9},{9,10},{10,1... | collective-permute-start | bytes 442376 | tf_op jit(solution)/shard_map/ppermute | solution.py:50
  23.4 4.3 %collective-permute-start.2 = (bf16[576,128]{1,0:T(8,128)(2,1)}, bf16[576,128]{1,0:T(8,128)(2,1)S(1)}, u32[]{:S(2)}, u32[]{:S(2)}) collective-permute-start(bf16[576,128]{1,0:T(8,128)(2,1)} %get-tuple-element.31), channel_id=1, source_target_pairs={{0,2},{1,3},{2,0},{3,1},{4,6},{5,7},{6,4},{7,5},{8,10},{9,11},{10,... | collective-permute-start | bytes 442376 | tf_op jit(solution)/shard_map/ppermute | solution.py:50
  27.7 3.1 %collective-permute-start.3 = (bf16[576,128]{1,0:T(8,128)(2,1)}, bf16[576,128]{1,0:T(8,128)(2,1)S(1)}, u32[]{:S(2)}, u32[]{:S(2)}) collective-permute-start(bf16[576,128]{1,0:T(8,128)(2,1)} %get-tuple-element.32), channel_id=1, source_target_pairs={{0,3},{1,0},{2,1},{3,2},{4,7},{5,4},{6,5},{7,6},{8,11},{9,8},{10,9... | collective-permute-start | bytes 442376 | tf_op jit(solution)/shard_map/ppermute | solution.py:50
  30.8 0.0 copy-start.3
  30.8 1.0 copy-done.3
  31.8 0.7 shard_map.195.refs_0_
  32.5 0.4 collective-permute-done.2.refs_2_
  32.9 1.4 collective-permute-done.3.refs_3_
  34.3 1.5 lift.1
  35.8 20.0 %all_to_all.35.got_ref = bf16[4,96,512]{2,1,0:T(8,128)(2,1)S(1)} all-to-all(bf16[4,96,512]{2,1,0:T(8,128)(2,1)S(1)} %lift.1), channel_id=1, replica_groups=mesh['zh'=4,'zl'=4,'c'=2,'y'=4,'x'=4] {'y'}, dimensions={0} | all-to-all | bytes 786432 | tf_op jit(solution)/shard_map/all_to_all | solution.py:31
  55.8 0.2 shard_map.197
  56.0 0.0 copy-start.4
  56.0 0.0 copy-start.6
  56.0 26.9 %all_to_all.36 = bf16[16,96,512]{2,1,0:T(8,128)(2,1)S(1)} all-to-all(bf16[16,96,512]{2,1,0:T(8,128)(2,1)S(1)} %shard_map.197), channel_id=1, replica_groups=mesh['zh'=4,'zl'=4,'c'=2,'y'=4,'x'=4] {'y','x'}, dimensions={0} | all-to-all | bytes 3145728 | tf_op jit(solution)/shard_map/all_to_all | solution.py:31
  82.9 1.4 contract.1
  84.3 0.0 copy-start.7
  84.3 13.2 %all_to_all.37.got_ref = bf16[8,32,384]{2,1,0:T(8,128)(2,1)S(1)} all-to-all(bf16[8,32,384]{2,1,0:T(8,128)(2,1)S(1)} %contract.1), channel_id=1, replica_groups=mesh['zh'=4,'zl'=4,'c'=2,'y'=4,'x'=4] {'zl','c'}, dimensions={0} | all-to-all | bytes 393216 | tf_op jit(solution)/shard_map/all_to_all | solution.py:31
  97.6 0.7 shard_map.198
  98.2 11.2 %all-to-all-start.4 = ((bf16[4,32,384]{2,1,0:T(8,128)(2,1)}), bf16[4,32,384]{2,1,0:T(8,128)(2,1)S(1)}, u32[]{:S(2)}, u32[]{:S(2)}) async-start(bf16[4,32,384]{2,1,0:T(8,128)(2,1)} %shard_map.198), calls=%async_computation.4 | async-start | bytes 196608 | tf_op jit(solution)/shard_map/all_to_all | solution.py:31
  109.4 12.1 %collective-permute-start.7 = (bf16[1,160,128]{2,1,0:T(8,128)(2,1)S(1)}, bf16[1,160,128]{2,1,0:T(8,128)(2,1)S(1)}, u32[]{:S(2)}, u32[]{:S(2)}) collective-permute-start(bf16[1,160,128]{2,1,0:T(8,128)(2,1)S(1)} %bitcast.6), channel_id=1, source_target_pairs={{0,256},{32,288},{64,320},{96,352},{128,384},{160,416},{192,448},{... | collective-permute-start | bytes 122888 | tf_op jit(solution)/shard_map/ppermute | solution.py:50
  121.5 2.0 %collective-permute-done.7 = bf16[1,160,128]{2,1,0:T(8,128)(2,1)S(1)} collective-permute-done((bf16[1,160,128]{2,1,0:T(8,128)(2,1)S(1)}, bf16[1,160,128]{2,1,0:T(8,128)(2,1)S(1)}, u32[]{:S(2)}, u32[]{:S(2)}) %collective-permute-start.7) | collective-permute-done | bytes 40992 | tf_op jit(solution)/shard_map/ppermute | solution.py:50
  123.5 7.4 %collective-permute-start.8 = (bf16[2,160,128]{2,1,0:T(8,128)(2,1)S(1)}, bf16[2,160,128]{2,1,0:T(8,128)(2,1)S(1)}, u32[]{:S(2)}, u32[]{:S(2)}) collective-permute-start(bf16[2,160,128]{2,1,0:T(8,128)(2,1)S(1)} %pad_maximum_fusion.2), channel_id=1, source_target_pairs={{0,128},{32,160},{64,192},{96,224},{128,256},{160,288},{192,320},{... | collective-permute-start | bytes 245768 | tf_op jit(solution)/shard_map/ppermute | solution.py:50
  130.9 0.7 shard_map.199
  131.6 6.8 %all-to-all-start.5 = ((bf16[8,32,384]{2,1,0:T(8,128)(2,1)}), bf16[8,32,384]{2,1,0:T(8,128)(2,1)S(1)}, u32[]{:S(2)}, u32[]{:S(2)}) async-start(bf16[8,32,384]{2,1,0:T(8,128)(2,1)} %shard_map.199), calls=%async_computation.5 | async-start | bytes 393216 | tf_op jit(solution)/shard_map/all_to_all | solution.py:31
  138.4 1.9 %collective-permute-start.4 = (bf16[8,96,256]{2,1,0:T(8,128)(2,1)}, bf16[8,96,256]{2,1,0:T(8,128)(2,1)S(1)}, u32[]{:S(2)}, u32[]{:S(2)}) collective-permute-start(bf16[8,96,256]{2,1,0:T(8,128)(2,1)} %all-to-all-done.blocks_ref.b0), channel_id=1, source_target_pairs={{0,4},{4,8},{8,12},{12,0},{1,5},{5,9},{9,13},{13,1},{2,6},{6,10},{... | collective-permute-start | bytes 1179656 | tf_op jit(solution)/shard_map/ppermute | solution.py:50
  140.3 2.0 %collective-permute-start.9 = (bf16[4,160,128]{2,1,0:T(8,128)(2,1)S(1)}, bf16[4,160,128]{2,1,0:T(8,128)(2,1)S(1)}, u32[]{:S(2)}, u32[]{:S(2)}) collective-permute-start(bf16[4,160,128]{2,1,0:T(8,128)(2,1)S(1)} %pad_maximum_fusion.1), channel_id=1, source_target_pairs={{0,16},{16,0},{1,17},{17,1},{2,18},{18,2},{3,19},{19,3},{4,20},{20... | collective-permute-start | bytes 491528 | tf_op jit(solution)/shard_map/ppermute | solution.py:50
  142.4 3.9 %collective-permute-start.5 = (bf16[8,96,256]{2,1,0:T(8,128)(2,1)}, bf16[8,96,256]{2,1,0:T(8,128)(2,1)S(1)}, u32[]{:S(2)}, u32[]{:S(2)}) collective-permute-start(bf16[8,96,256]{2,1,0:T(8,128)(2,1)} %all-to-all-done.blocks_ref.b0), channel_id=1, source_target_pairs={{0,8},{4,12},{8,0},{12,4},{1,9},{5,13},{9,1},{13,5},{2,10},{6,14},... | collective-permute-start | bytes 1179656 | tf_op jit(solution)/shard_map/ppermute | solution.py:50
  146.3 2.8 %collective-permute-start.6 = (bf16[8,96,256]{2,1,0:T(8,128)(2,1)}, bf16[8,96,256]{2,1,0:T(8,128)(2,1)S(1)}, u32[]{:S(2)}, u32[]{:S(2)}) collective-permute-start(bf16[8,96,256]{2,1,0:T(8,128)(2,1)} %all-to-all-done.blocks_ref.b0), channel_id=1, source_target_pairs={{0,12},{4,0},{8,4},{12,8},{1,13},{5,1},{9,5},{13,9},{2,14},{6,2},{... | collective-permute-start | bytes 1179656 | tf_op jit(solution)/shard_map/ppermute | solution.py:50
  149.2 3.5 %collective-permute-start.10 = (bf16[8,160,128]{2,1,0:T(8,128)(2,1)S(1)}, bf16[8,160,128]{2,1,0:T(8,128)(2,1)S(1)}, u32[]{:S(2)}, u32[]{:S(2)}) collective-permute-start(bf16[8,160,128]{2,1,0:T(8,128)(2,1)S(1)} %pad_maximum_fusion.h0), channel_id=1, source_target_pairs={{0,32},{32,64},{64,96},{96,128},{128,160},{160,192},{192,224},{224... | collective-permute-start | bytes 983048 | tf_op jit(solution)/shard_map/ppermute | solution.py:50
  152.8 4.0 %collective-permute-start.11 = (bf16[8,160,128]{2,1,0:T(8,128)(2,1)S(1)}, bf16[8,160,128]{2,1,0:T(8,128)(2,1)S(1)}, u32[]{:S(2)}, u32[]{:S(2)}) collective-permute-start(bf16[8,160,128]{2,1,0:T(8,128)(2,1)S(1)} %pad_maximum_fusion.h0), channel_id=1, source_target_pairs={{0,64},{32,96},{64,128},{96,160},{128,192},{160,224},{192,256},{22... | collective-permute-start | bytes 983048 | tf_op jit(solution)/shard_map/ppermute | solution.py:50
  156.8 3.9 %collective-permute-done.4.b1 = bf16[8,96,256]{2,1,0:T(8,128)(2,1)S(1)} collective-permute-done((bf16[8,96,256]{2,1,0:T(8,128)(2,1)}, bf16[8,96,256]{2,1,0:T(8,128)(2,1)S(1)}, u32[]{:S(2)}, u32[]{:S(2)}) %collective-permute-start.4) | collective-permute-done | bytes 393248 | tf_op jit(solution)/shard_map/ppermute | solution.py:50
  160.7 1.9 %collective-permute-start.12 = (bf16[8,160,128]{2,1,0:T(8,128)(2,1)S(1)}, bf16[8,160,128]{2,1,0:T(8,128)(2,1)S(1)}, u32[]{:S(2)}, u32[]{:S(2)}) collective-permute-start(bf16[8,160,128]{2,1,0:T(8,128)(2,1)S(1)} %pad_maximum_fusion.h0), channel_id=1, source_target_pairs={{0,480},{32,0},{64,32},{96,64},{128,96},{160,128},{192,160},{224,1... | collective-permute-start | bytes 983048 | tf_op jit(solution)/shard_map/ppermute | solution.py:50
  162.6 3.0 %collective-permute-done.6.b3 = bf16[8,96,256]{2,1,0:T(8,128)(2,1)S(1)} collective-permute-done((bf16[8,96,256]{2,1,0:T(8,128)(2,1)}, bf16[8,96,256]{2,1,0:T(8,128)(2,1)S(1)}, u32[]{:S(2)}, u32[]{:S(2)}) %collective-permute-start.6) | collective-permute-done | bytes 393248 | tf_op jit(solution)/shard_map/ppermute | solution.py:50
  165.6 2.6 %directions.1 = (f32[256,256]{1,0:T(8,128)}, f32[256,256]{1,0:T(8,128)}, f32[256,128]{1,0:T(8,128)}, f32[256,128]{1,0:T(8,128)}, f32[16,8,128]{2,1,0:T(8,128)}) custom-call(bf16[8,32,384]{2,1,0:T(8,128)(2,1)S(1)} %all-to-all-done.5.got_ref, f32[256,256]{1,0:T(8,128)S(1)} %copy-done.7, f32[256,256]{1,0:T(8,128)S(1)} %copy-done.8, f32[256,128]{1,0:T(8,128)S(1)} %copy-done.10, ...), custom_call_target="tpu_custom_call" | custom-call | flops 400000000 | bytes 4000000 | tf_op jit(solution)/shard_map/directions/pallas_call | solution.py:261
  168.3 0.7 copy-done
  169.0 4.4 %all-to-all-start.6 = ((f32[16,8,128]{2,1,0:T(8,128)}), f32[16,8,128]{2,1,0:T(8,128)}, u32[]{:S(2)}, u32[]{:S(2)}) async-start(f32[16,8,128]{2,1,0:T(8,128)} %get-tuple-element.33), calls=%async_computation.6 | async-start | bytes 131072 | tf_op jit(solution)/shard_map/all_to_all | solution.py:31
  173.5 0.7 copy-done.14
  174.2 0.1 copy-done.15
  174.3 0.6 copy-done.16
  174.9 4.4 %ready.1 = (f32[64,256]{1,0:T(8,128)}, f32[32,128]{1,0:T(8,128)}, bf16[2048,256]{1,0:T(8,128)(2,1)}, bf16[1024,128]{1,0:T(8,128)(2,1)}, bf16[2048,256]{1,0:T(8,128)(2,1)}, /*index=5*/bf16[1024,128]{1,0:T(8,128)(2,1)}) custom-call(f32[256,256]{1,0:T(8,128)} %get-tuple-element.23.mean_o, f32[256,256]{1,0:T(8,128)} %get-tuple-element.24.square_o, ...), custom_call_target="tpu_custom_call" | custom-call | flops 400000000 | bytes 4000000 | tf_op jit(solution)/shard_map/ready/pallas_call | solution.py:324
  179.3 0.7 all-to-all-done.6.total_ref
  180.0 3.8 %outputs.1 = (f32[64,256]{1,0:T(8,128)}, f32[64,256]{1,0:T(8,128)}, bf16[2048,256]{1,0:T(8,128)(2,1)}, f32[32,128]{1,0:T(8,128)}, f32[32,128]{1,0:T(8,128)}, /*index=5*/bf16[1024,128]{1,0:T(8,128)(2,1)}) custom-call(f32[16,8,128]{2,1,0:T(8,128)} %all-to-all-done.6.total_ref, f32[64,256]{1,0:T(8,128)} %weight_o.3, f32[32,128]{1,0:T(8,128)} %weight_v.3, ...), custom_call_target="tpu_custom_call" | custom-call | flops 10000000 | bytes 4000000 | tf_op jit(solution)/shard_map/outputs/pallas_call | solution.py:387
  (39 shorter events, 0.1 us)
Async XLA Ops:
  0.6 30.2 %copy-start.5 = (bf16[1536,64]{0,1:T(8,128)(2,1)S(1)}, bf16[1536,64]{0,1:T(8,128)(2,1)}, u32[]{:S(2)}) copy-start(bf16[1536,64]{0,1:T(8,128)(2,1)} %param.14) | copy-start | bytes 589828
  1.5 0.7 collective-permute-start
  2.9 31.4 %all-to-all-start = ((bf16[8,96,256]{2,1,0:T(8,128)(2,1)}), bf16[8,96,256]{2,1,0:T(8,128)(2,1)}, u32[]{:S(2)}, u32[]{:S(2)}) async-start(bf16[8,96,256]{2,1,0:T(8,128)(2,1)} %broadcast_in_dim.4), calls=%async_computation | async-start | bytes 786432 | tf_op jit(solution)/shard_map/all_to_all | solution.py:31
  20.1 12.4 %collective-permute-start.1 = (bf16[576,128]{1,0:T(8,128)(2,1)}, bf16[576,128]{1,0:T(8,128)(2,1)S(1)}, u32[]{:S(2)}, u32[]{:S(2)}) collective-permute-start(bf16[576,128]{1,0:T(8,128)(2,1)} %get-tuple-element.30), channel_id=1, source_target_pairs={{0,1},{1,2},{2,3},{3,0},{4,5},{5,6},{6,7},{7,4},{8,9},{9,10},{10,1... | collective-permute-start | bytes 442376 | tf_op jit(solution)/shard_map/ppermute | solution.py:50
  23.4 9.5 %collective-permute-start.2 = (bf16[576,128]{1,0:T(8,128)(2,1)}, bf16[576,128]{1,0:T(8,128)(2,1)S(1)}, u32[]{:S(2)}, u32[]{:S(2)}) collective-permute-start(bf16[576,128]{1,0:T(8,128)(2,1)} %get-tuple-element.31), channel_id=1, source_target_pairs={{0,2},{1,3},{2,0},{3,1},{4,6},{5,7},{6,4},{7,5},{8,10},{9,11},{10,... | collective-permute-start | bytes 442376 | tf_op jit(solution)/shard_map/ppermute | solution.py:50
  27.7 6.6 %collective-permute-start.3 = (bf16[576,128]{1,0:T(8,128)(2,1)}, bf16[576,128]{1,0:T(8,128)(2,1)S(1)}, u32[]{:S(2)}, u32[]{:S(2)}) collective-permute-start(bf16[576,128]{1,0:T(8,128)(2,1)} %get-tuple-element.32), channel_id=1, source_target_pairs={{0,3},{1,0},{2,1},{3,2},{4,7},{5,4},{6,5},{7,6},{8,11},{9,8},{10,9... | collective-permute-start | bytes 442376 | tf_op jit(solution)/shard_map/ppermute | solution.py:50
  30.8 1.0 copy-start.3
  56.0 27.0 %copy-start.4 = (bf16[1536,256]{1,0:T(8,128)(2,1)S(1)}, bf16[1536,256]{1,0:T(8,128)(2,1)}, u32[]{:S(2)}) copy-start(bf16[1536,256]{1,0:T(8,128)(2,1)} %cot_o.1) | copy-start | bytes 2359300
  56.0 26.9 %copy-start.6 = (bf16[1536,128]{1,0:T(8,128)(2,1)S(1)}, bf16[1536,128]{1,0:T(8,128)(2,1)}, u32[]{:S(2)}) copy-start(bf16[1536,128]{1,0:T(8,128)(2,1)} %cot_v.1) | copy-start | bytes 1179652
  82.9 26.5 %copy-start.9 = (f32[64,256]{1,0:T(8,128)S(1)}, f32[64,256]{1,0:T(8,128)}, u32[]{:S(2)}) copy-start(f32[64,256]{1,0:T(8,128)} %weight_o.3) | copy-start | bytes 196612
  82.9 26.5 %copy-start.12 = (f32[32,128]{1,0:T(8,128)S(1)}, f32[32,128]{1,0:T(8,128)}, u32[]{:S(2)}) copy-start(f32[32,128]{1,0:T(8,128)} %weight_v.3) | copy-start | bytes 49156
  84.3 81.3 %copy-start.7 = (f32[256,256]{1,0:T(8,128)S(1)}, f32[256,256]{1,0:T(8,128)}, u32[]{:S(2)}) copy-start(f32[256,256]{1,0:T(8,128)} %mean_o.1) | copy-start | bytes 786436
  84.3 81.3 %copy-start.8 = (f32[256,256]{1,0:T(8,128)S(1)}, f32[256,256]{1,0:T(8,128)}, u32[]{:S(2)}) copy-start(f32[256,256]{1,0:T(8,128)} %square_o.1) | copy-start | bytes 786436
  84.3 81.3 %copy-start.10 = (f32[256,128]{1,0:T(8,128)S(1)}, f32[256,128]{1,0:T(8,128)}, u32[]{:S(2)}) copy-start(f32[256,128]{1,0:T(8,128)} %mean_v.1) | copy-start | bytes 393220
  84.3 81.3 %copy-start.11 = (f32[256,128]{1,0:T(8,128)S(1)}, f32[256,128]{1,0:T(8,128)}, u32[]{:S(2)}) copy-start(f32[256,128]{1,0:T(8,128)} %square_v.1) | copy-start | bytes 393220
  98.2 32.7 %all-to-all-start.4 = ((bf16[4,32,384]{2,1,0:T(8,128)(2,1)}), bf16[4,32,384]{2,1,0:T(8,128)(2,1)S(1)}, u32[]{:S(2)}, u32[]{:S(2)}) async-start(bf16[4,32,384]{2,1,0:T(8,128)(2,1)} %shard_map.198), calls=%async_computation.4 | async-start | bytes 196608 | tf_op jit(solution)/shard_map/all_to_all | solution.py:31
  109.4 14.1 %collective-permute-start.7 = (bf16[1,160,128]{2,1,0:T(8,128)(2,1)S(1)}, bf16[1,160,128]{2,1,0:T(8,128)(2,1)S(1)}, u32[]{:S(2)}, u32[]{:S(2)}) collective-permute-start(bf16[1,160,128]{2,1,0:T(8,128)(2,1)S(1)} %bitcast.6), channel_id=1, source_target_pairs={{0,256},{32,288},{64,320},{96,352},{128,384},{160,416},{192,448},{... | collective-permute-start | bytes 122888 | tf_op jit(solution)/shard_map/ppermute | solution.py:50
  123.5 16.8 %collective-permute-start.8 = (bf16[2,160,128]{2,1,0:T(8,128)(2,1)S(1)}, bf16[2,160,128]{2,1,0:T(8,128)(2,1)S(1)}, u32[]{:S(2)}, u32[]{:S(2)}) collective-permute-start(bf16[2,160,128]{2,1,0:T(8,128)(2,1)S(1)} %pad_maximum_fusion.2), channel_id=1, source_target_pairs={{0,128},{32,160},{64,192},{96,224},{128,256},{160,288},{192,320},{... | collective-permute-start | bytes 245768 | tf_op jit(solution)/shard_map/ppermute | solution.py:50
  131.6 33.9 %all-to-all-start.5 = ((bf16[8,32,384]{2,1,0:T(8,128)(2,1)}), bf16[8,32,384]{2,1,0:T(8,128)(2,1)S(1)}, u32[]{:S(2)}, u32[]{:S(2)}) async-start(bf16[8,32,384]{2,1,0:T(8,128)(2,1)} %shard_map.199), calls=%async_computation.5 | async-start | bytes 393216 | tf_op jit(solution)/shard_map/all_to_all | solution.py:31
  138.4 22.3 %collective-permute-start.4 = (bf16[8,96,256]{2,1,0:T(8,128)(2,1)}, bf16[8,96,256]{2,1,0:T(8,128)(2,1)S(1)}, u32[]{:S(2)}, u32[]{:S(2)}) collective-permute-start(bf16[8,96,256]{2,1,0:T(8,128)(2,1)} %all-to-all-done.blocks_ref.b0), channel_id=1, source_target_pairs={{0,4},{4,8},{8,12},{12,0},{1,5},{5,9},{9,13},{13,1},{2,6},{6,10},{... | collective-permute-start | bytes 1179656 | tf_op jit(solution)/shard_map/ppermute | solution.py:50
  140.3 8.8 %collective-permute-start.9 = (bf16[4,160,128]{2,1,0:T(8,128)(2,1)S(1)}, bf16[4,160,128]{2,1,0:T(8,128)(2,1)S(1)}, u32[]{:S(2)}, u32[]{:S(2)}) collective-permute-start(bf16[4,160,128]{2,1,0:T(8,128)(2,1)S(1)} %pad_maximum_fusion.1), channel_id=1, source_target_pairs={{0,16},{16,0},{1,17},{17,1},{2,18},{18,2},{3,19},{19,3},{4,20},{20... | collective-permute-start | bytes 491528 | tf_op jit(solution)/shard_map/ppermute | solution.py:50
  142.4 20.2 %collective-permute-start.5 = (bf16[8,96,256]{2,1,0:T(8,128)(2,1)}, bf16[8,96,256]{2,1,0:T(8,128)(2,1)S(1)}, u32[]{:S(2)}, u32[]{:S(2)}) collective-permute-start(bf16[8,96,256]{2,1,0:T(8,128)(2,1)} %all-to-all-done.blocks_ref.b0), channel_id=1, source_target_pairs={{0,8},{4,12},{8,0},{12,4},{1,9},{5,13},{9,1},{13,5},{2,10},{6,14},... | collective-permute-start | bytes 1179656 | tf_op jit(solution)/shard_map/ppermute | solution.py:50
  146.3 19.2 %collective-permute-start.6 = (bf16[8,96,256]{2,1,0:T(8,128)(2,1)}, bf16[8,96,256]{2,1,0:T(8,128)(2,1)S(1)}, u32[]{:S(2)}, u32[]{:S(2)}) collective-permute-start(bf16[8,96,256]{2,1,0:T(8,128)(2,1)} %all-to-all-done.blocks_ref.b0), channel_id=1, source_target_pairs={{0,12},{4,0},{8,4},{12,8},{1,13},{5,1},{9,5},{13,9},{2,14},{6,2},{... | collective-permute-start | bytes 1179656 | tf_op jit(solution)/shard_map/ppermute | solution.py:50
  149.2 19.8 %copy-start.13 = (bf16[8,160,128]{2,1,0:T(8,128)(2,1)}, bf16[8,160,128]{2,1,0:T(8,128)(2,1)S(1)}, u32[]{:S(2)}) copy-start(bf16[8,160,128]{2,1,0:T(8,128)(2,1)S(1)} %pad_maximum_fusion.h0) | copy-start | bytes 983044
  149.2 24.2 %collective-permute-start.10 = (bf16[8,160,128]{2,1,0:T(8,128)(2,1)S(1)}, bf16[8,160,128]{2,1,0:T(8,128)(2,1)S(1)}, u32[]{:S(2)}, u32[]{:S(2)}) collective-permute-start(bf16[8,160,128]{2,1,0:T(8,128)(2,1)S(1)} %pad_maximum_fusion.h0), channel_id=1, source_target_pairs={{0,32},{32,64},{64,96},{96,128},{128,160},{160,192},{192,224},{224... | collective-permute-start | bytes 983048 | tf_op jit(solution)/shard_map/ppermute | solution.py:50
  152.8 20.7 %collective-permute-start.11 = (bf16[8,160,128]{2,1,0:T(8,128)(2,1)S(1)}, bf16[8,160,128]{2,1,0:T(8,128)(2,1)S(1)}, u32[]{:S(2)}, u32[]{:S(2)}) collective-permute-start(bf16[8,160,128]{2,1,0:T(8,128)(2,1)S(1)} %pad_maximum_fusion.h0), channel_id=1, source_target_pairs={{0,64},{32,96},{64,128},{96,160},{128,192},{160,224},{192,256},{22... | collective-permute-start | bytes 983048 | tf_op jit(solution)/shard_map/ppermute | solution.py:50
  160.7 12.8 %collective-permute-start.12 = (bf16[8,160,128]{2,1,0:T(8,128)(2,1)S(1)}, bf16[8,160,128]{2,1,0:T(8,128)(2,1)S(1)}, u32[]{:S(2)}, u32[]{:S(2)}) collective-permute-start(bf16[8,160,128]{2,1,0:T(8,128)(2,1)S(1)} %pad_maximum_fusion.h0), channel_id=1, source_target_pairs={{0,480},{32,0},{64,32},{96,64},{128,96},{160,128},{192,160},{224,1... | collective-permute-start | bytes 983048 | tf_op jit(solution)/shard_map/ppermute | solution.py:50
  162.6 5.7 %copy-start.1 = (bf16[8,96,256]{2,1,0:T(8,128)(2,1)}, bf16[8,96,256]{2,1,0:T(8,128)(2,1)S(1)}, u32[]{:S(2)}) copy-start(bf16[8,96,256]{2,1,0:T(8,128)(2,1)S(1)} %collective-permute-done.5.b2) | copy-start | bytes 1179652
  165.6 3.4 %copy-start.2 = (bf16[8,96,256]{2,1,0:T(8,128)(2,1)}, bf16[8,96,256]{2,1,0:T(8,128)(2,1)S(1)}, u32[]{:S(2)}) copy-start(bf16[8,96,256]{2,1,0:T(8,128)(2,1)S(1)} %collective-permute-done.6.b3) | copy-start | bytes 1179652
  168.2 0.7 copy-start
  169.0 11.0 %all-to-all-start.6 = ((f32[16,8,128]{2,1,0:T(8,128)}), f32[16,8,128]{2,1,0:T(8,128)}, u32[]{:S(2)}, u32[]{:S(2)}) async-start(f32[16,8,128]{2,1,0:T(8,128)} %get-tuple-element.33), calls=%async_computation.6 | async-start | bytes 131072 | tf_op jit(solution)/shard_map/all_to_all | solution.py:31
  173.5 0.7 copy-start.14
  173.5 0.8 copy-start.15
  174.2 0.7 copy-start.16

commit v10 on v9

--- a/solution.py
+++ b/solution.py
@@ -274,8 +274,8 @@
 
 
 def ready_kernel(
-    rows_o, rows_v, mean_o, square_o, mean_v, square_v, local_o, local_v, h0, h1, h2, h3, b0, b1, b2, b3,
-    step_o_out, step_v_out, update_o_out, update_v_out, old_o_out, old_v_out,
+    rows_o, rows_v, mean_o, square_o, mean_v, square_v, local_o, local_v, b0, b1, b2, b3,
+    step_o_out, step_v_out, update_o_out, update_v_out,
 ):
     uppers = []
     for mean, square, local, step_out in (
@@ -288,8 +288,7 @@
         step_out[...] = dot(local[...], upper) + dot(local[...], lower)
         uppers.append(upper)
     upper_o, upper_v = uppers
-    y, c = lax.axis_index("y"), lax.axis_index("c")
-    z = 4 * lax.axis_index("zh") + lax.axis_index("zl")
+    y = lax.axis_index("y")
     for k, ref in enumerate((b0, b1, b2, b3)):
         origin = lax.rem(y + 4 - k, 4)
         count = ref.shape[0]
@@ -304,6 +303,11 @@
             update_o_out[pl.ds(at, rows_o), :] = update_o[i * rows_o : (i + 1) * rows_o]
             at = pl.multiple_of(index * rows_v, rows_v)
             update_v_out[pl.ds(at, rows_v), :] = update_v[i * rows_v : (i + 1) * rows_v]
+
+
+def arrange_kernel(rows_o, rows_v, h0, h1, h2, h3, old_o_out, old_v_out):
+    c = lax.axis_index("c")
+    z = 4 * lax.axis_index("zh") + lax.axis_index("zl")
     for ref, step in zip((h0, h1, h2, h3), STEPS):
         for p in range(8):
             behind = (0, 8, 4, 12)[p & 3] + step
@@ -316,10 +320,21 @@
             old_v_out[pl.ds(at, rows_v), :] = ref[p, 2 * rows_o :]
 
 
-def ready(moments, local_o, local_v, held, segments):
+def arrange(rows_o, rows_v, held):
+    fs = 4 * held[0].shape[0]
+    shape = jax.ShapeDtypeStruct
+    return pl.pallas_call(
+        functools.partial(arrange_kernel, rows_o, rows_v),
+        out_shape=(shape((rows_o * fs, held[0].shape[2] * 2), BF), shape((rows_v * fs, held[0].shape[2]), BF)),
+        cost_estimate=pl.CostEstimate(flops=10**6, bytes_accessed=3 * 10**6, transcendentals=0),
+        compiler_params=pltpu.CompilerParams(vmem_limit_bytes=ROOM),
+        name="arrange",
+    )(*held)
+
+
+def ready(moments, local_o, local_v, fs, segments):
     rows_o, rows_v = local_o.shape[0], local_v.shape[0]
     cols_o, cols_v = moments[0].shape[1], moments[2].shape[1]
-    fs = 4 * held[0].shape[0]
     shape = jax.ShapeDtypeStruct
     return pl.pallas_call(
         functools.partial(ready_kernel, rows_o, rows_v),
@@ -328,13 +343,11 @@
             shape((rows_v, cols_v), F32),
             shape((rows_o * fs, cols_o), BF),
             shape((rows_v * fs, cols_v), BF),
-            shape((rows_o * fs, cols_o), BF),
-            shape((rows_v * fs, cols_v), BF),
         ),
         cost_estimate=pl.CostEstimate(flops=4 * 10**8, bytes_accessed=4 * 10**6, transcendentals=0),
         compiler_params=pltpu.CompilerParams(vmem_limit_bytes=WHOLE),
         name="ready",
-    )(*moments, local_o, local_v, *held, *segments)
+    )(*moments, local_o, local_v, *segments)
 
 
 def output_kernel(
@@ -460,15 +473,16 @@
     for k in range(1, ys):
         segments.append(shifted(blocks, "y", k))
 
+    old = arrange(rows_o, rows_v, held)
     mean_o, square_o, mean_v, square_v, total = directions(
         rows_o, tp, proj, out_mean, out_square, value_mean, value_square, segments
     )
     total = exchange(total, TP)
     moments = (mean_o, square_o, mean_v, square_v)
-    prepared = ready(moments, out_basis, value_basis, held, segments)
+    prepared = ready(moments, out_basis, value_basis, fs, segments)
     counts = (rows_o * fs * cols_o * tp, rows_v * fs * cols_v * tp)
     step_o, new_o, copy_o, step_v, new_v, copy_v = outputs(
-        counts, total, out_weight, value_up_matrix, *prepared
+        counts, total, out_weight, value_up_matrix, *prepared, *old
     )
     return (step_o, new_o, copy_o, mean_o, square_o, step_v, new_v, copy_v, mean_v, square_v)
 

time: 185 us -> 185 us (level)
  transfers between devices with their start and end apart: 17 -> 17, of which waited for: 6 -> 6; matrix products, arithmetic and copies ran while one was open for 0% -> 0% of each run, Pallas kernels for 6% -> 5%
where the time goes in v10:
time: 185 us; the launch traced here: 183 us
  starting transfers between devices  88.5 us (48%)
  blocking collectives  60.1 us (32%)
  Pallas kernels  17.2 us (9%)
  waiting for transfers between devices  11.8 us (6%)
  local copies, waits for them, and re-layouts  3.48 us (2%)
    all_to_all x3, blocking collectives, exchange(): return lax.all_to_all(value, axes, 0, 0, tiled=True)  60.1 us
    ppermute x12, starting transfers between devices, shifted(): lax.ppermute(value, axis, [(i, (i + by) % devices) for i in range(devices)])  50.3 us
    all_to_all x4, starting transfers between devices, exchange(): return lax.all_to_all(value, axes, 0, 0, tiled=True)  37.6 us
    ppermute x12, waiting for transfers between devices, shifted(): lax.ppermute(value, axis, [(i, (i + by) % devices) for i in range(devices)])  10.6 us
    pallas_call x1, Pallas kernels, outputs(): pl.pallas_call(functools.partial(output_kernel, counts, pieces), in_specs...  3.82 us
  transfers between devices with their start and end apart: 17, of which 6 were waited for; matrix products, arithmetic and copies ran while one was open for 0% of the time, Pallas kernels for 5%

profile of v10, /device:TPU:1, one launch (start us, length us, event | category | flops | bytes accessed | tf_op | source)
XLA Modules:
  0.0 183.1 jit_solution(7777057844915794245)
XLA Ops:
  0.6 0.0 copy-start.6
  0.7 0.8 pad_maximum_fusion.3
  1.5 0.7 collective-permute-start
  2.1 0.8 broadcast_in_dim.4
  2.9 15.3 %all-to-all-start = ((bf16[8,96,256]{2,1,0:T(8,128)(2,1)}), bf16[8,96,256]{2,1,0:T(8,128)(2,1)}, u32[]{:S(2)}, u32[]{:S(2)}) async-start(bf16[8,96,256]{2,1,0:T(8,128)(2,1)} %broadcast_in_dim.4), calls=%async_computation | async-start | bytes 786432 | tf_op jit(solution)/shard_map/all_to_all | solution.py:31
  18.2 2.0 %shard_map.196 = (bf16[576,128]{1,0:T(8,128)(2,1)}, bf16[576,128]{1,0:T(8,128)(2,1)}, bf16[576,128]{1,0:T(8,128)(2,1)}) custom-call(bf16[1536,128]{1,0:T(8,128)(2,1)} %attn_ref.3, bf16[64,1536]{1,0:T(8,128)(2,1)} %bitcast.4), custom_call_target="tpu_custom_call" | custom-call | flops 10000000 | bytes 1000000 | tf_op jit(solution)/shard_map/pallas_call | solution.py:86
  20.1 3.3 %collective-permute-start.1 = (bf16[576,128]{1,0:T(8,128)(2,1)}, bf16[576,128]{1,0:T(8,128)(2,1)S(1)}, u32[]{:S(2)}, u32[]{:S(2)}) collective-permute-start(bf16[576,128]{1,0:T(8,128)(2,1)} %get-tuple-element.30), channel_id=1, source_target_pairs={{0,1},{1,2},{2,3},{3,0},{4,5},{5,6},{6,7},{7,4},{8,9},{9,10},{10,1... | collective-permute-start | bytes 442376 | tf_op jit(solution)/shard_map/ppermute | solution.py:50
  23.4 4.3 %collective-permute-start.2 = (bf16[576,128]{1,0:T(8,128)(2,1)}, bf16[576,128]{1,0:T(8,128)(2,1)S(1)}, u32[]{:S(2)}, u32[]{:S(2)}) collective-permute-start(bf16[576,128]{1,0:T(8,128)(2,1)} %get-tuple-element.31), channel_id=1, source_target_pairs={{0,2},{1,3},{2,0},{3,1},{4,6},{5,7},{6,4},{7,5},{8,10},{9,11},{10,... | collective-permute-start | bytes 442376 | tf_op jit(solution)/shard_map/ppermute | solution.py:50
  27.7 3.1 %collective-permute-start.3 = (bf16[576,128]{1,0:T(8,128)(2,1)}, bf16[576,128]{1,0:T(8,128)(2,1)S(1)}, u32[]{:S(2)}, u32[]{:S(2)}) collective-permute-start(bf16[576,128]{1,0:T(8,128)(2,1)} %get-tuple-element.32), channel_id=1, source_target_pairs={{0,3},{1,0},{2,1},{3,2},{4,7},{5,4},{6,5},{7,6},{8,11},{9,8},{10,9... | collective-permute-start | bytes 442376 | tf_op jit(solution)/shard_map/ppermute | solution.py:50
  30.8 0.0 copy-start.3
  30.8 1.0 copy-done.3
  31.8 0.7 shard_map.195.refs_0_
  32.5 0.4 collective-permute-done.2.refs_2_
  32.9 1.4 collective-permute-done.3.refs_3_
  34.3 1.5 lift.1
  35.8 20.0 %all_to_all.35.got_ref = bf16[4,96,512]{2,1,0:T(8,128)(2,1)S(1)} all-to-all(bf16[4,96,512]{2,1,0:T(8,128)(2,1)S(1)} %lift.1), channel_id=1, replica_groups=mesh['zh'=4,'zl'=4,'c'=2,'y'=4,'x'=4] {'y'}, dimensions={0} | all-to-all | bytes 786432 | tf_op jit(solution)/shard_map/all_to_all | solution.py:31
  55.8 0.2 shard_map.197
  56.0 0.0 copy-start.5
  56.0 0.0 copy-start.7
  56.0 26.9 %all_to_all.36 = bf16[16,96,512]{2,1,0:T(8,128)(2,1)S(1)} all-to-all(bf16[16,96,512]{2,1,0:T(8,128)(2,1)S(1)} %shard_map.197), channel_id=1, replica_groups=mesh['zh'=4,'zl'=4,'c'=2,'y'=4,'x'=4] {'y','x'}, dimensions={0} | all-to-all | bytes 3145728 | tf_op jit(solution)/shard_map/all_to_all | solution.py:31
  82.9 1.4 contract.1
  84.3 0.0 copy-start.8
  84.3 0.0 copy-start.9
  84.3 13.2 %all_to_all.37.got_ref = bf16[8,32,384]{2,1,0:T(8,128)(2,1)S(1)} all-to-all(bf16[8,32,384]{2,1,0:T(8,128)(2,1)S(1)} %contract.1), channel_id=1, replica_groups=mesh['zh'=4,'zl'=4,'c'=2,'y'=4,'x'=4] {'zl','c'}, dimensions={0} | all-to-all | bytes 393216 | tf_op jit(solution)/shard_map/all_to_all | solution.py:31
  97.6 0.7 shard_map.198
  98.3 11.1 %all-to-all-start.4 = ((bf16[4,32,384]{2,1,0:T(8,128)(2,1)}), bf16[4,32,384]{2,1,0:T(8,128)(2,1)S(1)}, u32[]{:S(2)}, u32[]{:S(2)}) async-start(bf16[4,32,384]{2,1,0:T(8,128)(2,1)} %shard_map.198), calls=%async_computation.4 | async-start | bytes 196608 | tf_op jit(solution)/shard_map/all_to_all | solution.py:31
  109.4 12.1 %collective-permute-start.7 = (bf16[1,160,128]{2,1,0:T(8,128)(2,1)S(1)}, bf16[1,160,128]{2,1,0:T(8,128)(2,1)S(1)}, u32[]{:S(2)}, u32[]{:S(2)}) collective-permute-start(bf16[1,160,128]{2,1,0:T(8,128)(2,1)S(1)} %bitcast.6), channel_id=1, source_target_pairs={{0,256},{32,288},{64,320},{96,352},{128,384},{160,416},{192,448},{... | collective-permute-start | bytes 122888 | tf_op jit(solution)/shard_map/ppermute | solution.py:50
  121.5 2.0 %collective-permute-done.7 = bf16[1,160,128]{2,1,0:T(8,128)(2,1)S(1)} collective-permute-done((bf16[1,160,128]{2,1,0:T(8,128)(2,1)S(1)}, bf16[1,160,128]{2,1,0:T(8,128)(2,1)S(1)}, u32[]{:S(2)}, u32[]{:S(2)}) %collective-permute-start.7) | collective-permute-done | bytes 40992 | tf_op jit(solution)/shard_map/ppermute | solution.py:50
  123.5 7.4 %collective-permute-start.8 = (bf16[2,160,128]{2,1,0:T(8,128)(2,1)S(1)}, bf16[2,160,128]{2,1,0:T(8,128)(2,1)S(1)}, u32[]{:S(2)}, u32[]{:S(2)}) collective-permute-start(bf16[2,160,128]{2,1,0:T(8,128)(2,1)S(1)} %pad_maximum_fusion.2), channel_id=1, source_target_pairs={{0,128},{32,160},{64,192},{96,224},{128,256},{160,288},{192,320},{... | collective-permute-start | bytes 245768 | tf_op jit(solution)/shard_map/ppermute | solution.py:50
  130.9 0.7 shard_map.199
  131.6 6.8 %all-to-all-start.5 = ((bf16[8,32,384]{2,1,0:T(8,128)(2,1)}), bf16[8,32,384]{2,1,0:T(8,128)(2,1)S(1)}, u32[]{:S(2)}, u32[]{:S(2)}) async-start(bf16[8,32,384]{2,1,0:T(8,128)(2,1)} %shard_map.199), calls=%async_computation.5 | async-start | bytes 393216 | tf_op jit(solution)/shard_map/all_to_all | solution.py:31
  138.4 1.9 %collective-permute-start.4 = (bf16[8,96,256]{2,1,0:T(8,128)(2,1)}, bf16[8,96,256]{2,1,0:T(8,128)(2,1)S(1)}, u32[]{:S(2)}, u32[]{:S(2)}) collective-permute-start(bf16[8,96,256]{2,1,0:T(8,128)(2,1)} %all-to-all-done.blocks_ref.b0), channel_id=1, source_target_pairs={{0,4},{4,8},{8,12},{12,0},{1,5},{5,9},{9,13},{13,1},{2,6},{6,10},{... | collective-permute-start | bytes 1179656 | tf_op jit(solution)/shard_map/ppermute | solution.py:50
  140.3 2.0 %collective-permute-start.9 = (bf16[4,160,128]{2,1,0:T(8,128)(2,1)S(1)}, bf16[4,160,128]{2,1,0:T(8,128)(2,1)S(1)}, u32[]{:S(2)}, u32[]{:S(2)}) collective-permute-start(bf16[4,160,128]{2,1,0:T(8,128)(2,1)S(1)} %pad_maximum_fusion.1), channel_id=1, source_target_pairs={{0,16},{16,0},{1,17},{17,1},{2,18},{18,2},{3,19},{19,3},{4,20},{20... | collective-permute-start | bytes 491528 | tf_op jit(solution)/shard_map/ppermute | solution.py:50
  142.4 3.9 %collective-permute-start.5 = (bf16[8,96,256]{2,1,0:T(8,128)(2,1)}, bf16[8,96,256]{2,1,0:T(8,128)(2,1)S(1)}, u32[]{:S(2)}, u32[]{:S(2)}) collective-permute-start(bf16[8,96,256]{2,1,0:T(8,128)(2,1)} %all-to-all-done.blocks_ref.b0), channel_id=1, source_target_pairs={{0,8},{4,12},{8,0},{12,4},{1,9},{5,13},{9,1},{13,5},{2,10},{6,14},... | collective-permute-start | bytes 1179656 | tf_op jit(solution)/shard_map/ppermute | solution.py:50
  146.3 2.8 %collective-permute-start.6 = (bf16[8,96,256]{2,1,0:T(8,128)(2,1)}, bf16[8,96,256]{2,1,0:T(8,128)(2,1)S(1)}, u32[]{:S(2)}, u32[]{:S(2)}) collective-permute-start(bf16[8,96,256]{2,1,0:T(8,128)(2,1)} %all-to-all-done.blocks_ref.b0), channel_id=1, source_target_pairs={{0,12},{4,0},{8,4},{12,8},{1,13},{5,1},{9,5},{13,9},{2,14},{6,2},{... | collective-permute-start | bytes 1179656 | tf_op jit(solution)/shard_map/ppermute | solution.py:50
  149.2 3.5 %collective-permute-start.10 = (bf16[8,160,128]{2,1,0:T(8,128)(2,1)S(1)}, bf16[8,160,128]{2,1,0:T(8,128)(2,1)S(1)}, u32[]{:S(2)}, u32[]{:S(2)}) collective-permute-start(bf16[8,160,128]{2,1,0:T(8,128)(2,1)S(1)} %pad_maximum_fusion.h0), channel_id=1, source_target_pairs={{0,32},{32,64},{64,96},{96,128},{128,160},{160,192},{192,224},{224... | collective-permute-start | bytes 983048 | tf_op jit(solution)/shard_map/ppermute | solution.py:50
  152.8 4.0 %collective-permute-start.11 = (bf16[8,160,128]{2,1,0:T(8,128)(2,1)S(1)}, bf16[8,160,128]{2,1,0:T(8,128)(2,1)S(1)}, u32[]{:S(2)}, u32[]{:S(2)}) collective-permute-start(bf16[8,160,128]{2,1,0:T(8,128)(2,1)S(1)} %pad_maximum_fusion.h0), channel_id=1, source_target_pairs={{0,64},{32,96},{64,128},{96,160},{128,192},{160,224},{192,256},{22... | collective-permute-start | bytes 983048 | tf_op jit(solution)/shard_map/ppermute | solution.py:50
  156.8 3.9 %collective-permute-done.4.b1 = bf16[8,96,256]{2,1,0:T(8,128)(2,1)S(1)} collective-permute-done((bf16[8,96,256]{2,1,0:T(8,128)(2,1)}, bf16[8,96,256]{2,1,0:T(8,128)(2,1)S(1)}, u32[]{:S(2)}, u32[]{:S(2)}) %collective-permute-start.4) | collective-permute-done | bytes 393248 | tf_op jit(solution)/shard_map/ppermute | solution.py:50
  160.7 1.9 %collective-permute-start.12 = (bf16[8,160,128]{2,1,0:T(8,128)(2,1)S(1)}, bf16[8,160,128]{2,1,0:T(8,128)(2,1)S(1)}, u32[]{:S(2)}, u32[]{:S(2)}) collective-permute-start(bf16[8,160,128]{2,1,0:T(8,128)(2,1)S(1)} %pad_maximum_fusion.h0), channel_id=1, source_target_pairs={{0,480},{32,0},{64,32},{96,64},{128,96},{160,128},{192,160},{224,1... | collective-permute-start | bytes 983048 | tf_op jit(solution)/shard_map/ppermute | solution.py:50
  162.6 3.0 %collective-permute-done.6.b3 = bf16[8,96,256]{2,1,0:T(8,128)(2,1)S(1)} collective-permute-done((bf16[8,96,256]{2,1,0:T(8,128)(2,1)}, bf16[8,96,256]{2,1,0:T(8,128)(2,1)S(1)}, u32[]{:S(2)}, u32[]{:S(2)}) %collective-permute-start.6) | collective-permute-done | bytes 393248 | tf_op jit(solution)/shard_map/ppermute | solution.py:50
  165.6 2.6 %directions.1 = (f32[256,256]{1,0:T(8,128)}, f32[256,256]{1,0:T(8,128)}, f32[256,128]{1,0:T(8,128)}, f32[256,128]{1,0:T(8,128)}, f32[16,8,128]{2,1,0:T(8,128)}) custom-call(bf16[8,32,384]{2,1,0:T(8,128)(2,1)S(1)} %all-to-all-done.5.got_ref, f32[256,256]{1,0:T(8,128)S(1)} %copy-done.8, f32[256,256]{1,0:T(8,128)S(1)} %copy-done.9, f32[256,128]{1,0:T(8,128)S(1)} %copy-done.12, ...), custom_call_target="tpu_custom_call" | custom-call | flops 400000000 | bytes 4000000 | tf_op jit(solution)/shard_map/directions/pallas_call | solution.py:261
  168.2 4.4 %all-to-all-start.6 = ((f32[16,8,128]{2,1,0:T(8,128)}), f32[16,8,128]{2,1,0:T(8,128)}, u32[]{:S(2)}, u32[]{:S(2)}) async-start(f32[16,8,128]{2,1,0:T(8,128)} %get-tuple-element.33), calls=%async_computation.6 | async-start | bytes 131072 | tf_op jit(solution)/shard_map/all_to_all | solution.py:31
  172.7 0.3 arrange.1
  173.1 1.0 copy-done.4
  174.0 0.7 copy-done.11
  174.7 3.4 %ready.1 = (f32[64,256]{1,0:T(8,128)}, f32[32,128]{1,0:T(8,128)}, bf16[2048,256]{1,0:T(8,128)(2,1)}, bf16[1024,128]{1,0:T(8,128)(2,1)}) custom-call(f32[256,256]{1,0:T(8,128)} %get-tuple-element.23.mean_o, f32[256,256]{1,0:T(8,128)} %get-tuple-element.24.square_o, f32[256,128]{1,0:T(8,128)} %get-tuple-element.28.mean_v, ...), custom_call_target="tpu_custom_call" | custom-call | flops 400000000 | bytes 4000000 | tf_op jit(solution)/shard_map/ready/pallas_call | solution.py:339
  178.1 1.1 all-to-all-done.6.total_ref
  179.3 3.8 %outputs.1 = (f32[64,256]{1,0:T(8,128)}, f32[64,256]{1,0:T(8,128)}, bf16[2048,256]{1,0:T(8,128)(2,1)}, f32[32,128]{1,0:T(8,128)}, f32[32,128]{1,0:T(8,128)}, /*index=5*/bf16[1024,128]{1,0:T(8,128)(2,1)}) custom-call(f32[16,8,128]{2,1,0:T(8,128)} %all-to-all-done.6.total_ref, f32[64,256]{1,0:T(8,128)} %weight_o.3, f32[32,128]{1,0:T(8,128)} %weight_v.3, ...), custom_call_target="tpu_custom_call" | custom-call | flops 10000000 | bytes 4000000 | tf_op jit(solution)/shard_map/outputs/pallas_call | solution.py:400
  (36 shorter events, 0.1 us)
Async XLA Ops:
  0.6 30.2 %copy-start.6 = (bf16[1536,64]{0,1:T(8,128)(2,1)S(1)}, bf16[1536,64]{0,1:T(8,128)(2,1)}, u32[]{:S(2)}) copy-start(bf16[1536,64]{0,1:T(8,128)(2,1)} %param.14) | copy-start | bytes 589828
  1.5 0.7 collective-permute-start
  2.9 31.4 %all-to-all-start = ((bf16[8,96,256]{2,1,0:T(8,128)(2,1)}), bf16[8,96,256]{2,1,0:T(8,128)(2,1)}, u32[]{:S(2)}, u32[]{:S(2)}) async-start(bf16[8,96,256]{2,1,0:T(8,128)(2,1)} %broadcast_in_dim.4), calls=%async_computation | async-start | bytes 786432 | tf_op jit(solution)/shard_map/all_to_all | solution.py:31
  20.1 12.4 %collective-permute-start.1 = (bf16[576,128]{1,0:T(8,128)(2,1)}, bf16[576,128]{1,0:T(8,128)(2,1)S(1)}, u32[]{:S(2)}, u32[]{:S(2)}) collective-permute-start(bf16[576,128]{1,0:T(8,128)(2,1)} %get-tuple-element.30), channel_id=1, source_target_pairs={{0,1},{1,2},{2,3},{3,0},{4,5},{5,6},{6,7},{7,4},{8,9},{9,10},{10,1... | collective-permute-start | bytes 442376 | tf_op jit(solution)/shard_map/ppermute | solution.py:50
  23.4 9.5 %collective-permute-start.2 = (bf16[576,128]{1,0:T(8,128)(2,1)}, bf16[576,128]{1,0:T(8,128)(2,1)S(1)}, u32[]{:S(2)}, u32[]{:S(2)}) collective-permute-start(bf16[576,128]{1,0:T(8,128)(2,1)} %get-tuple-element.31), channel_id=1, source_target_pairs={{0,2},{1,3},{2,0},{3,1},{4,6},{5,7},{6,4},{7,5},{8,10},{9,11},{10,... | collective-permute-start | bytes 442376 | tf_op jit(solution)/shard_map/ppermute | solution.py:50
  27.7 6.6 %collective-permute-start.3 = (bf16[576,128]{1,0:T(8,128)(2,1)}, bf16[576,128]{1,0:T(8,128)(2,1)S(1)}, u32[]{:S(2)}, u32[]{:S(2)}) collective-permute-start(bf16[576,128]{1,0:T(8,128)(2,1)} %get-tuple-element.32), channel_id=1, source_target_pairs={{0,3},{1,0},{2,1},{3,2},{4,7},{5,4},{6,5},{7,6},{8,11},{9,8},{10,9... | collective-permute-start | bytes 442376 | tf_op jit(solution)/shard_map/ppermute | solution.py:50
  30.8 1.0 copy-start.3
  56.0 27.0 %copy-start.5 = (bf16[1536,256]{1,0:T(8,128)(2,1)S(1)}, bf16[1536,256]{1,0:T(8,128)(2,1)}, u32[]{:S(2)}) copy-start(bf16[1536,256]{1,0:T(8,128)(2,1)} %cot_o.1) | copy-start | bytes 2359300
  56.0 26.9 %copy-start.7 = (bf16[1536,128]{1,0:T(8,128)(2,1)S(1)}, bf16[1536,128]{1,0:T(8,128)(2,1)}, u32[]{:S(2)}) copy-start(bf16[1536,128]{1,0:T(8,128)(2,1)} %cot_v.1) | copy-start | bytes 1179652
  82.9 26.5 %copy-start.10 = (f32[64,256]{1,0:T(8,128)S(1)}, f32[64,256]{1,0:T(8,128)}, u32[]{:S(2)}) copy-start(f32[64,256]{1,0:T(8,128)} %weight_o.3) | copy-start | bytes 196612
  82.9 26.5 %copy-start.14 = (f32[32,128]{1,0:T(8,128)S(1)}, f32[32,128]{1,0:T(8,128)}, u32[]{:S(2)}) copy-start(f32[32,128]{1,0:T(8,128)} %weight_v.3) | copy-start | bytes 49156
  84.3 81.3 %copy-start.8 = (f32[256,256]{1,0:T(8,128)S(1)}, f32[256,256]{1,0:T(8,128)}, u32[]{:S(2)}) copy-start(f32[256,256]{1,0:T(8,128)} %mean_o.1) | copy-start | bytes 786436
  84.3 81.3 %copy-start.9 = (f32[256,256]{1,0:T(8,128)S(1)}, f32[256,256]{1,0:T(8,128)}, u32[]{:S(2)}) copy-start(f32[256,256]{1,0:T(8,128)} %square_o.1) | copy-start | bytes 786436
  84.3 81.3 %copy-start.12 = (f32[256,128]{1,0:T(8,128)S(1)}, f32[256,128]{1,0:T(8,128)}, u32[]{:S(2)}) copy-start(f32[256,128]{1,0:T(8,128)} %mean_v.1) | copy-start | bytes 393220
  84.3 81.3 %copy-start.13 = (f32[256,128]{1,0:T(8,128)S(1)}, f32[256,128]{1,0:T(8,128)}, u32[]{:S(2)}) copy-start(f32[256,128]{1,0:T(8,128)} %square_v.1) | copy-start | bytes 393220
  98.3 32.7 %all-to-all-start.4 = ((bf16[4,32,384]{2,1,0:T(8,128)(2,1)}), bf16[4,32,384]{2,1,0:T(8,128)(2,1)S(1)}, u32[]{:S(2)}, u32[]{:S(2)}) async-start(bf16[4,32,384]{2,1,0:T(8,128)(2,1)} %shard_map.198), calls=%async_computation.4 | async-start | bytes 196608 | tf_op jit(solution)/shard_map/all_to_all | solution.py:31
  109.4 14.1 %collective-permute-start.7 = (bf16[1,160,128]{2,1,0:T(8,128)(2,1)S(1)}, bf16[1,160,128]{2,1,0:T(8,128)(2,1)S(1)}, u32[]{:S(2)}, u32[]{:S(2)}) collective-permute-start(bf16[1,160,128]{2,1,0:T(8,128)(2,1)S(1)} %bitcast.6), channel_id=1, source_target_pairs={{0,256},{32,288},{64,320},{96,352},{128,384},{160,416},{192,448},{... | collective-permute-start | bytes 122888 | tf_op jit(solution)/shard_map/ppermute | solution.py:50
  123.5 16.8 %collective-permute-start.8 = (bf16[2,160,128]{2,1,0:T(8,128)(2,1)S(1)}, bf16[2,160,128]{2,1,0:T(8,128)(2,1)S(1)}, u32[]{:S(2)}, u32[]{:S(2)}) collective-permute-start(bf16[2,160,128]{2,1,0:T(8,128)(2,1)S(1)} %pad_maximum_fusion.2), channel_id=1, source_target_pairs={{0,128},{32,160},{64,192},{96,224},{128,256},{160,288},{192,320},{... | collective-permute-start | bytes 245768 | tf_op jit(solution)/shard_map/ppermute | solution.py:50
  131.6 33.9 %all-to-all-start.5 = ((bf16[8,32,384]{2,1,0:T(8,128)(2,1)}), bf16[8,32,384]{2,1,0:T(8,128)(2,1)S(1)}, u32[]{:S(2)}, u32[]{:S(2)}) async-start(bf16[8,32,384]{2,1,0:T(8,128)(2,1)} %shard_map.199), calls=%async_computation.5 | async-start | bytes 393216 | tf_op jit(solution)/shard_map/all_to_all | solution.py:31
  138.4 22.3 %collective-permute-start.4 = (bf16[8,96,256]{2,1,0:T(8,128)(2,1)}, bf16[8,96,256]{2,1,0:T(8,128)(2,1)S(1)}, u32[]{:S(2)}, u32[]{:S(2)}) collective-permute-start(bf16[8,96,256]{2,1,0:T(8,128)(2,1)} %all-to-all-done.blocks_ref.b0), channel_id=1, source_target_pairs={{0,4},{4,8},{8,12},{12,0},{1,5},{5,9},{9,13},{13,1},{2,6},{6,10},{... | collective-permute-start | bytes 1179656 | tf_op jit(solution)/shard_map/ppermute | solution.py:50
  140.3 8.8 %collective-permute-start.9 = (bf16[4,160,128]{2,1,0:T(8,128)(2,1)S(1)}, bf16[4,160,128]{2,1,0:T(8,128)(2,1)S(1)}, u32[]{:S(2)}, u32[]{:S(2)}) collective-permute-start(bf16[4,160,128]{2,1,0:T(8,128)(2,1)S(1)} %pad_maximum_fusion.1), channel_id=1, source_target_pairs={{0,16},{16,0},{1,17},{17,1},{2,18},{18,2},{3,19},{19,3},{4,20},{20... | collective-permute-start | bytes 491528 | tf_op jit(solution)/shard_map/ppermute | solution.py:50
  142.4 20.2 %collective-permute-start.5 = (bf16[8,96,256]{2,1,0:T(8,128)(2,1)}, bf16[8,96,256]{2,1,0:T(8,128)(2,1)S(1)}, u32[]{:S(2)}, u32[]{:S(2)}) collective-permute-start(bf16[8,96,256]{2,1,0:T(8,128)(2,1)} %all-to-all-done.blocks_ref.b0), channel_id=1, source_target_pairs={{0,8},{4,12},{8,0},{12,4},{1,9},{5,13},{9,1},{13,5},{2,10},{6,14},... | collective-permute-start | bytes 1179656 | tf_op jit(solution)/shard_map/ppermute | solution.py:50
  146.3 19.2 %collective-permute-start.6 = (bf16[8,96,256]{2,1,0:T(8,128)(2,1)}, bf16[8,96,256]{2,1,0:T(8,128)(2,1)S(1)}, u32[]{:S(2)}, u32[]{:S(2)}) collective-permute-start(bf16[8,96,256]{2,1,0:T(8,128)(2,1)} %all-to-all-done.blocks_ref.b0), channel_id=1, source_target_pairs={{0,12},{4,0},{8,4},{12,8},{1,13},{5,1},{9,5},{13,9},{2,14},{6,2},{... | collective-permute-start | bytes 1179656 | tf_op jit(solution)/shard_map/ppermute | solution.py:50
  149.2 23.5 %collective-permute-start.10 = (bf16[8,160,128]{2,1,0:T(8,128)(2,1)S(1)}, bf16[8,160,128]{2,1,0:T(8,128)(2,1)S(1)}, u32[]{:S(2)}, u32[]{:S(2)}) collective-permute-start(bf16[8,160,128]{2,1,0:T(8,128)(2,1)S(1)} %pad_maximum_fusion.h0), channel_id=1, source_target_pairs={{0,32},{32,64},{64,96},{96,128},{128,160},{160,192},{192,224},{224... | collective-permute-start | bytes 983048 | tf_op jit(solution)/shard_map/ppermute | solution.py:50
  152.8 19.9 %collective-permute-start.11 = (bf16[8,160,128]{2,1,0:T(8,128)(2,1)S(1)}, bf16[8,160,128]{2,1,0:T(8,128)(2,1)S(1)}, u32[]{:S(2)}, u32[]{:S(2)}) collective-permute-start(bf16[8,160,128]{2,1,0:T(8,128)(2,1)S(1)} %pad_maximum_fusion.h0), channel_id=1, source_target_pairs={{0,64},{32,96},{64,128},{96,160},{128,192},{160,224},{192,256},{22... | collective-permute-start | bytes 983048 | tf_op jit(solution)/shard_map/ppermute | solution.py:50
  160.7 12.3 %copy-start = (bf16[8,96,256]{2,1,0:T(8,128)(2,1)}, bf16[8,96,256]{2,1,0:T(8,128)(2,1)S(1)}, u32[]{:S(2)}) copy-start(bf16[8,96,256]{2,1,0:T(8,128)(2,1)S(1)} %collective-permute-done.4.b1) | copy-start | bytes 1179652
  160.7 12.0 %collective-permute-start.12 = (bf16[8,160,128]{2,1,0:T(8,128)(2,1)S(1)}, bf16[8,160,128]{2,1,0:T(8,128)(2,1)S(1)}, u32[]{:S(2)}, u32[]{:S(2)}) collective-permute-start(bf16[8,160,128]{2,1,0:T(8,128)(2,1)S(1)} %pad_maximum_fusion.h0), channel_id=1, source_target_pairs={{0,480},{32,0},{64,32},{96,64},{128,96},{160,128},{192,160},{224,1... | collective-permute-start | bytes 983048 | tf_op jit(solution)/shard_map/ppermute | solution.py:50
  162.6 10.4 %copy-start.1 = (bf16[8,96,256]{2,1,0:T(8,128)(2,1)}, bf16[8,96,256]{2,1,0:T(8,128)(2,1)S(1)}, u32[]{:S(2)}) copy-start(bf16[8,96,256]{2,1,0:T(8,128)(2,1)S(1)} %collective-permute-done.5.b2) | copy-start | bytes 1179652
  165.6 7.5 %copy-start.2 = (bf16[8,96,256]{2,1,0:T(8,128)(2,1)}, bf16[8,96,256]{2,1,0:T(8,128)(2,1)S(1)}, u32[]{:S(2)}) copy-start(bf16[8,96,256]{2,1,0:T(8,128)(2,1)S(1)} %collective-permute-done.6.b3) | copy-start | bytes 1179652
  168.2 11.0 %all-to-all-start.6 = ((f32[16,8,128]{2,1,0:T(8,128)}), f32[16,8,128]{2,1,0:T(8,128)}, u32[]{:S(2)}, u32[]{:S(2)}) async-start(f32[16,8,128]{2,1,0:T(8,128)} %get-tuple-element.33), calls=%async_computation.6 | async-start | bytes 131072 | tf_op jit(solution)/shard_map/all_to_all | solution.py:31
  173.0 1.0 copy-start.4
  174.0 0.7 copy-start.11

commit v11 on v10

--- a/solution.py
+++ b/solution.py
@@ -171,50 +171,23 @@
     )(got)
 
 
-def contract_kernel(lifted_ref, cot_o, cot_v, out_ref, total_o, total_v):
-    step = pl.program_id(0)
-    rank = total_o.shape[0]
+def contract_kernel(lifted_ref, cot_o, cot_v, out_ref):
+    rank = lifted_ref.shape[1] // 2
+    cols_o = cot_o.shape[1]
     dims = (((0,), (0,)), ((), ()))
-
-    def term(side, cot):
-        rows = lifted_ref[:, side * rank : (side + 1) * rank]
-        return lax.dot_general(rows, cot[...], dims, preferred_element_type=F32)
-
-    @pl.when(step == 0)
-    def _():
-        total_o[...] = term(0, cot_o)
-        total_v[...] = term(1, cot_v)
-
-    @pl.when(step > 0)
-    def _():
-        total_o[...] += term(0, cot_o)
-        total_v[...] += term(1, cot_v)
-
-    @pl.when(step == pl.num_programs(0) - 1)
-    def _():
-        cols_o = total_o.shape[1]
-        parts, each, _ = out_ref.shape
-        for p in range(parts):
-            out_ref[p, :, :cols_o] = total_o[p * each : (p + 1) * each].astype(BF)
-            out_ref[p, :, cols_o:] = total_v[p * each : (p + 1) * each].astype(BF)
-
-
-def contract(lifted, cot_o, cot_v, parts, steps):
-    tokens, both = lifted.shape
-    rank, cols_o, cols_v = both // 2, cot_o.shape[1], cot_v.shape[1]
-    rows = tokens // steps
-    shape = (parts, rank // parts, cols_o + cols_v)
+    total_o = lax.dot_general(lifted_ref[:, :rank], cot_o[...], dims, preferred_element_type=F32)
+    total_v = lax.dot_general(lifted_ref[:, rank:], cot_v[...], dims, preferred_element_type=F32)
+    parts, each, _ = out_ref.shape
+    for p in range(parts):
+        out_ref[p, :, :cols_o] = total_o[p * each : (p + 1) * each].astype(BF)
+        out_ref[p, :, cols_o:] = total_v[p * each : (p + 1) * each].astype(BF)
+
+
+def contract(lifted, cot_o, cot_v, parts):
+    rank = lifted.shape[1] // 2
     return pl.pallas_call(
         contract_kernel,
-        grid=(steps,),
-        in_specs=[
-            pl.BlockSpec((rows, both), lambda i: (i, 0)),
-            pl.BlockSpec((rows, cols_o), lambda i: (i, 0)),
-            pl.BlockSpec((rows, cols_v), lambda i: (i, 0)),
-        ],
-        out_specs=pl.BlockSpec(shape, lambda i: (0, 0, 0)),
-        out_shape=jax.ShapeDtypeStruct(shape, BF),
-        scratch_shapes=[pltpu.VMEM((rank, cols_o), F32), pltpu.VMEM((rank, cols_v), F32)],
+        out_shape=jax.ShapeDtypeStruct((parts, rank // parts, cot_o.shape[1] + cot_v.shape[1]), BF),
         cost_estimate=pl.CostEstimate(flops=3 * 10**8, bytes_accessed=3 * 10**6, transcendentals=0),
         compiler_params=pltpu.CompilerParams(vmem_limit_bytes=ROOM),
         name="contract",
@@ -464,7 +437,7 @@
     lifted = exchange(lifted, TP).reshape(tokens, 2 * rank)
 
     near = lax.axis_size(NEAR)
-    part = contract(lifted, out_cot, value_cot, near, 4)
+    part = contract(lifted, out_cot, value_cot, near)
     part = exchange(part, NEAR)
     part = exchange(summed_for(part, lax.axis_size("zh"), BF), "zh")
     proj = exchange(summed_for(part, near, BF), NEAR)

time: 185 us -> 184 us (level)
  no operation moved by 1% of the time
where the time goes in v11:
time: 184 us; the launch traced here: 182 us
  starting transfers between devices  88.5 us (48%)
  blocking collectives  60.1 us (33%)
  Pallas kernels  16.5 us (9%)
  waiting for transfers between devices  11.8 us (6%)
  local copies, waits for them, and re-layouts  3.48 us (2%)
    all_to_all x3, blocking collectives, exchange(): return lax.all_to_all(value, axes, 0, 0, tiled=True)  60.1 us
    ppermute x12, starting transfers between devices, shifted(): lax.ppermute(value, axis, [(i, (i + by) % devices) for i in range(devices)])  50.3 us
    all_to_all x4, starting transfers between devices, exchange(): return lax.all_to_all(value, axes, 0, 0, tiled=True)  37.6 us
    ppermute x12, waiting for transfers between devices, shifted(): lax.ppermute(value, axis, [(i, (i + by) % devices) for i in range(devices)])  10.6 us
    pallas_call x1, Pallas kernels, outputs(): pl.pallas_call(functools.partial(output_kernel, counts, pieces), in_specs...  3.82 us
  transfers between devices with their start and end apart: 17, of which 6 were waited for; matrix products, arithmetic and copies ran while one was open for 0% of the time, Pallas kernels for 5%

profile of v11, /device:TPU:1, one launch (start us, length us, event | category | flops | bytes accessed | tf_op | source)
XLA Modules:
  0.0 182.3 jit_solution(18349122604165369909)
XLA Ops:
  0.6 0.0 copy-start.6
  0.7 0.8 pad_maximum_fusion.3
  1.5 0.7 collective-permute-start
  2.1 0.8 broadcast_in_dim.4
  2.9 15.3 %all-to-all-start = ((bf16[8,96,256]{2,1,0:T(8,128)(2,1)}), bf16[8,96,256]{2,1,0:T(8,128)(2,1)}, u32[]{:S(2)}, u32[]{:S(2)}) async-start(bf16[8,96,256]{2,1,0:T(8,128)(2,1)} %broadcast_in_dim.4), calls=%async_computation | async-start | bytes 786432 | tf_op jit(solution)/shard_map/all_to_all | solution.py:31
  18.2 2.0 %shard_map.196 = (bf16[576,128]{1,0:T(8,128)(2,1)}, bf16[576,128]{1,0:T(8,128)(2,1)}, bf16[576,128]{1,0:T(8,128)(2,1)}) custom-call(bf16[1536,128]{1,0:T(8,128)(2,1)} %attn_ref.3, bf16[64,1536]{1,0:T(8,128)(2,1)} %bitcast.4), custom_call_target="tpu_custom_call" | custom-call | flops 10000000 | bytes 1000000 | tf_op jit(solution)/shard_map/pallas_call | solution.py:86
  20.1 3.3 %collective-permute-start.1 = (bf16[576,128]{1,0:T(8,128)(2,1)}, bf16[576,128]{1,0:T(8,128)(2,1)S(1)}, u32[]{:S(2)}, u32[]{:S(2)}) collective-permute-start(bf16[576,128]{1,0:T(8,128)(2,1)} %get-tuple-element.30), channel_id=1, source_target_pairs={{0,1},{1,2},{2,3},{3,0},{4,5},{5,6},{6,7},{7,4},{8,9},{9,10},{10,1... | collective-permute-start | bytes 442376 | tf_op jit(solution)/shard_map/ppermute | solution.py:50
  23.4 4.3 %collective-permute-start.2 = (bf16[576,128]{1,0:T(8,128)(2,1)}, bf16[576,128]{1,0:T(8,128)(2,1)S(1)}, u32[]{:S(2)}, u32[]{:S(2)}) collective-permute-start(bf16[576,128]{1,0:T(8,128)(2,1)} %get-tuple-element.31), channel_id=1, source_target_pairs={{0,2},{1,3},{2,0},{3,1},{4,6},{5,7},{6,4},{7,5},{8,10},{9,11},{10,... | collective-permute-start | bytes 442376 | tf_op jit(solution)/shard_map/ppermute | solution.py:50
  27.7 3.1 %collective-permute-start.3 = (bf16[576,128]{1,0:T(8,128)(2,1)}, bf16[576,128]{1,0:T(8,128)(2,1)S(1)}, u32[]{:S(2)}, u32[]{:S(2)}) collective-permute-start(bf16[576,128]{1,0:T(8,128)(2,1)} %get-tuple-element.32), channel_id=1, source_target_pairs={{0,3},{1,0},{2,1},{3,2},{4,7},{5,4},{6,5},{7,6},{8,11},{9,8},{10,9... | collective-permute-start | bytes 442376 | tf_op jit(solution)/shard_map/ppermute | solution.py:50
  30.8 0.0 copy-start.3
  30.8 1.0 copy-done.3
  31.8 0.7 shard_map.195.refs_0_
  32.5 0.4 collective-permute-done.2.refs_2_
  32.9 1.4 collective-permute-done.3.refs_3_
  34.3 1.5 lift.1
  35.8 20.0 %all_to_all.35.got_ref = bf16[4,96,512]{2,1,0:T(8,128)(2,1)S(1)} all-to-all(bf16[4,96,512]{2,1,0:T(8,128)(2,1)S(1)} %lift.1), channel_id=1, replica_groups=mesh['zh'=4,'zl'=4,'c'=2,'y'=4,'x'=4] {'y'}, dimensions={0} | all-to-all | bytes 786432 | tf_op jit(solution)/shard_map/all_to_all | solution.py:31
  55.8 0.2 shard_map.197
  56.0 0.0 copy-start.5
  56.0 0.0 copy-start.7
  56.0 26.9 %all_to_all.36 = bf16[16,96,512]{2,1,0:T(8,128)(2,1)S(1)} all-to-all(bf16[16,96,512]{2,1,0:T(8,128)(2,1)S(1)} %shard_map.197), channel_id=1, replica_groups=mesh['zh'=4,'zl'=4,'c'=2,'y'=4,'x'=4] {'y','x'}, dimensions={0} | all-to-all | bytes 3145728 | tf_op jit(solution)/shard_map/all_to_all | solution.py:31
  82.9 0.6 contract.1
  83.5 0.0 copy-start.8
  83.6 0.0 copy-start.9
  83.6 13.2 %all_to_all.37.got_ref = bf16[8,32,384]{2,1,0:T(8,128)(2,1)S(1)} all-to-all(bf16[8,32,384]{2,1,0:T(8,128)(2,1)S(1)} %contract.1), channel_id=1, replica_groups=mesh['zh'=4,'zl'=4,'c'=2,'y'=4,'x'=4] {'zl','c'}, dimensions={0} | all-to-all | bytes 393216 | tf_op jit(solution)/shard_map/all_to_all | solution.py:31
  96.8 0.7 shard_map.198
  97.5 11.1 %all-to-all-start.4 = ((bf16[4,32,384]{2,1,0:T(8,128)(2,1)}), bf16[4,32,384]{2,1,0:T(8,128)(2,1)S(1)}, u32[]{:S(2)}, u32[]{:S(2)}) async-start(bf16[4,32,384]{2,1,0:T(8,128)(2,1)} %shard_map.198), calls=%async_computation.4 | async-start | bytes 196608 | tf_op jit(solution)/shard_map/all_to_all | solution.py:31
  108.7 12.1 %collective-permute-start.7 = (bf16[1,160,128]{2,1,0:T(8,128)(2,1)S(1)}, bf16[1,160,128]{2,1,0:T(8,128)(2,1)S(1)}, u32[]{:S(2)}, u32[]{:S(2)}) collective-permute-start(bf16[1,160,128]{2,1,0:T(8,128)(2,1)S(1)} %bitcast.6), channel_id=1, source_target_pairs={{0,256},{32,288},{64,320},{96,352},{128,384},{160,416},{192,448},{... | collective-permute-start | bytes 122888 | tf_op jit(solution)/shard_map/ppermute | solution.py:50
  120.8 2.0 %collective-permute-done.7 = bf16[1,160,128]{2,1,0:T(8,128)(2,1)S(1)} collective-permute-done((bf16[1,160,128]{2,1,0:T(8,128)(2,1)S(1)}, bf16[1,160,128]{2,1,0:T(8,128)(2,1)S(1)}, u32[]{:S(2)}, u32[]{:S(2)}) %collective-permute-start.7) | collective-permute-done | bytes 40992 | tf_op jit(solution)/shard_map/ppermute | solution.py:50
  122.8 7.4 %collective-permute-start.8 = (bf16[2,160,128]{2,1,0:T(8,128)(2,1)S(1)}, bf16[2,160,128]{2,1,0:T(8,128)(2,1)S(1)}, u32[]{:S(2)}, u32[]{:S(2)}) collective-permute-start(bf16[2,160,128]{2,1,0:T(8,128)(2,1)S(1)} %pad_maximum_fusion.2), channel_id=1, source_target_pairs={{0,128},{32,160},{64,192},{96,224},{128,256},{160,288},{192,320},{... | collective-permute-start | bytes 245768 | tf_op jit(solution)/shard_map/ppermute | solution.py:50
  130.2 0.7 shard_map.199
  130.9 6.8 %all-to-all-start.5 = ((bf16[8,32,384]{2,1,0:T(8,128)(2,1)}), bf16[8,32,384]{2,1,0:T(8,128)(2,1)S(1)}, u32[]{:S(2)}, u32[]{:S(2)}) async-start(bf16[8,32,384]{2,1,0:T(8,128)(2,1)} %shard_map.199), calls=%async_computation.5 | async-start | bytes 393216 | tf_op jit(solution)/shard_map/all_to_all | solution.py:31
  137.6 1.9 %collective-permute-start.4 = (bf16[8,96,256]{2,1,0:T(8,128)(2,1)}, bf16[8,96,256]{2,1,0:T(8,128)(2,1)S(1)}, u32[]{:S(2)}, u32[]{:S(2)}) collective-permute-start(bf16[8,96,256]{2,1,0:T(8,128)(2,1)} %all-to-all-done.blocks_ref.b0), channel_id=1, source_target_pairs={{0,4},{4,8},{8,12},{12,0},{1,5},{5,9},{9,13},{13,1},{2,6},{6,10},{... | collective-permute-start | bytes 1179656 | tf_op jit(solution)/shard_map/ppermute | solution.py:50
  139.6 2.0 %collective-permute-start.9 = (bf16[4,160,128]{2,1,0:T(8,128)(2,1)S(1)}, bf16[4,160,128]{2,1,0:T(8,128)(2,1)S(1)}, u32[]{:S(2)}, u32[]{:S(2)}) collective-permute-start(bf16[4,160,128]{2,1,0:T(8,128)(2,1)S(1)} %pad_maximum_fusion.1), channel_id=1, source_target_pairs={{0,16},{16,0},{1,17},{17,1},{2,18},{18,2},{3,19},{19,3},{4,20},{20... | collective-permute-start | bytes 491528 | tf_op jit(solution)/shard_map/ppermute | solution.py:50
  141.6 3.9 %collective-permute-start.5 = (bf16[8,96,256]{2,1,0:T(8,128)(2,1)}, bf16[8,96,256]{2,1,0:T(8,128)(2,1)S(1)}, u32[]{:S(2)}, u32[]{:S(2)}) collective-permute-start(bf16[8,96,256]{2,1,0:T(8,128)(2,1)} %all-to-all-done.blocks_ref.b0), channel_id=1, source_target_pairs={{0,8},{4,12},{8,0},{12,4},{1,9},{5,13},{9,1},{13,5},{2,10},{6,14},... | collective-permute-start | bytes 1179656 | tf_op jit(solution)/shard_map/ppermute | solution.py:50
  145.6 2.8 %collective-permute-start.6 = (bf16[8,96,256]{2,1,0:T(8,128)(2,1)}, bf16[8,96,256]{2,1,0:T(8,128)(2,1)S(1)}, u32[]{:S(2)}, u32[]{:S(2)}) collective-permute-start(bf16[8,96,256]{2,1,0:T(8,128)(2,1)} %all-to-all-done.blocks_ref.b0), channel_id=1, source_target_pairs={{0,12},{4,0},{8,4},{12,8},{1,13},{5,1},{9,5},{13,9},{2,14},{6,2},{... | collective-permute-start | bytes 1179656 | tf_op jit(solution)/shard_map/ppermute | solution.py:50
  148.5 3.5 %collective-permute-start.10 = (bf16[8,160,128]{2,1,0:T(8,128)(2,1)S(1)}, bf16[8,160,128]{2,1,0:T(8,128)(2,1)S(1)}, u32[]{:S(2)}, u32[]{:S(2)}) collective-permute-start(bf16[8,160,128]{2,1,0:T(8,128)(2,1)S(1)} %pad_maximum_fusion.h0), channel_id=1, source_target_pairs={{0,32},{32,64},{64,96},{96,128},{128,160},{160,192},{192,224},{224... | collective-permute-start | bytes 983048 | tf_op jit(solution)/shard_map/ppermute | solution.py:50
  152.0 4.0 %collective-permute-start.11 = (bf16[8,160,128]{2,1,0:T(8,128)(2,1)S(1)}, bf16[8,160,128]{2,1,0:T(8,128)(2,1)S(1)}, u32[]{:S(2)}, u32[]{:S(2)}) collective-permute-start(bf16[8,160,128]{2,1,0:T(8,128)(2,1)S(1)} %pad_maximum_fusion.h0), channel_id=1, source_target_pairs={{0,64},{32,96},{64,128},{96,160},{128,192},{160,224},{192,256},{22... | collective-permute-start | bytes 983048 | tf_op jit(solution)/shard_map/ppermute | solution.py:50
  156.0 3.9 %collective-permute-done.4.b1 = bf16[8,96,256]{2,1,0:T(8,128)(2,1)S(1)} collective-permute-done((bf16[8,96,256]{2,1,0:T(8,128)(2,1)}, bf16[8,96,256]{2,1,0:T(8,128)(2,1)S(1)}, u32[]{:S(2)}, u32[]{:S(2)}) %collective-permute-start.4) | collective-permute-done | bytes 393248 | tf_op jit(solution)/shard_map/ppermute | solution.py:50
  159.9 1.9 %collective-permute-start.12 = (bf16[8,160,128]{2,1,0:T(8,128)(2,1)S(1)}, bf16[8,160,128]{2,1,0:T(8,128)(2,1)S(1)}, u32[]{:S(2)}, u32[]{:S(2)}) collective-permute-start(bf16[8,160,128]{2,1,0:T(8,128)(2,1)S(1)} %pad_maximum_fusion.h0), channel_id=1, source_target_pairs={{0,480},{32,0},{64,32},{96,64},{128,96},{160,128},{192,160},{224,1... | collective-permute-start | bytes 983048 | tf_op jit(solution)/shard_map/ppermute | solution.py:50
  161.9 3.0 %collective-permute-done.6.b3 = bf16[8,96,256]{2,1,0:T(8,128)(2,1)S(1)} collective-permute-done((bf16[8,96,256]{2,1,0:T(8,128)(2,1)}, bf16[8,96,256]{2,1,0:T(8,128)(2,1)S(1)}, u32[]{:S(2)}, u32[]{:S(2)}) %collective-permute-start.6) | collective-permute-done | bytes 393248 | tf_op jit(solution)/shard_map/ppermute | solution.py:50
  164.9 2.6 %directions.1 = (f32[256,256]{1,0:T(8,128)}, f32[256,256]{1,0:T(8,128)}, f32[256,128]{1,0:T(8,128)}, f32[256,128]{1,0:T(8,128)}, f32[16,8,128]{2,1,0:T(8,128)}) custom-call(bf16[8,32,384]{2,1,0:T(8,128)(2,1)S(1)} %all-to-all-done.5.got_ref, f32[256,256]{1,0:T(8,128)S(1)} %copy-done.8, f32[256,256]{1,0:T(8,128)S(1)} %copy-done.9, f32[256,128]{1,0:T(8,128)S(1)} %copy-done.12, ...), custom_call_target="tpu_custom_call" | custom-call | flops 400000000 | bytes 4000000 | tf_op jit(solution)/shard_map/directions/pallas_call | solution.py:234
  167.5 4.4 %all-to-all-start.6 = ((f32[16,8,128]{2,1,0:T(8,128)}), f32[16,8,128]{2,1,0:T(8,128)}, u32[]{:S(2)}, u32[]{:S(2)}) async-start(f32[16,8,128]{2,1,0:T(8,128)} %get-tuple-element.33), calls=%async_computation.6 | async-start | bytes 131072 | tf_op jit(solution)/shard_map/all_to_all | solution.py:31
  172.0 0.3 arrange.1
  172.3 1.0 copy-done.4
  173.3 0.7 copy-done.11
  174.0 3.4 %ready.1 = (f32[64,256]{1,0:T(8,128)}, f32[32,128]{1,0:T(8,128)}, bf16[2048,256]{1,0:T(8,128)(2,1)}, bf16[1024,128]{1,0:T(8,128)(2,1)}) custom-call(f32[256,256]{1,0:T(8,128)} %get-tuple-element.23.mean_o, f32[256,256]{1,0:T(8,128)} %get-tuple-element.24.square_o, f32[256,128]{1,0:T(8,128)} %get-tuple-element.28.mean_v, ...), custom_call_target="tpu_custom_call" | custom-call | flops 400000000 | bytes 4000000 | tf_op jit(solution)/shard_map/ready/pallas_call | solution.py:312
  177.4 1.1 all-to-all-done.6.total_ref
  178.5 3.8 %outputs.1 = (f32[64,256]{1,0:T(8,128)}, f32[64,256]{1,0:T(8,128)}, bf16[2048,256]{1,0:T(8,128)(2,1)}, f32[32,128]{1,0:T(8,128)}, f32[32,128]{1,0:T(8,128)}, /*index=5*/bf16[1024,128]{1,0:T(8,128)(2,1)}) custom-call(f32[16,8,128]{2,1,0:T(8,128)} %all-to-all-done.6.total_ref, f32[64,256]{1,0:T(8,128)} %weight_o.3, f32[32,128]{1,0:T(8,128)} %weight_v.3, ...), custom_call_target="tpu_custom_call" | custom-call | flops 10000000 | bytes 4000000 | tf_op jit(solution)/shard_map/outputs/pallas_call | solution.py:373
  (36 shorter events, 0.1 us)
Async XLA Ops:
  0.6 30.2 %copy-start.6 = (bf16[1536,64]{0,1:T(8,128)(2,1)S(1)}, bf16[1536,64]{0,1:T(8,128)(2,1)}, u32[]{:S(2)}) copy-start(bf16[1536,64]{0,1:T(8,128)(2,1)} %param.14) | copy-start | bytes 589828
  1.5 0.7 collective-permute-start
  2.9 31.4 %all-to-all-start = ((bf16[8,96,256]{2,1,0:T(8,128)(2,1)}), bf16[8,96,256]{2,1,0:T(8,128)(2,1)}, u32[]{:S(2)}, u32[]{:S(2)}) async-start(bf16[8,96,256]{2,1,0:T(8,128)(2,1)} %broadcast_in_dim.4), calls=%async_computation | async-start | bytes 786432 | tf_op jit(solution)/shard_map/all_to_all | solution.py:31
  20.1 12.4 %collective-permute-start.1 = (bf16[576,128]{1,0:T(8,128)(2,1)}, bf16[576,128]{1,0:T(8,128)(2,1)S(1)}, u32[]{:S(2)}, u32[]{:S(2)}) collective-permute-start(bf16[576,128]{1,0:T(8,128)(2,1)} %get-tuple-element.30), channel_id=1, source_target_pairs={{0,1},{1,2},{2,3},{3,0},{4,5},{5,6},{6,7},{7,4},{8,9},{9,10},{10,1... | collective-permute-start | bytes 442376 | tf_op jit(solution)/shard_map/ppermute | solution.py:50
  23.4 9.5 %collective-permute-start.2 = (bf16[576,128]{1,0:T(8,128)(2,1)}, bf16[576,128]{1,0:T(8,128)(2,1)S(1)}, u32[]{:S(2)}, u32[]{:S(2)}) collective-permute-start(bf16[576,128]{1,0:T(8,128)(2,1)} %get-tuple-element.31), channel_id=1, source_target_pairs={{0,2},{1,3},{2,0},{3,1},{4,6},{5,7},{6,4},{7,5},{8,10},{9,11},{10,... | collective-permute-start | bytes 442376 | tf_op jit(solution)/shard_map/ppermute | solution.py:50
  27.7 6.6 %collective-permute-start.3 = (bf16[576,128]{1,0:T(8,128)(2,1)}, bf16[576,128]{1,0:T(8,128)(2,1)S(1)}, u32[]{:S(2)}, u32[]{:S(2)}) collective-permute-start(bf16[576,128]{1,0:T(8,128)(2,1)} %get-tuple-element.32), channel_id=1, source_target_pairs={{0,3},{1,0},{2,1},{3,2},{4,7},{5,4},{6,5},{7,6},{8,11},{9,8},{10,9... | collective-permute-start | bytes 442376 | tf_op jit(solution)/shard_map/ppermute | solution.py:50
  30.8 1.0 copy-start.3
  56.0 27.0 %copy-start.5 = (bf16[1536,256]{1,0:T(8,128)(2,1)S(1)}, bf16[1536,256]{1,0:T(8,128)(2,1)}, u32[]{:S(2)}) copy-start(bf16[1536,256]{1,0:T(8,128)(2,1)} %cot_o.1) | copy-start | bytes 2359300
  56.0 26.9 %copy-start.7 = (bf16[1536,128]{1,0:T(8,128)(2,1)S(1)}, bf16[1536,128]{1,0:T(8,128)(2,1)}, u32[]{:S(2)}) copy-start(bf16[1536,128]{1,0:T(8,128)(2,1)} %cot_v.1) | copy-start | bytes 1179652
  82.9 25.7 %copy-start.10 = (f32[64,256]{1,0:T(8,128)S(1)}, f32[64,256]{1,0:T(8,128)}, u32[]{:S(2)}) copy-start(f32[64,256]{1,0:T(8,128)} %weight_o.3) | copy-start | bytes 196612
  82.9 25.7 %copy-start.14 = (f32[32,128]{1,0:T(8,128)S(1)}, f32[32,128]{1,0:T(8,128)}, u32[]{:S(2)}) copy-start(f32[32,128]{1,0:T(8,128)} %weight_v.3) | copy-start | bytes 49156
  83.5 81.3 %copy-start.8 = (f32[256,256]{1,0:T(8,128)S(1)}, f32[256,256]{1,0:T(8,128)}, u32[]{:S(2)}) copy-start(f32[256,256]{1,0:T(8,128)} %mean_o.1) | copy-start | bytes 786436
  83.6 81.3 %copy-start.9 = (f32[256,256]{1,0:T(8,128)S(1)}, f32[256,256]{1,0:T(8,128)}, u32[]{:S(2)}) copy-start(f32[256,256]{1,0:T(8,128)} %square_o.1) | copy-start | bytes 786436
  83.6 81.3 %copy-start.12 = (f32[256,128]{1,0:T(8,128)S(1)}, f32[256,128]{1,0:T(8,128)}, u32[]{:S(2)}) copy-start(f32[256,128]{1,0:T(8,128)} %mean_v.1) | copy-start | bytes 393220
  83.6 81.3 %copy-start.13 = (f32[256,128]{1,0:T(8,128)S(1)}, f32[256,128]{1,0:T(8,128)}, u32[]{:S(2)}) copy-start(f32[256,128]{1,0:T(8,128)} %square_v.1) | copy-start | bytes 393220
  97.5 32.7 %all-to-all-start.4 = ((bf16[4,32,384]{2,1,0:T(8,128)(2,1)}), bf16[4,32,384]{2,1,0:T(8,128)(2,1)S(1)}, u32[]{:S(2)}, u32[]{:S(2)}) async-start(bf16[4,32,384]{2,1,0:T(8,128)(2,1)} %shard_map.198), calls=%async_computation.4 | async-start | bytes 196608 | tf_op jit(solution)/shard_map/all_to_all | solution.py:31
  108.7 14.1 %collective-permute-start.7 = (bf16[1,160,128]{2,1,0:T(8,128)(2,1)S(1)}, bf16[1,160,128]{2,1,0:T(8,128)(2,1)S(1)}, u32[]{:S(2)}, u32[]{:S(2)}) collective-permute-start(bf16[1,160,128]{2,1,0:T(8,128)(2,1)S(1)} %bitcast.6), channel_id=1, source_target_pairs={{0,256},{32,288},{64,320},{96,352},{128,384},{160,416},{192,448},{... | collective-permute-start | bytes 122888 | tf_op jit(solution)/shard_map/ppermute | solution.py:50
  122.8 16.8 %collective-permute-start.8 = (bf16[2,160,128]{2,1,0:T(8,128)(2,1)S(1)}, bf16[2,160,128]{2,1,0:T(8,128)(2,1)S(1)}, u32[]{:S(2)}, u32[]{:S(2)}) collective-permute-start(bf16[2,160,128]{2,1,0:T(8,128)(2,1)S(1)} %pad_maximum_fusion.2), channel_id=1, source_target_pairs={{0,128},{32,160},{64,192},{96,224},{128,256},{160,288},{192,320},{... | collective-permute-start | bytes 245768 | tf_op jit(solution)/shard_map/ppermute | solution.py:50
  130.9 33.9 %all-to-all-start.5 = ((bf16[8,32,384]{2,1,0:T(8,128)(2,1)}), bf16[8,32,384]{2,1,0:T(8,128)(2,1)S(1)}, u32[]{:S(2)}, u32[]{:S(2)}) async-start(bf16[8,32,384]{2,1,0:T(8,128)(2,1)} %shard_map.199), calls=%async_computation.5 | async-start | bytes 393216 | tf_op jit(solution)/shard_map/all_to_all | solution.py:31
  137.6 22.3 %collective-permute-start.4 = (bf16[8,96,256]{2,1,0:T(8,128)(2,1)}, bf16[8,96,256]{2,1,0:T(8,128)(2,1)S(1)}, u32[]{:S(2)}, u32[]{:S(2)}) collective-permute-start(bf16[8,96,256]{2,1,0:T(8,128)(2,1)} %all-to-all-done.blocks_ref.b0), channel_id=1, source_target_pairs={{0,4},{4,8},{8,12},{12,0},{1,5},{5,9},{9,13},{13,1},{2,6},{6,10},{... | collective-permute-start | bytes 1179656 | tf_op jit(solution)/shard_map/ppermute | solution.py:50
  139.6 8.8 %collective-permute-start.9 = (bf16[4,160,128]{2,1,0:T(8,128)(2,1)S(1)}, bf16[4,160,128]{2,1,0:T(8,128)(2,1)S(1)}, u32[]{:S(2)}, u32[]{:S(2)}) collective-permute-start(bf16[4,160,128]{2,1,0:T(8,128)(2,1)S(1)} %pad_maximum_fusion.1), channel_id=1, source_target_pairs={{0,16},{16,0},{1,17},{17,1},{2,18},{18,2},{3,19},{19,3},{4,20},{20... | collective-permute-start | bytes 491528 | tf_op jit(solution)/shard_map/ppermute | solution.py:50
  141.6 20.2 %collective-permute-start.5 = (bf16[8,96,256]{2,1,0:T(8,128)(2,1)}, bf16[8,96,256]{2,1,0:T(8,128)(2,1)S(1)}, u32[]{:S(2)}, u32[]{:S(2)}) collective-permute-start(bf16[8,96,256]{2,1,0:T(8,128)(2,1)} %all-to-all-done.blocks_ref.b0), channel_id=1, source_target_pairs={{0,8},{4,12},{8,0},{12,4},{1,9},{5,13},{9,1},{13,5},{2,10},{6,14},... | collective-permute-start | bytes 1179656 | tf_op jit(solution)/shard_map/ppermute | solution.py:50
  145.6 19.2 %collective-permute-start.6 = (bf16[8,96,256]{2,1,0:T(8,128)(2,1)}, bf16[8,96,256]{2,1,0:T(8,128)(2,1)S(1)}, u32[]{:S(2)}, u32[]{:S(2)}) collective-permute-start(bf16[8,96,256]{2,1,0:T(8,128)(2,1)} %all-to-all-done.blocks_ref.b0), channel_id=1, source_target_pairs={{0,12},{4,0},{8,4},{12,8},{1,13},{5,1},{9,5},{13,9},{2,14},{6,2},{... | collective-permute-start | bytes 1179656 | tf_op jit(solution)/shard_map/ppermute | solution.py:50
  148.5 23.5 %collective-permute-start.10 = (bf16[8,160,128]{2,1,0:T(8,128)(2,1)S(1)}, bf16[8,160,128]{2,1,0:T(8,128)(2,1)S(1)}, u32[]{:S(2)}, u32[]{:S(2)}) collective-permute-start(bf16[8,160,128]{2,1,0:T(8,128)(2,1)S(1)} %pad_maximum_fusion.h0), channel_id=1, source_target_pairs={{0,32},{32,64},{64,96},{96,128},{128,160},{160,192},{192,224},{224... | collective-permute-start | bytes 983048 | tf_op jit(solution)/shard_map/ppermute | solution.py:50
  152.0 19.9 %collective-permute-start.11 = (bf16[8,160,128]{2,1,0:T(8,128)(2,1)S(1)}, bf16[8,160,128]{2,1,0:T(8,128)(2,1)S(1)}, u32[]{:S(2)}, u32[]{:S(2)}) collective-permute-start(bf16[8,160,128]{2,1,0:T(8,128)(2,1)S(1)} %pad_maximum_fusion.h0), channel_id=1, source_target_pairs={{0,64},{32,96},{64,128},{96,160},{128,192},{160,224},{192,256},{22... | collective-permute-start | bytes 983048 | tf_op jit(solution)/shard_map/ppermute | solution.py:50
  159.9 12.4 %copy-start = (bf16[8,96,256]{2,1,0:T(8,128)(2,1)}, bf16[8,96,256]{2,1,0:T(8,128)(2,1)S(1)}, u32[]{:S(2)}) copy-start(bf16[8,96,256]{2,1,0:T(8,128)(2,1)S(1)} %collective-permute-done.4.b1) | copy-start | bytes 1179652
  159.9 12.0 %collective-permute-start.12 = (bf16[8,160,128]{2,1,0:T(8,128)(2,1)S(1)}, bf16[8,160,128]{2,1,0:T(8,128)(2,1)S(1)}, u32[]{:S(2)}, u32[]{:S(2)}) collective-permute-start(bf16[8,160,128]{2,1,0:T(8,128)(2,1)S(1)} %pad_maximum_fusion.h0), channel_id=1, source_target_pairs={{0,480},{32,0},{64,32},{96,64},{128,96},{160,128},{192,160},{224,1... | collective-permute-start | bytes 983048 | tf_op jit(solution)/shard_map/ppermute | solution.py:50
  161.9 10.4 %copy-start.1 = (bf16[8,96,256]{2,1,0:T(8,128)(2,1)}, bf16[8,96,256]{2,1,0:T(8,128)(2,1)S(1)}, u32[]{:S(2)}) copy-start(bf16[8,96,256]{2,1,0:T(8,128)(2,1)S(1)} %collective-permute-done.5.b2) | copy-start | bytes 1179652
  164.8 7.5 %copy-start.2 = (bf16[8,96,256]{2,1,0:T(8,128)(2,1)}, bf16[8,96,256]{2,1,0:T(8,128)(2,1)S(1)}, u32[]{:S(2)}) copy-start(bf16[8,96,256]{2,1,0:T(8,128)(2,1)S(1)} %collective-permute-done.6.b3) | copy-start | bytes 1179652
  167.5 11.0 %all-to-all-start.6 = ((f32[16,8,128]{2,1,0:T(8,128)}), f32[16,8,128]{2,1,0:T(8,128)}, u32[]{:S(2)}, u32[]{:S(2)}) async-start(f32[16,8,128]{2,1,0:T(8,128)} %get-tuple-element.33), calls=%async_computation.6 | async-start | bytes 131072 | tf_op jit(solution)/shard_map/all_to_all | solution.py:31
  172.3 1.0 copy-start.4
  173.3 0.7 copy-start.11
